TPU v7x, 32 devices: a whole 2x2x4 slice. The times are simulated.
32 devices in a mesh: grp: 2 (over y), sp: 4 (over z), tp: 4 (over x, core).
Axes of the slice: x: 2, y: 2, z: 4, core: 2. Of those that a mesh axis runs over, the one named last changes fastest.
Arguments:
- hidden: bfloat16 [3072, 2048], P(('grp', 'sp'), 'tp'), parts along dimension 0, may hold values from -45 to 45
- norm_gain: bfloat16 [2048], replicated, may hold values from 0.099609375 to 1.8984375
- w_query: bfloat16 [2048, 1024], P(None, 'tp'), may hold values from -0.125 to 0.125
- w_key: bfloat16 [2048, 1024], P(None, 'tp'), may hold values from -0.125 to 0.125
- w_value: bfloat16 [2048, 1024], P(None, 'tp'), may hold values from -0.125 to 0.125
- query_gain: float32 [8, 128], P('tp'), may hold values from 0.3 to 16
- key_gain: float32 [8, 128], P('tp'), may hold values from 0.3 to 16
- w_out: bfloat16 [1024, 2048], P('tp'), may hold values from -1.5 to 1.5
Outputs:
- mixed: bfloat16 [3072, 2048], P(('grp', 'sp'), 'tp'), parts along dimension 0
- log_total: float32 [3072, 8], P(('grp', 'sp'), 'tp'), parts along dimension 0
There are 2 independent parts, one for each index of `grp`. A program takes and returns all parts, laid end to end along the dimension named above; an argument that names none is the same for every part. Nothing has to cross between parts.
All inputs are finite; a program needn't handle non-finite values.
Results may differ from a plain program's by a relative error of at most 0.015.
The roundings to bfloat16 on the way count: a program that leaves them out, or rounds other values in their place, can miss the bound.
Values may be sent and summed in bfloat16 or wider, within the bound.
No kernel may reach another device: no remote copies, remote signals or barrier semaphores. Data moves between devices by JAX's collectives and lax.ppermute only.
A program may use at most 64 MiB of HBM per device.

v0:
```python
import math

import jax
import jax.numpy as jnp
from jax import lax
from jax.sharding import PartitionSpec as P

D = 2048
KEYS_BEHIND = 128
MIDDLE_DILATION = 4
WIDEST_DILATION = 16


EPSILON = 1e-06
ROTARY_BASE = 500000.0


def from_behind(value, axis, steps):
    count = lax.axis_size(axis)
    initial, last = (max(0, -steps), min(count, count - steps))
    return lax.ppermute(value, axis, [(source, source + steps) for source in range(initial, last)])


def rotate(values, positions):
    head_width = values.shape[-1]
    inverse = ROTARY_BASE ** (-jnp.arange(0, head_width, 2, dtype=jnp.float32) / head_width)
    angles = positions[:, None] * inverse[None, :]
    cosine = jnp.cos(angles)[:, None, :]
    sine = jnp.sin(angles)[:, None, :]
    half_width = head_width // 2
    first_half = values[..., :half_width]
    second_half = values[..., half_width:]
    return jnp.concatenate(
        [first_half * cosine - second_half * sine, second_half * cosine + first_half * sine],
        axis=-1,
    )


def head_norm(values, gains):
    normed = values * lax.rsqrt(jnp.mean(values * values, axis=-1, keepdims=True) + EPSILON)
    return normed * gains[None, :, :]


def earlier_pairs(own_pair, token_rows):
    distant_shards = (KEYS_BEHIND * WIDEST_DILATION + token_rows - 1) // token_rows
    pieces = [own_pair]
    for distance in range(1, distant_shards + 1):
        pieces.insert(0, from_behind(own_pair, "sp", distance))
    buffer = jnp.concatenate(pieces, axis=1)
    return buffer


def local_branch(query, key_rows, value_rows, dilation_step, first_pos):
    token_rows, head_count, head_width = query.shape
    reach_rows = KEYS_BEHIND * dilation_step
    buffer_rows = key_rows.shape[0]
    class_rows = token_rows // dilation_step
    class_keys = class_rows + KEYS_BEHIND
    window_start = buffer_rows - token_rows - reach_rows
    key_window = key_rows[window_start:]
    value_window = value_rows[window_start:]
    query_class = query.reshape(class_rows, dilation_step, head_count, head_width).transpose(
        1, 0, 2, 3
    )
    key_class = key_window.reshape(class_keys, dilation_step, head_count, head_width).transpose(
        1, 0, 2, 3
    )
    value_class = value_window.reshape(class_keys, dilation_step, head_count, head_width).transpose(
        1, 0, 2, 3
    )
    block_rows = math.gcd(class_rows, KEYS_BEHIND) if class_rows > KEYS_BEHIND else class_rows
    block_count = class_rows // block_rows
    query_blocks = query_class.reshape(
        dilation_step, block_count, block_rows, head_count, head_width
    )
    key_blocks = jnp.stack(
        [
            key_class[:, number * block_rows : number * block_rows + block_rows + KEYS_BEHIND]
            for number in range(block_count)
        ],
        axis=1,
    )
    value_blocks = jnp.stack(
        [
            value_class[:, number * block_rows : number * block_rows + block_rows + KEYS_BEHIND]
            for number in range(block_count)
        ],
        axis=1,
    )
    scores = jnp.einsum(
        "rnqhd,rnkhd->rnhqk", query_blocks, key_blocks, preferred_element_type=jnp.float32
    ) * head_width ** (-0.5)
    row_index = jnp.arange(block_rows, dtype=jnp.int32)[:, None]
    col_index = jnp.arange(block_rows + KEYS_BEHIND, dtype=jnp.int32)[None, :]
    distance = KEYS_BEHIND + row_index - col_index
    in_band = (distance >= 0) & (distance <= KEYS_BEHIND)
    class_index = jnp.arange(block_count, dtype=jnp.int32)[:, None] * block_rows + col_index
    residue = jnp.arange(dilation_step, dtype=jnp.int32)[:, None, None]
    key_position = first_pos - reach_rows + class_index[None] * dilation_step + residue
    allowed = in_band[None, None, None, :, :] & (key_position >= 0)[:, :, None, None, :]
    scores = jnp.where(allowed, scores, -jnp.inf)
    row_max = jnp.max(scores, axis=-1, keepdims=True)
    weights = jnp.exp(scores - row_max)
    weight_sum = jnp.sum(weights, axis=-1)
    weighted = jnp.einsum(
        "rnhqk,rnkhd->rnqhd",
        weights.astype(jnp.bfloat16),
        value_blocks,
        preferred_element_type=jnp.float32,
    )
    branch_out = weighted / jnp.transpose(weight_sum, (0, 1, 3, 2))[..., None]
    branch_out = branch_out.reshape(dilation_step, class_rows, head_count, head_width).transpose(
        1, 0, 2, 3
    )
    branch_out = branch_out.reshape(token_rows, head_count, head_width)
    log_sum = jnp.transpose(row_max[..., 0] + jnp.log(weight_sum), (0, 1, 3, 2))
    log_sum = (
        log_sum.reshape(dilation_step, class_rows, head_count)
        .transpose(1, 0, 2)
        .reshape(token_rows, head_count)
    )
    return (branch_out, log_sum)


def local(hidden, norm_gain, w_query, w_key, w_value, query_gain, key_gain, w_out):
    token_rows = hidden.shape[0]
    local_width = w_query.shape[1]
    head_count = query_gain.shape[0]
    head_width = query_gain.shape[1]
    gain_full = norm_gain.astype(jnp.float32)
    raw_piece = lax.all_gather(hidden, "tp", axis=1, tiled=True).astype(jnp.float32)
    scaled = (raw_piece * gain_full[None, :]).astype(jnp.bfloat16)

    def add_product(weight):
        return jnp.dot(scaled, weight, preferred_element_type=jnp.float32)

    query_raw = add_product(w_query)
    key_raw = add_product(w_key)
    value_raw = add_product(w_value)
    squares = jnp.sum(raw_piece * raw_piece, axis=1)
    row_scale = lax.rsqrt(squares / D + EPSILON)[:, None]
    first_pos = lax.axis_index("sp") * token_rows
    positions = (jnp.arange(token_rows, dtype=jnp.int32) + first_pos).astype(jnp.float32)
    query = rotate(
        head_norm((query_raw * row_scale).reshape(token_rows, head_count, head_width), query_gain),
        positions,
    ).astype(jnp.bfloat16)
    key_now = rotate(
        head_norm((key_raw * row_scale).reshape(token_rows, head_count, head_width), key_gain),
        positions,
    ).astype(jnp.bfloat16)
    value_now = (value_raw * row_scale).astype(jnp.bfloat16)
    own_pair = jnp.stack([key_now.reshape(token_rows, local_width), value_now], axis=0)
    buffer = earlier_pairs(own_pair, token_rows)
    key_rows = buffer[0].reshape(-1, head_count, head_width)
    value_rows = buffer[1].reshape(-1, head_count, head_width)
    branch_outs = []
    branch_logs = []
    for dilation_step in (1, MIDDLE_DILATION, WIDEST_DILATION):
        branch_out, log_sum = local_branch(query, key_rows, value_rows, dilation_step, first_pos)
        branch_outs.append(branch_out)
        branch_logs.append(log_sum)
    stacked_logs = jnp.stack(branch_logs, axis=0)
    peak = jnp.max(stacked_logs, axis=0)
    log_total = peak + jnp.log(jnp.sum(jnp.exp(stacked_logs - peak[None]), axis=0))
    shares = jnp.exp(stacked_logs - log_total[None])
    attended = jnp.sum(shares[..., None] * jnp.stack(branch_outs, axis=0), axis=0)
    attended = attended.astype(jnp.bfloat16).reshape(token_rows, local_width)
    column_block = lax.all_to_all(w_out, "tp", split_axis=1, concat_axis=0, tiled=True)
    mixed = jnp.dot(
        lax.all_gather(attended, "tp", axis=1, tiled=True),
        column_block,
        preferred_element_type=jnp.float32,
    )
    return (mixed.astype(jnp.bfloat16), log_total)


def solution(mesh):
    placed = (
        P(("grp", "sp"), "tp"),
        P(),
        P(None, "tp"),
        P(None, "tp"),
        P(None, "tp"),
        P("tp", None),
        P("tp", None),
        P("tp", None),
    )
    return jax.shard_map(
        local,
        mesh=mesh,
        in_specs=placed,
        out_specs=(P(("grp", "sp"), "tp"), P(("grp", "sp"), "tp")),
        check_vma=False,
    )
```

profile of v0, /device:TPU:15, one launch (start us, length us, event | category | flops | bytes accessed | tf_op | source)
XLA Modules:
  0.0 133.7 jit_solution(7337849643305904054)
XLA Ops:
  7.2 0.7 all-gather.2.cloned.1.call-update
  7.9 2.3 %copy.167 = bf16[256,2048]{0,1:T(8,128)(2,1)} copy(bf16[256,2048]{1,0:T(8,128)(2,1)} %param.15) | data formatting | bytes 2097152 | tf_op args[7]
  10.2 4.4 %all-to-all-start = ((bf16[256,4,512]{0,2,1:T(8,128)(2,1)}), bf16[256,4,512]{0,2,1:T(8,128)(2,1)S(1)}, u32[]{:S(2)}, u32[]{:S(2)}) async-start(bf16[256,4,512]{0,2,1:T(8,128)(2,1)} %bitcast.65), calls=%async_computation | async-start | bytes 2097152 | tf_op jit(solution)/shard_map/all_to_all | solution.py:169
  15.1 0.7 broadcast_and_fusion.1
  15.8 0.7 broadcast_and_fusion.2
  16.5 1.4 %multiply_cosine_fusion = (f32[384,64]{1,0:T(8,128)S(1)}, f32[384,64]{1,0:T(8,128)}) fusion(f32[64]{0:T(128)S(1)} %multiply_power_fusion, f32[384]{0:T(512)S(1)} %add_convert_fusion.2), kind=kLoop, calls=%fused_computation.71 | loop fusion | flops 24576 | bytes 198400 | tf_op jit(solution)/shard_map/cos | solution.py:28
  17.9 19.5 %all-gather.2.cloned.1.call-done = bf16[384,2048]{1,0:T(8,128)(2,1)} async-done(((bf16[384,512]{1,0:T(8,128)(2,1)}), bf16[384,2048]{1,0:T(8,128)(2,1)}) %all-gather.2.cloned.1.call-update) | async-done | bytes 1572880 | tf_op jit(solution)/shard_map/all_gather | solution.py:131
  37.5 1.9 %fusion.1 = f32[384]{0:T(512)S(1)} fusion(bf16[384,2048]{1,0:T(8,128)(2,1)} %all-gather.2.cloned.1.call-done), kind=kLoop, calls=%fused_computation.3 | loop fusion | flops 2358912 | bytes 1574400 | tf_op jit(solution)/shard_map/reduce_sum | solution.py:140
  39.4 0.8 multiply_reduce_fusion
  40.4 2.5 %multiply_reduce_fusion.1 = (f32[384,2]{0,1:T(2,128)S(1)}, f32[384,256]{0,1:T(8,128)S(1)}) fusion(f32[384]{0:T(512)S(1)} %add_rsqrt_fusion.2, bf16[2048,256]{1,0:T(8,128)(2,1)} %param.10, bf16[384,2048]{1,0:T(8,128)(2,1)} %all-gather.2.cloned.1.call-done, f32[2048]{0:T(1024)S(1)} %convert_element_type.58), kind=kOutput, calls=%fused_computation.69 | convolution fusion | flops 405306624 | bytes 3027456 | tf_op jit(solution)/shard_map/dot_general | solution.py:135
  43.3 1.3 subtract_convert_fusion.1
  44.9 2.5 %fusion.20 = bf16[1,384,256]{1,2,0:T(8,128)(2,1)S(1)} fusion(bf16[2048,256]{1,0:T(8,128)(2,1)} %param.12, bf16[384,2048]{1,0:T(8,128)(2,1)} %all-gather.2.cloned.1.call-done, f32[2048]{0:T(1024)S(1)} %convert_element_type.58, f32[384]{0:T(512)S(1)} %add_rsqrt_fusion.2), kind=kOutput, calls=%fused_computation.25 | convolution fusion | flops 405209088 | bytes 2827776 | tf_op jit(solution)/shard_map/dot_general | solution.py:135
  47.5 0.8 pad_maximum_fusion.2
  48.3 0.7 collective-permute-start.2
  49.0 1.4 %collective-permute-start.3 = (bf16[2,384,256]{1,2,0:T(8,128)(2,1)}, bf16[2,384,256]{1,2,0:T(8,128)(2,1)}, u32[]{:S(2)}, u32[]{:S(2)}) collective-permute-start(bf16[2,384,256]{1,2,0:T(8,128)(2,1)} %pad_maximum_fusion.2), channel_id=1, source_target_pairs={{0,12},{1,13},{2,14},{3,15},{16,28},{17,29},{18,30},{19,31}} | collective-permute-start | bytes 1179656 | tf_op jit(solution)/shard_map/ppermute | solution.py:21
  50.4 0.7 broadcast_and_fusion
  51.1 1.3 copy.168
  52.4 4.1 %collective-permute-start.1 = (bf16[2,384,256]{1,2,0:T(8,128)(2,1)}, bf16[2,384,256]{1,2,0:T(8,128)(2,1)S(1)}, u32[]{:S(2)}, u32[]{:S(2)}) collective-permute-start(bf16[2,384,256]{1,2,0:T(8,128)(2,1)} %pad_maximum_fusion.2), channel_id=1, source_target_pairs={{0,8},{4,12},{1,9},{5,13},{2,10},{6,14},{3,11},{7,15},{16,24},{20,... | collective-permute-start | bytes 1179656 | tf_op jit(solution)/shard_map/ppermute | solution.py:21
  56.5 2.1 %collective-permute-start = (bf16[2,384,256]{1,2,0:T(8,128)(2,1)}, bf16[2,384,256]{1,2,0:T(8,128)(2,1)S(1)}, u32[]{:S(2)}, u32[]{:S(2)}) collective-permute-start(bf16[2,384,256]{1,2,0:T(8,128)(2,1)} %pad_maximum_fusion.2), channel_id=1, source_target_pairs={{0,4},{4,8},{8,12},{1,5},{5,9},{9,13},{2,6},{6,10},{10,14},{3,7},{... | collective-permute-start | bytes 1179656 | tf_op jit(solution)/shard_map/ppermute | solution.py:21
  58.6 0.7 copy.150
  59.3 0.7 copy.149
  60.1 0.7 copy.145
  60.8 0.7 copy.144
  61.7 1.1 constant_dynamic-update-slice_fusion.3
  62.7 17.4 %collective-permute-done.1 = bf16[2,384,256]{1,2,0:T(8,128)(2,1)S(1)} collective-permute-done((bf16[2,384,256]{1,2,0:T(8,128)(2,1)}, bf16[2,384,256]{1,2,0:T(8,128)(2,1)S(1)}, u32[]{:S(2)}, u32[]{:S(2)}) %collective-permute-start.1) | collective-permute-done | bytes 393248 | tf_op jit(solution)/shard_map/ppermute | solution.py:21
  80.2 8.4 %collective-permute-done = bf16[2,384,256]{1,2,0:T(8,128)(2,1)S(1)} collective-permute-done((bf16[2,384,256]{1,2,0:T(8,128)(2,1)}, bf16[2,384,256]{1,2,0:T(8,128)(2,1)S(1)}, u32[]{:S(2)}, u32[]{:S(2)}) %collective-permute-start) | collective-permute-done | bytes 393248 | tf_op jit(solution)/shard_map/ppermute | solution.py:21
  88.7 0.6 copy-done.3
  89.6 1.5 %copy.151 = bf16[1,2432,256]{2,1,0:T(8,128)(2,1)} copy(bf16[1,2432,256]{1,2,0:T(8,128)(2,1)S(1)} %get-tuple-element.2) | data formatting | bytes 2490368 | tf_op jit(solution)/shard_map/slice | solution.py:60
  91.0 2.9 %reshape.537 = bf16[152,16,2,128]{3,2,1,0:T(2,128)(2,1)S(1)} reshape(bf16[1,2432,256]{2,1,0:T(8,128)(2,1)} %copy.151) | data formatting | bytes 2490368 | tf_op jit(solution)/shard_map/reshape | solution.py:65
  93.9 2.0 %fusion.85 = (f32[16,2,24]{2,1,0:T(2,128)S(1)}, f32[16,2,24,152]{3,2,1,0:T(8,128)S(1)}) fusion(bf16[152,16,2,128]{3,2,1,0:T(2,128)(2,1)S(1)} %reshape.537, bf16[24,16,2,64]{3,0,2,1:T(8,128)(2,1)} %copy.150, bf16[24,16,2,64]{3,0,2,1:T(8,128)(2,1)} %copy.149, pred[16,24,152]{2,1,0:T(8,128)(4,1)} %broadcast_and_fusion), kind=kOutput, calls=%fused_computation.142 | convolution fusion | flops 30627072 | bytes 1970176 | tf_op jit(solution)/shard_map/rnqhd,rnkhd->rnhqk/dot_general | solution.py:90
  95.9 0.9 copy-done.5
  97.2 0.6 copy-done.21
  97.8 0.7 stack_reshape.14
  98.5 0.7 stack.54
  99.2 2.1 %maximum_maximum_fusion = (bf16[1,896,256]{1,2,0:T(8,128)(2,1)S(1)}, bf16[1,896,256]{1,2,0:T(8,128)(2,1)}) fusion(bf16[1,384,256]{1,2,0:T(8,128)(2,1)} %copy-done.7, bf16[1,384,256]{1,2,0:T(8,128)(2,1)} %bitcast.176, bf16[2,384,256]{1,2,0:T(8,128)(2,1)} %copy-done.3, bf16[2,384,256]{1,2,0:T(8,128)(2,1)} %copy-done.15), kind=kLoop, calls=%fused_computation.43 | loop fusion | flops 3670016 | bytes 2097152 | tf_op jit(solution)/shard_map/slice | solution.py:60
  101.7 1.5 %fusion.86 = (f32[4,2,96]{2,1,0:T(2,128)S(1)}, f32[4,2,96,224]{3,2,1,0:T(8,128)S(1)}) fusion(bf16[224,4,2,128]{3,2,1,0:T(2,128)(2,1)S(1)} %reshape.535, bf16[96,4,2,64]{3,0,2,1:T(8,128)(2,1)S(1)} %copy-done.18, bf16[96,4,2,64]{3,0,2,1:T(8,128)(2,1)} %copy.144, pred[4,96,224]{2,1,0:T(8,128)(4,1)S(1)} %copy-done.20), kind=kOutput, calls=%fused_computation.143 | convolution fusion | flops 44948736 | bytes 1432576 | tf_op jit(solution)/shard_map/rnqhd,rnkhd->rnhqk/dot_general | solution.py:90
  103.5 0.5 copy-done.16
  104.2 0.7 stack_reshape.13
  104.9 0.7 stack.53
  105.6 0.8 copy.163
  106.4 1.2 reshape.542
  107.6 2.1 %fusion.29 = f32[24,16,2,128]{3,0,2,1:T(8,128)S(1)} fusion(bf16[152,16,2,128]{3,2,1,0:T(2,128)(2,1)} %reshape.542, f32[16,2,24,152]{3,2,1,0:T(8,128)S(1)} %copy-done.6, f32[16,2,24]{2,1,0:T(2,128)S(1)} %get-tuple-element.26, f32[16,24,2]{1,2,0:T(2,128)} %bitcast.200), kind=kOutput, calls=%fused_computation.30 | convolution fusion | flops 30216192 | bytes 2111488 | tf_op jit(solution)/shard_map/rnhqk,rnkhd->rnqhd/dot_general | solution.py:105
  110.2 0.6 copy-done.17
  113.1 0.4 fusion.87
  113.9 0.6 fusion.25
  114.7 0.4 fusion.16
  115.2 9.0 %all_gather.7 = bf16[384,1024]{0,1:T(8,128)(2,1)S(1)} all-gather(bf16[384,256]{0,1:T(8,128)(2,1)S(1)} %bitcast.191), channel_id=1, replica_groups=mesh['grp'=2,'sp'=4,'tp'=4] {'tp'}, dimensions={1}, use_global_device_ids=true | all-gather | bytes 983040 | tf_op jit(solution)/shard_map/all_gather | solution.py:171
  124.3 2.6 %convolution_convert_fusion = bf16[384,512]{1,0:T(8,128)(2,1)} fusion(bf16[384,1024]{0,1:T(8,128)(2,1)S(1)} %all_gather.7, bf16[1024,512]{1,0:T(8,128)(2,1)} %bitcast.190), kind=kOutput, calls=%fused_computation.10 | convolution fusion | flops 402849792 | bytes 2228224 | tf_op jit(solution)/shard_map/dot_general | solution.py:170
  (127 shorter events, 6.6 us)
Async XLA Ops:
  7.2 32.2 %copy-start = (bf16[2048,256]{1,0:T(8,128)(2,1)S(1)}, bf16[2048,256]{1,0:T(8,128)(2,1)}, u32[]{:S(2)}) copy-start(bf16[2048,256]{1,0:T(8,128)(2,1)} %param.11) | copy-start | bytes 3145732
  7.2 30.3 %all-gather.2.cloned.1.call-start = ((), (), s32[]{:S(2)}) async-start(), calls=%async_computation.1 | async-start | bytes 1966080 | tf_op jit(solution)/shard_map/all_gather | solution.py:131
  10.2 4.5 %copy-start.31 = (bf16[2048]{0:T(1024)(128)(2,1)S(1)}, bf16[2048]{0:T(1024)(128)(2,1)}, u32[]{:S(2)}) copy-start(bf16[2048]{0:T(1024)(128)(2,1)} %param.9) | copy-start | bytes 12292
  10.2 40.9 %all-to-all-start = ((bf16[256,4,512]{0,2,1:T(8,128)(2,1)}), bf16[256,4,512]{0,2,1:T(8,128)(2,1)S(1)}, u32[]{:S(2)}, u32[]{:S(2)}) async-start(bf16[256,4,512]{0,2,1:T(8,128)(2,1)} %bitcast.65), calls=%async_computation | async-start | bytes 2097152 | tf_op jit(solution)/shard_map/all_to_all | solution.py:169
  37.4 1.9 %copy-start.14 = (bf16[384,2048]{1,0:T(8,128)(2,1)S(1)}, bf16[384,2048]{1,0:T(8,128)(2,1)}, u32[]{:S(2)}) copy-start(bf16[384,2048]{1,0:T(8,128)(2,1)} %all-gather.2.cloned.1.call-done) | copy-start | bytes 4718596
  40.4 2.7 %copy-start.32 = (f32[2,128]{1,0:T(2,128)S(1)}, f32[2,128]{1,0:T(2,128)}, u32[]{:S(2)}) copy-start(f32[2,128]{1,0:T(2,128)} %param.14) | copy-start | bytes 3076
  40.4 2.7 %copy-start.33 = (f32[2,128]{1,0:T(2,128)S(1)}, f32[2,128]{1,0:T(2,128)}, u32[]{:S(2)}) copy-start(f32[2,128]{1,0:T(2,128)} %param.13) | copy-start | bytes 3076
  44.6 15.5 %copy-start.12 = (bf16[384,2,64]{2,0,1:T(8,128)(2,1)}, bf16[384,2,64]{2,0,1:T(8,128)(2,1)S(1)}, u32[]{:S(2)}) copy-start(bf16[384,2,64]{2,0,1:T(8,128)(2,1)S(1)} %get-tuple-element.9) | copy-start | bytes 294916
  44.6 16.2 %copy-start.10 = (bf16[384,2,64]{2,0,1:T(8,128)(2,1)}, bf16[384,2,64]{2,0,1:T(8,128)(2,1)S(1)}, u32[]{:S(2)}) copy-start(bf16[384,2,64]{2,0,1:T(8,128)(2,1)S(1)} %get-tuple-element.8) | copy-start | bytes 294916
  44.9 43.7 %copy-start.1 = (bf16[384,2,128]{0,2,1:T(8,128)(2,1)}, bf16[384,2,128]{0,2,1:T(8,128)(2,1)S(1)}, u32[]{:S(2)}) copy-start(bf16[384,2,128]{0,2,1:T(8,128)(2,1)S(1)} %copy.139) | copy-start | bytes 589828
  47.5 41.2 %copy-start.7 = (bf16[1,384,256]{1,2,0:T(8,128)(2,1)}, bf16[1,384,256]{1,2,0:T(8,128)(2,1)S(1)}, u32[]{:S(2)}) copy-start(bf16[1,384,256]{1,2,0:T(8,128)(2,1)S(1)} %fusion.20) | copy-start | bytes 589828
  48.3 13.2 %collective-permute-start.2 = (bf16[2,384,256]{1,2,0:T(8,128)(2,1)}, bf16[2,384,256]{1,2,0:T(8,128)(2,1)S(1)}, u32[]{:S(2)}, u32[]{:S(2)}) collective-permute-start(bf16[2,384,256]{1,2,0:T(8,128)(2,1)} %pad_maximum_fusion.2), channel_id=1, source_target_pairs={} | collective-permute-start | bytes 1179656 | tf_op jit(solution)/shard_map/ppermute | solution.py:21
  49.0 12.7 %collective-permute-start.3 = (bf16[2,384,256]{1,2,0:T(8,128)(2,1)}, bf16[2,384,256]{1,2,0:T(8,128)(2,1)}, u32[]{:S(2)}, u32[]{:S(2)}) collective-permute-start(bf16[2,384,256]{1,2,0:T(8,128)(2,1)} %pad_maximum_fusion.2), channel_id=1, source_target_pairs={{0,12},{1,13},{2,14},{3,15},{16,28},{17,29},{18,30},{19,31}} | collective-permute-start | bytes 1179656 | tf_op jit(solution)/shard_map/ppermute | solution.py:21
  52.4 27.8 %collective-permute-start.1 = (bf16[2,384,256]{1,2,0:T(8,128)(2,1)}, bf16[2,384,256]{1,2,0:T(8,128)(2,1)S(1)}, u32[]{:S(2)}, u32[]{:S(2)}) collective-permute-start(bf16[2,384,256]{1,2,0:T(8,128)(2,1)} %pad_maximum_fusion.2), channel_id=1, source_target_pairs={{0,8},{4,12},{1,9},{5,13},{2,10},{6,14},{3,11},{7,15},{16,24},{20,... | collective-permute-start | bytes 1179656 | tf_op jit(solution)/shard_map/ppermute | solution.py:21
  56.5 32.1 %collective-permute-start = (bf16[2,384,256]{1,2,0:T(8,128)(2,1)}, bf16[2,384,256]{1,2,0:T(8,128)(2,1)S(1)}, u32[]{:S(2)}, u32[]{:S(2)}) collective-permute-start(bf16[2,384,256]{1,2,0:T(8,128)(2,1)} %pad_maximum_fusion.2), channel_id=1, source_target_pairs={{0,4},{4,8},{8,12},{1,5},{5,9},{9,13},{2,6},{6,10},{10,14},{3,7},{... | collective-permute-start | bytes 1179656 | tf_op jit(solution)/shard_map/ppermute | solution.py:21
  80.1 8.5 %copy-start.15 = (bf16[2,384,256]{1,2,0:T(8,128)(2,1)}, bf16[2,384,256]{1,2,0:T(8,128)(2,1)S(1)}, u32[]{:S(2)}) copy-start(bf16[2,384,256]{1,2,0:T(8,128)(2,1)S(1)} %collective-permute-done.1) | copy-start | bytes 1179652
  88.6 0.7 copy-start.3
  95.9 0.9 copy-start.5
  97.1 0.6 copy-start.21
  99.2 2.5 %copy-start.18 = (bf16[96,4,2,64]{3,0,2,1:T(8,128)(2,1)S(1)}, bf16[96,4,2,64]{3,0,2,1:T(8,128)(2,1)}, u32[]{:S(2)}) copy-start(bf16[96,4,2,64]{3,0,2,1:T(8,128)(2,1)} %copy.145) | copy-start | bytes 294916
  99.2 2.5 %copy-start.20 = (pred[4,96,224]{2,1,0:T(8,128)(4,1)S(1)}, pred[4,96,224]{2,1,0:T(8,128)(4,1)}, u32[]{:S(2)}) copy-start(pred[4,96,224]{2,1,0:T(8,128)(4,1)} %broadcast_and_fusion.1) | copy-start | bytes 258052
  103.1 0.9 copy-start.16
  103.1 2.5 %copy-start.24 = (f32[4,2,96]{2,1,0:T(2,128)}, f32[4,2,96]{2,1,0:T(2,128)S(1)}, u32[]{:S(2)}) copy-start(f32[4,2,96]{2,1,0:T(2,128)S(1)} %get-tuple-element.28) | copy-start | bytes 9220
  104.0 1.6 %copy-start.26 = (f32[4,2,96]{2,1,0:T(2,128)}, f32[4,2,96]{2,1,0:T(2,128)S(1)}, u32[]{:S(2)}) copy-start(f32[4,2,96]{2,1,0:T(2,128)S(1)} %fusion.35) | copy-start | bytes 9220
  106.4 1.3 copy-start.6
  107.6 2.2 %copy-start.9 = (bf16[1,896,256]{1,2,0:T(8,128)(2,1)S(1)}, bf16[1,896,256]{1,2,0:T(8,128)(2,1)}, u32[]{:S(2)}) copy-start(bf16[1,896,256]{1,2,0:T(8,128)(2,1)} %get-tuple-element.5) | copy-start | bytes 1376260
  109.7 1.1 copy-start.17
  109.7 1.1 copy-start.25
  109.7 1.1 copy-start.27
  110.8 0.9 copy-start.2
  110.8 1.1 copy-start.4
  110.8 1.1 copy-start.8
  112.0 0.9 copy-start.11
  112.0 1.0 copy-start.13
  112.0 1.1 copy-start.19
  113.9 0.7 copy-start.28
  113.9 0.7 copy-start.29
  113.9 0.7 copy-start.22
  113.9 0.7 copy-start.23
  114.6 12.2 %copy-start.30 = (f32[384,2]{0,1:T(2,128)}, f32[384,2]{0,1:T(2,128)S(1)}, u32[]{:S(2)}) copy-start(f32[384,2]{0,1:T(2,128)S(1)} %log_add_fusion) | copy-start | bytes 9220
Sparse Core Ops, SparseCore 0:
  9.5 27.8 all-gather.1
where the time goes:
time: 136 us; the launch traced here: 134 us
  waiting for transfers between devices  46 us (34%)
  local copies, waits for them, and re-layouts  23.9 us (18%)
  matrix products  15.2 us (11%)
  between operations  14.8 us (11%)
  starting transfers between devices  12.8 us (9%)
  other arithmetic  12 us (9%)
  blocking collectives  9.02 us (7%)
    ppermute x4, waiting for transfers between devices, from_behind(): lax.ppermute(value, axis, [(source, source + steps) for source in range(i...  25.8 us
    all_gather x1, waiting for transfers between devices, local(): lax.all_gather(hidden, 'tp', axis=1, tiled=True).astype(jnp.float32)  19.5 us
    all_gather x1, blocking collectives, local(): lax.all_gather(attended, 'tp', axis=1, tiled=True)  9.02 us
    unnamed x81, local copies, waits for them, and re-layouts  8.51 us
    ppermute x4, starting transfers between devices, from_behind(): lax.ppermute(value, axis, [(source, source + steps) for source in range(i...  8.29 us
    dot_general x3, matrix products, add_product(): return jnp.dot(scaled, weight, preferred_element_type=jnp.float32)  5.79 us
    all_to_all x1, starting transfers between devices, local(): lax.all_to_all(w_out, 'tp', split_axis=1, concat_axis=0, tiled=True)  4.43 us
    dot_general x3, matrix products, local_branch(): jnp.einsum('rnqhd,rnkhd->rnhqk', query_blocks, key_blocks, preferred_elem...  3.85 us
  transfers between devices with their start and end apart: 6, of which 3 were waited for; matrix products, arithmetic and copies ran while one was open for 17% of the time, Pallas kernels for 0%

commit v1 on v0

v1 whole, which is shorter than its diff:
```python
import functools
import math

import jax
import jax.numpy as jnp
from jax import lax
from jax.experimental import pallas as pl
from jax.experimental.pallas import tpu as pltpu
from jax.sharding import PartitionSpec as P

KEYS_BEHIND = 128
DILATIONS = (1, 4, 16)
EPSILON = 1e-06
ROTARY_BASE = 500000.0
MASKED = -1e30
ROW_BLOCK = 128

VMEM = pl.BlockSpec(memory_space=pltpu.VMEM)
SMEM = pl.BlockSpec(memory_space=pltpu.SMEM)


def swap(value, distance):
    count = lax.axis_size("tp")
    return lax.ppermute(value, "tp", [(i, i ^ distance) for i in range(count)])


def shift(value, steps):
    count = lax.axis_size("sp")
    return lax.ppermute(value, "sp", [(s, s + steps) for s in range(count - steps)])


def gather_blocks(block):
    count = lax.axis_size("tp")
    blocks = {0: block}
    distance = count // 2
    while distance:
        for k in list(blocks):
            blocks[k ^ distance] = swap(blocks[k], distance)
        distance //= 2
    return [blocks[k] for k in range(count)]


def turn_tables(positions, head_width):
    inverse = ROTARY_BASE ** (-jnp.arange(0, head_width, 2, dtype=jnp.float32) / head_width)
    angles = positions[:, None] * inverse[None, :]
    cosine = jnp.cos(angles)
    sine = jnp.sin(angles)
    return jnp.concatenate([cosine, cosine], 1), jnp.concatenate([-sine, sine], 1)


def project_kernel(where, *refs, count, head_count, width):
    hidden = refs[:count]
    gain, wq, wk, wv, qg, kg, cosine, sine, q_out, kv_out = refs[count:]
    me = where[0]
    piece = hidden[0].shape[1]
    rows = hidden[0].shape[0]
    head_width = qg.shape[1]
    for start in range(0, rows, ROW_BLOCK):
        span = pl.ds(start, ROW_BLOCK)
        sums = [None, None, None]
        squares = None
        for k in range(count):
            source = me ^ k
            raw = hidden[k][span, :].astype(jnp.float32)
            scaled = (raw * gain[pl.ds(source, 1), :]).astype(jnp.bfloat16)
            part = jnp.sum(raw * raw, axis=1, keepdims=True)
            squares = part if squares is None else squares + part
            at = pl.ds(pl.multiple_of(source * piece, piece), piece)
            for n, weight in enumerate((wq, wk, wv)):
                product = jnp.dot(scaled, weight[at, :], preferred_element_type=jnp.float32)
                sums[n] = product if sums[n] is None else sums[n] + product
        scale = lax.rsqrt(squares / width + EPSILON)
        turn_c = cosine[span, :]
        turn_s = sine[span, :]
        for n, (gains, out) in enumerate(((qg, q_out), (kg, kv_out.at[0]))):
            total = sums[n] * scale
            for h in range(head_count):
                values = total[:, h * head_width : (h + 1) * head_width]
                mean = jnp.mean(values * values, axis=1, keepdims=True)
                values = values * lax.rsqrt(mean + EPSILON) * gains[h : h + 1, :]
                turned = values * turn_c + pltpu.roll(values, head_width // 2, 1) * turn_s
                out[span, h * head_width : (h + 1) * head_width] = turned.astype(jnp.bfloat16)
        kv_out.at[1][span, :] = (sums[2] * scale).astype(jnp.bfloat16)


def project(where, blocks, gain, weights, gains, tables):
    rows, piece = blocks[0].shape
    count = len(blocks)
    local_width = weights[0].shape[1]
    head_count = gains[0].shape[0]
    return pl.pallas_call(
        functools.partial(
            project_kernel, count=count, head_count=head_count, width=piece * count
        ),
        out_shape=(
            jax.ShapeDtypeStruct((rows, local_width), jnp.bfloat16),
            jax.ShapeDtypeStruct((2, rows, local_width), jnp.bfloat16),
        ),
        in_specs=[SMEM] + [VMEM] * (count + 8),
        out_specs=(VMEM, VMEM),
        name="project",
    )(where, *blocks, gain, *weights, *gains, *tables)


def pair_bias(rows, distance):
    row = lax.broadcasted_iota(jnp.int32, (rows, rows), 0)
    col = lax.broadcasted_iota(jnp.int32, (rows, rows), 1)
    behind = row - col + distance * rows
    times = jnp.zeros((rows, rows), jnp.int32)
    for dilation in DILATIONS:
        read = (behind >= 0) & (behind <= KEYS_BEHIND * dilation) & (behind % dilation == 0)
        times = times + read.astype(jnp.int32)
    return jnp.where(
        times == 0,
        MASKED,
        jnp.where(times == 3, math.log2(3.0), (times - 1).astype(jnp.float32)),
    )


def attend_kernel(where, *refs, distance, first, last, head_width, factor):
    if first:
        q, kv, bias = refs[:3]
        outs = refs[3:]
    else:
        q, kv, bias, top_in, sum_in, acc_in = refs[:6]
        outs = refs[6:]
    rows, local_width = q.shape
    head_count = local_width // head_width

    def work(active):
        for start in range(0, rows, ROW_BLOCK):
            span = pl.ds(start, ROW_BLOCK)
            keys = start + ROW_BLOCK if distance == 0 else rows
            for h in range(head_count):
                lanes = slice(h * head_width, (h + 1) * head_width)
                if not first:
                    top = top_in[span, h : h + 1]
                    total = sum_in[span, h : h + 1]
                    acc = acc_in[span, lanes]
                if active:
                    scores = lax.dot_general(
                        q[span, lanes],
                        kv[0, :keys, lanes],
                        (((1,), (1,)), ((), ())),
                        preferred_element_type=jnp.float32,
                    )
                    scores = scores * factor + bias[span, :keys]
                    peak = jnp.max(scores, axis=1, keepdims=True)
                    if not first:
                        peak = jnp.maximum(peak, top)
                    weights = jnp.exp2(scores - peak)
                    part = jnp.sum(weights, axis=1, keepdims=True)
                    out = jnp.dot(
                        weights.astype(jnp.bfloat16),
                        kv[1, :keys, lanes],
                        preferred_element_type=jnp.float32,
                    )
                    if not first:
                        decay = jnp.exp2(top - peak)
                        part = part + total * decay
                        out = out + acc * decay
                    top, total, acc = peak, part, out
                if last:
                    outs[0][span, lanes] = (acc / total).astype(jnp.bfloat16)
                    outs[1][span, h : h + 1] = top * math.log(2.0) + jnp.log(total)
                else:
                    outs[0][span, h : h + 1] = top
                    outs[1][span, h : h + 1] = total
                    outs[2][span, lanes] = acc

    if first:
        work(True)
    else:
        pl.when(where[1] >= distance)(lambda: work(True))
        pl.when(where[1] < distance)(lambda: work(False))


def attend(where, q, kv, bias, carry, distance, last, head_width):
    rows, local_width = q.shape
    head_count = local_width // head_width
    first = carry is None
    if last:
        shapes = (
            jax.ShapeDtypeStruct((rows, local_width), jnp.bfloat16),
            jax.ShapeDtypeStruct((rows, head_count), jnp.float32),
        )
    else:
        shapes = (
            jax.ShapeDtypeStruct((rows, head_count), jnp.float32),
            jax.ShapeDtypeStruct((rows, head_count), jnp.float32),
            jax.ShapeDtypeStruct((rows, local_width), jnp.float32),
        )
    extra = () if first else carry
    return pl.pallas_call(
        functools.partial(
            attend_kernel,
            distance=distance,
            first=first,
            last=last,
            head_width=head_width,
            factor=head_width ** (-0.5) * math.log2(math.e),
        ),
        out_shape=shapes,
        in_specs=[SMEM] + [VMEM] * (3 + len(extra)),
        out_specs=(VMEM,) * len(shapes),
        name=f"attend{distance}",
    )(where, q, kv, bias, *extra)


def mix_kernel(where, attended, *refs):
    pieces, out = refs[:-1], refs[-1]
    me = where[0]
    for start in range(0, out.shape[0], ROW_BLOCK):
        span = pl.ds(start, ROW_BLOCK)
        total = None
        for k, piece in enumerate(pieces):
            product = jnp.dot(
                attended[me ^ k, span, :], piece[...], preferred_element_type=jnp.float32
            )
            total = product if total is None else total + product
        out[span, :] = total.astype(jnp.bfloat16)


def local(hidden, norm_gain, w_query, w_key, w_value, query_gain, key_gain, w_out):
    rows, piece = hidden.shape
    head_width = query_gain.shape[1]
    count = lax.axis_size("tp")
    shards = lax.axis_size("sp")
    me = lax.axis_index("tp")
    shard = lax.axis_index("sp")
    where = jnp.stack([me, shard]).astype(jnp.int32)

    positions = (jnp.arange(rows, dtype=jnp.int32) + shard * rows).astype(jnp.float32)
    tables = turn_tables(positions, head_width)
    gain = norm_gain.astype(jnp.float32).reshape(count, piece)
    reach = -(-KEYS_BEHIND * DILATIONS[-1] // rows)
    distances = range(1, min(shards - 1, reach) + 1)

    blocks = gather_blocks(hidden)
    q, kv = project(
        where, blocks, gain, (w_query, w_key, w_value), (query_gain, key_gain), tables
    )
    w_late, _ = lax.optimization_barrier((w_out, kv))
    others = [shift(kv, d) for d in distances]

    columns = w_out.shape[1] // count
    slices = [
        lax.dynamic_slice_in_dim(w_late, (me ^ k) * columns, columns, axis=1) for k in range(count)
    ]
    pieces = [slices[0]] + [swap(slices[k], k) for k in range(1, count)]

    carry = attend(where, q, kv, pair_bias(rows, 0), None, 0, not others, head_width)
    for d, other in zip(distances, others):
        carry = attend(where, q, other, pair_bias(rows, d), carry, d, d == len(others), head_width)
    attended, log_total = carry

    gathered = lax.all_gather(attended, "tp", axis=0, tiled=False)
    mixed = pl.pallas_call(
        mix_kernel,
        out_shape=jax.ShapeDtypeStruct((rows, columns), jnp.bfloat16),
        in_specs=[SMEM] + [VMEM] * (1 + count),
        out_specs=VMEM,
        name="mix",
    )(where, gathered, *pieces)
    return mixed, log_total


def solution(mesh):
    placed = (
        P(("grp", "sp"), "tp"),
        P(),
        P(None, "tp"),
        P(None, "tp"),
        P(None, "tp"),
        P("tp", None),
        P("tp", None),
        P("tp", None),
    )
    return jax.shard_map(
        local,
        mesh=mesh,
        in_specs=placed,
        out_specs=(P(("grp", "sp"), "tp"), P(("grp", "sp"), "tp")),
        check_vma=False,
    )
```

time: 136 us -> 86.2 us (0.63)
  the two profiles are of different devices: /device:TPU:15 before, /device:TPU:29 now
where the time goes in v1:
time: 86.2 us; the launch traced here: 85.8 us
  Pallas kernels  25.7 us (30%)
  waiting for transfers between devices  24.1 us (28%)
  starting transfers between devices  11.2 us (13%)
  blocking collectives  9.8 us (11%)
  other arithmetic  7.28 us (8%)
  local copies, waits for them, and re-layouts  6.96 us (8%)
    ppermute x3, waiting for transfers between devices, shift(): lax.ppermute(value, 'sp', [(s, s + steps) for s in range(count - steps)])  19.1 us
    pallas_call x4, Pallas kernels, attend(): pl.pallas_call(functools.partial(attend_kernel, distance=distance, first=...  17.5 us
    all_gather x1, blocking collectives, local(): gathered = lax.all_gather(attended, 'tp', axis=0, tiled=False)  9.8 us
    ppermute x6, starting transfers between devices, swap(): return lax.ppermute(value, 'tp', [(i, i ^ distance) for i in range(count)])  7.22 us
    unnamed x25, local copies, waits for them, and re-layouts  5.55 us
    pallas_call x1, Pallas kernels, project(): pl.pallas_call(functools.partial(project_kernel, count=count, head_count=...  5.5 us
    ppermute x6, waiting for transfers between devices, swap(): return lax.ppermute(value, 'tp', [(i, i ^ distance) for i in range(count)])  5.03 us
    select_n x4, other arithmetic, pair_bias(): jnp.where(times == 0, MASKED, jnp.where(times == 3, math.log2(3.0), (time...  4.9 us
  transfers between devices with their start and end apart: 9, of which 3 were waited for; matrix products, arithmetic and copies ran while one was open for 12% of the time, Pallas kernels for 20%

profile of v1, /device:TPU:29, one launch (start us, length us, event | category | flops | bytes accessed | tf_op | source)
XLA Modules:
  0.0 85.8 jit_solution(1958526295767094214)
XLA Ops:
  0.6 1.3 %collective-permute-start.1 = (bf16[384,512]{1,0:T(8,128)(2,1)}, bf16[384,512]{1,0:T(8,128)(2,1)S(1)}, u32[]{:S(2)}, u32[]{:S(2)}) collective-permute-start(bf16[384,512]{1,0:T(8,128)(2,1)} %refs_0_.1), channel_id=1, source_target_pairs={{0,2},{1,3},{2,0},{3,1},{4,6},{5,7},{6,4},{7,5},{8,10},{9,11},{10,... | collective-permute-start | bytes 1179656 | tf_op jit(solution)/shard_map/ppermute | solution.py:24
  1.9 1.0 %collective-permute-start = (bf16[384,512]{1,0:T(8,128)(2,1)}, bf16[384,512]{1,0:T(8,128)(2,1)S(1)}, u32[]{:S(2)}, u32[]{:S(2)}) collective-permute-start(bf16[384,512]{1,0:T(8,128)(2,1)} %refs_0_.1), channel_id=1, source_target_pairs={{0,1},{1,0},{2,3},{3,2},{4,5},{5,4},{6,7},{7,6},{8,9},{9,8},{10,11... | collective-permute-start | bytes 1179656 | tf_op jit(solution)/shard_map/ppermute | solution.py:24
  2.9 0.0 copy-start.11
  2.9 0.7 copy-done.11
  3.6 0.6 reshape.24.refs_4_
  4.2 0.8 fusion.68
  4.9 0.9 %pad_maximum_fusion = (f32[384,128]{1,0:T(8,128)}, f32[384,128]{1,0:T(8,128)}) fusion(f32[384,64]{1,0:T(8,128)S(1)} %get-tuple-element.38, f32[384,64]{1,0:T(8,128)S(1)} %get-tuple-element.37, f32[384,64]{1,0:T(8,128)S(1)} %get-tuple-element.36), kind=kLoop, calls=%fused_computation.99 | loop fusion | flops 98304 | bytes 688128 | tf_op jit(solution)/shard_map/concatenate | solution.py:48
  5.9 5.0 %collective-permute-done.1.refs_2_ = bf16[384,512]{1,0:T(8,128)(2,1)S(1)} collective-permute-done((bf16[384,512]{1,0:T(8,128)(2,1)}, bf16[384,512]{1,0:T(8,128)(2,1)S(1)}, u32[]{:S(2)}, u32[]{:S(2)}) %collective-permute-start.1) | collective-permute-done | bytes 393248 | tf_op jit(solution)/shard_map/ppermute | solution.py:24
  10.9 1.5 %collective-permute-start.2 = (bf16[384,512]{1,0:T(8,128)(2,1)S(1)}, bf16[384,512]{1,0:T(8,128)(2,1)S(1)}, u32[]{:S(2)}, u32[]{:S(2)}) collective-permute-start(bf16[384,512]{1,0:T(8,128)(2,1)S(1)} %collective-permute-done.1.refs_2_), channel_id=1, source_target_pairs={{0,1},{1,0},{2,3},{3,2},{4,5},{5,4},{6,7},{7,6},{8,9},{9,8},{10,11... | collective-permute-start | bytes 1179656 | tf_op jit(solution)/shard_map/ppermute | solution.py:24
  12.4 0.7 pad_add_fusion.where
  13.1 1.4 %select_select_fusion.1.refs_2_ = f32[384,384]{1,0:T(8,128)} fusion(), kind=kLoop, calls=%fused_computation.32 | loop fusion | flops 6340608 | bytes 589824 | tf_op jit(solution)/shard_map/jit(_where)/select_n | solution.py:113
  14.5 1.2 %select_select_fusion.2.refs_2_ = f32[384,384]{1,0:T(8,128)} fusion(), kind=kLoop, calls=%fused_computation.36 | loop fusion | flops 6340608 | bytes 589824 | tf_op jit(solution)/shard_map/jit(_where)/select_n | solution.py:113
  15.7 0.0 copy-done.1
  15.7 0.0 collective-permute-done.refs_1_
  15.7 0.0 collective-permute-done.2.refs_3_
  15.7 0.0 copy-start.3
  15.7 0.7 copy-done.2
  16.4 0.1 copy-done.3
  16.5 5.5 %project.1 = (bf16[384,256]{1,0:T(8,128)(2,1)}, bf16[2,384,256]{2,1,0:T(8,128)(2,1)}) custom-call(s32[2]{0:T(128)} %pad_add_fusion.where, bf16[384,512]{1,0:T(8,128)(2,1)} %refs_0_.1, bf16[384,512]{1,0:T(8,128)(2,1)} %copy-done.2, bf16[384,512]{1,0:T(8,128)(2,1)} %copy-done.1, bf16[384,512]{1,0:T(8,128)(2,1)} %copy-done.3, f32[4,512]{1,0:T(4,128)} %reshape.24.refs_4_, ...), custom_call_target="tpu_custom_call" | custom-call | tf_op jit(solution)/shard_map/project/pallas_call | solution.py:91
  22.0 1.4 %collective-permute-start.5 = (bf16[2,384,256]{2,1,0:T(8,128)(2,1)}, bf16[2,384,256]{2,1,0:T(8,128)(2,1)S(1)}, u32[]{:S(2)}, u32[]{:S(2)}) collective-permute-start(bf16[2,384,256]{2,1,0:T(8,128)(2,1)} %get-tuple-element.17.refs_1_), channel_id=1, source_target_pairs={{0,4},{4,8},{8,12},{1,5},{5,9},{9,13},{2,6},{6,10},{10,14},{3,7},{... | collective-permute-start | bytes 1179656 | tf_op jit(solution)/shard_map/ppermute | solution.py:29
  23.5 1.3 %collective-permute-start.4 = (bf16[2,384,256]{2,1,0:T(8,128)(2,1)}, bf16[2,384,256]{2,1,0:T(8,128)(2,1)S(1)}, u32[]{:S(2)}, u32[]{:S(2)}) collective-permute-start(bf16[2,384,256]{2,1,0:T(8,128)(2,1)} %get-tuple-element.17.refs_1_), channel_id=1, source_target_pairs={{0,8},{4,12},{1,9},{5,13},{2,10},{6,14},{3,11},{7,15},{16,24},{20,... | collective-permute-start | bytes 1179656 | tf_op jit(solution)/shard_map/ppermute | solution.py:29
  24.8 1.3 %collective-permute-start.3 = (bf16[2,384,256]{2,1,0:T(8,128)(2,1)}, bf16[2,384,256]{2,1,0:T(8,128)(2,1)S(1)}, u32[]{:S(2)}, u32[]{:S(2)}) collective-permute-start(bf16[2,384,256]{2,1,0:T(8,128)(2,1)} %get-tuple-element.17.refs_1_), channel_id=1, source_target_pairs={{0,12},{1,13},{2,14},{3,15},{16,28},{17,29},{18,30},{19,31}} | collective-permute-start | bytes 1179656 | tf_op jit(solution)/shard_map/ppermute | solution.py:29
  26.1 1.2 %select_select_fusion.refs_2_ = f32[384,384]{1,0:T(8,128)} fusion(), kind=kLoop, calls=%fused_computation.28 | loop fusion | flops 6193152 | bytes 589824 | tf_op jit(solution)/shard_map/jit(_where)/select_n | solution.py:113
  27.3 1.2 %select_select_fusion.3.refs_2_ = f32[384,384]{1,0:T(8,128)} fusion(), kind=kLoop, calls=%fused_computation.40 | loop fusion | flops 6340608 | bytes 589824 | tf_op jit(solution)/shard_map/jit(_where)/select_n | solution.py:113
  28.4 0.0 copy-done
  28.4 0.8 constant_dynamic-slice_fusion
  29.2 0.1 collective-permute-start.6
  29.3 1.2 %collective-permute-start.7 = (bf16[256,512]{1,0:T(8,128)(2,1)S(1)}, bf16[256,512]{1,0:T(8,128)(2,1)S(1)}, u32[]{:S(2)}, u32[]{:S(2)}) collective-permute-start(bf16[256,512]{1,0:T(8,128)(2,1)S(1)} %get-tuple-element.33), channel_id=1, source_target_pairs={{0,2},{1,3},{2,0},{3,1},{4,6},{5,7},{6,4},{7,5},{8,10},{9,11},{10,... | collective-permute-start | bytes 786440 | tf_op jit(solution)/shard_map/ppermute | solution.py:24
  30.5 3.7 %attend0.1 = (f32[384,2]{1,0:T(8,128)}, f32[384,2]{1,0:T(8,128)}, f32[384,256]{1,0:T(8,128)}) custom-call(s32[2]{0:T(128)} %pad_add_fusion.where, bf16[384,256]{1,0:T(8,128)(2,1)} %get-tuple-element.16.refs_0_, bf16[2,384,256]{2,1,0:T(8,128)(2,1)} %get-tuple-element.17.refs_1_, f32[384,384]{1,0:T(8,128)} %select_select_fusion.refs_2_), custom_call_target="tpu_custom_call" | custom-call | tf_op jit(solution)/shard_map/attend0/pallas_call | solution.py:194
  34.2 0.7 collective-permute-done.5.refs_1_
  34.9 2.2 %collective-permute-start.8 = (bf16[256,512]{1,0:T(8,128)(2,1)S(1)}, bf16[256,512]{1,0:T(8,128)(2,1)S(1)}, u32[]{:S(2)}, u32[]{:S(2)}) collective-permute-start(bf16[256,512]{1,0:T(8,128)(2,1)S(1)} %get-tuple-element.32), channel_id=1, source_target_pairs={{0,3},{1,2},{2,1},{3,0},{4,7},{5,6},{6,5},{7,4},{8,11},{9,10},{10,... | collective-permute-start | bytes 786440 | tf_op jit(solution)/shard_map/ppermute | solution.py:24
  37.1 4.6 %attend1.1 = (f32[384,2]{1,0:T(8,128)}, f32[384,2]{1,0:T(8,128)}, f32[384,256]{1,0:T(8,128)}) custom-call(s32[2]{0:T(128)} %pad_add_fusion.where, bf16[384,256]{1,0:T(8,128)(2,1)} %get-tuple-element.16.refs_0_, bf16[2,384,256]{2,1,0:T(8,128)(2,1)} %copy-done.6, f32[384,384]{1,0:T(8,128)} %select_select_fusion.1.refs_2_, f32[384,2]{1,0:T(8,128)} %get-tuple-element.18.refs_3_, ...), custom_call_target="tpu_custom_call" | custom-call | tf_op jit(solution)/shard_map/attend1/pallas_call | solution.py:194
  41.7 18.4 %collective-permute-done.4.refs_1_ = bf16[2,384,256]{2,1,0:T(8,128)(2,1)S(1)} collective-permute-done((bf16[2,384,256]{2,1,0:T(8,128)(2,1)}, bf16[2,384,256]{2,1,0:T(8,128)(2,1)S(1)}, u32[]{:S(2)}, u32[]{:S(2)}) %collective-permute-start.4) | collective-permute-done | bytes 393248 | tf_op jit(solution)/shard_map/ppermute | solution.py:29
  60.1 0.7 copy-done.5
  60.8 4.6 %attend2.1 = (f32[384,2]{1,0:T(8,128)}, f32[384,2]{1,0:T(8,128)}, f32[384,256]{1,0:T(8,128)}) custom-call(s32[2]{0:T(128)} %pad_add_fusion.where, bf16[384,256]{1,0:T(8,128)(2,1)} %get-tuple-element.16.refs_0_, bf16[2,384,256]{2,1,0:T(8,128)(2,1)} %copy-done.5, f32[384,384]{1,0:T(8,128)} %select_select_fusion.2.refs_2_, f32[384,2]{1,0:T(8,128)} %get-tuple-element.21.refs_3_, ...), custom_call_target="tpu_custom_call" | custom-call | tf_op jit(solution)/shard_map/attend2/pallas_call | solution.py:194
  65.4 0.0 collective-permute-done.3.refs_1_
  65.4 0.7 copy-done.4
  66.2 4.6 %attend3.1 = (bf16[384,256]{1,0:T(8,128)(2,1)}, f32[384,2]{1,0:T(8,128)}) custom-call(s32[2]{0:T(128)} %pad_add_fusion.where, bf16[384,256]{1,0:T(8,128)(2,1)} %get-tuple-element.16.refs_0_, bf16[2,384,256]{2,1,0:T(8,128)(2,1)} %copy-done.4, f32[384,384]{1,0:T(8,128)} %select_select_fusion.3.refs_2_, f32[384,2]{1,0:T(8,128)} %get-tuple-element.24.refs_3_, ...), custom_call_target="tpu_custom_call" | custom-call | tf_op jit(solution)/shard_map/attend3/pallas_call | solution.py:194
  70.7 1.7 %copy.10 = f32[384,2]{0,1:T(2,128)} copy(f32[384,2]{1,0:T(8,128)} %get-tuple-element.31) | data formatting | bytes 6144
  72.4 9.8 %all-gather = bf16[1536,256]{1,0:T(8,128)(2,1)} all-gather(bf16[384,256]{1,0:T(8,128)(2,1)S(1)} %copy-done.10), channel_id=2, replica_groups=mesh['grp'=2,'sp'=4,'tp'=4] {'tp'}, dimensions={0}, use_global_device_ids=true | all-gather | bytes 983040 | tf_op jit(solution)/shard_map/all_gather | solution.py:257
  82.2 0.0 collective-permute-done.6.refs_1_
  82.2 0.0 collective-permute-done.7.refs_2_
  82.2 0.0 collective-permute-done.8.refs_3_
  82.2 0.0 copy-start.9
  82.2 0.7 copy-done.7
  82.9 0.1 copy-done.8
  83.0 0.1 copy-done.9
  83.1 2.8 %mix.1 = bf16[384,512]{1,0:T(8,128)(2,1)} custom-call(s32[2]{0:T(128)} %pad_add_fusion.where, bf16[4,384,256]{2,1,0:T(8,128)(2,1)} %bitcast.3, bf16[256,512]{1,0:T(8,128)(2,1)} %get-tuple-element.35.refs_0_, bf16[256,512]{1,0:T(8,128)(2,1)} %copy-done.7, bf16[256,512]{1,0:T(8,128)(2,1)} %copy-done.8, bf16[256,512]{1,0:T(8,128)(2,1)} %copy-done.9), custom_call_target="tpu_custom_call" | custom-call | tf_op jit(solution)/shard_map/mix/pallas_call | solution.py:258
  (13 shorter events, 0.0 us)
Async XLA Ops:
  0.6 10.3 %collective-permute-start.1 = (bf16[384,512]{1,0:T(8,128)(2,1)}, bf16[384,512]{1,0:T(8,128)(2,1)S(1)}, u32[]{:S(2)}, u32[]{:S(2)}) collective-permute-start(bf16[384,512]{1,0:T(8,128)(2,1)} %refs_0_.1), channel_id=1, source_target_pairs={{0,2},{1,3},{2,0},{3,1},{4,6},{5,7},{6,4},{7,5},{8,10},{9,11},{10,... | collective-permute-start | bytes 1179656 | tf_op jit(solution)/shard_map/ppermute | solution.py:24
  1.9 13.8 %collective-permute-start = (bf16[384,512]{1,0:T(8,128)(2,1)}, bf16[384,512]{1,0:T(8,128)(2,1)S(1)}, u32[]{:S(2)}, u32[]{:S(2)}) collective-permute-start(bf16[384,512]{1,0:T(8,128)(2,1)} %refs_0_.1), channel_id=1, source_target_pairs={{0,1},{1,0},{2,3},{3,2},{4,5},{5,4},{6,7},{7,6},{8,9},{9,8},{10,11... | collective-permute-start | bytes 1179656 | tf_op jit(solution)/shard_map/ppermute | solution.py:24
  2.9 0.7 copy-start.11
  10.9 4.8 %copy-start.1 = (bf16[384,512]{1,0:T(8,128)(2,1)}, bf16[384,512]{1,0:T(8,128)(2,1)S(1)}, u32[]{:S(2)}) copy-start(bf16[384,512]{1,0:T(8,128)(2,1)S(1)} %collective-permute-done.1.refs_2_) | copy-start | bytes 1179652
  10.9 4.8 %collective-permute-start.2 = (bf16[384,512]{1,0:T(8,128)(2,1)S(1)}, bf16[384,512]{1,0:T(8,128)(2,1)S(1)}, u32[]{:S(2)}, u32[]{:S(2)}) collective-permute-start(bf16[384,512]{1,0:T(8,128)(2,1)S(1)} %collective-permute-done.1.refs_2_), channel_id=1, source_target_pairs={{0,1},{1,0},{2,3},{3,2},{4,5},{5,4},{6,7},{7,6},{8,9},{9,8},{10,11... | collective-permute-start | bytes 1179656 | tf_op jit(solution)/shard_map/ppermute | solution.py:24
  15.7 0.7 copy-start.2
  15.7 0.9 %copy-start.3 = (bf16[384,512]{1,0:T(8,128)(2,1)}, bf16[384,512]{1,0:T(8,128)(2,1)S(1)}, u32[]{:S(2)}) copy-start(bf16[384,512]{1,0:T(8,128)(2,1)S(1)} %collective-permute-done.2.refs_3_) | copy-start | bytes 1179652
  22.0 6.4 %copy-start = (bf16[256,2048]{1,0:T(8,128)(2,1)S(1)}, bf16[256,2048]{1,0:T(8,128)(2,1)}, u32[]{:S(2)}) copy-start(bf16[256,2048]{1,0:T(8,128)(2,1)} %param.15) | copy-start | bytes 3145732
  22.0 12.8 %collective-permute-start.5 = (bf16[2,384,256]{2,1,0:T(8,128)(2,1)}, bf16[2,384,256]{2,1,0:T(8,128)(2,1)S(1)}, u32[]{:S(2)}, u32[]{:S(2)}) collective-permute-start(bf16[2,384,256]{2,1,0:T(8,128)(2,1)} %get-tuple-element.17.refs_1_), channel_id=1, source_target_pairs={{0,4},{4,8},{8,12},{1,5},{5,9},{9,13},{2,6},{6,10},{10,14},{3,7},{... | collective-permute-start | bytes 1179656 | tf_op jit(solution)/shard_map/ppermute | solution.py:29
  23.5 36.6 %collective-permute-start.4 = (bf16[2,384,256]{2,1,0:T(8,128)(2,1)}, bf16[2,384,256]{2,1,0:T(8,128)(2,1)S(1)}, u32[]{:S(2)}, u32[]{:S(2)}) collective-permute-start(bf16[2,384,256]{2,1,0:T(8,128)(2,1)} %get-tuple-element.17.refs_1_), channel_id=1, source_target_pairs={{0,8},{4,12},{1,9},{5,13},{2,10},{6,14},{3,11},{7,15},{16,24},{20,... | collective-permute-start | bytes 1179656 | tf_op jit(solution)/shard_map/ppermute | solution.py:29
  24.8 40.6 %collective-permute-start.3 = (bf16[2,384,256]{2,1,0:T(8,128)(2,1)}, bf16[2,384,256]{2,1,0:T(8,128)(2,1)S(1)}, u32[]{:S(2)}, u32[]{:S(2)}) collective-permute-start(bf16[2,384,256]{2,1,0:T(8,128)(2,1)} %get-tuple-element.17.refs_1_), channel_id=1, source_target_pairs={{0,12},{1,13},{2,14},{3,15},{16,28},{17,29},{18,30},{19,31}} | collective-permute-start | bytes 1179656 | tf_op jit(solution)/shard_map/ppermute | solution.py:29
  29.2 53.0 %collective-permute-start.6 = (bf16[256,512]{1,0:T(8,128)(2,1)S(1)}, bf16[256,512]{1,0:T(8,128)(2,1)S(1)}, u32[]{:S(2)}, u32[]{:S(2)}) collective-permute-start(bf16[256,512]{1,0:T(8,128)(2,1)S(1)} %get-tuple-element.34), channel_id=1, source_target_pairs={{0,1},{1,0},{2,3},{3,2},{4,5},{5,4},{6,7},{7,6},{8,9},{9,8},{10,11... | collective-permute-start | bytes 786440 | tf_op jit(solution)/shard_map/ppermute | solution.py:24
  29.3 52.9 %collective-permute-start.7 = (bf16[256,512]{1,0:T(8,128)(2,1)S(1)}, bf16[256,512]{1,0:T(8,128)(2,1)S(1)}, u32[]{:S(2)}, u32[]{:S(2)}) collective-permute-start(bf16[256,512]{1,0:T(8,128)(2,1)S(1)} %get-tuple-element.33), channel_id=1, source_target_pairs={{0,2},{1,3},{2,0},{3,1},{4,6},{5,7},{6,4},{7,5},{8,10},{9,11},{10,... | collective-permute-start | bytes 786440 | tf_op jit(solution)/shard_map/ppermute | solution.py:24
  34.9 2.2 %copy-start.6 = (bf16[2,384,256]{2,1,0:T(8,128)(2,1)}, bf16[2,384,256]{2,1,0:T(8,128)(2,1)S(1)}, u32[]{:S(2)}) copy-start(bf16[2,384,256]{2,1,0:T(8,128)(2,1)S(1)} %collective-permute-done.5.refs_1_) | copy-start | bytes 1179652
  34.9 47.3 %collective-permute-start.8 = (bf16[256,512]{1,0:T(8,128)(2,1)S(1)}, bf16[256,512]{1,0:T(8,128)(2,1)S(1)}, u32[]{:S(2)}, u32[]{:S(2)}) collective-permute-start(bf16[256,512]{1,0:T(8,128)(2,1)S(1)} %get-tuple-element.32), channel_id=1, source_target_pairs={{0,3},{1,2},{2,1},{3,0},{4,7},{5,6},{6,5},{7,4},{8,11},{9,10},{10,... | collective-permute-start | bytes 786440 | tf_op jit(solution)/shard_map/ppermute | solution.py:24
  60.0 0.7 copy-start.5
  65.4 0.7 copy-start.4
  70.7 1.7 %copy-start.10 = (bf16[384,256]{1,0:T(8,128)(2,1)S(1)}, bf16[384,256]{1,0:T(8,128)(2,1)}, u32[]{:S(2)}) copy-start(bf16[384,256]{1,0:T(8,128)(2,1)} %get-tuple-element.27) | copy-start | bytes 589828
  82.2 0.7 copy-start.7
  82.2 0.8 copy-start.8
  82.2 0.9 copy-start.9

commit v2 on v0

v2 whole, which is shorter than its diff:
```python
import functools
import math

import jax
import jax.numpy as jnp
from jax import lax
from jax.experimental import pallas as pl
from jax.experimental.pallas import tpu as pltpu
from jax.sharding import PartitionSpec as P

KEYS_BEHIND = 128
DILATIONS = (1, 4, 16)
EPSILON = 1e-06
ROTARY_BASE = 500000.0
MASKED = -1e30
LANES = 128
LOG2_E = math.log2(math.e)

VMEM = pl.BlockSpec(memory_space=pltpu.VMEM)
SMEM = pl.BlockSpec(memory_space=pltpu.SMEM)


def shape_of(shape, dtype):
    return jax.ShapeDtypeStruct(shape, dtype)


def call(body, name, where, operands, outs, limit=24 << 20):
    return pl.pallas_call(
        body,
        out_shape=tuple(outs),
        in_specs=[SMEM] + [VMEM] * len(operands),
        out_specs=(VMEM,) * len(outs),
        compiler_params=pltpu.CompilerParams(vmem_limit_bytes=limit),
        name=name,
    )(where, *operands)


def wide(column):
    return jnp.broadcast_to(column, (column.shape[0], LANES))


def pair_bias(rows, distance):
    row = lax.broadcasted_iota(jnp.int32, (rows, rows), 0)
    col = lax.broadcasted_iota(jnp.int32, (rows, rows), 1)
    behind = row - col + distance * rows
    times = jnp.zeros((rows, rows), jnp.int32)
    for dilation in DILATIONS:
        read = (behind >= 0) & (behind <= KEYS_BEHIND * dilation)
        read = read & ((behind & (dilation - 1)) == 0)
        times = times + read.astype(jnp.int32)
    return jnp.where(
        times == 0,
        MASKED,
        jnp.where(times == 3, math.log2(3.0), (times - 1).astype(jnp.float32)),
    )


def sums_of(where, hidden, gain, weights, offsets):
    me = where[0]
    sums = [None] * len(weights)
    squares = None
    for block, k in zip(hidden, offsets):
        piece = block.shape[1]
        source = me ^ k
        raw = block[...].astype(jnp.float32)
        scaled = (raw * gain[pl.ds(source, 1), :]).astype(jnp.bfloat16)
        part = jnp.sum(raw * raw, axis=1, keepdims=True)
        squares = part if squares is None else squares + part
        at = pl.ds(pl.multiple_of(source * piece, piece), piece)
        for n, weight in enumerate(weights):
            product = jnp.dot(scaled, weight[at, :], preferred_element_type=jnp.float32)
            sums[n] = product if sums[n] is None else sums[n] + product
    return sums, squares


def early_kernel(where, *refs, offsets, kinds, biases):
    count = len(offsets)
    hidden = refs[:count]
    gain = refs[count]
    weights = refs[count + 1 : count + 1 + kinds]
    outs = refs[count + 1 + kinds :]
    sums, squares = sums_of(where, hidden, gain, weights, offsets)
    for out, total in zip(outs[:kinds], sums):
        out[...] = total
    outs[kinds][...] = wide(squares)
    for d, out in zip(biases, outs[kinds + 1 :]):
        out[...] = pair_bias(out.shape[0], d)


def head_turn(values, gains, cosine, sine):
    mean = jnp.mean(values * values, axis=1, keepdims=True)
    values = values * lax.rsqrt(mean + EPSILON) * gains
    return values * cosine + pltpu.roll(values, values.shape[1] // 2, 1) * sine


def late_kernel(where, *refs, offsets, kinds, width):
    count = len(offsets)
    hidden = refs[:count]
    gain = refs[count]
    weights = refs[count + 1 : count + 1 + kinds]
    rest = refs[count + 1 + kinds :]
    before = rest[:kinds]
    squares_before = rest[kinds]
    gains = rest[kinds + 1 : 2 * kinds]
    cosine, sine = rest[2 * kinds : 2 * kinds + 2]
    outs = rest[2 * kinds + 2 :]
    sums, squares = sums_of(where, hidden, gain, weights, offsets)
    scale = lax.rsqrt((squares + squares_before[...]) / width + EPSILON)
    head_width = gains[0].shape[1]
    turn_c = cosine[...]
    turn_s = sine[...]
    for n in range(kinds):
        for start in range(0, sums[n].shape[1], head_width):
            lanes = slice(start, start + head_width)
            h = start // head_width
            values = (sums[n][:, lanes] + before[n][:, lanes]) * scale
            if n < kinds - 1:
                values = head_turn(values, gains[n][h : h + 1, :], turn_c, turn_s)
            outs[n][:, lanes] = values.astype(jnp.bfloat16)


def softmax_part(q, blocks, lanes, factor):
    scores = []
    for key, _, bias in blocks:
        product = lax.dot_general(
            q[:, lanes], key[:, lanes], (((1,), (1,)), ((), ())), preferred_element_type=jnp.float32
        )
        scores.append(product * factor + bias)
    top = functools.reduce(
        jnp.maximum, [jnp.max(s, axis=1, keepdims=True) for s in scores]
    )
    total = None
    acc = None
    for s, (_, value, _) in zip(scores, blocks):
        weights = jnp.exp2(s - top)
        part = jnp.sum(weights, axis=1, keepdims=True)
        out = jnp.dot(
            weights.astype(jnp.bfloat16), value[:, lanes], preferred_element_type=jnp.float32
        )
        total = part if total is None else total + part
        acc = out if acc is None else acc + out
    return top, total, acc


def merge(parts):
    top = functools.reduce(jnp.maximum, [part[0] for part in parts])
    total = None
    acc = None
    for part_top, part_total, part_acc in parts:
        decay = jnp.exp2(part_top - top)
        total = part_total * decay if total is None else total + part_total * decay
        acc = part_acc * decay if acc is None else acc + part_acc * decay
    return acc / total, top + jnp.log2(total)


def head_lanes(q, head_width):
    count = q.shape[1] // head_width
    return [slice(h * head_width, (h + 1) * head_width) for h in range(count)]


def part_kernel(where, q, key, value, bias, tops, totals, accs, *, head_width, factor):
    for lanes in head_lanes(q, head_width):
        blocks = [(key, value, bias[...])]
        top, total, acc = softmax_part(q, blocks, lanes, factor)
        tops[:, lanes] = wide(top)
        totals[:, lanes] = wide(total)
        accs[:, lanes] = acc


def help_kernel(where, q, *refs, blocks, head_width, factor, helper):
    out, logs = refs[3 * blocks :]

    @pl.when(where[1] == helper)
    def _():
        for h, lanes in enumerate(head_lanes(q, head_width)):
            ready = [(refs[3 * n], refs[3 * n + 1], refs[3 * n + 2][...]) for n in range(blocks)]
            top, total, acc = softmax_part(q, ready, lanes, factor)
            out[:, lanes] = (acc / total).astype(jnp.bfloat16)
            logs[h : h + 1, :] = wide(top + jnp.log2(total)).T[:1, :]


def final_kernel(where, q, *refs, far, only, helped, head_width, factor):
    shard = where[1]
    near = refs[:6]
    kvs = refs[6 : 6 + 3 * len(far)]
    given = refs[6 + 3 * len(far) : -2]
    attended, logs = refs[-2:]
    rows = q.shape[0]

    def finish(use_far, use_given):
        for h, lanes in enumerate(head_lanes(q, head_width)):
            before = jnp.where(shard >= 1, near[3][:, lanes], MASKED)
            parts = [
                (near[0][:, lanes], near[1][:, lanes], near[2][:, lanes]),
                (before, near[4][:, lanes], near[5][:, lanes]),
            ]
            if use_far:
                blocks = [
                    (
                        kvs[3 * n],
                        kvs[3 * n + 1],
                        jnp.where(shard >= d, kvs[3 * n + 2][...], MASKED),
                    )
                    for n, d in enumerate(far)
                ]
                top, total, acc = softmax_part(q, blocks, lanes, factor)
                parts.append((wide(top), wide(total), acc))
            if use_given:
                top = jnp.broadcast_to(given[1][h : h + 1, :], (LANES, rows)).T
                parts.append((top, jnp.ones_like(top), given[0][:, lanes].astype(jnp.float32)))
            out, log_sum = merge(parts)
            attended[:, lanes] = out.astype(jnp.bfloat16)
            logs[h : h + 1, :] = (log_sum * math.log(2.0)).T[:1, :]

    with_far = (shard == only) if only is not None else (shard >= 2)
    with_given = (shard == helped) if helped is not None else (shard < 0)
    if far:
        pl.when(with_far)(lambda: finish(True, False))
    if helped is not None:
        pl.when(with_given)(lambda: finish(False, True))
    pl.when(jnp.logical_not(with_far | with_given))(lambda: finish(False, False))


def mix_kernel(where, attended, *refs):
    pieces, out = refs[:-1], refs[-1]
    me = where[0]
    total = None
    for k, piece in enumerate(pieces):
        product = jnp.dot(attended[me ^ k], piece[...], preferred_element_type=jnp.float32)
        total = product if total is None else total + product
    out[...] = total.astype(jnp.bfloat16)


def swap(value, distance):
    count = lax.axis_size("tp")
    return lax.ppermute(value, "tp", [(i, i ^ distance) for i in range(count)])


def behind(value, steps):
    count = lax.axis_size("sp")
    return lax.ppermute(value, "sp", [(s, s + steps) for s in range(count - steps)])


def near_blocks(block):
    blocks = {0: block}
    distance = lax.axis_size("tp") // 4
    while distance:
        for k in list(blocks):
            blocks[k ^ distance] = swap(blocks[k], distance)
        distance //= 2
    return [blocks[k] for k in sorted(blocks)]


def turn_tables(positions, head_width):
    inverse = ROTARY_BASE ** (-jnp.arange(0, head_width, 2, dtype=jnp.float32) / head_width)
    angles = positions[:, None] * inverse[None, :]
    cosine = jnp.cos(angles)
    sine = jnp.sin(angles)
    return jnp.concatenate([cosine, cosine], 1), jnp.concatenate([-sine, sine], 1)


def local(hidden, norm_gain, w_query, w_key, w_value, query_gain, key_gain, w_out):
    rows, piece = hidden.shape
    head_count, head_width = query_gain.shape
    local_width = head_count * head_width
    count = lax.axis_size("tp")
    shards = lax.axis_size("sp")
    half = count // 2
    me = lax.axis_index("tp")
    shard = lax.axis_index("sp")
    where = jnp.stack([me, shard]).astype(jnp.int32)
    factor = head_width ** (-0.5) * LOG2_E
    reach = -(-KEYS_BEHIND * DILATIONS[-1] // rows)
    distances = list(range(min(shards - 1, reach) + 1))
    helped = shards - 1 if shards == 4 and reach >= shards - 1 else None
    far = [2] if helped is not None else distances[2:]

    first = shard * rows
    steps = jnp.arange(rows, dtype=jnp.int32)
    tables = turn_tables((steps + first).astype(jnp.float32), head_width)
    tables_before = turn_tables((steps + first - rows).astype(jnp.float32), head_width)
    gain = norm_gain.astype(jnp.float32).reshape(count, piece)
    gains = (query_gain, key_gain)
    weights = (w_query, w_key, w_value)
    sums = shape_of((rows, local_width), jnp.float32)
    half_sum = shape_of((rows, local_width), jnp.bfloat16)
    lane_wide = shape_of((rows, LANES), jnp.float32)
    square = shape_of((rows, rows), jnp.float32)
    early = tuple(range(half))
    late = tuple(range(half, count))

    def begin(name, blocks, kinds, biases):
        return call(
            functools.partial(early_kernel, offsets=early, kinds=kinds, biases=biases),
            name,
            where,
            [*blocks, gain, *weights[3 - kinds :]],
            [sums] * kinds + [lane_wide] + [square] * len(biases),
        )

    def finish(name, blocks, kinds, begun, turn):
        return call(
            functools.partial(late_kernel, offsets=late, kinds=kinds, width=piece * count),
            name,
            where,
            [*blocks, gain, *weights[3 - kinds :], *begun, *gains[3 - kinds :], *turn],
            [half_sum] * kinds,
        )

    across = swap(hidden, half)
    own_near = near_blocks(hidden)
    before = behind(hidden, 1)

    begun = begin("early_own", own_near, 3, tuple(distances))
    biases = begun[4:]
    own_far = near_blocks(across)
    before_across = swap(before, half)
    q, key, value = finish("late_own", own_far, 3, begun[:4], tables)

    if helped is not None:
        visitor = lax.ppermute(q, "sp", [(helped, 1)])
        far_keys = [
            (lax.ppermute(key, "sp", [(0, 2)]), lax.ppermute(value, "sp", [(0, 2)]), biases[2])
        ]
    else:
        far_keys = [(behind(key, d), behind(value, d), biases[d]) for d in far]

    begun_before = begin("early_before", near_blocks(before), 2, ())
    own_part = call(
        functools.partial(part_kernel, head_width=head_width, factor=factor),
        "own_part",
        where,
        [q, key, value, biases[0]],
        [sums] * 3,
    )
    key_before, value_before = finish(
        "late_before", near_blocks(before_across), 2, begun_before, tables_before
    )
    given = []
    if helped is not None:
        out, logs = call(
            functools.partial(
                help_kernel, blocks=2, head_width=head_width, factor=factor, helper=1
            ),
            "help",
            where,
            [visitor, key, value, biases[2], key_before, value_before, biases[3]],
            [half_sum, shape_of((8, rows), jnp.float32)],
        )
        given = [lax.ppermute(out, "sp", [(1, helped)]), lax.ppermute(logs, "sp", [(1, helped)])]
    before_part = call(
        functools.partial(part_kernel, head_width=head_width, factor=factor),
        "before_part",
        where,
        [q, key_before, value_before, biases[1]],
        [sums] * 3,
    )

    columns = w_out.shape[1] // count
    w_late, _ = lax.optimization_barrier((w_out, before_across))
    slices = [
        lax.dynamic_slice_in_dim(w_late, (me ^ k) * columns, columns, axis=1) for k in range(count)
    ]
    pieces = [slices[0]] + [swap(slices[k], k) for k in range(1, count)]

    attended, logs = call(
        functools.partial(
            final_kernel,
            far=tuple(far),
            only=2 if helped is not None else None,
            helped=helped,
            head_width=head_width,
            factor=factor,
        ),
        "final",
        where,
        [q, *own_part, *before_part, *[x for block in far_keys for x in block], *given],
        [half_sum, shape_of((head_count, rows), jnp.float32)],
    )
    gathered = lax.all_gather(attended, "tp", axis=0, tiled=False)
    (mixed,) = call(
        mix_kernel, "mix", where, [gathered, *pieces], [shape_of((rows, columns), jnp.bfloat16)]
    )
    return mixed, logs.T


def solution(mesh):
    placed = (
        P(("grp", "sp"), "tp"),
        P(),
        P(None, "tp"),
        P(None, "tp"),
        P(None, "tp"),
        P("tp", None),
        P("tp", None),
        P("tp", None),
    )
    return jax.shard_map(
        local,
        mesh=mesh,
        in_specs=placed,
        out_specs=(P(("grp", "sp"), "tp"), P(("grp", "sp"), "tp")),
        check_vma=False,
    )
```

time: 136 us -> 75 us (0.55); the launches traced: 134 us -> 74.6 us
  waiting for transfers between devices: 46 us -> 12.8 us
  local copies, waits for them, and re-layouts: 23.9 us -> 4.79 us
  Pallas kernels: 0 us -> 17.1 us
  matrix products: 15.2 us -> 0 us
  between operations: 14.8 us -> 0.92 us
  other arithmetic: 12 us -> 2.7 us
  starting transfers between devices: 12.8 us -> 20.6 us
  blocking collectives: 9.02 us -> 15.7 us
    all_gather x1 -> x0, waiting for transfers between devices: 19.5 us -> none  [local(): lax.all_gather(hidden, 'tp', axis=1, tiled=True).astype(jnp.float32)]
    pallas_call x0 -> x9, Pallas kernels: none -> 17.1 us  [call(): pl.pallas_call(body, out_shape=tuple(outs), in_specs=[SMEM] + [VMEM] * le...]
    dot_general x10 -> x0, matrix products: 15.2 us -> none  [the longest x3 5.79 us: add_product(): return jnp.dot(scaled, weight, preferred_element_type=jnp.float32)]
    ppermute x4 -> x15, waiting for transfers between devices: 25.8 us -> 12.8 us  [the longest x1 7.43 us: behind(): lax.ppermute(value, 'sp', [(s, s + steps) for s in range(count - steps)])]
    ppermute x4 -> x15, starting transfers between devices: 8.29 us -> 20.6 us  [the longest x9 8.46 us: swap(): return lax.ppermute(value, 'tp', [(i, i ^ distance) for i in range(count)])]
    all_gather x1, blocking collectives: 9.02 us -> 15.7 us  [local(): gathered = lax.all_gather(attended, 'tp', axis=0, tiled=False)]
    reshape x6 -> x1, local copies, waits for them, and re-layouts: 4.62 us -> 0.01 us  [local(): gain = norm_gain.astype(jnp.float32).reshape(count, piece)]
    all_to_all x1 -> x0, starting transfers between devices: 4.43 us -> none  [local(): lax.all_to_all(w_out, 'tp', split_axis=1, concat_axis=0, tiled=True)]
  transfers between devices with their start and end apart: 6 -> 15, of which waited for: 3 -> 4; matrix products, arithmetic and copies ran while one was open for 17% -> 4% of each run, Pallas kernels for 0% -> 20%
where the time goes in v2:
time: 75 us; the launch traced here: 74.6 us
  starting transfers between devices  20.6 us (27%)
  Pallas kernels  17.1 us (23%)
  blocking collectives  15.7 us (21%)
  waiting for transfers between devices  12.8 us (17%)
  local copies, waits for them, and re-layouts  4.79 us (6%)
  other arithmetic  2.7 us (4%)
  between operations  0.92 us (1%)
    pallas_call x9, Pallas kernels, call(): pl.pallas_call(body, out_shape=tuple(outs), in_specs=[SMEM] + [VMEM] * le...  17.1 us
    all_gather x1, blocking collectives, local(): gathered = lax.all_gather(attended, 'tp', axis=0, tiled=False)  15.7 us
    ppermute x9, starting transfers between devices, swap(): return lax.ppermute(value, 'tp', [(i, i ^ distance) for i in range(count)])  8.46 us
    ppermute x1, waiting for transfers between devices, behind(): lax.ppermute(value, 'sp', [(s, s + steps) for s in range(count - steps)])  7.43 us
    ppermute x9, waiting for transfers between devices, swap(): return lax.ppermute(value, 'tp', [(i, i ^ distance) for i in range(count)])  5.03 us
    unnamed x34, local copies, waits for them, and re-layouts  4.67 us
    ppermute x1, starting transfers between devices, local(): lax.ppermute(out, 'sp', [(1, helped)])  3.49 us
    ppermute x1, starting transfers between devices, behind(): lax.ppermute(value, 'sp', [(s, s + steps) for s in range(count - steps)])  3.21 us
  transfers between devices with their start and end apart: 15, of which 4 were waited for; matrix products, arithmetic and copies ran while one was open for 4% of the time, Pallas kernels for 20%

profile of v2, /device:TPU:15, one launch (start us, length us, event | category | flops | bytes accessed | tf_op | source)
XLA Modules:
  0.0 74.6 jit_solution(13949320425315668875)
XLA Ops:
  0.6 3.2 %collective-permute-start.3 = (bf16[384,512]{1,0:T(8,128)(2,1)}, bf16[384,512]{1,0:T(8,128)(2,1)}, u32[]{:S(2)}, u32[]{:S(2)}) collective-permute-start(bf16[384,512]{1,0:T(8,128)(2,1)} %refs_0_.1), channel_id=1, source_target_pairs={{0,4},{4,8},{8,12},{1,5},{5,9},{9,13},{2,6},{6,10},{10,14},{3,7},{... | collective-permute-start | bytes 1179656 | tf_op jit(solution)/shard_map/ppermute | solution.py:241
  3.8 0.3 collective-permute-start
  4.2 1.2 %collective-permute-start.2 = (bf16[384,512]{1,0:T(8,128)(2,1)}, bf16[384,512]{1,0:T(8,128)(2,1)S(1)}, u32[]{:S(2)}, u32[]{:S(2)}) collective-permute-start(bf16[384,512]{1,0:T(8,128)(2,1)} %refs_0_.1), channel_id=1, source_target_pairs={{0,1},{1,0},{2,3},{3,2},{4,5},{5,4},{6,7},{7,6},{8,9},{9,8},{10,11... | collective-permute-start | bytes 1179656 | tf_op jit(solution)/shard_map/ppermute | solution.py:236
  5.4 7.4 %collective-permute-done.3.refs_0_ = bf16[384,512]{1,0:T(8,128)(2,1)} collective-permute-done((bf16[384,512]{1,0:T(8,128)(2,1)}, bf16[384,512]{1,0:T(8,128)(2,1)}, u32[]{:S(2)}, u32[]{:S(2)}) %collective-permute-start.3) | collective-permute-done | bytes 393248 | tf_op jit(solution)/shard_map/ppermute | solution.py:241
  12.8 0.3 collective-permute-start.4
  13.1 0.8 %collective-permute-done.refs_0_ = bf16[384,512]{1,0:T(8,128)(2,1)} collective-permute-done((bf16[384,512]{1,0:T(8,128)(2,1)}, bf16[384,512]{1,0:T(8,128)(2,1)}, u32[]{:S(2)}, u32[]{:S(2)}) %collective-permute-start) | collective-permute-done | bytes 393248 | tf_op jit(solution)/shard_map/ppermute | solution.py:236
  13.9 1.8 %collective-permute-start.1 = (bf16[384,512]{1,0:T(8,128)(2,1)}, bf16[384,512]{1,0:T(8,128)(2,1)}, u32[]{:S(2)}, u32[]{:S(2)}) collective-permute-start(bf16[384,512]{1,0:T(8,128)(2,1)} %collective-permute-done.refs_0_), channel_id=1, source_target_pairs={{0,1},{1,0},{2,3},{3,2},{4,5},{5,4},{6,7},{7,6},{8,9},{9,8},{10,11... | collective-permute-start | bytes 1179656 | tf_op jit(solution)/shard_map/ppermute | solution.py:236
  15.8 2.1 %fusion.1 = (f32[384,64]{1,0:T(8,128)}, f32[384,64]{1,0:T(8,128)}, f32[384,64]{1,0:T(8,128)}, f32[384,64]{1,0:T(8,128)S(1)}, f32[384,64]{1,0:T(8,128)S(1)}, /*index=5*/f32[384,64]{1,0:T(8,128)S(1)}) fusion(f32[64]{0:T(128)S(1)} %multiply_power_fusion, f32[384]{0:T(512)S(1)} %get-tuple-element.69, f32[384]{0:T(512)S(1)} %get-tuple-element.70), kind=kLoop, calls=%fused_computation.9 | loop fusion | flops 98304 | bytes 593152 | tf_op jit(solution)/shard_map/neg | solution.py:259
  17.9 0.1 pad_maximum_fusion.refs_12_
  18.0 0.1 collective-permute-start.6
  18.1 4.2 %collective-permute-done.4.refs_0_ = bf16[384,512]{1,0:T(8,128)(2,1)} collective-permute-done((bf16[384,512]{1,0:T(8,128)(2,1)}, bf16[384,512]{1,0:T(8,128)(2,1)}, u32[]{:S(2)}, u32[]{:S(2)}) %collective-permute-start.4) | collective-permute-done | bytes 393248 | tf_op jit(solution)/shard_map/ppermute | solution.py:236
  22.3 2.4 %collective-permute-start.5 = (bf16[384,512]{1,0:T(8,128)(2,1)}, bf16[384,512]{1,0:T(8,128)(2,1)}, u32[]{:S(2)}, u32[]{:S(2)}) collective-permute-start(bf16[384,512]{1,0:T(8,128)(2,1)} %collective-permute-done.4.refs_0_), channel_id=1, source_target_pairs={{0,1},{1,0},{2,3},{3,2},{4,5},{5,4},{6,7},{7,6},{8,9},{9,8},{10,11... | collective-permute-start | bytes 1179656 | tf_op jit(solution)/shard_map/ppermute | solution.py:236
  24.7 0.1 pad_add_fusion.where
  24.8 0.1 pad_maximum_fusion.1.refs_13_
  24.9 0.0 copy-start.2
  24.9 1.2 %copy-done.2 = bf16[2048,256]{1,0:T(8,128)(2,1)S(1)} copy-done((bf16[2048,256]{1,0:T(8,128)(2,1)S(1)}, bf16[2048,256]{1,0:T(8,128)(2,1)}, u32[]{:S(2)}) %copy-start.2) | copy-done | bytes 1048600
  26.2 1.0 %copy-done.9 = bf16[384,512]{1,0:T(8,128)(2,1)S(1)} copy-done((bf16[384,512]{1,0:T(8,128)(2,1)S(1)}, bf16[384,512]{1,0:T(8,128)(2,1)}, u32[]{:S(2)}) %copy-start.9) | copy-done | bytes 393240
  27.2 2.8 %early_own.1 = (f32[384,256]{1,0:T(8,128)S(1)}, f32[384,256]{1,0:T(8,128)S(1)}, f32[384,256]{1,0:T(8,128)S(1)}, f32[384,128]{1,0:T(8,128)S(1)}, f32[384,384]{1,0...) custom-call(s32[2]{0:T(128)S(1)} %pad_add_fusion.where, ...), custom_call_target="tpu_custom_call" | custom-call | tf_op jit(solution)/shard_map/early_own/pallas_call | solution.py:28
  30.0 0.8 %copy-done.7 = f32[384,384]{1,0:T(8,128)} copy-done((f32[384,384]{1,0:T(8,128)}, f32[384,384]{1,0:T(8,128)S(1)}, u32[]{:S(2)}) %copy-start.7) | copy-done | bytes 589848
  30.8 0.7 copy-done.10
  31.5 2.3 %late_own.1 = (bf16[384,256]{1,0:T(8,128)(2,1)S(1)}, bf16[384,256]{1,0:T(8,128)(2,1)S(1)}, bf16[384,256]{1,0:T(8,128)(2,1)S(1)}) custom-call(s32[2]{0:T(128)S(1)} %pad_add_fusion.where, bf16[384,512]{1,0:T(8,128)(2,1)} %collective-permute-done.refs_0_, bf16[384,512]{1,0:T(8,128)(2,1)} %collective-permute-done.1.refs_1_, f32[4,512]{1,0:T(4,128)S(1)} %reshape.28.refs_2_, ...), custom_call_target="tpu_custom_call" | custom-call | tf_op jit(solution)/shard_map/late_own/pallas_call | solution.py:28
  33.9 1.3 %collective-permute-start.9 = (bf16[384,256]{1,0:T(8,128)(2,1)S(1)}, bf16[384,256]{1,0:T(8,128)(2,1)S(1)}, u32[]{:S(2)}, u32[]{:S(2)}) collective-permute-start(bf16[384,256]{1,0:T(8,128)(2,1)S(1)} %get-tuple-element.33.q), channel_id=1, source_target_pairs={{12,4},{13,5},{14,6},{15,7},{28,20},{29,21},{30,22},{31,23}} | collective-permute-start | bytes 589832 | tf_op jit(solution)/shard_map/ppermute | solution.py:321
  35.2 0.0 copy-start.14
  35.2 0.1 pad_maximum_fusion.2.refs_9_
  35.3 0.8 %copy-done.14 = f32[384,64]{1,0:T(8,128)S(1)} copy-done((f32[384,64]{1,0:T(8,128)S(1)}, f32[384,64]{1,0:T(8,128)}, u32[]{:S(2)}) %copy-start.14) | copy-done | bytes 98328
  36.1 0.1 copy-done.15
  36.2 0.1 pad_maximum_fusion.3.refs_10_
  36.3 1.3 %collective-permute-start.7 = (bf16[384,256]{1,0:T(8,128)(2,1)S(1)}, bf16[384,256]{1,0:T(8,128)(2,1)}, u32[]{:S(2)}, u32[]{:S(2)}) collective-permute-start(bf16[384,256]{1,0:T(8,128)(2,1)S(1)} %get-tuple-element.34.key.refs_0_), channel_id=1, source_target_pairs={{0,8},{1,9},{2,10},{3,11},{16,24},{17,25},{18,26},{19,27}} | collective-permute-start | bytes 589832 | tf_op jit(solution)/shard_map/ppermute | solution.py:323
  37.7 1.3 %collective-permute-start.8 = (bf16[384,256]{1,0:T(8,128)(2,1)S(1)}, bf16[384,256]{1,0:T(8,128)(2,1)}, u32[]{:S(2)}, u32[]{:S(2)}) collective-permute-start(bf16[384,256]{1,0:T(8,128)(2,1)S(1)} %get-tuple-element.35.value.refs_1_), channel_id=1, source_target_pairs={{0,8},{1,9},{2,10},{3,11},{16,24},{17,25},{18,26},{19,27}} | collective-permute-start | bytes 589832 | tf_op jit(solution)/shard_map/ppermute | solution.py:323
  39.0 1.7 %early_before.1 = (f32[384,256]{1,0:T(8,128)S(1)}, f32[384,256]{1,0:T(8,128)S(1)}, f32[384,128]{1,0:T(8,128)S(1)}) custom-call(s32[2]{0:T(128)S(1)} %pad_add_fusion.where, bf16[384,512]{1,0:T(8,128)(2,1)} %collective-permute-done.3.refs_0_, bf16[384,512]{1,0:T(8,128)(2,1)} %collective-permute-done.6.refs_1_, f32[4,512]{1,0:T(4,128)S(1)} %reshape.28.refs_2_, ...), custom_call_target="tpu_custom_call" | custom-call | tf_op jit(solution)/shard_map/early_before/pallas_call | solution.py:28
  40.7 0.0 collective-permute-done.5.refs_1_
  40.7 2.1 %late_before.1 = (bf16[384,256]{1,0:T(8,128)(2,1)S(1)}, bf16[384,256]{1,0:T(8,128)(2,1)S(1)}) custom-call(s32[2]{0:T(128)S(1)} %pad_add_fusion.where, bf16[384,512]{1,0:T(8,128)(2,1)} %collective-permute-done.4.refs_0_, bf16[384,512]{1,0:T(8,128)(2,1)} %collective-permute-done.5.refs_1_, f32[4,512]{1,0:T(4,128)S(1)} %reshape.28.refs_2_, ...), custom_call_target="tpu_custom_call" | custom-call | tf_op jit(solution)/shard_map/late_before/pallas_call | solution.py:28
  42.8 0.0 copy-start.3
  42.8 0.3 collective-permute-done.9.q
  43.1 1.8 %help.1 = (bf16[384,256]{1,0:T(8,128)(2,1)S(1)}, f32[8,384]{1,0:T(8,128)S(1)}) custom-call(s32[2]{0:T(128)S(1)} %pad_add_fusion.where, bf16[384,256]{1,0:T(8,128)(2,1)S(1)} %collective-permute-done.9.q, bf16[384,256]{1,0:T(8,128)(2,1)S(1)} %get-tuple-element.34.key.refs_0_, bf16[384,256]{1,0:T(8,128)(2,1)S(1)} %get-tuple-element.35.value.refs_1_, ...), custom_call_target="tpu_custom_call" | custom-call | tf_op jit(solution)/shard_map/help/pallas_call | solution.py:28
  44.9 3.5 %collective-permute-start.10 = (bf16[384,256]{1,0:T(8,128)(2,1)S(1)}, bf16[384,256]{1,0:T(8,128)(2,1)S(1)}, u32[]{:S(2)}, u32[]{:S(2)}) collective-permute-start(bf16[384,256]{1,0:T(8,128)(2,1)S(1)} %get-tuple-element.51), channel_id=1, source_target_pairs={{4,12},{5,13},{6,14},{7,15},{20,28},{21,29},{22,30},{23,31}} | collective-permute-start | bytes 589832 | tf_op jit(solution)/shard_map/ppermute | solution.py:350
  48.4 1.4 %collective-permute-start.11 = (f32[8,384]{1,0:T(8,128)S(1)}, f32[8,384]{1,0:T(8,128)S(1)}, u32[]{:S(2)}, u32[]{:S(2)}) collective-permute-start(f32[8,384]{1,0:T(8,128)S(1)} %get-tuple-element.52), channel_id=1, source_target_pairs={{4,12},{5,13},{6,14},{7,15},{20,28},{21,29},{22,30},{23,31}} | collective-permute-start | bytes 36872 | tf_op jit(solution)/shard_map/ppermute | solution.py:350
  49.8 0.1 constant_dynamic-slice_fusion
  50.0 0.0 copy-start.4
  50.0 1.4 %own_part.1 = (f32[384,256]{1,0:T(8,128)S(1)}, f32[384,256]{1,0:T(8,128)S(1)}, f32[384,256]{1,0:T(8,128)S(1)}) custom-call(s32[2]{0:T(128)S(1)} %pad_add_fusion.where, bf16[384,256]{1,0:T(8,128)(2,1)S(1)} %get-tuple-element.33.q, bf16[384,256]{1,0:T(8,128)(2,1)S(1)} %get-tuple-element.34.key.refs_0_, bf16[384,256]{1,0:T(8,128)(2,1)S(1)} %get-tuple-element.35.value.refs_1_, ...), custom_call_target="tpu_custom_call" | custom-call | tf_op jit(solution)/shard_map/own_part/pallas_call | solution.py:28
  51.4 0.6 collective-permute-start.12
  52.0 1.3 %before_part.1 = (f32[384,256]{1,0:T(8,128)S(1)}, f32[384,256]{1,0:T(8,128)S(1)}, f32[384,256]{1,0:T(8,128)S(1)}) custom-call(s32[2]{0:T(128)S(1)} %pad_add_fusion.where, bf16[384,256]{1,0:T(8,128)(2,1)S(1)} %get-tuple-element.33.q, bf16[384,256]{1,0:T(8,128)(2,1)S(1)} %get-tuple-element.43.key.refs_3_, bf16[384,256]{1,0:T(8,128)(2,1)S(1)} %copy-done.4, ...), custom_call_target="tpu_custom_call" | custom-call | tf_op jit(solution)/shard_map/before_part/pallas_call | solution.py:28
  53.4 0.3 collective-permute-start.13
  53.7 1.4 %collective-permute-start.14 = (bf16[256,512]{1,0:T(8,128)(2,1)S(1)}, bf16[256,512]{1,0:T(8,128)(2,1)S(1)}, u32[]{:S(2)}, u32[]{:S(2)}) collective-permute-start(bf16[256,512]{1,0:T(8,128)(2,1)S(1)} %get-tuple-element.56), channel_id=1, source_target_pairs={{0,3},{1,2},{2,1},{3,0},{4,7},{5,6},{6,5},{7,4},{8,11},{9,10},{10,... | collective-permute-start | bytes 786440 | tf_op jit(solution)/shard_map/ppermute | solution.py:236
  55.1 0.0 collective-permute-done.10.refs_9_
  55.1 1.9 %final.1 = (bf16[384,256]{1,0:T(8,128)(2,1)S(1)}, f32[2,384]{1,0:T(2,128)}) custom-call(s32[2]{0:T(128)S(1)} %pad_add_fusion.where, bf16[384,256]{1,0:T(8,128)(2,1)S(1)} %get-tuple-element.33.q, f32[384,256]{1,0:T(8,128)S(1)} %get-tuple-element.37.refs_0_, f32[384,256]{1,0:T(8,128)S(1)} %get-tuple-element.38.refs_1_, ...), custom_call_target="tpu_custom_call" | custom-call | tf_op jit(solution)/shard_map/final/pallas_call | solution.py:28
  57.0 15.7 %all-gather = bf16[1536,256]{1,0:T(8,128)(2,1)S(1)} all-gather(bf16[384,256]{1,0:T(8,128)(2,1)S(1)} %get-tuple-element.53), channel_id=2, replica_groups=mesh['grp'=2,'sp'=4,'tp'=4] {'tp'}, dimensions={0}, use_global_device_ids=true | all-gather | bytes 983040 | tf_op jit(solution)/shard_map/all_gather | solution.py:380
  72.7 1.9 %mix.1 = bf16[384,512]{1,0:T(8,128)(2,1)} custom-call(s32[2]{0:T(128)S(1)} %pad_add_fusion.where, bf16[4,384,256]{2,1,0:T(8,128)(2,1)S(1)} %bitcast.4, bf16[256,512]{1,0:T(8,128)(2,1)S(1)} %get-tuple-element.59.refs_0_, bf16[256,512]{1,0:T(8,128)(2,1)S(1)} %collective-permute-done.12.refs_1_, bf16[256,512]{1,0:T(8,128)(2,1)S(1)} %collective-permute-done.13.refs_2_, ...), custom_call_target="tpu_custom_call" | custom-call | tf_op jit(solution)/shard_map/mix/pallas_call | solution.py:28
  (36 shorter events, 0.1 us)
Async XLA Ops:
  0.6 12.2 %collective-permute-start.3 = (bf16[384,512]{1,0:T(8,128)(2,1)}, bf16[384,512]{1,0:T(8,128)(2,1)}, u32[]{:S(2)}, u32[]{:S(2)}) collective-permute-start(bf16[384,512]{1,0:T(8,128)(2,1)} %refs_0_.1), channel_id=1, source_target_pairs={{0,4},{4,8},{8,12},{1,5},{5,9},{9,13},{2,6},{6,10},{10,14},{3,7},{... | collective-permute-start | bytes 1179656 | tf_op jit(solution)/shard_map/ppermute | solution.py:241
  3.8 10.1 %collective-permute-start = (bf16[384,512]{1,0:T(8,128)(2,1)}, bf16[384,512]{1,0:T(8,128)(2,1)}, u32[]{:S(2)}, u32[]{:S(2)}) collective-permute-start(bf16[384,512]{1,0:T(8,128)(2,1)} %refs_0_.1), channel_id=1, source_target_pairs={{0,2},{1,3},{2,0},{3,1},{4,6},{5,7},{6,4},{7,5},{8,10},{9,11},{10,... | collective-permute-start | bytes 1179656 | tf_op jit(solution)/shard_map/ppermute | solution.py:236
  4.2 20.7 %collective-permute-start.2 = (bf16[384,512]{1,0:T(8,128)(2,1)}, bf16[384,512]{1,0:T(8,128)(2,1)S(1)}, u32[]{:S(2)}, u32[]{:S(2)}) collective-permute-start(bf16[384,512]{1,0:T(8,128)(2,1)} %refs_0_.1), channel_id=1, source_target_pairs={{0,1},{1,0},{2,3},{3,2},{4,5},{5,4},{6,7},{7,6},{8,9},{9,8},{10,11... | collective-permute-start | bytes 1179656 | tf_op jit(solution)/shard_map/ppermute | solution.py:236
  5.4 19.4 %copy-start.16 = (bf16[2048]{0:T(1024)(128)(2,1)S(1)}, bf16[2048]{0:T(1024)(128)(2,1)}, u32[]{:S(2)}) copy-start(bf16[2048]{0:T(1024)(128)(2,1)} %param.9) | copy-start | bytes 12292
  12.8 9.5 %collective-permute-start.4 = (bf16[384,512]{1,0:T(8,128)(2,1)}, bf16[384,512]{1,0:T(8,128)(2,1)}, u32[]{:S(2)}, u32[]{:S(2)}) collective-permute-start(bf16[384,512]{1,0:T(8,128)(2,1)} %collective-permute-done.3.refs_0_), channel_id=1, source_target_pairs={{0,2},{1,3},{2,0},{3,1},{4,6},{5,7},{6,4},{7,5},{8,10},{9,11},{10,... | collective-permute-start | bytes 1179656 | tf_op jit(solution)/shard_map/ppermute | solution.py:236
  13.9 16.8 %collective-permute-start.1 = (bf16[384,512]{1,0:T(8,128)(2,1)}, bf16[384,512]{1,0:T(8,128)(2,1)}, u32[]{:S(2)}, u32[]{:S(2)}) collective-permute-start(bf16[384,512]{1,0:T(8,128)(2,1)} %collective-permute-done.refs_0_), channel_id=1, source_target_pairs={{0,1},{1,0},{2,3},{3,2},{4,5},{5,4},{6,7},{7,6},{8,9},{9,8},{10,11... | collective-permute-start | bytes 1179656 | tf_op jit(solution)/shard_map/ppermute | solution.py:236
  15.8 9.2 %copy-start = (bf16[2048,256]{1,0:T(8,128)(2,1)S(1)}, bf16[2048,256]{1,0:T(8,128)(2,1)}, u32[]{:S(2)}) copy-start(bf16[2048,256]{1,0:T(8,128)(2,1)} %refs_3_.7) | copy-start | bytes 3145732
  15.8 9.2 %copy-start.1 = (bf16[2048,256]{1,0:T(8,128)(2,1)S(1)}, bf16[2048,256]{1,0:T(8,128)(2,1)}, u32[]{:S(2)}) copy-start(bf16[2048,256]{1,0:T(8,128)(2,1)} %refs_4_.7) | copy-start | bytes 3145732
  18.0 21.0 %collective-permute-start.6 = (bf16[384,512]{1,0:T(8,128)(2,1)}, bf16[384,512]{1,0:T(8,128)(2,1)}, u32[]{:S(2)}, u32[]{:S(2)}) collective-permute-start(bf16[384,512]{1,0:T(8,128)(2,1)} %collective-permute-done.3.refs_0_), channel_id=1, source_target_pairs={{0,1},{1,0},{2,3},{3,2},{4,5},{5,4},{6,7},{7,6},{8,9},{9,8},{10,11... | collective-permute-start | bytes 1179656 | tf_op jit(solution)/shard_map/ppermute | solution.py:236
  22.3 18.4 %collective-permute-start.5 = (bf16[384,512]{1,0:T(8,128)(2,1)}, bf16[384,512]{1,0:T(8,128)(2,1)}, u32[]{:S(2)}, u32[]{:S(2)}) collective-permute-start(bf16[384,512]{1,0:T(8,128)(2,1)} %collective-permute-done.4.refs_0_), channel_id=1, source_target_pairs={{0,1},{1,0},{2,3},{3,2},{4,5},{5,4},{6,7},{7,6},{8,9},{9,8},{10,11... | collective-permute-start | bytes 1179656 | tf_op jit(solution)/shard_map/ppermute | solution.py:236
  24.9 1.2 %copy-start.2 = (bf16[2048,256]{1,0:T(8,128)(2,1)S(1)}, bf16[2048,256]{1,0:T(8,128)(2,1)}, u32[]{:S(2)}) copy-start(bf16[2048,256]{1,0:T(8,128)(2,1)} %refs_3_.5) | copy-start | bytes 3145732
  26.2 1.0 %copy-start.9 = (bf16[384,512]{1,0:T(8,128)(2,1)S(1)}, bf16[384,512]{1,0:T(8,128)(2,1)}, u32[]{:S(2)}) copy-start(bf16[384,512]{1,0:T(8,128)(2,1)} %refs_0_.1) | copy-start | bytes 1179652
  27.2 3.6 %copy-start.11 = (f32[2,128]{1,0:T(2,128)S(1)}, f32[2,128]{1,0:T(2,128)}, u32[]{:S(2)}) copy-start(f32[2,128]{1,0:T(2,128)} %refs_10_.1) | copy-start | bytes 3076
  30.0 0.8 %copy-start.7 = (f32[384,384]{1,0:T(8,128)}, f32[384,384]{1,0:T(8,128)S(1)}, u32[]{:S(2)}) copy-start(f32[384,384]{1,0:T(8,128)S(1)} %get-tuple-element.36.bias) | copy-start | bytes 1769476
  30.8 3.1 %copy-start.5 = (f32[384,384]{1,0:T(8,128)}, f32[384,384]{1,0:T(8,128)S(1)}, u32[]{:S(2)}) copy-start(f32[384,384]{1,0:T(8,128)S(1)} %get-tuple-element.45.bias) | copy-start | bytes 1769476
  30.8 0.7 copy-start.10
  31.5 3.7 %copy-start.13 = (f32[384,64]{1,0:T(8,128)S(1)}, f32[384,64]{1,0:T(8,128)}, u32[]{:S(2)}) copy-start(f32[384,64]{1,0:T(8,128)} %get-tuple-element.61) | copy-start | bytes 294916
  33.9 9.2 %collective-permute-start.9 = (bf16[384,256]{1,0:T(8,128)(2,1)S(1)}, bf16[384,256]{1,0:T(8,128)(2,1)S(1)}, u32[]{:S(2)}, u32[]{:S(2)}) collective-permute-start(bf16[384,256]{1,0:T(8,128)(2,1)S(1)} %get-tuple-element.33.q), channel_id=1, source_target_pairs={{12,4},{13,5},{14,6},{15,7},{28,20},{29,21},{30,22},{31,23}} | collective-permute-start | bytes 589832 | tf_op jit(solution)/shard_map/ppermute | solution.py:321
  35.2 0.9 %copy-start.14 = (f32[384,64]{1,0:T(8,128)S(1)}, f32[384,64]{1,0:T(8,128)}, u32[]{:S(2)}) copy-start(f32[384,64]{1,0:T(8,128)} %get-tuple-element.60) | copy-start | bytes 294916
  35.2 1.0 %copy-start.15 = (f32[384,64]{1,0:T(8,128)S(1)}, f32[384,64]{1,0:T(8,128)}, u32[]{:S(2)}) copy-start(f32[384,64]{1,0:T(8,128)} %get-tuple-element.62) | copy-start | bytes 294916
  36.3 17.0 %collective-permute-start.7 = (bf16[384,256]{1,0:T(8,128)(2,1)S(1)}, bf16[384,256]{1,0:T(8,128)(2,1)}, u32[]{:S(2)}, u32[]{:S(2)}) collective-permute-start(bf16[384,256]{1,0:T(8,128)(2,1)S(1)} %get-tuple-element.34.key.refs_0_), channel_id=1, source_target_pairs={{0,8},{1,9},{2,10},{3,11},{16,24},{17,25},{18,26},{19,27}} | collective-permute-start | bytes 589832 | tf_op jit(solution)/shard_map/ppermute | solution.py:323
  37.7 16.0 %collective-permute-start.8 = (bf16[384,256]{1,0:T(8,128)(2,1)S(1)}, bf16[384,256]{1,0:T(8,128)(2,1)}, u32[]{:S(2)}, u32[]{:S(2)}) collective-permute-start(bf16[384,256]{1,0:T(8,128)(2,1)S(1)} %get-tuple-element.35.value.refs_1_), channel_id=1, source_target_pairs={{0,8},{1,9},{2,10},{3,11},{16,24},{17,25},{18,26},{19,27}} | collective-permute-start | bytes 589832 | tf_op jit(solution)/shard_map/ppermute | solution.py:323
  42.8 2.1 %copy-start.3 = (bf16[384,256]{1,0:T(8,128)(2,1)}, bf16[384,256]{1,0:T(8,128)(2,1)S(1)}, u32[]{:S(2)}) copy-start(bf16[384,256]{1,0:T(8,128)(2,1)S(1)} %get-tuple-element.44.value.refs_4_) | copy-start | bytes 589828
  43.1 6.7 %copy-start.12 = (bf16[256,2048]{1,0:T(8,128)(2,1)S(1)}, bf16[256,2048]{1,0:T(8,128)(2,1)}, u32[]{:S(2)}) copy-start(bf16[256,2048]{1,0:T(8,128)(2,1)} %param.15) | copy-start | bytes 3145732
  44.9 10.2 %collective-permute-start.10 = (bf16[384,256]{1,0:T(8,128)(2,1)S(1)}, bf16[384,256]{1,0:T(8,128)(2,1)S(1)}, u32[]{:S(2)}, u32[]{:S(2)}) collective-permute-start(bf16[384,256]{1,0:T(8,128)(2,1)S(1)} %get-tuple-element.51), channel_id=1, source_target_pairs={{4,12},{5,13},{6,14},{7,15},{20,28},{21,29},{22,30},{23,31}} | collective-permute-start | bytes 589832 | tf_op jit(solution)/shard_map/ppermute | solution.py:350
  48.4 1.6 %copy-start.8 = (f32[384,384]{1,0:T(8,128)S(1)}, f32[384,384]{1,0:T(8,128)}, u32[]{:S(2)}) copy-start(f32[384,384]{1,0:T(8,128)} %copy-done.7) | copy-start | bytes 1769476
  48.4 6.7 %collective-permute-start.11 = (f32[8,384]{1,0:T(8,128)S(1)}, f32[8,384]{1,0:T(8,128)S(1)}, u32[]{:S(2)}, u32[]{:S(2)}) collective-permute-start(f32[8,384]{1,0:T(8,128)S(1)} %get-tuple-element.52), channel_id=1, source_target_pairs={{4,12},{5,13},{6,14},{7,15},{20,28},{21,29},{22,30},{23,31}} | collective-permute-start | bytes 36872 | tf_op jit(solution)/shard_map/ppermute | solution.py:350
  50.0 2.0 %copy-start.4 = (bf16[384,256]{1,0:T(8,128)(2,1)S(1)}, bf16[384,256]{1,0:T(8,128)(2,1)}, u32[]{:S(2)}) copy-start(bf16[384,256]{1,0:T(8,128)(2,1)} %copy-done.3) | copy-start | bytes 589828
  50.0 2.0 %copy-start.6 = (f32[384,384]{1,0:T(8,128)S(1)}, f32[384,384]{1,0:T(8,128)}, u32[]{:S(2)}) copy-start(f32[384,384]{1,0:T(8,128)} %copy-done.5) | copy-start | bytes 1769476
  51.4 21.3 %collective-permute-start.12 = (bf16[256,512]{1,0:T(8,128)(2,1)S(1)}, bf16[256,512]{1,0:T(8,128)(2,1)S(1)}, u32[]{:S(2)}, u32[]{:S(2)}) collective-permute-start(bf16[256,512]{1,0:T(8,128)(2,1)S(1)} %get-tuple-element.58), channel_id=1, source_target_pairs={{0,1},{1,0},{2,3},{3,2},{4,5},{5,4},{6,7},{7,6},{8,9},{9,8},{10,11... | collective-permute-start | bytes 786440 | tf_op jit(solution)/shard_map/ppermute | solution.py:236
  53.4 19.3 %collective-permute-start.13 = (bf16[256,512]{1,0:T(8,128)(2,1)S(1)}, bf16[256,512]{1,0:T(8,128)(2,1)S(1)}, u32[]{:S(2)}, u32[]{:S(2)}) collective-permute-start(bf16[256,512]{1,0:T(8,128)(2,1)S(1)} %get-tuple-element.57), channel_id=1, source_target_pairs={{0,2},{1,3},{2,0},{3,1},{4,6},{5,7},{6,4},{7,5},{8,10},{9,11},{10,... | collective-permute-start | bytes 786440 | tf_op jit(solution)/shard_map/ppermute | solution.py:236
  53.7 19.0 %collective-permute-start.14 = (bf16[256,512]{1,0:T(8,128)(2,1)S(1)}, bf16[256,512]{1,0:T(8,128)(2,1)S(1)}, u32[]{:S(2)}, u32[]{:S(2)}) collective-permute-start(bf16[256,512]{1,0:T(8,128)(2,1)S(1)} %get-tuple-element.56), channel_id=1, source_target_pairs={{0,3},{1,2},{2,1},{3,0},{4,7},{5,6},{6,5},{7,4},{8,11},{9,10},{10,... | collective-permute-start | bytes 786440 | tf_op jit(solution)/shard_map/ppermute | solution.py:236

commit v3 on v2

--- a/solution.py
+++ b/solution.py
@@ -7,6 +7,7 @@
 from jax.experimental import pallas as pl
 from jax.experimental.pallas import tpu as pltpu
 from jax.sharding import PartitionSpec as P
+
 
 KEYS_BEHIND = 128
 DILATIONS = (1, 4, 16)
@@ -16,6 +17,7 @@
 LANES = 128
 LOG2_E = math.log2(math.e)
 
+
 VMEM = pl.BlockSpec(memory_space=pltpu.VMEM)
 SMEM = pl.BlockSpec(memory_space=pltpu.SMEM)
 
@@ -24,14 +26,13 @@
     return jax.ShapeDtypeStruct(shape, dtype)
 
 
-def call(body, name, where, operands, outs, limit=24 << 20):
+def call(body, where, operands, outs, limit=24 << 20):
     return pl.pallas_call(
         body,
         out_shape=tuple(outs),
         in_specs=[SMEM] + [VMEM] * len(operands),
         out_specs=(VMEM,) * len(outs),
         compiler_params=pltpu.CompilerParams(vmem_limit_bytes=limit),
-        name=name,
     )(where, *operands)
 
 
@@ -104,11 +105,12 @@
     gains = rest[kinds + 1 : 2 * kinds]
     cosine, sine = rest[2 * kinds : 2 * kinds + 2]
     outs = rest[2 * kinds + 2 :]
+    outs = [*outs[:-1], outs[-1].at[0], outs[-1].at[1]]
     sums, squares = sums_of(where, hidden, gain, weights, offsets)
     scale = lax.rsqrt((squares + squares_before[...]) / width + EPSILON)
     head_width = gains[0].shape[1]
-    turn_c = cosine[...]
-    turn_s = sine[...]
+    turn_c = jnp.concatenate([cosine[...], cosine[...]], axis=1)
+    turn_s = jnp.concatenate([-sine[...], sine[...]], axis=1)
     for n in range(kinds):
         for start in range(0, sums[n].shape[1], head_width):
             lanes = slice(start, start + head_width)
@@ -121,21 +123,20 @@
 
 def softmax_part(q, blocks, lanes, factor):
     scores = []
-    for key, _, bias in blocks:
+    for kv, bias in blocks:
         product = lax.dot_general(
-            q[:, lanes], key[:, lanes], (((1,), (1,)), ((), ())), preferred_element_type=jnp.float32
+            q[:, lanes], kv[0, :, lanes], (((1,), (1,)), ((), ())),
+            preferred_element_type=jnp.float32,
         )
         scores.append(product * factor + bias)
-    top = functools.reduce(
-        jnp.maximum, [jnp.max(s, axis=1, keepdims=True) for s in scores]
-    )
+    top = functools.reduce(jnp.maximum, [jnp.max(s, axis=1, keepdims=True) for s in scores])
     total = None
     acc = None
-    for s, (_, value, _) in zip(scores, blocks):
+    for s, (kv, _) in zip(scores, blocks):
         weights = jnp.exp2(s - top)
         part = jnp.sum(weights, axis=1, keepdims=True)
         out = jnp.dot(
-            weights.astype(jnp.bfloat16), value[:, lanes], preferred_element_type=jnp.float32
+            weights.astype(jnp.bfloat16), kv[1, :, lanes], preferred_element_type=jnp.float32
         )
         total = part if total is None else total + part
         acc = out if acc is None else acc + out
@@ -158,9 +159,9 @@
     return [slice(h * head_width, (h + 1) * head_width) for h in range(count)]
 
 
-def part_kernel(where, q, key, value, bias, tops, totals, accs, *, head_width, factor):
+def part_kernel(where, q, kv, bias, tops, totals, accs, *, head_width, factor):
     for lanes in head_lanes(q, head_width):
-        blocks = [(key, value, bias[...])]
+        blocks = [(kv, bias[...])]
         top, total, acc = softmax_part(q, blocks, lanes, factor)
         tops[:, lanes] = wide(top)
         totals[:, lanes] = wide(total)
@@ -168,12 +169,12 @@
 
 
 def help_kernel(where, q, *refs, blocks, head_width, factor, helper):
-    out, logs = refs[3 * blocks :]
+    out, logs = refs[2 * blocks :]
 
     @pl.when(where[1] == helper)
     def _():
         for h, lanes in enumerate(head_lanes(q, head_width)):
-            ready = [(refs[3 * n], refs[3 * n + 1], refs[3 * n + 2][...]) for n in range(blocks)]
+            ready = [(refs[2 * n], refs[2 * n + 1][...]) for n in range(blocks)]
             top, total, acc = softmax_part(q, ready, lanes, factor)
             out[:, lanes] = (acc / total).astype(jnp.bfloat16)
             logs[h : h + 1, :] = wide(top + jnp.log2(total)).T[:1, :]
@@ -182,8 +183,8 @@
 def final_kernel(where, q, *refs, far, only, helped, head_width, factor):
     shard = where[1]
     near = refs[:6]
-    kvs = refs[6 : 6 + 3 * len(far)]
-    given = refs[6 + 3 * len(far) : -2]
+    kvs = refs[6 : 6 + 2 * len(far)]
+    given = refs[6 + 2 * len(far) : -2]
     attended, logs = refs[-2:]
     rows = q.shape[0]
 
@@ -196,11 +197,7 @@
             ]
             if use_far:
                 blocks = [
-                    (
-                        kvs[3 * n],
-                        kvs[3 * n + 1],
-                        jnp.where(shard >= d, kvs[3 * n + 2][...], MASKED),
-                    )
+                    (kvs[2 * n], jnp.where(shard >= d, kvs[2 * n + 1][...], MASKED))
                     for n, d in enumerate(far)
                 ]
                 top, total, acc = softmax_part(q, blocks, lanes, factor)
@@ -236,9 +233,13 @@
     return lax.ppermute(value, "tp", [(i, i ^ distance) for i in range(count)])
 
 
+def send(value, pairs):
+    return lax.ppermute(value, "sp", pairs)
+
+
 def behind(value, steps):
     count = lax.axis_size("sp")
-    return lax.ppermute(value, "sp", [(s, s + steps) for s in range(count - steps)])
+    return send(value, [(s, s + steps) for s in range(count - steps)])
 
 
 def near_blocks(block):
@@ -254,12 +255,10 @@
 def turn_tables(positions, head_width):
     inverse = ROTARY_BASE ** (-jnp.arange(0, head_width, 2, dtype=jnp.float32) / head_width)
     angles = positions[:, None] * inverse[None, :]
-    cosine = jnp.cos(angles)
-    sine = jnp.sin(angles)
-    return jnp.concatenate([cosine, cosine], 1), jnp.concatenate([-sine, sine], 1)
-
-
-def local(hidden, norm_gain, w_query, w_key, w_value, query_gain, key_gain, w_out):
+    return jnp.cos(angles), jnp.sin(angles)
+
+
+def layer(hidden, norm_gain, w_query, w_key, w_value, query_gain, key_gain, w_out):
     rows, piece = hidden.shape
     head_count, head_width = query_gain.shape
     local_width = head_count * head_width
@@ -284,84 +283,78 @@
     weights = (w_query, w_key, w_value)
     sums = shape_of((rows, local_width), jnp.float32)
     half_sum = shape_of((rows, local_width), jnp.bfloat16)
+    pair = shape_of((2, rows, local_width), jnp.bfloat16)
     lane_wide = shape_of((rows, LANES), jnp.float32)
     square = shape_of((rows, rows), jnp.float32)
     early = tuple(range(half))
     late = tuple(range(half, count))
-
-    def begin(name, blocks, kinds, biases):
+    columns = w_out.shape[1] // count
+    slices = [
+        lax.dynamic_slice_in_dim(w_out, (me ^ k) * columns, columns, axis=1)
+        for k in range(count)
+    ]
+
+    def begin(blocks, kinds, biases):
         return call(
             functools.partial(early_kernel, offsets=early, kinds=kinds, biases=biases),
-            name,
             where,
             [*blocks, gain, *weights[3 - kinds :]],
             [sums] * kinds + [lane_wide] + [square] * len(biases),
         )
 
-    def finish(name, blocks, kinds, begun, turn):
+    def finish(blocks, kinds, begun, turn):
         return call(
             functools.partial(late_kernel, offsets=late, kinds=kinds, width=piece * count),
-            name,
             where,
             [*blocks, gain, *weights[3 - kinds :], *begun, *gains[3 - kinds :], *turn],
-            [half_sum] * kinds,
+            [half_sum] * (kinds - 2) + [pair],
+        )
+
+    def part(kv, bias):
+        return call(
+            functools.partial(part_kernel, head_width=head_width, factor=factor),
+            where,
+            [q, kv, bias],
+            [sums] * 3,
         )
 
     across = swap(hidden, half)
     own_near = near_blocks(hidden)
     before = behind(hidden, 1)
 
-    begun = begin("early_own", own_near, 3, tuple(distances))
+    begun = begin(own_near, 3, tuple(distances))
     biases = begun[4:]
     own_far = near_blocks(across)
     before_across = swap(before, half)
-    q, key, value = finish("late_own", own_far, 3, begun[:4], tables)
+    q, kv = finish(own_far, 3, begun[:4], tables)
 
     if helped is not None:
-        visitor = lax.ppermute(q, "sp", [(helped, 1)])
-        far_keys = [
-            (lax.ppermute(key, "sp", [(0, 2)]), lax.ppermute(value, "sp", [(0, 2)]), biases[2])
-        ]
+        visitor = send(q, [(helped, 1)])
+        far_blocks = [(send(kv, [(0, 2)]), biases[2])]
     else:
-        far_keys = [(behind(key, d), behind(value, d), biases[d]) for d in far]
-
-    begun_before = begin("early_before", near_blocks(before), 2, ())
-    own_part = call(
-        functools.partial(part_kernel, head_width=head_width, factor=factor),
-        "own_part",
-        where,
-        [q, key, value, biases[0]],
-        [sums] * 3,
-    )
-    key_before, value_before = finish(
-        "late_before", near_blocks(before_across), 2, begun_before, tables_before
-    )
+        far_blocks = [(behind(kv, d), biases[d]) for d in far]
+
+    begun_before = begin(near_blocks(before), 2, ())
+    own_part = part(kv, biases[0])
+    (kv_before,) = finish(near_blocks(before_across), 2, begun_before, tables_before)
     given = []
     if helped is not None:
         out, logs = call(
             functools.partial(
                 help_kernel, blocks=2, head_width=head_width, factor=factor, helper=1
             ),
-            "help",
             where,
-            [visitor, key, value, biases[2], key_before, value_before, biases[3]],
+            [visitor, kv, biases[2], kv_before, biases[3]],
             [half_sum, shape_of((8, rows), jnp.float32)],
         )
-        given = [lax.ppermute(out, "sp", [(1, helped)]), lax.ppermute(logs, "sp", [(1, helped)])]
-    before_part = call(
-        functools.partial(part_kernel, head_width=head_width, factor=factor),
-        "before_part",
-        where,
-        [q, key_before, value_before, biases[1]],
-        [sums] * 3,
-    )
-
-    columns = w_out.shape[1] // count
-    w_late, _ = lax.optimization_barrier((w_out, before_across))
-    slices = [
-        lax.dynamic_slice_in_dim(w_late, (me ^ k) * columns, columns, axis=1) for k in range(count)
-    ]
-    pieces = [slices[0]] + [swap(slices[k], k) for k in range(1, count)]
+        given = [send(out, [(1, helped)]), send(logs, [(1, helped)])]
+    before_part = part(kv_before, biases[1])
+
+    w_first, _ = lax.optimization_barrier((slices[-1], begun[3]))
+    *w_rest, _ = lax.optimization_barrier((*slices[1:-1], begun_before[2]))
+    pieces = [slices[0]]
+    pieces += [swap(w_rest[k - 1], k) for k in range(1, count - 1)]
+    pieces += [swap(w_first, count - 1)]
 
     attended, logs = call(
         functools.partial(
@@ -372,14 +365,13 @@
             head_width=head_width,
             factor=factor,
         ),
-        "final",
         where,
-        [q, *own_part, *before_part, *[x for block in far_keys for x in block], *given],
+        [q, *own_part, *before_part, *[x for block in far_blocks for x in block], *given],
         [half_sum, shape_of((head_count, rows), jnp.float32)],
     )
     gathered = lax.all_gather(attended, "tp", axis=0, tiled=False)
     (mixed,) = call(
-        mix_kernel, "mix", where, [gathered, *pieces], [shape_of((rows, columns), jnp.bfloat16)]
+        mix_kernel, where, [gathered, *pieces], [shape_of((rows, columns), jnp.bfloat16)]
     )
     return mixed, logs.T
 
@@ -396,7 +388,7 @@
         P("tp", None),
     )
     return jax.shard_map(
-        local,
+        layer,
         mesh=mesh,
         in_specs=placed,
         out_specs=(P(("grp", "sp"), "tp"), P(("grp", "sp"), "tp")),

time: 75 us -> 72.5 us (0.967)
  waiting for transfers between devices: 12.8 us -> 19.2 us
  starting transfers between devices: 20.6 us -> 15.9 us
  blocking collectives: 15.7 us -> 13.2 us
  Pallas kernels: 17.1 us -> 15.5 us
  other arithmetic: 2.7 us -> 1.52 us
  local copies, waits for them, and re-layouts: 4.79 us -> 5.61 us
    ppermute x6 -> x5, waiting for transfers between devices: 7.73 us -> 13.1 us  [send(): return lax.ppermute(value, 'sp', pairs)]
    ppermute x6 -> x5, starting transfers between devices: 12.1 us -> 7.78 us  [send(): return lax.ppermute(value, 'sp', pairs)]
    all_gather x1, blocking collectives: 15.7 us -> 13.2 us  [layer(): gathered = lax.all_gather(attended, 'tp', axis=0, tiled=False)]
    neg x1 -> x0, other arithmetic: 2.14 us -> none  [turn_tables(): -sine]
    pallas_call x9, Pallas kernels: 17.1 us -> 15.5 us  [call(): pl.pallas_call(body, out_shape=tuple(outs), in_specs=[SMEM] + [VMEM] * le...]
    sin x0 -> x1, other arithmetic: none -> 1.43 us  [turn_tables(): return (jnp.cos(angles), jnp.sin(angles))]
    dynamic_slice x1, local copies, waits for them, and re-layouts: 0.11 us -> 1.27 us  [layer(): lax.dynamic_slice_in_dim(w_out, (me ^ k) * columns, columns, axis=1)]
    ppermute x9, waiting for transfers between devices: 5.03 us -> 6.08 us  [swap(): return lax.ppermute(value, 'tp', [(i, i ^ distance) for i in range(count)])]
  transfers between devices with their start and end apart: 15 -> 14, of which waited for: 4 -> 3; matrix products, arithmetic and copies ran while one was open for 4% -> 4% of each run, Pallas kernels for 20% -> 19%
where the time goes in v3:
time: 72.5 us; the launch traced here: 71.7 us
  waiting for transfers between devices  19.2 us (26%)
  starting transfers between devices  15.9 us (22%)
  Pallas kernels  15.5 us (21%)
  blocking collectives  13.2 us (18%)
  local copies, waits for them, and re-layouts  5.61 us (8%)
  other arithmetic  1.52 us (2%)
  between operations  0.86 us (1%)
    pallas_call x9, Pallas kernels, call(): pl.pallas_call(body, out_shape=tuple(outs), in_specs=[SMEM] + [VMEM] * le...  15.5 us
    all_gather x1, blocking collectives, layer(): gathered = lax.all_gather(attended, 'tp', axis=0, tiled=False)  13.2 us
    ppermute x5, waiting for transfers between devices, send(): return lax.ppermute(value, 'sp', pairs)  13.1 us
    ppermute x9, starting transfers between devices, swap(): return lax.ppermute(value, 'tp', [(i, i ^ distance) for i in range(count)])  8.08 us
    ppermute x5, starting transfers between devices, send(): return lax.ppermute(value, 'sp', pairs)  7.78 us
    ppermute x9, waiting for transfers between devices, swap(): return lax.ppermute(value, 'tp', [(i, i ^ distance) for i in range(count)])  6.08 us
    unnamed x18, local copies, waits for them, and re-layouts  4.33 us
  transfers between devices with their start and end apart: 14, of which 3 were waited for; matrix products, arithmetic and copies ran while one was open for 4% of the time, Pallas kernels for 19%

profile of v3, /device:TPU:15, one launch (start us, length us, event | category | flops | bytes accessed | tf_op | source)
XLA Modules:
  0.0 71.7 jit_solution(14892075451147840559)
XLA Ops:
  0.6 3.2 %collective-permute-start.3 = (bf16[384,512]{1,0:T(8,128)(2,1)}, bf16[384,512]{1,0:T(8,128)(2,1)S(1)}, u32[]{:S(2)}, u32[]{:S(2)}) collective-permute-start(bf16[384,512]{1,0:T(8,128)(2,1)} %refs_0_.1), channel_id=1, source_target_pairs={{0,4},{4,8},{8,12},{1,5},{5,9},{9,13},{2,6},{6,10},{10,14},{3,7},{... | collective-permute-start | bytes 1179656 | tf_op jit(solution)/shard_map/ppermute | solution.py:237
  3.8 0.3 collective-permute-start
  4.2 8.6 %collective-permute-done.3.refs_0_ = bf16[384,512]{1,0:T(8,128)(2,1)S(1)} collective-permute-done((bf16[384,512]{1,0:T(8,128)(2,1)}, bf16[384,512]{1,0:T(8,128)(2,1)S(1)}, u32[]{:S(2)}, u32[]{:S(2)}) %collective-permute-start.3) | collective-permute-done | bytes 393248 | tf_op jit(solution)/shard_map/ppermute | solution.py:237
  12.7 0.3 collective-permute-start.4
  13.0 1.8 %collective-permute-start.2 = (bf16[384,512]{1,0:T(8,128)(2,1)}, bf16[384,512]{1,0:T(8,128)(2,1)S(1)}, u32[]{:S(2)}, u32[]{:S(2)}) collective-permute-start(bf16[384,512]{1,0:T(8,128)(2,1)} %refs_0_.1), channel_id=1, source_target_pairs={{0,1},{1,0},{2,3},{3,2},{4,5},{5,4},{6,7},{7,6},{8,9},{9,8},{10,11... | collective-permute-start | bytes 1179656 | tf_op jit(solution)/shard_map/ppermute | solution.py:233
  14.8 0.0 collective-permute-done.refs_0_
  14.8 0.8 %collective-permute-start.1 = (bf16[384,512]{1,0:T(8,128)(2,1)S(1)}, bf16[384,512]{1,0:T(8,128)(2,1)}, u32[]{:S(2)}, u32[]{:S(2)}) collective-permute-start(bf16[384,512]{1,0:T(8,128)(2,1)S(1)} %collective-permute-done.refs_0_), channel_id=1, source_target_pairs={{0,1},{1,0},{2,3},{3,2},{4,5},{5,4},{6,7},{7,6},{8,9},{9,8},{10,11... | collective-permute-start | bytes 1179656 | tf_op jit(solution)/shard_map/ppermute | solution.py:233
  15.7 0.1 pad_add_fusion.where
  15.7 0.1 collective-permute-start.6
  15.8 6.1 %collective-permute-done.4.refs_0_ = bf16[384,512]{1,0:T(8,128)(2,1)S(1)} collective-permute-done((bf16[384,512]{1,0:T(8,128)(2,1)S(1)}, bf16[384,512]{1,0:T(8,128)(2,1)S(1)}, u32[]{:S(2)}, u32[]{:S(2)}) %collective-permute-start.4) | collective-permute-done | bytes 393248 | tf_op jit(solution)/shard_map/ppermute | solution.py:233
  21.9 2.4 %collective-permute-start.5 = (bf16[384,512]{1,0:T(8,128)(2,1)S(1)}, bf16[384,512]{1,0:T(8,128)(2,1)S(1)}, u32[]{:S(2)}, u32[]{:S(2)}) collective-permute-start(bf16[384,512]{1,0:T(8,128)(2,1)S(1)} %collective-permute-done.4.refs_0_), channel_id=1, source_target_pairs={{0,1},{1,0},{2,3},{3,2},{4,5},{5,4},{6,7},{7,6},{8,9},{9,8},{10,11... | collective-permute-start | bytes 1179656 | tf_op jit(solution)/shard_map/ppermute | solution.py:233
  24.3 1.4 %multiply_sine_fusion = (f32[384,64]{1,0:T(8,128)S(1)}, f32[384,64]{1,0:T(8,128)S(1)}, f32[384,64]{1,0:T(8,128)S(1)}, f32[384,64]{1,0:T(8,128)S(1)}) fusion(f32[384]{0:T(512)S(1)} %get-tuple-element.64, f32[64]{0:T(128)S(1)} %multiply_power_fusion, f32[384]{0:T(512)S(1)} %get-tuple-element.65), kind=kLoop, calls=%fused_computation | loop fusion | flops 49152 | bytes 396544 | tf_op jit(solution)/shard_map/sin | solution.py:258
  25.7 0.0 collective-permute-done.2.refs_1_
  25.7 0.0 copy-done.5
  25.7 0.0 copy-start
  25.7 1.2 %copy-done = bf16[2048,256]{1,0:T(8,128)(2,1)S(1)} copy-done((bf16[2048,256]{1,0:T(8,128)(2,1)S(1)}, bf16[2048,256]{1,0:T(8,128)(2,1)}, u32[]{:S(2)}) %copy-start) | copy-done | bytes 1048600
  27.0 1.2 %copy-done.2 = bf16[2048,256]{1,0:T(8,128)(2,1)S(1)} copy-done((bf16[2048,256]{1,0:T(8,128)(2,1)S(1)}, bf16[2048,256]{1,0:T(8,128)(2,1)}, u32[]{:S(2)}) %copy-start.2) | copy-done | bytes 1048600
  28.2 1.2 %copy-done.4 = bf16[2048,256]{1,0:T(8,128)(2,1)S(1)} copy-done((bf16[2048,256]{1,0:T(8,128)(2,1)S(1)}, bf16[2048,256]{1,0:T(8,128)(2,1)}, u32[]{:S(2)}) %copy-start.4) | copy-done | bytes 1048600
  29.4 2.8 %shard_map.95 = (f32[384,256]{1,0:T(8,128)S(1)}, f32[384,256]{1,0:T(8,128)S(1)}, f32[384,256]{1,0:T(8,128)S(1)}, f32[384,128]{1,0:T(8,128)S(1)}, f32[384,384]{1,...) custom-call(s32[2]{0:T(128)S(1)} %pad_add_fusion.where, ...), custom_call_target="tpu_custom_call" | custom-call | tf_op jit(solution)/shard_map/pallas_call | solution.py:30
  32.2 0.0 collective-permute-done.1.refs_1_
  32.2 0.0 copy-start.6
  32.3 0.6 copy-done.6
  32.9 2.3 %shard_map.96 = (bf16[384,256]{1,0:T(8,128)(2,1)S(1)}, bf16[2,384,256]{2,1,0:T(8,128)(2,1)S(1)}) custom-call(s32[2]{0:T(128)S(1)} %pad_add_fusion.where, bf16[384,512]{1,0:T(8,128)(2,1)S(1)} %collective-permute-done.refs_0_, bf16[384,512]{1,0:T(8,128)(2,1)} %collective-permute-done.1.refs_1_, f32[4,512]{1,0:T(4,128)S(1)} %reshape.28.refs_2_, ...), custom_call_target="tpu_custom_call" | custom-call | tf_op jit(solution)/shard_map/pallas_call | solution.py:30
  35.2 1.3 %collective-permute-start.8 = (bf16[384,256]{1,0:T(8,128)(2,1)S(1)}, bf16[384,256]{1,0:T(8,128)(2,1)S(1)}, u32[]{:S(2)}, u32[]{:S(2)}) collective-permute-start(bf16[384,256]{1,0:T(8,128)(2,1)S(1)} %get-tuple-element.32.q), channel_id=1, source_target_pairs={{12,4},{13,5},{14,6},{15,7},{28,20},{29,21},{30,22},{31,23}} | collective-permute-start | bytes 589832 | tf_op jit(solution)/shard_map/ppermute | solution.py:237
  36.5 0.7 collective-permute-start.7
  37.2 0.0 collective-permute-done.6.refs_1_
  37.2 1.1 %shard_map.98 = (f32[384,256]{1,0:T(8,128)S(1)}, f32[384,256]{1,0:T(8,128)S(1)}, f32[384,128]{1,0:T(8,128)S(1)}) custom-call(s32[2]{0:T(128)S(1)} %pad_add_fusion.where, bf16[384,512]{1,0:T(8,128)(2,1)S(1)} %collective-permute-done.3.refs_0_, bf16[384,512]{1,0:T(8,128)(2,1)S(1)} %collective-permute-done.6.refs_1_, f32[4,512]{1,0:T(4,128)S(1)} %reshape.28.refs_2_, ...), custom_call_target="tpu_custom_call" | custom-call | tf_op jit(solution)/shard_map/pallas_call | solution.py:30
  38.3 0.0 collective-permute-done.5.refs_1_
  38.3 1.5 %shard_map.99.kv.refs_2_ = bf16[2,384,256]{2,1,0:T(8,128)(2,1)S(1)} custom-call(s32[2]{0:T(128)S(1)} %pad_add_fusion.where, bf16[384,512]{1,0:T(8,128)(2,1)S(1)} %collective-permute-done.4.refs_0_, bf16[384,512]{1,0:T(8,128)(2,1)S(1)} %collective-permute-done.5.refs_1_, f32[4,512]{1,0:T(4,128)S(1)} %reshape.28.refs_2_, bf16[2048,256]{1,0:T(8,128)(2,1)S(1)} %copy-done.1, ...), custom_call_target="tpu_custom_call" | custom-call | tf_op jit(solution)/shard_map/pallas_call | solution.py:30
  39.8 4.6 %collective-permute-done.8.q = bf16[384,256]{1,0:T(8,128)(2,1)S(1)} collective-permute-done((bf16[384,256]{1,0:T(8,128)(2,1)S(1)}, bf16[384,256]{1,0:T(8,128)(2,1)S(1)}, u32[]{:S(2)}, u32[]{:S(2)}) %collective-permute-start.8) | collective-permute-done | bytes 196640 | tf_op jit(solution)/shard_map/ppermute | solution.py:237
  44.4 1.8 %shard_map.101 = (bf16[384,256]{1,0:T(8,128)(2,1)S(1)}, f32[8,384]{1,0:T(8,128)S(1)}) custom-call(s32[2]{0:T(128)S(1)} %pad_add_fusion.where, bf16[384,256]{1,0:T(8,128)(2,1)S(1)} %collective-permute-done.8.q, bf16[2,384,256]{2,1,0:T(8,128)(2,1)S(1)} %get-tuple-element.33.kv.refs_0_, f32[384,384]{1,0:T(8,128)S(1)} %get-tuple-element.45.refs_1_.refs_7_, ...), custom_call_target="tpu_custom_call" | custom-call | tf_op jit(solution)/shard_map/pallas_call | solution.py:30
  46.2 1.3 %collective-permute-start.9 = (bf16[384,256]{1,0:T(8,128)(2,1)S(1)}, bf16[384,256]{1,0:T(8,128)(2,1)S(1)}, u32[]{:S(2)}, u32[]{:S(2)}) collective-permute-start(bf16[384,256]{1,0:T(8,128)(2,1)S(1)} %get-tuple-element.47), channel_id=1, source_target_pairs={{4,12},{5,13},{6,14},{7,15},{20,28},{21,29},{22,30},{23,31}} | collective-permute-start | bytes 589832 | tf_op jit(solution)/shard_map/ppermute | solution.py:237
  47.5 1.3 %collective-permute-start.10 = (f32[8,384]{1,0:T(8,128)S(1)}, f32[8,384]{1,0:T(8,128)S(1)}, u32[]{:S(2)}, u32[]{:S(2)}) collective-permute-start(f32[8,384]{1,0:T(8,128)S(1)} %get-tuple-element.48), channel_id=1, source_target_pairs={{4,12},{5,13},{6,14},{7,15},{20,28},{21,29},{22,30},{23,31}} | collective-permute-start | bytes 36872 | tf_op jit(solution)/shard_map/ppermute | solution.py:237
  48.8 1.3 %constant_dynamic-slice_fusion = (bf16[256,512]{1,0:T(8,128)(2,1)S(1)}, bf16[256,512]{1,0:T(8,128)(2,1)S(1)}, bf16[256,512]{1,0:T(8,128)(2,1)S(1)}, bf16[256,512]{1,0:T(8,128)(2,1)S(1)}) fusion(bf16[256,2048]{1,0:T(8,128)(2,1)} %param.15, s32[]{:T(128)S(6)} %select_n.15, s32[]{:T(128)S(6)} %select_n.13, s32[]{:T(128)S(6)} %select_n.12, s32[]{:T(128)S(6)} %select_n.14), kind=kLoop, calls=%fused_computation.7 | loop fusion | bytes 2097168 | tf_op jit(solution)/shard_map/dynamic_slice | solution.py:293
  50.1 1.1 %collective-permute-start.13 = (bf16[256,512]{1,0:T(8,128)(2,1)S(1)}, bf16[256,512]{1,0:T(8,128)(2,1)S(1)}, u32[]{:S(2)}, u32[]{:S(2)}) collective-permute-start(bf16[256,512]{1,0:T(8,128)(2,1)S(1)} %get-tuple-element.52), channel_id=1, source_target_pairs={{0,3},{1,2},{2,1},{3,0},{4,7},{5,6},{6,5},{7,4},{8,11},{9,10},{10,... | collective-permute-start | bytes 786440 | tf_op jit(solution)/shard_map/ppermute | solution.py:233
  51.2 1.3 %shard_map.97 = (f32[384,256]{1,0:T(8,128)S(1)}, f32[384,256]{1,0:T(8,128)S(1)}, f32[384,256]{1,0:T(8,128)S(1)}) custom-call(s32[2]{0:T(128)S(1)} %pad_add_fusion.where, bf16[384,256]{1,0:T(8,128)(2,1)S(1)} %get-tuple-element.32.q, bf16[2,384,256]{2,1,0:T(8,128)(2,1)S(1)} %get-tuple-element.33.kv.refs_0_, f32[384,384]{1,0:T(8,128)S(1)} %get-tuple-element.34.bias), custom_call_target="tpu_custom_call" | custom-call | tf_op jit(solution)/shard_map/pallas_call | solution.py:30
  52.5 0.1 collective-permute-start.11
  52.6 1.4 %shard_map.100 = (f32[384,256]{1,0:T(8,128)S(1)}, f32[384,256]{1,0:T(8,128)S(1)}, f32[384,256]{1,0:T(8,128)S(1)}) custom-call(s32[2]{0:T(128)S(1)} %pad_add_fusion.where, bf16[384,256]{1,0:T(8,128)(2,1)S(1)} %get-tuple-element.32.q, bf16[2,384,256]{2,1,0:T(8,128)(2,1)S(1)} %shard_map.99.kv.refs_2_, f32[384,384]{1,0:T(8,128)S(1)} %get-tuple-element.41.bias), custom_call_target="tpu_custom_call" | custom-call | tf_op jit(solution)/shard_map/pallas_call | solution.py:30
  54.0 0.0 collective-permute-done.7.refs_6_
  54.0 1.3 %collective-permute-start.12 = (bf16[256,512]{1,0:T(8,128)(2,1)S(1)}, bf16[256,512]{1,0:T(8,128)(2,1)S(1)}, u32[]{:S(2)}, u32[]{:S(2)}) collective-permute-start(bf16[256,512]{1,0:T(8,128)(2,1)S(1)} %get-tuple-element.51), channel_id=1, source_target_pairs={{0,2},{1,3},{2,0},{3,1},{4,6},{5,7},{6,4},{7,5},{8,10},{9,11},{10,... | collective-permute-start | bytes 786440 | tf_op jit(solution)/shard_map/ppermute | solution.py:233
  55.2 0.0 collective-permute-done.10.refs_9_
  55.2 0.0 collective-permute-done.9.refs_8_
  55.2 1.4 %shard_map.102 = (bf16[384,256]{1,0:T(8,128)(2,1)S(1)}, f32[2,384]{1,0:T(2,128)}) custom-call(s32[2]{0:T(128)S(1)} %pad_add_fusion.where, bf16[384,256]{1,0:T(8,128)(2,1)S(1)} %get-tuple-element.32.q, f32[384,256]{1,0:T(8,128)S(1)} %get-tuple-element.35.refs_0_, f32[384,256]{1,0:T(8,128)S(1)} %get-tuple-element.36.refs_1_, ...), custom_call_target="tpu_custom_call" | custom-call | tf_op jit(solution)/shard_map/pallas_call | solution.py:30
  56.7 13.2 %all-gather = bf16[1536,256]{1,0:T(8,128)(2,1)S(1)} all-gather(bf16[384,256]{1,0:T(8,128)(2,1)S(1)} %get-tuple-element.49), channel_id=2, replica_groups=mesh['grp'=2,'sp'=4,'tp'=4] {'tp'}, dimensions={0}, use_global_device_ids=true | all-gather | bytes 983040 | tf_op jit(solution)/shard_map/all_gather | solution.py:372
  69.8 0.0 collective-permute-done.13.refs_3_
  69.8 0.0 collective-permute-done.11.refs_1_
  69.8 0.0 collective-permute-done.12.refs_2_
  69.8 1.9 %shard_map.103 = bf16[384,512]{1,0:T(8,128)(2,1)} custom-call(s32[2]{0:T(128)S(1)} %pad_add_fusion.where, bf16[4,384,256]{2,1,0:T(8,128)(2,1)S(1)} %bitcast.4, bf16[256,512]{1,0:T(8,128)(2,1)S(1)} %get-tuple-element.56.refs_0_, bf16[256,512]{1,0:T(8,128)(2,1)S(1)} %collective-permute-done.11.refs_1_, bf16[256,512]{1,0:T(8,128)(2,1)S(1)} %collective-permute-done.12.refs_2_, ...), custom_call_target="tpu_custom_call" | custom-call | tf_op jit(solution)/shard_map/pallas_call | solution.py:30
  (14 shorter events, 0.0 us)
Async XLA Ops:
  0.6 12.1 %collective-permute-start.3 = (bf16[384,512]{1,0:T(8,128)(2,1)}, bf16[384,512]{1,0:T(8,128)(2,1)S(1)}, u32[]{:S(2)}, u32[]{:S(2)}) collective-permute-start(bf16[384,512]{1,0:T(8,128)(2,1)} %refs_0_.1), channel_id=1, source_target_pairs={{0,4},{4,8},{8,12},{1,5},{5,9},{9,13},{2,6},{6,10},{10,14},{3,7},{... | collective-permute-start | bytes 1179656 | tf_op jit(solution)/shard_map/ppermute | solution.py:237
  3.8 11.0 %collective-permute-start = (bf16[384,512]{1,0:T(8,128)(2,1)}, bf16[384,512]{1,0:T(8,128)(2,1)S(1)}, u32[]{:S(2)}, u32[]{:S(2)}) collective-permute-start(bf16[384,512]{1,0:T(8,128)(2,1)} %refs_0_.1), channel_id=1, source_target_pairs={{0,2},{1,3},{2,0},{3,1},{4,6},{5,7},{6,4},{7,5},{8,10},{9,11},{10,... | collective-permute-start | bytes 1179656 | tf_op jit(solution)/shard_map/ppermute | solution.py:233
  12.7 9.1 %collective-permute-start.4 = (bf16[384,512]{1,0:T(8,128)(2,1)S(1)}, bf16[384,512]{1,0:T(8,128)(2,1)S(1)}, u32[]{:S(2)}, u32[]{:S(2)}) collective-permute-start(bf16[384,512]{1,0:T(8,128)(2,1)S(1)} %collective-permute-done.3.refs_0_), channel_id=1, source_target_pairs={{0,2},{1,3},{2,0},{3,1},{4,6},{5,7},{6,4},{7,5},{8,10},{9,11},{10,... | collective-permute-start | bytes 1179656 | tf_op jit(solution)/shard_map/ppermute | solution.py:233
  13.0 12.7 %collective-permute-start.2 = (bf16[384,512]{1,0:T(8,128)(2,1)}, bf16[384,512]{1,0:T(8,128)(2,1)S(1)}, u32[]{:S(2)}, u32[]{:S(2)}) collective-permute-start(bf16[384,512]{1,0:T(8,128)(2,1)} %refs_0_.1), channel_id=1, source_target_pairs={{0,1},{1,0},{2,3},{3,2},{4,5},{5,4},{6,7},{7,6},{8,9},{9,8},{10,11... | collective-permute-start | bytes 1179656 | tf_op jit(solution)/shard_map/ppermute | solution.py:233
  14.8 0.9 %copy-start.8 = (bf16[2048]{0:T(1024)(128)(2,1)S(1)}, bf16[2048]{0:T(1024)(128)(2,1)}, u32[]{:S(2)}) copy-start(bf16[2048]{0:T(1024)(128)(2,1)} %param.9) | copy-start | bytes 12292
  14.8 17.4 %collective-permute-start.1 = (bf16[384,512]{1,0:T(8,128)(2,1)S(1)}, bf16[384,512]{1,0:T(8,128)(2,1)}, u32[]{:S(2)}, u32[]{:S(2)}) collective-permute-start(bf16[384,512]{1,0:T(8,128)(2,1)S(1)} %collective-permute-done.refs_0_), channel_id=1, source_target_pairs={{0,1},{1,0},{2,3},{3,2},{4,5},{5,4},{6,7},{7,6},{8,9},{9,8},{10,11... | collective-permute-start | bytes 1179656 | tf_op jit(solution)/shard_map/ppermute | solution.py:233
  15.7 21.4 %collective-permute-start.6 = (bf16[384,512]{1,0:T(8,128)(2,1)S(1)}, bf16[384,512]{1,0:T(8,128)(2,1)S(1)}, u32[]{:S(2)}, u32[]{:S(2)}) collective-permute-start(bf16[384,512]{1,0:T(8,128)(2,1)S(1)} %collective-permute-done.3.refs_0_), channel_id=1, source_target_pairs={{0,1},{1,0},{2,3},{3,2},{4,5},{5,4},{6,7},{7,6},{8,9},{9,8},{10,11... | collective-permute-start | bytes 1179656 | tf_op jit(solution)/shard_map/ppermute | solution.py:233
  21.9 16.4 %collective-permute-start.5 = (bf16[384,512]{1,0:T(8,128)(2,1)S(1)}, bf16[384,512]{1,0:T(8,128)(2,1)S(1)}, u32[]{:S(2)}, u32[]{:S(2)}) collective-permute-start(bf16[384,512]{1,0:T(8,128)(2,1)S(1)} %collective-permute-done.4.refs_0_), channel_id=1, source_target_pairs={{0,1},{1,0},{2,3},{3,2},{4,5},{5,4},{6,7},{7,6},{8,9},{9,8},{10,11... | collective-permute-start | bytes 1179656 | tf_op jit(solution)/shard_map/ppermute | solution.py:233
  24.3 1.4 %copy-start.5 = (bf16[384,512]{1,0:T(8,128)(2,1)S(1)}, bf16[384,512]{1,0:T(8,128)(2,1)}, u32[]{:S(2)}) copy-start(bf16[384,512]{1,0:T(8,128)(2,1)} %refs_0_.1) | copy-start | bytes 1179652
  25.7 1.2 %copy-start = (bf16[2048,256]{1,0:T(8,128)(2,1)S(1)}, bf16[2048,256]{1,0:T(8,128)(2,1)}, u32[]{:S(2)}) copy-start(bf16[2048,256]{1,0:T(8,128)(2,1)} %refs_3_.7) | copy-start | bytes 3145732
  27.0 1.2 %copy-start.2 = (bf16[2048,256]{1,0:T(8,128)(2,1)S(1)}, bf16[2048,256]{1,0:T(8,128)(2,1)}, u32[]{:S(2)}) copy-start(bf16[2048,256]{1,0:T(8,128)(2,1)} %refs_4_.7) | copy-start | bytes 3145732
  28.2 1.2 %copy-start.4 = (bf16[2048,256]{1,0:T(8,128)(2,1)S(1)}, bf16[2048,256]{1,0:T(8,128)(2,1)}, u32[]{:S(2)}) copy-start(bf16[2048,256]{1,0:T(8,128)(2,1)} %refs_3_.5) | copy-start | bytes 3145732
  29.4 2.8 %copy-start.1 = (bf16[2048,256]{1,0:T(8,128)(2,1)S(1)}, bf16[2048,256]{1,0:T(8,128)(2,1)}, u32[]{:S(2)}) copy-start(bf16[2048,256]{1,0:T(8,128)(2,1)} %refs_3_.7) | copy-start | bytes 3145732
  29.4 2.8 %copy-start.3 = (bf16[2048,256]{1,0:T(8,128)(2,1)S(1)}, bf16[2048,256]{1,0:T(8,128)(2,1)}, u32[]{:S(2)}) copy-start(bf16[2048,256]{1,0:T(8,128)(2,1)} %refs_4_.7) | copy-start | bytes 3145732
  29.4 2.9 %copy-start.7 = (f32[2,128]{1,0:T(2,128)S(1)}, f32[2,128]{1,0:T(2,128)}, u32[]{:S(2)}) copy-start(f32[2,128]{1,0:T(2,128)} %refs_10_.1) | copy-start | bytes 3076
  32.2 0.7 copy-start.6
  35.2 9.2 %collective-permute-start.8 = (bf16[384,256]{1,0:T(8,128)(2,1)S(1)}, bf16[384,256]{1,0:T(8,128)(2,1)S(1)}, u32[]{:S(2)}, u32[]{:S(2)}) collective-permute-start(bf16[384,256]{1,0:T(8,128)(2,1)S(1)} %get-tuple-element.32.q), channel_id=1, source_target_pairs={{12,4},{13,5},{14,6},{15,7},{28,20},{29,21},{30,22},{31,23}} | collective-permute-start | bytes 589832 | tf_op jit(solution)/shard_map/ppermute | solution.py:237
  36.5 17.5 %collective-permute-start.7 = (bf16[2,384,256]{2,1,0:T(8,128)(2,1)S(1)}, bf16[2,384,256]{2,1,0:T(8,128)(2,1)S(1)}, u32[]{:S(2)}, u32[]{:S(2)}) collective-permute-start(bf16[2,384,256]{2,1,0:T(8,128)(2,1)S(1)} %get-tuple-element.33.kv.refs_0_), channel_id=1, source_target_pairs={{0,8},{1,9},{2,10},{3,11},{16,24},{17,25},{18,26},{19,27}} | collective-permute-start | bytes 1179656 | tf_op jit(solution)/shard_map/ppermute | solution.py:237
  46.2 9.1 %collective-permute-start.9 = (bf16[384,256]{1,0:T(8,128)(2,1)S(1)}, bf16[384,256]{1,0:T(8,128)(2,1)S(1)}, u32[]{:S(2)}, u32[]{:S(2)}) collective-permute-start(bf16[384,256]{1,0:T(8,128)(2,1)S(1)} %get-tuple-element.47), channel_id=1, source_target_pairs={{4,12},{5,13},{6,14},{7,15},{20,28},{21,29},{22,30},{23,31}} | collective-permute-start | bytes 589832 | tf_op jit(solution)/shard_map/ppermute | solution.py:237
  47.5 7.7 %collective-permute-start.10 = (f32[8,384]{1,0:T(8,128)S(1)}, f32[8,384]{1,0:T(8,128)S(1)}, u32[]{:S(2)}, u32[]{:S(2)}) collective-permute-start(f32[8,384]{1,0:T(8,128)S(1)} %get-tuple-element.48), channel_id=1, source_target_pairs={{4,12},{5,13},{6,14},{7,15},{20,28},{21,29},{22,30},{23,31}} | collective-permute-start | bytes 36872 | tf_op jit(solution)/shard_map/ppermute | solution.py:237
  50.1 19.7 %collective-permute-start.13 = (bf16[256,512]{1,0:T(8,128)(2,1)S(1)}, bf16[256,512]{1,0:T(8,128)(2,1)S(1)}, u32[]{:S(2)}, u32[]{:S(2)}) collective-permute-start(bf16[256,512]{1,0:T(8,128)(2,1)S(1)} %get-tuple-element.52), channel_id=1, source_target_pairs={{0,3},{1,2},{2,1},{3,0},{4,7},{5,6},{6,5},{7,4},{8,11},{9,10},{10,... | collective-permute-start | bytes 786440 | tf_op jit(solution)/shard_map/ppermute | solution.py:233
  52.5 17.3 %collective-permute-start.11 = (bf16[256,512]{1,0:T(8,128)(2,1)S(1)}, bf16[256,512]{1,0:T(8,128)(2,1)S(1)}, u32[]{:S(2)}, u32[]{:S(2)}) collective-permute-start(bf16[256,512]{1,0:T(8,128)(2,1)S(1)} %get-tuple-element.50), channel_id=1, source_target_pairs={{0,1},{1,0},{2,3},{3,2},{4,5},{5,4},{6,7},{7,6},{8,9},{9,8},{10,11... | collective-permute-start | bytes 786440 | tf_op jit(solution)/shard_map/ppermute | solution.py:233
  54.0 15.9 %collective-permute-start.12 = (bf16[256,512]{1,0:T(8,128)(2,1)S(1)}, bf16[256,512]{1,0:T(8,128)(2,1)S(1)}, u32[]{:S(2)}, u32[]{:S(2)}) collective-permute-start(bf16[256,512]{1,0:T(8,128)(2,1)S(1)} %get-tuple-element.51), channel_id=1, source_target_pairs={{0,2},{1,3},{2,0},{3,1},{4,6},{5,7},{6,4},{7,5},{8,10},{9,11},{10,... | collective-permute-start | bytes 786440 | tf_op jit(solution)/shard_map/ppermute | solution.py:233

commit v4 on v3

--- a/solution.py
+++ b/solution.py
@@ -74,17 +74,20 @@
     return sums, squares
 
 
-def early_kernel(where, *refs, offsets, kinds, biases):
+def early_kernel(where, *refs, offsets, kinds, biases, copies):
     count = len(offsets)
     hidden = refs[:count]
     gain = refs[count]
     weights = refs[count + 1 : count + 1 + kinds]
-    outs = refs[count + 1 + kinds :]
+    small = refs[count + 1 + kinds : count + 1 + kinds + copies]
+    outs = refs[count + 1 + kinds + copies :]
     sums, squares = sums_of(where, hidden, gain, weights, offsets)
     for out, total in zip(outs[:kinds], sums):
         out[...] = total
     outs[kinds][...] = wide(squares)
-    for d, out in zip(biases, outs[kinds + 1 :]):
+    for ref, out in zip(small, outs[kinds + 1 :]):
+        out[...] = ref[...]
+    for d, out in zip(biases, outs[kinds + 1 + copies :]):
         out[...] = pair_bias(out.shape[0], d)
 
 
@@ -159,9 +162,14 @@
     return [slice(h * head_width, (h + 1) * head_width) for h in range(count)]
 
 
-def part_kernel(where, q, kv, bias, tops, totals, accs, *, head_width, factor):
+def near_kernel(where, q, *refs, distances, head_width, factor):
+    count = len(distances)
+    tops, totals, accs = refs[2 * count :]
     for lanes in head_lanes(q, head_width):
-        blocks = [(kv, bias[...])]
+        blocks = []
+        for n, d in enumerate(distances):
+            bias = refs[2 * n + 1][...]
+            blocks.append((refs[2 * n], jnp.where(where[1] >= d, bias, MASKED) if d else bias))
         top, total, acc = softmax_part(q, blocks, lanes, factor)
         tops[:, lanes] = wide(top)
         totals[:, lanes] = wide(total)
@@ -182,19 +190,15 @@
 
 def final_kernel(where, q, *refs, far, only, helped, head_width, factor):
     shard = where[1]
-    near = refs[:6]
-    kvs = refs[6 : 6 + 2 * len(far)]
-    given = refs[6 + 2 * len(far) : -2]
+    near = refs[:3]
+    kvs = refs[3 : 3 + 2 * len(far)]
+    given = refs[3 + 2 * len(far) : -2]
     attended, logs = refs[-2:]
     rows = q.shape[0]
 
     def finish(use_far, use_given):
         for h, lanes in enumerate(head_lanes(q, head_width)):
-            before = jnp.where(shard >= 1, near[3][:, lanes], MASKED)
-            parts = [
-                (near[0][:, lanes], near[1][:, lanes], near[2][:, lanes]),
-                (before, near[4][:, lanes], near[5][:, lanes]),
-            ]
+            parts = [tuple(ref[:, lanes] for ref in near)]
             if use_far:
                 blocks = [
                     (kvs[2 * n], jnp.where(shard >= d, kvs[2 * n + 1][...], MASKED))
@@ -207,7 +211,7 @@
                 parts.append((top, jnp.ones_like(top), given[0][:, lanes].astype(jnp.float32)))
             out, log_sum = merge(parts)
             attended[:, lanes] = out.astype(jnp.bfloat16)
-            logs[h : h + 1, :] = (log_sum * math.log(2.0)).T[:1, :]
+            logs[:, lanes] = log_sum
 
     with_far = (shard == only) if only is not None else (shard >= 2)
     with_given = (shard == helped) if helped is not None else (shard < 0)
@@ -218,14 +222,25 @@
     pl.when(jnp.logical_not(with_far | with_given))(lambda: finish(False, False))
 
 
-def mix_kernel(where, attended, *refs):
-    pieces, out = refs[:-1], refs[-1]
-    me = where[0]
+def products(blocks, pieces):
     total = None
-    for k, piece in enumerate(pieces):
-        product = jnp.dot(attended[me ^ k], piece[...], preferred_element_type=jnp.float32)
+    for block, piece in zip(blocks, pieces):
+        product = jnp.dot(block[...], piece[...], preferred_element_type=jnp.float32)
         total = product if total is None else total + product
-    out[...] = total.astype(jnp.bfloat16)
+    return total
+
+
+def mix_early_kernel(where, logs, *refs, count):
+    total, rows = refs[2 * count :]
+    total[...] = products(refs[:count], refs[count : 2 * count])
+    for h in range(rows.shape[0]):
+        lanes = slice(h * LANES, (h + 1) * LANES)
+        rows[h : h + 1, :] = (logs[:, lanes] * math.log(2.0)).T[:1, :]
+
+
+def mix_late_kernel(where, before, *refs, count):
+    total = before[...] + products(refs[:count], refs[count : 2 * count])
+    refs[-1][...] = total.astype(jnp.bfloat16)
 
 
 def swap(value, distance):
@@ -294,12 +309,17 @@
         for k in range(count)
     ]
 
-    def begin(blocks, kinds, biases):
+    def begin(blocks, kinds, biases, copied):
         return call(
-            functools.partial(early_kernel, offsets=early, kinds=kinds, biases=biases),
+            functools.partial(
+                early_kernel, offsets=early, kinds=kinds, biases=biases, copies=len(copied)
+            ),
             where,
-            [*blocks, gain, *weights[3 - kinds :]],
-            [sums] * kinds + [lane_wide] + [square] * len(biases),
+            [*blocks, gain, *weights[3 - kinds :], *copied],
+            [sums] * kinds
+            + [lane_wide]
+            + [shape_of(x.shape, x.dtype) for x in copied]
+            + [square] * len(biases),
         )
 
     def finish(blocks, kinds, begun, turn):
@@ -310,20 +330,13 @@
             [half_sum] * (kinds - 2) + [pair],
         )
 
-    def part(kv, bias):
-        return call(
-            functools.partial(part_kernel, head_width=head_width, factor=factor),
-            where,
-            [q, kv, bias],
-            [sums] * 3,
-        )
-
     across = swap(hidden, half)
     own_near = near_blocks(hidden)
     before = behind(hidden, 1)
 
-    begun = begin(own_near, 3, tuple(distances))
-    biases = begun[4:]
+    begun = begin(own_near, 3, tuple(distances), gains)
+    gains = begun[4:6]
+    biases = begun[6:]
     own_far = near_blocks(across)
     before_across = swap(before, half)
     q, kv = finish(own_far, 3, begun[:4], tables)
@@ -334,8 +347,7 @@
     else:
         far_blocks = [(behind(kv, d), biases[d]) for d in far]
 
-    begun_before = begin(near_blocks(before), 2, ())
-    own_part = part(kv, biases[0])
+    begun_before = begin(near_blocks(before), 2, (), ())
     (kv_before,) = finish(near_blocks(before_across), 2, begun_before, tables_before)
     given = []
     if helped is not None:
@@ -348,9 +360,16 @@
             [half_sum, shape_of((8, rows), jnp.float32)],
         )
         given = [send(out, [(1, helped)]), send(logs, [(1, helped)])]
-    before_part = part(kv_before, biases[1])
-
-    w_first, _ = lax.optimization_barrier((slices[-1], begun[3]))
+    near = call(
+        functools.partial(
+            near_kernel, distances=(0, 1), head_width=head_width, factor=factor
+        ),
+        where,
+        [q, kv, biases[0], kv_before, biases[1]],
+        [sums] * 3,
+    )
+
+    w_first, _ = lax.optimization_barrier((slices[-1], begun_before[2]))
     *w_rest, _ = lax.optimization_barrier((*slices[1:-1], begun_before[2]))
     pieces = [slices[0]]
     pieces += [swap(w_rest[k - 1], k) for k in range(1, count - 1)]
@@ -366,14 +385,24 @@
             factor=factor,
         ),
         where,
-        [q, *own_part, *before_part, *[x for block in far_blocks for x in block], *given],
-        [half_sum, shape_of((head_count, rows), jnp.float32)],
-    )
-    gathered = lax.all_gather(attended, "tp", axis=0, tiled=False)
+        [q, *near, *[x for block in far_blocks for x in block], *given],
+        [half_sum, sums],
+    )
+    attended_across = swap(attended, half)
+    mixed_shape = (rows, columns)
+    partial_mix, log_rows = call(
+        functools.partial(mix_early_kernel, count=half),
+        where,
+        [logs, *near_blocks(attended), *pieces[:half]],
+        [shape_of(mixed_shape, jnp.float32), shape_of((head_count, rows), jnp.float32)],
+    )
     (mixed,) = call(
-        mix_kernel, where, [gathered, *pieces], [shape_of((rows, columns), jnp.bfloat16)]
-    )
-    return mixed, logs.T
+        functools.partial(mix_late_kernel, count=half),
+        where,
+        [partial_mix, *near_blocks(attended_across), *pieces[half:]],
+        [shape_of(mixed_shape, jnp.bfloat16)],
+    )
+    return mixed, log_rows.T
 
 
 def solution(mesh):

time: 72.5 us -> 73.3 us (1.011)
  blocking collectives: 13.2 us -> 0 us
  waiting for transfers between devices: 19.2 us -> 28.5 us
  starting transfers between devices: 15.9 us -> 21.4 us
  local copies, waits for them, and re-layouts: 5.61 us -> 3.97 us
    all_gather x1 -> x0, blocking collectives: 13.2 us -> none  [layer(): gathered = lax.all_gather(attended, 'tp', axis=0, tiled=False)]
    ppermute x9 -> x12, waiting for transfers between devices: 6.08 us -> 14.4 us  [swap(): return lax.ppermute(value, 'tp', [(i, i ^ distance) for i in range(count)])]
    ppermute x9 -> x12, starting transfers between devices: 8.08 us -> 13.6 us  [swap(): return lax.ppermute(value, 'tp', [(i, i ^ distance) for i in range(count)])]
    dynamic_slice x1, local copies, waits for them, and re-layouts: 1.27 us -> 0.1 us  [layer(): lax.dynamic_slice_in_dim(w_out, (me ^ k) * columns, columns, axis=1)]
    ppermute x5, waiting for transfers between devices: 13.1 us -> 14.1 us  [send(): return lax.ppermute(value, 'sp', pairs)]
    unnamed x18 -> x20, local copies, waits for them, and re-layouts: 4.33 us -> 3.86 us
  transfers between devices with their start and end apart: 14 -> 17, of which waited for: 3 -> 7; matrix products, arithmetic and copies ran while one was open for 4% -> 2% of each run, Pallas kernels for 19% -> 19%
where the time goes in v4:
time: 73.3 us; the launch traced here: 72 us
  waiting for transfers between devices  28.5 us (39%)
  starting transfers between devices  21.4 us (29%)
  Pallas kernels  15.8 us (22%)
  local copies, waits for them, and re-layouts  3.97 us (5%)
  other arithmetic  1.52 us (2%)
  between operations  0.85 us (1%)
    pallas_call x9, Pallas kernels, call(): pl.pallas_call(body, out_shape=tuple(outs), in_specs=[SMEM] + [VMEM] * le...  15.8 us
    ppermute x12, waiting for transfers between devices, swap(): return lax.ppermute(value, 'tp', [(i, i ^ distance) for i in range(count)])  14.4 us
    ppermute x5, waiting for transfers between devices, send(): return lax.ppermute(value, 'sp', pairs)  14.1 us
    ppermute x12, starting transfers between devices, swap(): return lax.ppermute(value, 'tp', [(i, i ^ distance) for i in range(count)])  13.6 us
    ppermute x5, starting transfers between devices, send(): return lax.ppermute(value, 'sp', pairs)  7.76 us
    unnamed x20, local copies, waits for them, and re-layouts  3.86 us
  transfers between devices with their start and end apart: 17, of which 7 were waited for; matrix products, arithmetic and copies ran while one was open for 2% of the time, Pallas kernels for 19%

profile of v4, /device:TPU:15, one launch (start us, length us, event | category | flops | bytes accessed | tf_op | source)
XLA Modules:
  0.0 72.0 jit_solution(5208013931213390764)
XLA Ops:
  0.6 3.2 %collective-permute-start.3 = (bf16[384,512]{1,0:T(8,128)(2,1)}, bf16[384,512]{1,0:T(8,128)(2,1)S(1)}, u32[]{:S(2)}, u32[]{:S(2)}) collective-permute-start(bf16[384,512]{1,0:T(8,128)(2,1)} %refs_0_.1), channel_id=1, source_target_pairs={{0,4},{4,8},{8,12},{1,5},{5,9},{9,13},{2,6},{6,10},{10,14},{3,7},{... | collective-permute-start | bytes 1179656 | tf_op jit(solution)/shard_map/ppermute | solution.py:252
  3.8 0.3 collective-permute-start
  4.2 8.6 %collective-permute-done.3.refs_0_ = bf16[384,512]{1,0:T(8,128)(2,1)S(1)} collective-permute-done((bf16[384,512]{1,0:T(8,128)(2,1)}, bf16[384,512]{1,0:T(8,128)(2,1)S(1)}, u32[]{:S(2)}, u32[]{:S(2)}) %collective-permute-start.3) | collective-permute-done | bytes 393248 | tf_op jit(solution)/shard_map/ppermute | solution.py:252
  12.7 0.3 collective-permute-start.4
  13.0 1.8 %collective-permute-start.2 = (bf16[384,512]{1,0:T(8,128)(2,1)}, bf16[384,512]{1,0:T(8,128)(2,1)S(1)}, u32[]{:S(2)}, u32[]{:S(2)}) collective-permute-start(bf16[384,512]{1,0:T(8,128)(2,1)} %refs_0_.1), channel_id=1, source_target_pairs={{0,1},{1,0},{2,3},{3,2},{4,5},{5,4},{6,7},{7,6},{8,9},{9,8},{10,11... | collective-permute-start | bytes 1179656 | tf_op jit(solution)/shard_map/ppermute | solution.py:248
  14.8 0.8 %collective-permute-start.1 = (bf16[384,512]{1,0:T(8,128)(2,1)S(1)}, bf16[384,512]{1,0:T(8,128)(2,1)}, u32[]{:S(2)}, u32[]{:S(2)}) collective-permute-start(bf16[384,512]{1,0:T(8,128)(2,1)S(1)} %collective-permute-done.refs_0_), channel_id=1, source_target_pairs={{0,1},{1,0},{2,3},{3,2},{4,5},{5,4},{6,7},{7,6},{8,9},{9,8},{10,11... | collective-permute-start | bytes 1179656 | tf_op jit(solution)/shard_map/ppermute | solution.py:248
  15.7 0.1 pad_add_fusion.where
  15.7 0.1 collective-permute-start.6
  15.8 6.1 %collective-permute-done.4.refs_0_ = bf16[384,512]{1,0:T(8,128)(2,1)S(1)} collective-permute-done((bf16[384,512]{1,0:T(8,128)(2,1)S(1)}, bf16[384,512]{1,0:T(8,128)(2,1)S(1)}, u32[]{:S(2)}, u32[]{:S(2)}) %collective-permute-start.4) | collective-permute-done | bytes 393248 | tf_op jit(solution)/shard_map/ppermute | solution.py:248
  21.9 2.4 %collective-permute-start.5 = (bf16[384,512]{1,0:T(8,128)(2,1)S(1)}, bf16[384,512]{1,0:T(8,128)(2,1)S(1)}, u32[]{:S(2)}, u32[]{:S(2)}) collective-permute-start(bf16[384,512]{1,0:T(8,128)(2,1)S(1)} %collective-permute-done.4.refs_0_), channel_id=1, source_target_pairs={{0,1},{1,0},{2,3},{3,2},{4,5},{5,4},{6,7},{7,6},{8,9},{9,8},{10,11... | collective-permute-start | bytes 1179656 | tf_op jit(solution)/shard_map/ppermute | solution.py:248
  24.3 1.4 %multiply_sine_fusion = (f32[384,64]{1,0:T(8,128)S(1)}, f32[384,64]{1,0:T(8,128)S(1)}, f32[384,64]{1,0:T(8,128)S(1)}, f32[384,64]{1,0:T(8,128)S(1)}) fusion(f32[384]{0:T(512)S(1)} %get-tuple-element.66, f32[64]{0:T(128)S(1)} %multiply_power_fusion, f32[384]{0:T(512)S(1)} %get-tuple-element.67), kind=kLoop, calls=%fused_computation | loop fusion | flops 49152 | bytes 396544 | tf_op jit(solution)/shard_map/sin | solution.py:273
  25.7 0.0 collective-permute-done.2.refs_1_
  25.7 0.0 copy-start
  25.8 1.2 %copy-done = bf16[2048,256]{1,0:T(8,128)(2,1)S(1)} copy-done((bf16[2048,256]{1,0:T(8,128)(2,1)S(1)}, bf16[2048,256]{1,0:T(8,128)(2,1)}, u32[]{:S(2)}) %copy-start) | copy-done | bytes 1048600
  27.0 1.2 %copy-done.2 = bf16[2048,256]{1,0:T(8,128)(2,1)S(1)} copy-done((bf16[2048,256]{1,0:T(8,128)(2,1)S(1)}, bf16[2048,256]{1,0:T(8,128)(2,1)}, u32[]{:S(2)}) %copy-start.2) | copy-done | bytes 1048600
  28.2 1.2 %copy-done.4 = bf16[2048,256]{1,0:T(8,128)(2,1)S(1)} copy-done((bf16[2048,256]{1,0:T(8,128)(2,1)S(1)}, bf16[2048,256]{1,0:T(8,128)(2,1)}, u32[]{:S(2)}) %copy-start.4) | copy-done | bytes 1048600
  29.4 2.8 %shard_map.95 = (f32[384,256]{1,0:T(8,128)S(1)}, f32[384,256]{1,0:T(8,128)S(1)}, f32[384,256]{1,0:T(8,128)S(1)}, f32[384,128]{1,0:T(8,128)S(1)}, f32[2,128]{1,0:...) custom-call(s32[2]{0:T(128)S(1)} %pad_add_fusion.where, ...), custom_call_target="tpu_custom_call" | custom-call | tf_op jit(solution)/shard_map/pallas_call | solution.py:30
  32.2 0.0 collective-permute-done.1.refs_1_
  32.3 2.3 %shard_map.96 = (bf16[384,256]{1,0:T(8,128)(2,1)S(1)}, bf16[2,384,256]{2,1,0:T(8,128)(2,1)S(1)}) custom-call(s32[2]{0:T(128)S(1)} %pad_add_fusion.where, bf16[384,512]{1,0:T(8,128)(2,1)S(1)} %collective-permute-done.refs_0_, bf16[384,512]{1,0:T(8,128)(2,1)} %collective-permute-done.1.refs_1_, f32[4,512]{1,0:T(4,128)S(1)} %reshape.28.refs_2_, ...), custom_call_target="tpu_custom_call" | custom-call | tf_op jit(solution)/shard_map/pallas_call | solution.py:30
  34.6 1.3 %collective-permute-start.8 = (bf16[384,256]{1,0:T(8,128)(2,1)S(1)}, bf16[384,256]{1,0:T(8,128)(2,1)S(1)}, u32[]{:S(2)}, u32[]{:S(2)}) collective-permute-start(bf16[384,256]{1,0:T(8,128)(2,1)S(1)} %get-tuple-element.35.q), channel_id=1, source_target_pairs={{12,4},{13,5},{14,6},{15,7},{28,20},{29,21},{30,22},{31,23}} | collective-permute-start | bytes 589832 | tf_op jit(solution)/shard_map/ppermute | solution.py:252
  35.9 0.7 collective-permute-start.7
  36.6 0.0 collective-permute-done.6.refs_1_
  36.6 1.1 %shard_map.97 = (f32[384,256]{1,0:T(8,128)S(1)}, f32[384,256]{1,0:T(8,128)S(1)}, f32[384,128]{1,0:T(8,128)S(1)}) custom-call(s32[2]{0:T(128)S(1)} %pad_add_fusion.where, bf16[384,512]{1,0:T(8,128)(2,1)S(1)} %collective-permute-done.3.refs_0_, bf16[384,512]{1,0:T(8,128)(2,1)S(1)} %collective-permute-done.6.refs_1_, f32[4,512]{1,0:T(4,128)S(1)} %reshape.28.refs_2_, ...), custom_call_target="tpu_custom_call" | custom-call | tf_op jit(solution)/shard_map/pallas_call | solution.py:30
  37.7 0.0 collective-permute-done.5.refs_1_
  37.7 1.5 %shard_map.98.refs_2_ = bf16[2,384,256]{2,1,0:T(8,128)(2,1)S(1)} custom-call(s32[2]{0:T(128)S(1)} %pad_add_fusion.where, bf16[384,512]{1,0:T(8,128)(2,1)S(1)} %collective-permute-done.4.refs_0_, bf16[384,512]{1,0:T(8,128)(2,1)S(1)} %collective-permute-done.5.refs_1_, f32[4,512]{1,0:T(4,128)S(1)} %reshape.28.refs_2_, bf16[2048,256]{1,0:T(8,128)(2,1)S(1)} %copy-done.1, ...), custom_call_target="tpu_custom_call" | custom-call | tf_op jit(solution)/shard_map/pallas_call | solution.py:30
  39.2 4.6 %collective-permute-done.8.q = bf16[384,256]{1,0:T(8,128)(2,1)S(1)} collective-permute-done((bf16[384,256]{1,0:T(8,128)(2,1)S(1)}, bf16[384,256]{1,0:T(8,128)(2,1)S(1)}, u32[]{:S(2)}, u32[]{:S(2)}) %collective-permute-start.8) | collective-permute-done | bytes 196640 | tf_op jit(solution)/shard_map/ppermute | solution.py:252
  43.8 2.4 %shard_map.100 = (bf16[384,256]{1,0:T(8,128)(2,1)}, f32[8,384]{1,0:T(8,128)S(1)}) custom-call(s32[2]{0:T(128)S(1)} %pad_add_fusion.where, bf16[384,256]{1,0:T(8,128)(2,1)S(1)} %collective-permute-done.8.q, bf16[2,384,256]{2,1,0:T(8,128)(2,1)S(1)} %get-tuple-element.36.refs_0_, f32[384,384]{1,0:T(8,128)S(1)} %get-tuple-element.45.refs_1_.refs_4_, ...), custom_call_target="tpu_custom_call" | custom-call | tf_op jit(solution)/shard_map/pallas_call | solution.py:30
  46.3 1.3 %collective-permute-start.9 = (bf16[384,256]{1,0:T(8,128)(2,1)}, bf16[384,256]{1,0:T(8,128)(2,1)S(1)}, u32[]{:S(2)}, u32[]{:S(2)}) collective-permute-start(bf16[384,256]{1,0:T(8,128)(2,1)} %get-tuple-element.47), channel_id=1, source_target_pairs={{4,12},{5,13},{6,14},{7,15},{20,28},{21,29},{22,30},{23,31}} | collective-permute-start | bytes 589832 | tf_op jit(solution)/shard_map/ppermute | solution.py:252
  47.6 1.3 %collective-permute-start.10 = (f32[8,384]{1,0:T(8,128)S(1)}, f32[8,384]{1,0:T(8,128)S(1)}, u32[]{:S(2)}, u32[]{:S(2)}) collective-permute-start(f32[8,384]{1,0:T(8,128)S(1)} %get-tuple-element.48), channel_id=1, source_target_pairs={{4,12},{5,13},{6,14},{7,15},{20,28},{21,29},{22,30},{23,31}} | collective-permute-start | bytes 36872 | tf_op jit(solution)/shard_map/ppermute | solution.py:252
  48.9 1.8 %shard_map.99 = (f32[384,256]{1,0:T(8,128)S(1)}, f32[384,256]{1,0:T(8,128)S(1)}, f32[384,256]{1,0:T(8,128)S(1)}) custom-call(s32[2]{0:T(128)S(1)} %pad_add_fusion.where, bf16[384,256]{1,0:T(8,128)(2,1)S(1)} %get-tuple-element.35.q, bf16[2,384,256]{2,1,0:T(8,128)(2,1)S(1)} %get-tuple-element.36.refs_0_, f32[384,384]{1,0:T(8,128)S(1)} %get-tuple-element.37.refs_1_, ...), custom_call_target="tpu_custom_call" | custom-call | tf_op jit(solution)/shard_map/pallas_call | solution.py:30
  50.7 1.0 %collective-permute-done.10.refs_6_ = f32[8,384]{1,0:T(8,128)S(1)} collective-permute-done((f32[8,384]{1,0:T(8,128)S(1)}, f32[8,384]{1,0:T(8,128)S(1)}, u32[]{:S(2)}, u32[]{:S(2)}) %collective-permute-start.10) | collective-permute-done | bytes 12320 | tf_op jit(solution)/shard_map/ppermute | solution.py:252
  51.7 0.0 collective-permute-done.9.refs_5_
  51.7 0.7 %shard_map.101 = (bf16[384,256]{1,0:T(8,128)(2,1)S(1)}, f32[384,256]{1,0:T(8,128)S(1)}) custom-call(s32[2]{0:T(128)S(1)} %pad_add_fusion.where, bf16[384,256]{1,0:T(8,128)(2,1)S(1)} %get-tuple-element.35.q, f32[384,256]{1,0:T(8,128)S(1)} %get-tuple-element.42.refs_0_, f32[384,256]{1,0:T(8,128)S(1)} %get-tuple-element.43.refs_1_, ...), custom_call_target="tpu_custom_call" | custom-call | tf_op jit(solution)/shard_map/pallas_call | solution.py:30
  52.5 0.3 collective-permute-start.13
  52.8 0.2 copy-done.8
  53.0 0.1 constant_dynamic-slice_fusion
  53.1 1.6 %collective-permute-start.12 = (bf16[256,512]{1,0:T(8,128)(2,1)S(1)}, bf16[256,512]{1,0:T(8,128)(2,1)S(1)}, u32[]{:S(2)}, u32[]{:S(2)}) collective-permute-start(bf16[256,512]{1,0:T(8,128)(2,1)S(1)} %get-tuple-element.51), channel_id=1, source_target_pairs={{0,1},{1,0},{2,3},{3,2},{4,5},{5,4},{6,7},{7,6},{8,9},{9,8},{10,11... | collective-permute-start | bytes 786440 | tf_op jit(solution)/shard_map/ppermute | solution.py:248
  54.6 1.2 %collective-permute-start.15 = (bf16[256,512]{1,0:T(8,128)(2,1)S(1)}, bf16[256,512]{1,0:T(8,128)(2,1)S(1)}, u32[]{:S(2)}, u32[]{:S(2)}) collective-permute-start(bf16[256,512]{1,0:T(8,128)(2,1)S(1)} %get-tuple-element.53), channel_id=1, source_target_pairs={{0,2},{1,3},{2,0},{3,1},{4,6},{5,7},{6,4},{7,5},{8,10},{9,11},{10,... | collective-permute-start | bytes 786440 | tf_op jit(solution)/shard_map/ppermute | solution.py:248
  55.9 0.5 collective-permute-start.16
  56.4 0.2 collective-permute-start.11
  56.5 1.0 %collective-permute-done.13.refs_0_ = bf16[384,256]{1,0:T(8,128)(2,1)S(1)} collective-permute-done((bf16[384,256]{1,0:T(8,128)(2,1)S(1)}, bf16[384,256]{1,0:T(8,128)(2,1)S(1)}, u32[]{:S(2)}, u32[]{:S(2)}) %collective-permute-start.13) | collective-permute-done | bytes 196640 | tf_op jit(solution)/shard_map/ppermute | solution.py:248
  57.6 4.2 %collective-permute-start.14 = (bf16[384,256]{1,0:T(8,128)(2,1)S(1)}, bf16[384,256]{1,0:T(8,128)(2,1)S(1)}, u32[]{:S(2)}, u32[]{:S(2)}) collective-permute-start(bf16[384,256]{1,0:T(8,128)(2,1)S(1)} %collective-permute-done.13.refs_0_), channel_id=1, source_target_pairs={{0,1},{1,0},{2,3},{3,2},{4,5},{5,4},{6,7},{7,6},{8,9},{9,8},{10,11... | collective-permute-start | bytes 589832 | tf_op jit(solution)/shard_map/ppermute | solution.py:248
  61.7 0.0 collective-permute-done.11.refs_1_
  61.7 1.4 %shard_map.102 = (f32[384,512]{1,0:T(8,128)S(1)}, f32[2,384]{1,0:T(2,128)}) custom-call(s32[2]{0:T(128)S(1)} %pad_add_fusion.where, f32[384,256]{1,0:T(8,128)S(1)} %get-tuple-element.49.logs, bf16[384,256]{1,0:T(8,128)(2,1)S(1)} %get-tuple-element.50.refs_0_, bf16[384,256]{1,0:T(8,128)(2,1)S(1)} %collective-permute-done.11.refs_1_, ...), custom_call_target="tpu_custom_call" | custom-call | tf_op jit(solution)/shard_map/pallas_call | solution.py:30
  63.1 0.1 collective-permute-done.15.refs_2_
  63.2 7.2 %collective-permute-done.16.refs_3_ = bf16[256,512]{1,0:T(8,128)(2,1)S(1)} collective-permute-done((bf16[256,512]{1,0:T(8,128)(2,1)S(1)}, bf16[256,512]{1,0:T(8,128)(2,1)S(1)}, u32[]{:S(2)}, u32[]{:S(2)}) %collective-permute-start.16) | collective-permute-done | bytes 262176 | tf_op jit(solution)/shard_map/ppermute | solution.py:248
  70.4 0.0 collective-permute-done.14.refs_1_
  70.4 1.7 %shard_map.103 = bf16[384,512]{1,0:T(8,128)(2,1)} custom-call(s32[2]{0:T(128)S(1)} %pad_add_fusion.where, f32[384,512]{1,0:T(8,128)S(1)} %get-tuple-element.52.before, bf16[384,256]{1,0:T(8,128)(2,1)S(1)} %collective-permute-done.13.refs_0_, bf16[384,256]{1,0:T(8,128)(2,1)S(1)} %collective-permute-done.14.refs_1_, ...), custom_call_target="tpu_custom_call" | custom-call | tf_op jit(solution)/shard_map/pallas_call | solution.py:30
  (21 shorter events, 0.1 us)
Async XLA Ops:
  0.6 12.1 %collective-permute-start.3 = (bf16[384,512]{1,0:T(8,128)(2,1)}, bf16[384,512]{1,0:T(8,128)(2,1)S(1)}, u32[]{:S(2)}, u32[]{:S(2)}) collective-permute-start(bf16[384,512]{1,0:T(8,128)(2,1)} %refs_0_.1), channel_id=1, source_target_pairs={{0,4},{4,8},{8,12},{1,5},{5,9},{9,13},{2,6},{6,10},{10,14},{3,7},{... | collective-permute-start | bytes 1179656 | tf_op jit(solution)/shard_map/ppermute | solution.py:252
  3.8 11.0 %collective-permute-start = (bf16[384,512]{1,0:T(8,128)(2,1)}, bf16[384,512]{1,0:T(8,128)(2,1)S(1)}, u32[]{:S(2)}, u32[]{:S(2)}) collective-permute-start(bf16[384,512]{1,0:T(8,128)(2,1)} %refs_0_.1), channel_id=1, source_target_pairs={{0,2},{1,3},{2,0},{3,1},{4,6},{5,7},{6,4},{7,5},{8,10},{9,11},{10,... | collective-permute-start | bytes 1179656 | tf_op jit(solution)/shard_map/ppermute | solution.py:248
  12.7 9.1 %collective-permute-start.4 = (bf16[384,512]{1,0:T(8,128)(2,1)S(1)}, bf16[384,512]{1,0:T(8,128)(2,1)S(1)}, u32[]{:S(2)}, u32[]{:S(2)}) collective-permute-start(bf16[384,512]{1,0:T(8,128)(2,1)S(1)} %collective-permute-done.3.refs_0_), channel_id=1, source_target_pairs={{0,2},{1,3},{2,0},{3,1},{4,6},{5,7},{6,4},{7,5},{8,10},{9,11},{10,... | collective-permute-start | bytes 1179656 | tf_op jit(solution)/shard_map/ppermute | solution.py:248
  13.0 12.7 %collective-permute-start.2 = (bf16[384,512]{1,0:T(8,128)(2,1)}, bf16[384,512]{1,0:T(8,128)(2,1)S(1)}, u32[]{:S(2)}, u32[]{:S(2)}) collective-permute-start(bf16[384,512]{1,0:T(8,128)(2,1)} %refs_0_.1), channel_id=1, source_target_pairs={{0,1},{1,0},{2,3},{3,2},{4,5},{5,4},{6,7},{7,6},{8,9},{9,8},{10,11... | collective-permute-start | bytes 1179656 | tf_op jit(solution)/shard_map/ppermute | solution.py:248
  14.8 0.9 %copy-start.9 = (bf16[2048]{0:T(1024)(128)(2,1)S(1)}, bf16[2048]{0:T(1024)(128)(2,1)}, u32[]{:S(2)}) copy-start(bf16[2048]{0:T(1024)(128)(2,1)} %param.9) | copy-start | bytes 12292
  14.8 17.4 %collective-permute-start.1 = (bf16[384,512]{1,0:T(8,128)(2,1)S(1)}, bf16[384,512]{1,0:T(8,128)(2,1)}, u32[]{:S(2)}, u32[]{:S(2)}) collective-permute-start(bf16[384,512]{1,0:T(8,128)(2,1)S(1)} %collective-permute-done.refs_0_), channel_id=1, source_target_pairs={{0,1},{1,0},{2,3},{3,2},{4,5},{5,4},{6,7},{7,6},{8,9},{9,8},{10,11... | collective-permute-start | bytes 1179656 | tf_op jit(solution)/shard_map/ppermute | solution.py:248
  15.7 20.8 %collective-permute-start.6 = (bf16[384,512]{1,0:T(8,128)(2,1)S(1)}, bf16[384,512]{1,0:T(8,128)(2,1)S(1)}, u32[]{:S(2)}, u32[]{:S(2)}) collective-permute-start(bf16[384,512]{1,0:T(8,128)(2,1)S(1)} %collective-permute-done.3.refs_0_), channel_id=1, source_target_pairs={{0,1},{1,0},{2,3},{3,2},{4,5},{5,4},{6,7},{7,6},{8,9},{9,8},{10,11... | collective-permute-start | bytes 1179656 | tf_op jit(solution)/shard_map/ppermute | solution.py:248
  21.9 15.8 %collective-permute-start.5 = (bf16[384,512]{1,0:T(8,128)(2,1)S(1)}, bf16[384,512]{1,0:T(8,128)(2,1)S(1)}, u32[]{:S(2)}, u32[]{:S(2)}) collective-permute-start(bf16[384,512]{1,0:T(8,128)(2,1)S(1)} %collective-permute-done.4.refs_0_), channel_id=1, source_target_pairs={{0,1},{1,0},{2,3},{3,2},{4,5},{5,4},{6,7},{7,6},{8,9},{9,8},{10,11... | collective-permute-start | bytes 1179656 | tf_op jit(solution)/shard_map/ppermute | solution.py:248
  24.3 1.5 %copy-start.5 = (bf16[384,512]{1,0:T(8,128)(2,1)S(1)}, bf16[384,512]{1,0:T(8,128)(2,1)}, u32[]{:S(2)}) copy-start(bf16[384,512]{1,0:T(8,128)(2,1)} %refs_0_.1) | copy-start | bytes 1179652
  24.3 1.5 %copy-start.6 = (f32[2,128]{1,0:T(2,128)S(1)}, f32[2,128]{1,0:T(2,128)}, u32[]{:S(2)}) copy-start(f32[2,128]{1,0:T(2,128)} %refs_6_.1) | copy-start | bytes 3076
  24.3 1.5 %copy-start.7 = (f32[2,128]{1,0:T(2,128)S(1)}, f32[2,128]{1,0:T(2,128)}, u32[]{:S(2)}) copy-start(f32[2,128]{1,0:T(2,128)} %refs_7_.1) | copy-start | bytes 3076
  25.7 1.2 %copy-start = (bf16[2048,256]{1,0:T(8,128)(2,1)S(1)}, bf16[2048,256]{1,0:T(8,128)(2,1)}, u32[]{:S(2)}) copy-start(bf16[2048,256]{1,0:T(8,128)(2,1)} %refs_3_.7) | copy-start | bytes 3145732
  27.0 1.2 %copy-start.2 = (bf16[2048,256]{1,0:T(8,128)(2,1)S(1)}, bf16[2048,256]{1,0:T(8,128)(2,1)}, u32[]{:S(2)}) copy-start(bf16[2048,256]{1,0:T(8,128)(2,1)} %refs_4_.7) | copy-start | bytes 3145732
  28.2 1.2 %copy-start.4 = (bf16[2048,256]{1,0:T(8,128)(2,1)S(1)}, bf16[2048,256]{1,0:T(8,128)(2,1)}, u32[]{:S(2)}) copy-start(bf16[2048,256]{1,0:T(8,128)(2,1)} %refs_3_.5) | copy-start | bytes 3145732
  29.4 2.8 %copy-start.1 = (bf16[2048,256]{1,0:T(8,128)(2,1)S(1)}, bf16[2048,256]{1,0:T(8,128)(2,1)}, u32[]{:S(2)}) copy-start(bf16[2048,256]{1,0:T(8,128)(2,1)} %refs_3_.7) | copy-start | bytes 3145732
  29.4 2.8 %copy-start.3 = (bf16[2048,256]{1,0:T(8,128)(2,1)S(1)}, bf16[2048,256]{1,0:T(8,128)(2,1)}, u32[]{:S(2)}) copy-start(bf16[2048,256]{1,0:T(8,128)(2,1)} %refs_4_.7) | copy-start | bytes 3145732
  34.6 9.2 %collective-permute-start.8 = (bf16[384,256]{1,0:T(8,128)(2,1)S(1)}, bf16[384,256]{1,0:T(8,128)(2,1)S(1)}, u32[]{:S(2)}, u32[]{:S(2)}) collective-permute-start(bf16[384,256]{1,0:T(8,128)(2,1)S(1)} %get-tuple-element.35.q), channel_id=1, source_target_pairs={{12,4},{13,5},{14,6},{15,7},{28,20},{29,21},{30,22},{31,23}} | collective-permute-start | bytes 589832 | tf_op jit(solution)/shard_map/ppermute | solution.py:252
  35.9 14.9 %collective-permute-start.7 = (bf16[2,384,256]{2,1,0:T(8,128)(2,1)S(1)}, bf16[2,384,256]{2,1,0:T(8,128)(2,1)S(1)}, u32[]{:S(2)}, u32[]{:S(2)}) collective-permute-start(bf16[2,384,256]{2,1,0:T(8,128)(2,1)S(1)} %get-tuple-element.36.refs_0_), channel_id=1, source_target_pairs={{0,8},{1,9},{2,10},{3,11},{16,24},{17,25},{18,26},{19,27}} | collective-permute-start | bytes 1179656 | tf_op jit(solution)/shard_map/ppermute | solution.py:252
  46.3 5.5 %collective-permute-start.9 = (bf16[384,256]{1,0:T(8,128)(2,1)}, bf16[384,256]{1,0:T(8,128)(2,1)S(1)}, u32[]{:S(2)}, u32[]{:S(2)}) collective-permute-start(bf16[384,256]{1,0:T(8,128)(2,1)} %get-tuple-element.47), channel_id=1, source_target_pairs={{4,12},{5,13},{6,14},{7,15},{20,28},{21,29},{22,30},{23,31}} | collective-permute-start | bytes 589832 | tf_op jit(solution)/shard_map/ppermute | solution.py:252
  47.6 4.2 %collective-permute-start.10 = (f32[8,384]{1,0:T(8,128)S(1)}, f32[8,384]{1,0:T(8,128)S(1)}, u32[]{:S(2)}, u32[]{:S(2)}) collective-permute-start(f32[8,384]{1,0:T(8,128)S(1)} %get-tuple-element.48), channel_id=1, source_target_pairs={{4,12},{5,13},{6,14},{7,15},{20,28},{21,29},{22,30},{23,31}} | collective-permute-start | bytes 36872 | tf_op jit(solution)/shard_map/ppermute | solution.py:252
  51.7 1.2 %copy-start.8 = (bf16[256,2048]{1,0:T(8,128)(2,1)S(1)}, bf16[256,2048]{1,0:T(8,128)(2,1)}, u32[]{:S(2)}) copy-start(bf16[256,2048]{1,0:T(8,128)(2,1)} %param.15) | copy-start | bytes 3145732
  52.5 5.1 %collective-permute-start.13 = (bf16[384,256]{1,0:T(8,128)(2,1)S(1)}, bf16[384,256]{1,0:T(8,128)(2,1)S(1)}, u32[]{:S(2)}, u32[]{:S(2)}) collective-permute-start(bf16[384,256]{1,0:T(8,128)(2,1)S(1)} %get-tuple-element.50.refs_0_), channel_id=1, source_target_pairs={{0,2},{1,3},{2,0},{3,1},{4,6},{5,7},{6,4},{7,5},{8,10},{9,11},{10,... | collective-permute-start | bytes 589832 | tf_op jit(solution)/shard_map/ppermute | solution.py:248
  53.1 8.7 %collective-permute-start.12 = (bf16[256,512]{1,0:T(8,128)(2,1)S(1)}, bf16[256,512]{1,0:T(8,128)(2,1)S(1)}, u32[]{:S(2)}, u32[]{:S(2)}) collective-permute-start(bf16[256,512]{1,0:T(8,128)(2,1)S(1)} %get-tuple-element.51), channel_id=1, source_target_pairs={{0,1},{1,0},{2,3},{3,2},{4,5},{5,4},{6,7},{7,6},{8,9},{9,8},{10,11... | collective-permute-start | bytes 786440 | tf_op jit(solution)/shard_map/ppermute | solution.py:248
  54.6 8.5 %collective-permute-start.15 = (bf16[256,512]{1,0:T(8,128)(2,1)S(1)}, bf16[256,512]{1,0:T(8,128)(2,1)S(1)}, u32[]{:S(2)}, u32[]{:S(2)}) collective-permute-start(bf16[256,512]{1,0:T(8,128)(2,1)S(1)} %get-tuple-element.53), channel_id=1, source_target_pairs={{0,2},{1,3},{2,0},{3,1},{4,6},{5,7},{6,4},{7,5},{8,10},{9,11},{10,... | collective-permute-start | bytes 786440 | tf_op jit(solution)/shard_map/ppermute | solution.py:248
  55.9 14.5 %collective-permute-start.16 = (bf16[256,512]{1,0:T(8,128)(2,1)S(1)}, bf16[256,512]{1,0:T(8,128)(2,1)S(1)}, u32[]{:S(2)}, u32[]{:S(2)}) collective-permute-start(bf16[256,512]{1,0:T(8,128)(2,1)S(1)} %get-tuple-element.54), channel_id=1, source_target_pairs={{0,3},{1,2},{2,1},{3,0},{4,7},{5,6},{6,5},{7,4},{8,11},{9,10},{10,... | collective-permute-start | bytes 786440 | tf_op jit(solution)/shard_map/ppermute | solution.py:248
  56.4 5.4 %collective-permute-start.11 = (bf16[384,256]{1,0:T(8,128)(2,1)S(1)}, bf16[384,256]{1,0:T(8,128)(2,1)S(1)}, u32[]{:S(2)}, u32[]{:S(2)}) collective-permute-start(bf16[384,256]{1,0:T(8,128)(2,1)S(1)} %get-tuple-element.50.refs_0_), channel_id=1, source_target_pairs={{0,1},{1,0},{2,3},{3,2},{4,5},{5,4},{6,7},{7,6},{8,9},{9,8},{10,11... | collective-permute-start | bytes 589832 | tf_op jit(solution)/shard_map/ppermute | solution.py:248
  57.6 12.8 %collective-permute-start.14 = (bf16[384,256]{1,0:T(8,128)(2,1)S(1)}, bf16[384,256]{1,0:T(8,128)(2,1)S(1)}, u32[]{:S(2)}, u32[]{:S(2)}) collective-permute-start(bf16[384,256]{1,0:T(8,128)(2,1)S(1)} %collective-permute-done.13.refs_0_), channel_id=1, source_target_pairs={{0,1},{1,0},{2,3},{3,2},{4,5},{5,4},{6,7},{7,6},{8,9},{9,8},{10,11... | collective-permute-start | bytes 589832 | tf_op jit(solution)/shard_map/ppermute | solution.py:248

commit v5 on v4

--- a/solution.py
+++ b/solution.py
@@ -19,21 +19,20 @@
 
 
 VMEM = pl.BlockSpec(memory_space=pltpu.VMEM)
-SMEM = pl.BlockSpec(memory_space=pltpu.SMEM)
 
 
 def shape_of(shape, dtype):
     return jax.ShapeDtypeStruct(shape, dtype)
 
 
-def call(body, where, operands, outs, limit=24 << 20):
+def call(body, operands, outs, limit=24 << 20):
     return pl.pallas_call(
         body,
         out_shape=tuple(outs),
-        in_specs=[SMEM] + [VMEM] * len(operands),
+        in_specs=[VMEM] * len(operands),
         out_specs=(VMEM,) * len(outs),
         compiler_params=pltpu.CompilerParams(vmem_limit_bytes=limit),
-    )(where, *operands)
+    )(*operands)
 
 
 def wide(column):
@@ -56,8 +55,8 @@
     )
 
 
-def sums_of(where, hidden, gain, weights, offsets):
-    me = where[0]
+def sums_of(hidden, gain, weights, offsets):
+    me = lax.axis_index("tp")
     sums = [None] * len(weights)
     squares = None
     for block, k in zip(hidden, offsets):
@@ -74,14 +73,14 @@
     return sums, squares
 
 
-def early_kernel(where, *refs, offsets, kinds, biases, copies):
+def early_kernel(*refs, offsets, kinds, biases, copies):
     count = len(offsets)
     hidden = refs[:count]
     gain = refs[count]
     weights = refs[count + 1 : count + 1 + kinds]
     small = refs[count + 1 + kinds : count + 1 + kinds + copies]
     outs = refs[count + 1 + kinds + copies :]
-    sums, squares = sums_of(where, hidden, gain, weights, offsets)
+    sums, squares = sums_of(hidden, gain, weights, offsets)
     for out, total in zip(outs[:kinds], sums):
         out[...] = total
     outs[kinds][...] = wide(squares)
@@ -97,7 +96,7 @@
     return values * cosine + pltpu.roll(values, values.shape[1] // 2, 1) * sine
 
 
-def late_kernel(where, *refs, offsets, kinds, width):
+def late_kernel(*refs, offsets, kinds, width):
     count = len(offsets)
     hidden = refs[:count]
     gain = refs[count]
@@ -109,7 +108,7 @@
     cosine, sine = rest[2 * kinds : 2 * kinds + 2]
     outs = rest[2 * kinds + 2 :]
     outs = [*outs[:-1], outs[-1].at[0], outs[-1].at[1]]
-    sums, squares = sums_of(where, hidden, gain, weights, offsets)
+    sums, squares = sums_of(hidden, gain, weights, offsets)
     scale = lax.rsqrt((squares + squares_before[...]) / width + EPSILON)
     head_width = gains[0].shape[1]
     turn_c = jnp.concatenate([cosine[...], cosine[...]], axis=1)
@@ -162,24 +161,24 @@
     return [slice(h * head_width, (h + 1) * head_width) for h in range(count)]
 
 
-def near_kernel(where, q, *refs, distances, head_width, factor):
+def near_kernel(q, *refs, distances, head_width, factor):
     count = len(distances)
     tops, totals, accs = refs[2 * count :]
     for lanes in head_lanes(q, head_width):
         blocks = []
         for n, d in enumerate(distances):
             bias = refs[2 * n + 1][...]
-            blocks.append((refs[2 * n], jnp.where(where[1] >= d, bias, MASKED) if d else bias))
+            blocks.append((refs[2 * n], jnp.where(lax.axis_index("sp") >= d, bias, MASKED) if d else bias))
         top, total, acc = softmax_part(q, blocks, lanes, factor)
         tops[:, lanes] = wide(top)
         totals[:, lanes] = wide(total)
         accs[:, lanes] = acc
 
 
-def help_kernel(where, q, *refs, blocks, head_width, factor, helper):
+def help_kernel(q, *refs, blocks, head_width, factor, helper):
     out, logs = refs[2 * blocks :]
 
-    @pl.when(where[1] == helper)
+    @pl.when(lax.axis_index("sp") == helper)
     def _():
         for h, lanes in enumerate(head_lanes(q, head_width)):
             ready = [(refs[2 * n], refs[2 * n + 1][...]) for n in range(blocks)]
@@ -188,8 +187,16 @@
             logs[h : h + 1, :] = wide(top + jnp.log2(total)).T[:1, :]
 
 
-def final_kernel(where, q, *refs, far, only, helped, head_width, factor):
-    shard = where[1]
+def late_help_kernel(*refs, late_count, late, help_now):
+    late_in, rest = refs[:late_count], refs[late_count:]
+    q, kv, bias, bias_before = rest[:4]
+    kv_before, out, logs = rest[4:]
+    late(*late_in, kv_before)
+    help_now(q, kv, bias, kv_before, bias_before, out, logs)
+
+
+def final_kernel(q, *refs, far, only, helped, head_width, factor):
+    shard = lax.axis_index("sp")
     near = refs[:3]
     kvs = refs[3 : 3 + 2 * len(far)]
     given = refs[3 + 2 * len(far) : -2]
@@ -230,7 +237,7 @@
     return total
 
 
-def mix_early_kernel(where, logs, *refs, count):
+def mix_early_kernel(logs, *refs, count):
     total, rows = refs[2 * count :]
     total[...] = products(refs[:count], refs[count : 2 * count])
     for h in range(rows.shape[0]):
@@ -238,8 +245,13 @@
         rows[h : h + 1, :] = (logs[:, lanes] * math.log(2.0)).T[:1, :]
 
 
-def mix_late_kernel(where, before, *refs, count):
-    total = before[...] + products(refs[:count], refs[count : 2 * count])
+def mix_late_kernel(before, *refs, count, shared):
+    blocks = [ref[...] for ref in refs[:count]]
+    if shared:
+        crossed = lax.axis_index("grp") == 0
+        low, high = blocks
+        blocks = [jnp.where(crossed, high, low), jnp.where(crossed, low, high)]
+    total = before[...] + products(blocks, refs[count : 2 * count])
     refs[-1][...] = total.astype(jnp.bfloat16)
 
 
@@ -282,7 +294,6 @@
     half = count // 2
     me = lax.axis_index("tp")
     shard = lax.axis_index("sp")
-    where = jnp.stack([me, shard]).astype(jnp.int32)
     factor = head_width ** (-0.5) * LOG2_E
     reach = -(-KEYS_BEHIND * DILATIONS[-1] // rows)
     distances = list(range(min(shards - 1, reach) + 1))
@@ -304,17 +315,21 @@
     early = tuple(range(half))
     late = tuple(range(half, count))
     columns = w_out.shape[1] // count
-    slices = [
-        lax.dynamic_slice_in_dim(w_out, (me ^ k) * columns, columns, axis=1)
-        for k in range(count)
-    ]
+    copies = lax.axis_size("grp")
+    copy = lax.axis_index("grp")
+    shared = copies == 2 and count == 4
+
+    def piece_for(k):
+        return lax.dynamic_slice_in_dim(w_out, (me ^ k) * columns, columns, axis=1)
+
+    own_slice, near_slice = piece_for(0), [piece_for(k) for k in range(1, half)]
+    far_slice = [piece_for(3 - copy)] if shared else [piece_for(k) for k in late]
 
     def begin(blocks, kinds, biases, copied):
         return call(
             functools.partial(
                 early_kernel, offsets=early, kinds=kinds, biases=biases, copies=len(copied)
             ),
-            where,
             [*blocks, gain, *weights[3 - kinds :], *copied],
             [sums] * kinds
             + [lane_wide]
@@ -325,7 +340,6 @@
     def finish(blocks, kinds, begun, turn):
         return call(
             functools.partial(late_kernel, offsets=late, kinds=kinds, width=piece * count),
-            where,
             [*blocks, gain, *weights[3 - kinds :], *begun, *gains[3 - kinds :], *turn],
             [half_sum] * (kinds - 2) + [pair],
         )
@@ -348,32 +362,43 @@
         far_blocks = [(behind(kv, d), biases[d]) for d in far]
 
     begun_before = begin(near_blocks(before), 2, (), ())
-    (kv_before,) = finish(near_blocks(before_across), 2, begun_before, tables_before)
+    before_far = near_blocks(before_across)
     given = []
-    if helped is not None:
-        out, logs = call(
+    if helped is None:
+        (kv_before,) = finish(before_far, 2, begun_before, tables_before)
+    else:
+        operands = [*before_far, gain, *weights[1:], *begun_before, gains[1], *tables_before]
+        kv_before, out, logs = call(
             functools.partial(
-                help_kernel, blocks=2, head_width=head_width, factor=factor, helper=1
+                late_help_kernel,
+                late_count=len(operands),
+                late=functools.partial(late_kernel, offsets=late, kinds=2, width=piece * count),
+                help_now=functools.partial(
+                    help_kernel, blocks=2, head_width=head_width, factor=factor, helper=1
+                ),
             ),
-            where,
-            [visitor, kv, biases[2], kv_before, biases[3]],
-            [half_sum, shape_of((8, rows), jnp.float32)],
+            [*operands, visitor, kv, biases[2], biases[3]],
+            [pair, half_sum, shape_of((8, rows), jnp.float32)],
         )
         given = [send(out, [(1, helped)]), send(logs, [(1, helped)])]
     near = call(
         functools.partial(
             near_kernel, distances=(0, 1), head_width=head_width, factor=factor
         ),
-        where,
         [q, kv, biases[0], kv_before, biases[1]],
         [sums] * 3,
     )
 
-    w_first, _ = lax.optimization_barrier((slices[-1], begun_before[2]))
-    *w_rest, _ = lax.optimization_barrier((*slices[1:-1], begun_before[2]))
-    pieces = [slices[0]]
-    pieces += [swap(w_rest[k - 1], k) for k in range(1, count - 1)]
-    pieces += [swap(w_first, count - 1)]
+    *far_slice, _ = lax.optimization_barrier((*far_slice, begun_before[2]))
+    *near_slice, _ = lax.optimization_barrier((*near_slice, begun_before[2]))
+    near_pieces = [own_slice] + [swap(x, k + 1) for k, x in enumerate(near_slice)]
+    if shared:
+        routes = [(g * 4 + t, g * 4 + (t ^ (3 - g))) for g in range(2) for t in range(4)]
+        fetched = lax.ppermute(far_slice[0], ("grp", "tp"), routes)
+        other = lax.ppermute(fetched, "grp", [(0, 1), (1, 0)])
+        far_pieces = [fetched, other]
+    else:
+        far_pieces = [swap(x, k) for k, x in zip(late, far_slice)]
 
     attended, logs = call(
         functools.partial(
@@ -384,7 +409,6 @@
             head_width=head_width,
             factor=factor,
         ),
-        where,
         [q, *near, *[x for block in far_blocks for x in block], *given],
         [half_sum, sums],
     )
@@ -392,14 +416,12 @@
     mixed_shape = (rows, columns)
     partial_mix, log_rows = call(
         functools.partial(mix_early_kernel, count=half),
-        where,
-        [logs, *near_blocks(attended), *pieces[:half]],
+        [logs, *near_blocks(attended), *near_pieces],
         [shape_of(mixed_shape, jnp.float32), shape_of((head_count, rows), jnp.float32)],
     )
     (mixed,) = call(
-        functools.partial(mix_late_kernel, count=half),
-        where,
-        [partial_mix, *near_blocks(attended_across), *pieces[half:]],
+        functools.partial(mix_late_kernel, count=half, shared=shared),
+        [partial_mix, *near_blocks(attended_across), *far_pieces],
         [shape_of(mixed_shape, jnp.bfloat16)],
     )
     return mixed, log_rows.T

time: 73.3 us -> 69.3 us (0.945)
  the two profiles are of different devices: /device:TPU:15 before, /device:TPU:8 now
where the time goes in v5:
time: 69.3 us; the launch traced here: 68.8 us
  waiting for transfers between devices  29.7 us (43%)
  Pallas kernels  15.9 us (23%)
  starting transfers between devices  15.6 us (23%)
  local copies, waits for them, and re-layouts  5.3 us (8%)
  other arithmetic  1.45 us (2%)
  between operations  0.84 us (1%)
    pallas_call x8, Pallas kernels, call(): pl.pallas_call(body, out_shape=tuple(outs), in_specs=[VMEM] * len(operand...  15.9 us
    ppermute x5, waiting for transfers between devices, send(): return lax.ppermute(value, 'sp', pairs)  14 us
    ppermute x10, waiting for transfers between devices, swap(): return lax.ppermute(value, 'tp', [(i, i ^ distance) for i in range(count)])  11.5 us
    ppermute x5, starting transfers between devices, send(): return lax.ppermute(value, 'sp', pairs)  8.89 us
    ppermute x10, starting transfers between devices, swap(): return lax.ppermute(value, 'tp', [(i, i ^ distance) for i in range(count)])  5.12 us
    unnamed x30, local copies, waits for them, and re-layouts  4.52 us
    ppermute x1, waiting for transfers between devices, layer(): other = lax.ppermute(fetched, 'grp', [(0, 1), (1, 0)])  2.7 us
    sin x1, other arithmetic, turn_tables(): return (jnp.cos(angles), jnp.sin(angles))  1.43 us
  transfers between devices with their start and end apart: 17, of which 7 were waited for; matrix products, arithmetic and copies ran while one was open for 3% of the time, Pallas kernels for 22%

profile of v5, /device:TPU:8, one launch (start us, length us, event | category | flops | bytes accessed | tf_op | source)
XLA Modules:
  0.0 68.8 jit_solution(18213948505060448932)
XLA Ops:
  0.6 3.5 %collective-permute-start.3 = (bf16[384,512]{1,0:T(8,128)(2,1)}, bf16[384,512]{1,0:T(8,128)(2,1)}, u32[]{:S(2)}, u32[]{:S(2)}) collective-permute-start(bf16[384,512]{1,0:T(8,128)(2,1)} %refs_0_.1), channel_id=1, source_target_pairs={{0,4},{4,8},{8,12},{1,5},{5,9},{9,13},{2,6},{6,10},{10,14},{3,7},{... | collective-permute-start | bytes 1179656 | tf_op jit(solution)/shard_map/ppermute | solution.py:264
  4.1 1.6 %collective-permute-start = (bf16[384,512]{1,0:T(8,128)(2,1)}, bf16[384,512]{1,0:T(8,128)(2,1)}, u32[]{:S(2)}, u32[]{:S(2)}) collective-permute-start(bf16[384,512]{1,0:T(8,128)(2,1)} %refs_0_.1), channel_id=1, source_target_pairs={{0,2},{1,3},{2,0},{3,1},{4,6},{5,7},{6,4},{7,5},{8,10},{9,11},{10,... | collective-permute-start | bytes 1179656 | tf_op jit(solution)/shard_map/ppermute | solution.py:260
  5.7 8.0 %collective-permute-done.3.refs_0_ = bf16[384,512]{1,0:T(8,128)(2,1)} collective-permute-done((bf16[384,512]{1,0:T(8,128)(2,1)}, bf16[384,512]{1,0:T(8,128)(2,1)}, u32[]{:S(2)}, u32[]{:S(2)}) %collective-permute-start.3) | collective-permute-done | bytes 393248 | tf_op jit(solution)/shard_map/ppermute | solution.py:264
  13.7 1.5 %collective-permute-start.4 = (bf16[384,512]{1,0:T(8,128)(2,1)}, bf16[384,512]{1,0:T(8,128)(2,1)}, u32[]{:S(2)}, u32[]{:S(2)}) collective-permute-start(bf16[384,512]{1,0:T(8,128)(2,1)} %collective-permute-done.3.refs_0_), channel_id=1, source_target_pairs={{0,2},{1,3},{2,0},{3,1},{4,6},{5,7},{6,4},{7,5},{8,10},{9,11},{10,... | collective-permute-start | bytes 1179656 | tf_op jit(solution)/shard_map/ppermute | solution.py:260
  15.2 0.0 collective-permute-start.2
  15.2 0.0 collective-permute-done.refs_0_
  15.2 0.5 collective-permute-start.1
  15.7 0.7 %reshape.28.refs_2_ = f32[4,512]{1,0:T(4,128)S(1)} reshape(bf16[2048]{0:T(1024)(128)(2,1)} %param.9) | data formatting | bytes 12288 | tf_op jit(solution)/shard_map/reshape | solution.py:307
  16.4 0.0 collective-permute-start.6
  16.4 7.6 %collective-permute-done.4.refs_0_ = bf16[384,512]{1,0:T(8,128)(2,1)} collective-permute-done((bf16[384,512]{1,0:T(8,128)(2,1)}, bf16[384,512]{1,0:T(8,128)(2,1)}, u32[]{:S(2)}, u32[]{:S(2)}) %collective-permute-start.4) | collective-permute-done | bytes 393248 | tf_op jit(solution)/shard_map/ppermute | solution.py:260
  24.0 0.0 collective-permute-start.5
  24.0 1.4 %multiply_sine_fusion = (f32[384,64]{1,0:T(8,128)S(1)}, f32[384,64]{1,0:T(8,128)S(1)}, f32[384,64]{1,0:T(8,128)S(1)}, f32[384,64]{1,0:T(8,128)S(1)}) fusion(f32[384]{0:T(512)S(1)} %get-tuple-element.65, f32[64]{0:T(128)S(1)} %multiply_power_fusion, f32[384]{0:T(512)S(1)} %get-tuple-element.66), kind=kLoop, calls=%fused_computation | loop fusion | flops 49152 | bytes 396544 | tf_op jit(solution)/shard_map/sin | solution.py:285
  25.5 0.0 collective-permute-done.2.refs_1_
  25.5 0.0 copy-start
  25.5 1.2 %copy-done = bf16[2048,256]{1,0:T(8,128)(2,1)S(1)} copy-done((bf16[2048,256]{1,0:T(8,128)(2,1)S(1)}, bf16[2048,256]{1,0:T(8,128)(2,1)}, u32[]{:S(2)}) %copy-start) | copy-done | bytes 1048600
  26.7 1.2 %copy-done.2 = bf16[2048,256]{1,0:T(8,128)(2,1)S(1)} copy-done((bf16[2048,256]{1,0:T(8,128)(2,1)S(1)}, bf16[2048,256]{1,0:T(8,128)(2,1)}, u32[]{:S(2)}) %copy-start.2) | copy-done | bytes 1048600
  28.0 1.2 %copy-done.4 = bf16[2048,256]{1,0:T(8,128)(2,1)S(1)} copy-done((bf16[2048,256]{1,0:T(8,128)(2,1)S(1)}, bf16[2048,256]{1,0:T(8,128)(2,1)}, u32[]{:S(2)}) %copy-start.4) | copy-done | bytes 1048600
  29.2 2.3 %shard_map.95 = (f32[384,256]{1,0:T(8,128)S(1)}, f32[384,256]{1,0:T(8,128)S(1)}, f32[384,256]{1,0:T(8,128)S(1)}, f32[384,128]{1,0:T(8,128)S(1)}, f32[2,128]{1,0:...) custom-call(bf16[384,512]{1,0:T(8,128)(2,1)S(1)} %copy-done.11, ...), custom_call_target="tpu_custom_call" | custom-call | tf_op jit(solution)/shard_map/pallas_call | solution.py:29
  31.5 0.8 %copy-done.7 = f32[384,384]{1,0:T(8,128)} copy-done((f32[384,384]{1,0:T(8,128)}, f32[384,384]{1,0:T(8,128)S(1)}, u32[]{:S(2)}) %copy-start.7) | copy-done | bytes 589848
  32.3 0.0 collective-permute-done.1.refs_1_
  32.3 3.0 %shard_map.96 = (bf16[384,256]{1,0:T(8,128)(2,1)}, bf16[2,384,256]{2,1,0:T(8,128)(2,1)S(1)}) custom-call(bf16[384,512]{1,0:T(8,128)(2,1)} %collective-permute-done.refs_0_, bf16[384,512]{1,0:T(8,128)(2,1)} %collective-permute-done.1.refs_1_, f32[4,512]{1,0:T(4,128)S(1)} %reshape.28.refs_2_, bf16[2048,256]{1,0:T(8,128)(2,1)S(1)} %copy-done.4, ...), custom_call_target="tpu_custom_call" | custom-call | tf_op jit(solution)/shard_map/pallas_call | solution.py:29
  35.3 1.3 %collective-permute-start.7 = (bf16[384,256]{1,0:T(8,128)(2,1)}, bf16[384,256]{1,0:T(8,128)(2,1)}, u32[]{:S(2)}, u32[]{:S(2)}) collective-permute-start(bf16[384,256]{1,0:T(8,128)(2,1)} %get-tuple-element.35.q), channel_id=1, source_target_pairs={{12,4},{13,5},{14,6},{15,7},{28,20},{29,21},{30,22},{31,23}} | collective-permute-start | bytes 589832 | tf_op jit(solution)/shard_map/ppermute | solution.py:264
  36.6 1.4 %collective-permute-start.8 = (bf16[2,384,256]{2,1,0:T(8,128)(2,1)S(1)}, bf16[2,384,256]{2,1,0:T(8,128)(2,1)}, u32[]{:S(2)}, u32[]{:S(2)}) collective-permute-start(bf16[2,384,256]{2,1,0:T(8,128)(2,1)S(1)} %get-tuple-element.36.refs_12_.refs_0_), channel_id=1, source_target_pairs={{0,8},{1,9},{2,10},{3,11},{16,24},{17,25},{18,26},{19,27}} | collective-permute-start | bytes 1179656 | tf_op jit(solution)/shard_map/ppermute | solution.py:264
  38.0 0.0 collective-permute-done.6.refs_1_
  38.0 1.8 %shard_map.97 = (f32[384,256]{1,0:T(8,128)S(1)}, f32[384,256]{1,0:T(8,128)S(1)}, f32[384,128]{1,0:T(8,128)S(1)}) custom-call(bf16[384,512]{1,0:T(8,128)(2,1)} %collective-permute-done.3.refs_0_, bf16[384,512]{1,0:T(8,128)(2,1)} %collective-permute-done.6.refs_1_, f32[4,512]{1,0:T(4,128)S(1)} %reshape.28.refs_2_, bf16[2048,256]{1,0:T(8,128)(2,1)S(1)} %copy-done.1, ...), custom_call_target="tpu_custom_call" | custom-call | tf_op jit(solution)/shard_map/pallas_call | solution.py:29
  39.8 5.9 %collective-permute-done.7.refs_11_ = bf16[384,256]{1,0:T(8,128)(2,1)} collective-permute-done((bf16[384,256]{1,0:T(8,128)(2,1)}, bf16[384,256]{1,0:T(8,128)(2,1)}, u32[]{:S(2)}, u32[]{:S(2)}) %collective-permute-start.7) | collective-permute-done | bytes 196640 | tf_op jit(solution)/shard_map/ppermute | solution.py:264
  45.7 0.0 collective-permute-done.5.refs_1_
  45.7 3.4 %shard_map.98 = (bf16[2,384,256]{2,1,0:T(8,128)(2,1)S(1)}, bf16[384,256]{1,0:T(8,128)(2,1)S(1)}, f32[8,384]{1,0:T(8,128)S(1)}) custom-call(bf16[384,512]{1,0:T(8,128)(2,1)} %collective-permute-done.4.refs_0_, bf16[384,512]{1,0:T(8,128)(2,1)} %collective-permute-done.5.refs_1_, f32[4,512]{1,0:T(4,128)S(1)} %reshape.28.refs_2_, ...), custom_call_target="tpu_custom_call" | custom-call | tf_op jit(solution)/shard_map/pallas_call | solution.py:29
  49.2 1.4 %collective-permute-start.9 = (bf16[384,256]{1,0:T(8,128)(2,1)S(1)}, bf16[384,256]{1,0:T(8,128)(2,1)S(1)}, u32[]{:S(2)}, u32[]{:S(2)}) collective-permute-start(bf16[384,256]{1,0:T(8,128)(2,1)S(1)} %get-tuple-element.48), channel_id=1, source_target_pairs={{4,12},{5,13},{6,14},{7,15},{20,28},{21,29},{22,30},{23,31}} | collective-permute-start | bytes 589832 | tf_op jit(solution)/shard_map/ppermute | solution.py:264
  50.7 0.1 constant_dynamic-slice_fusion
  50.7 0.8 %collective-permute-start.15 = (bf16[256,512]{1,0:T(8,128)(2,1)S(1)}, bf16[256,512]{1,0:T(8,128)(2,1)S(1)}, u32[]{:S(2)}, u32[]{:S(2)}) collective-permute-start(bf16[256,512]{1,0:T(8,128)(2,1)S(1)} %get-tuple-element.54), channel_id=1, source_target_pairs={{0,3},{1,2},{2,1},{3,0},{16,18},{17,19},{18,16},{19,17},{4,7},{5,6... | collective-permute-start | bytes 786440 | tf_op jit(solution)/shard_map/ppermute | solution.py:397
  51.5 1.3 %collective-permute-start.10 = (f32[8,384]{1,0:T(8,128)S(1)}, f32[8,384]{1,0:T(8,128)S(1)}, u32[]{:S(2)}, u32[]{:S(2)}) collective-permute-start(f32[8,384]{1,0:T(8,128)S(1)} %get-tuple-element.49), channel_id=1, source_target_pairs={{4,12},{5,13},{6,14},{7,15},{20,28},{21,29},{22,30},{23,31}} | collective-permute-start | bytes 36872 | tf_op jit(solution)/shard_map/ppermute | solution.py:264
  52.8 2.2 %shard_map.99 = (f32[384,256]{1,0:T(8,128)S(1)}, f32[384,256]{1,0:T(8,128)S(1)}, f32[384,256]{1,0:T(8,128)S(1)}) custom-call(bf16[384,256]{1,0:T(8,128)(2,1)} %get-tuple-element.35.q, bf16[2,384,256]{2,1,0:T(8,128)(2,1)S(1)} %get-tuple-element.36.refs_12_.refs_0_, f32[384,384]{1,0:T(8,128)S(1)} %copy-done.8, ...), custom_call_target="tpu_custom_call" | custom-call | tf_op jit(solution)/shard_map/pallas_call | solution.py:29
  55.1 0.0 collective-permute-done.8.refs_3_
  55.1 0.1 collective-permute-done.10.refs_6_
  55.1 1.3 %shard_map.100 = (bf16[384,256]{1,0:T(8,128)(2,1)S(1)}, f32[384,256]{1,0:T(8,128)S(1)}) custom-call(bf16[384,256]{1,0:T(8,128)(2,1)} %get-tuple-element.35.q, f32[384,256]{1,0:T(8,128)S(1)} %get-tuple-element.45.refs_0_, f32[384,256]{1,0:T(8,128)S(1)} %get-tuple-element.46.refs_1_, f32[384,256]{1,0:T(8,128)S(1)} %get-tuple-element.47.refs_2_, ...), custom_call_target="tpu_custom_call" | custom-call | tf_op jit(solution)/shard_map/pallas_call | solution.py:29
  56.4 1.5 %collective-permute-start.13 = (bf16[384,256]{1,0:T(8,128)(2,1)S(1)}, bf16[384,256]{1,0:T(8,128)(2,1)S(1)}, u32[]{:S(2)}, u32[]{:S(2)}) collective-permute-start(bf16[384,256]{1,0:T(8,128)(2,1)S(1)} %get-tuple-element.51.refs_0_), channel_id=1, source_target_pairs={{0,2},{1,3},{2,0},{3,1},{4,6},{5,7},{6,4},{7,5},{8,10},{9,11},{10,... | collective-permute-start | bytes 589832 | tf_op jit(solution)/shard_map/ppermute | solution.py:260
  57.9 0.0 collective-permute-start.12
  57.9 1.4 %collective-permute-done.15.refs_2_ = bf16[256,512]{1,0:T(8,128)(2,1)S(1)} collective-permute-done((bf16[256,512]{1,0:T(8,128)(2,1)S(1)}, bf16[256,512]{1,0:T(8,128)(2,1)S(1)}, u32[]{:S(2)}, u32[]{:S(2)}) %collective-permute-start.15) | collective-permute-done | bytes 262176 | tf_op jit(solution)/shard_map/ppermute | solution.py:397
  59.4 0.8 %collective-permute-start.16 = (bf16[256,512]{1,0:T(8,128)(2,1)S(1)}, bf16[256,512]{1,0:T(8,128)(2,1)S(1)}, u32[]{:S(2)}, u32[]{:S(2)}) collective-permute-start(bf16[256,512]{1,0:T(8,128)(2,1)S(1)} %collective-permute-done.15.refs_2_), channel_id=1, source_target_pairs={{0,16},{16,0},{1,17},{17,1},{2,18},{18,2},{3,19},{19,3},{4,20},{20... | collective-permute-start | bytes 786440 | tf_op jit(solution)/shard_map/ppermute | solution.py:398
  60.2 0.0 collective-permute-start.11
  60.2 3.9 %collective-permute-done.13.refs_0_ = bf16[384,256]{1,0:T(8,128)(2,1)S(1)} collective-permute-done((bf16[384,256]{1,0:T(8,128)(2,1)S(1)}, bf16[384,256]{1,0:T(8,128)(2,1)S(1)}, u32[]{:S(2)}, u32[]{:S(2)}) %collective-permute-start.13) | collective-permute-done | bytes 196640 | tf_op jit(solution)/shard_map/ppermute | solution.py:260
  64.1 0.0 collective-permute-start.14
  64.1 0.0 collective-permute-done.12.refs_3_
  64.1 0.0 collective-permute-done.11.refs_1_
  64.1 0.9 %shard_map.101 = (f32[384,512]{1,0:T(8,128)S(1)}, f32[2,384]{1,0:T(2,128)}) custom-call(f32[384,256]{1,0:T(8,128)S(1)} %get-tuple-element.50.logs, bf16[384,256]{1,0:T(8,128)(2,1)S(1)} %get-tuple-element.51.refs_0_, bf16[384,256]{1,0:T(8,128)(2,1)S(1)} %collective-permute-done.11.refs_1_, bf16[256,512]{1,0:T(8,128)(2,1)S(1)} %get-tuple-element.57.refs_2_, ...), custom_call_target="tpu_custom_call" | custom-call | tf_op jit(solution)/shard_map/pallas_call | solution.py:29
  65.0 2.7 %collective-permute-done.16.refs_3_ = bf16[256,512]{1,0:T(8,128)(2,1)S(1)} collective-permute-done((bf16[256,512]{1,0:T(8,128)(2,1)S(1)}, bf16[256,512]{1,0:T(8,128)(2,1)S(1)}, u32[]{:S(2)}, u32[]{:S(2)}) %collective-permute-start.16) | collective-permute-done | bytes 262176 | tf_op jit(solution)/shard_map/ppermute | solution.py:398
  67.7 1.1 %shard_map.102 = bf16[384,512]{1,0:T(8,128)(2,1)} custom-call(f32[384,512]{1,0:T(8,128)S(1)} %get-tuple-element.53.before, bf16[384,256]{1,0:T(8,128)(2,1)S(1)} %collective-permute-done.13.refs_0_, bf16[384,256]{1,0:T(8,128)(2,1)S(1)} %collective-permute-done.14.refs_1_, bf16[256,512]{1,0:T(8,128)(2,1)S(1)} %collective-permute-done.15.refs_2_, ...), custom_call_target="tpu_custom_call" | custom-call | tf_op jit(solution)/shard_map/pallas_call | solution.py:29
  (29 shorter events, 0.1 us)
Async XLA Ops:
  0.6 13.1 %collective-permute-start.3 = (bf16[384,512]{1,0:T(8,128)(2,1)}, bf16[384,512]{1,0:T(8,128)(2,1)}, u32[]{:S(2)}, u32[]{:S(2)}) collective-permute-start(bf16[384,512]{1,0:T(8,128)(2,1)} %refs_0_.1), channel_id=1, source_target_pairs={{0,4},{4,8},{8,12},{1,5},{5,9},{9,13},{2,6},{6,10},{10,14},{3,7},{... | collective-permute-start | bytes 1179656 | tf_op jit(solution)/shard_map/ppermute | solution.py:264
  4.1 11.1 %collective-permute-start = (bf16[384,512]{1,0:T(8,128)(2,1)}, bf16[384,512]{1,0:T(8,128)(2,1)}, u32[]{:S(2)}, u32[]{:S(2)}) collective-permute-start(bf16[384,512]{1,0:T(8,128)(2,1)} %refs_0_.1), channel_id=1, source_target_pairs={{0,2},{1,3},{2,0},{3,1},{4,6},{5,7},{6,4},{7,5},{8,10},{9,11},{10,... | collective-permute-start | bytes 1179656 | tf_op jit(solution)/shard_map/ppermute | solution.py:260
  13.7 10.3 %collective-permute-start.4 = (bf16[384,512]{1,0:T(8,128)(2,1)}, bf16[384,512]{1,0:T(8,128)(2,1)}, u32[]{:S(2)}, u32[]{:S(2)}) collective-permute-start(bf16[384,512]{1,0:T(8,128)(2,1)} %collective-permute-done.3.refs_0_), channel_id=1, source_target_pairs={{0,2},{1,3},{2,0},{3,1},{4,6},{5,7},{6,4},{7,5},{8,10},{9,11},{10,... | collective-permute-start | bytes 1179656 | tf_op jit(solution)/shard_map/ppermute | solution.py:260
  15.2 10.3 %collective-permute-start.2 = (bf16[384,512]{1,0:T(8,128)(2,1)}, bf16[384,512]{1,0:T(8,128)(2,1)S(1)}, u32[]{:S(2)}, u32[]{:S(2)}) collective-permute-start(bf16[384,512]{1,0:T(8,128)(2,1)} %refs_0_.1), channel_id=1, source_target_pairs={{0,1},{1,0},{2,3},{3,2},{4,5},{5,4},{6,7},{7,6},{8,9},{9,8},{10,11... | collective-permute-start | bytes 1179656 | tf_op jit(solution)/shard_map/ppermute | solution.py:260
  15.2 17.1 %collective-permute-start.1 = (bf16[384,512]{1,0:T(8,128)(2,1)}, bf16[384,512]{1,0:T(8,128)(2,1)}, u32[]{:S(2)}, u32[]{:S(2)}) collective-permute-start(bf16[384,512]{1,0:T(8,128)(2,1)} %collective-permute-done.refs_0_), channel_id=1, source_target_pairs={{0,1},{1,0},{2,3},{3,2},{4,5},{5,4},{6,7},{7,6},{8,9},{9,8},{10,11... | collective-permute-start | bytes 1179656 | tf_op jit(solution)/shard_map/ppermute | solution.py:260
  16.4 21.6 %collective-permute-start.6 = (bf16[384,512]{1,0:T(8,128)(2,1)}, bf16[384,512]{1,0:T(8,128)(2,1)}, u32[]{:S(2)}, u32[]{:S(2)}) collective-permute-start(bf16[384,512]{1,0:T(8,128)(2,1)} %collective-permute-done.3.refs_0_), channel_id=1, source_target_pairs={{0,1},{1,0},{2,3},{3,2},{4,5},{5,4},{6,7},{7,6},{8,9},{9,8},{10,11... | collective-permute-start | bytes 1179656 | tf_op jit(solution)/shard_map/ppermute | solution.py:260
  24.0 21.7 %collective-permute-start.5 = (bf16[384,512]{1,0:T(8,128)(2,1)}, bf16[384,512]{1,0:T(8,128)(2,1)}, u32[]{:S(2)}, u32[]{:S(2)}) collective-permute-start(bf16[384,512]{1,0:T(8,128)(2,1)} %collective-permute-done.4.refs_0_), channel_id=1, source_target_pairs={{0,1},{1,0},{2,3},{3,2},{4,5},{5,4},{6,7},{7,6},{8,9},{9,8},{10,11... | collective-permute-start | bytes 1179656 | tf_op jit(solution)/shard_map/ppermute | solution.py:260
  24.0 1.5 %copy-start.11 = (bf16[384,512]{1,0:T(8,128)(2,1)S(1)}, bf16[384,512]{1,0:T(8,128)(2,1)}, u32[]{:S(2)}) copy-start(bf16[384,512]{1,0:T(8,128)(2,1)} %refs_0_.1) | copy-start | bytes 1179652
  24.0 1.5 %copy-start.12 = (f32[2,128]{1,0:T(2,128)S(1)}, f32[2,128]{1,0:T(2,128)}, u32[]{:S(2)}) copy-start(f32[2,128]{1,0:T(2,128)} %refs_6_.1) | copy-start | bytes 3076
  24.0 1.5 %copy-start.13 = (f32[2,128]{1,0:T(2,128)S(1)}, f32[2,128]{1,0:T(2,128)}, u32[]{:S(2)}) copy-start(f32[2,128]{1,0:T(2,128)} %refs_7_.1) | copy-start | bytes 3076
  25.5 1.2 %copy-start = (bf16[2048,256]{1,0:T(8,128)(2,1)S(1)}, bf16[2048,256]{1,0:T(8,128)(2,1)}, u32[]{:S(2)}) copy-start(bf16[2048,256]{1,0:T(8,128)(2,1)} %refs_3_.7) | copy-start | bytes 3145732
  26.7 1.2 %copy-start.2 = (bf16[2048,256]{1,0:T(8,128)(2,1)S(1)}, bf16[2048,256]{1,0:T(8,128)(2,1)}, u32[]{:S(2)}) copy-start(bf16[2048,256]{1,0:T(8,128)(2,1)} %refs_4_.7) | copy-start | bytes 3145732
  28.0 1.2 %copy-start.4 = (bf16[2048,256]{1,0:T(8,128)(2,1)S(1)}, bf16[2048,256]{1,0:T(8,128)(2,1)}, u32[]{:S(2)}) copy-start(bf16[2048,256]{1,0:T(8,128)(2,1)} %refs_3_.5) | copy-start | bytes 3145732
  29.2 3.1 %copy-start.1 = (bf16[2048,256]{1,0:T(8,128)(2,1)S(1)}, bf16[2048,256]{1,0:T(8,128)(2,1)}, u32[]{:S(2)}) copy-start(bf16[2048,256]{1,0:T(8,128)(2,1)} %refs_3_.7) | copy-start | bytes 3145732
  29.2 3.1 %copy-start.3 = (bf16[2048,256]{1,0:T(8,128)(2,1)S(1)}, bf16[2048,256]{1,0:T(8,128)(2,1)}, u32[]{:S(2)}) copy-start(bf16[2048,256]{1,0:T(8,128)(2,1)} %refs_4_.7) | copy-start | bytes 3145732
  31.5 0.8 %copy-start.7 = (f32[384,384]{1,0:T(8,128)}, f32[384,384]{1,0:T(8,128)S(1)}, u32[]{:S(2)}) copy-start(f32[384,384]{1,0:T(8,128)S(1)} %get-tuple-element.37.refs_1_) | copy-start | bytes 1769476
  32.3 3.0 %copy-start.5 = (f32[384,384]{1,0:T(8,128)}, f32[384,384]{1,0:T(8,128)S(1)}, u32[]{:S(2)}) copy-start(f32[384,384]{1,0:T(8,128)S(1)} %get-tuple-element.42.refs_14_) | copy-start | bytes 1769476
  32.3 3.0 %copy-start.9 = (f32[384,384]{1,0:T(8,128)}, f32[384,384]{1,0:T(8,128)S(1)}, u32[]{:S(2)}) copy-start(f32[384,384]{1,0:T(8,128)S(1)} %get-tuple-element.44.refs_3_) | copy-start | bytes 1769476
  35.3 10.4 %collective-permute-start.7 = (bf16[384,256]{1,0:T(8,128)(2,1)}, bf16[384,256]{1,0:T(8,128)(2,1)}, u32[]{:S(2)}, u32[]{:S(2)}) collective-permute-start(bf16[384,256]{1,0:T(8,128)(2,1)} %get-tuple-element.35.q), channel_id=1, source_target_pairs={{12,4},{13,5},{14,6},{15,7},{28,20},{29,21},{30,22},{31,23}} | collective-permute-start | bytes 589832 | tf_op jit(solution)/shard_map/ppermute | solution.py:264
  36.6 18.4 %collective-permute-start.8 = (bf16[2,384,256]{2,1,0:T(8,128)(2,1)S(1)}, bf16[2,384,256]{2,1,0:T(8,128)(2,1)}, u32[]{:S(2)}, u32[]{:S(2)}) collective-permute-start(bf16[2,384,256]{2,1,0:T(8,128)(2,1)S(1)} %get-tuple-element.36.refs_12_.refs_0_), channel_id=1, source_target_pairs={{0,8},{1,9},{2,10},{3,11},{16,24},{17,25},{18,26},{19,27}} | collective-permute-start | bytes 1179656 | tf_op jit(solution)/shard_map/ppermute | solution.py:264
  38.0 7.7 %copy-start.6 = (f32[384,384]{1,0:T(8,128)S(1)}, f32[384,384]{1,0:T(8,128)}, u32[]{:S(2)}) copy-start(f32[384,384]{1,0:T(8,128)} %copy-done.5) | copy-start | bytes 1769476
  45.7 4.9 %copy-start.14 = (bf16[256,2048]{1,0:T(8,128)(2,1)S(1)}, bf16[256,2048]{1,0:T(8,128)(2,1)}, u32[]{:S(2)}) copy-start(bf16[256,2048]{1,0:T(8,128)(2,1)} %param.15) | copy-start | bytes 3145732
  49.2 3.6 %copy-start.8 = (f32[384,384]{1,0:T(8,128)S(1)}, f32[384,384]{1,0:T(8,128)}, u32[]{:S(2)}) copy-start(f32[384,384]{1,0:T(8,128)} %copy-done.7) | copy-start | bytes 1769476
  49.2 3.6 %copy-start.10 = (f32[384,384]{1,0:T(8,128)S(1)}, f32[384,384]{1,0:T(8,128)}, u32[]{:S(2)}) copy-start(f32[384,384]{1,0:T(8,128)} %copy-done.9) | copy-start | bytes 1769476
  49.2 5.9 %collective-permute-start.9 = (bf16[384,256]{1,0:T(8,128)(2,1)S(1)}, bf16[384,256]{1,0:T(8,128)(2,1)S(1)}, u32[]{:S(2)}, u32[]{:S(2)}) collective-permute-start(bf16[384,256]{1,0:T(8,128)(2,1)S(1)} %get-tuple-element.48), channel_id=1, source_target_pairs={{4,12},{5,13},{6,14},{7,15},{20,28},{21,29},{22,30},{23,31}} | collective-permute-start | bytes 589832 | tf_op jit(solution)/shard_map/ppermute | solution.py:264
  50.7 8.6 %collective-permute-start.15 = (bf16[256,512]{1,0:T(8,128)(2,1)S(1)}, bf16[256,512]{1,0:T(8,128)(2,1)S(1)}, u32[]{:S(2)}, u32[]{:S(2)}) collective-permute-start(bf16[256,512]{1,0:T(8,128)(2,1)S(1)} %get-tuple-element.54), channel_id=1, source_target_pairs={{0,3},{1,2},{2,1},{3,0},{16,18},{17,19},{18,16},{19,17},{4,7},{5,6... | collective-permute-start | bytes 786440 | tf_op jit(solution)/shard_map/ppermute | solution.py:397
  51.5 3.6 %collective-permute-start.10 = (f32[8,384]{1,0:T(8,128)S(1)}, f32[8,384]{1,0:T(8,128)S(1)}, u32[]{:S(2)}, u32[]{:S(2)}) collective-permute-start(f32[8,384]{1,0:T(8,128)S(1)} %get-tuple-element.49), channel_id=1, source_target_pairs={{4,12},{5,13},{6,14},{7,15},{20,28},{21,29},{22,30},{23,31}} | collective-permute-start | bytes 36872 | tf_op jit(solution)/shard_map/ppermute | solution.py:264
  56.4 7.7 %collective-permute-start.13 = (bf16[384,256]{1,0:T(8,128)(2,1)S(1)}, bf16[384,256]{1,0:T(8,128)(2,1)S(1)}, u32[]{:S(2)}, u32[]{:S(2)}) collective-permute-start(bf16[384,256]{1,0:T(8,128)(2,1)S(1)} %get-tuple-element.51.refs_0_), channel_id=1, source_target_pairs={{0,2},{1,3},{2,0},{3,1},{4,6},{5,7},{6,4},{7,5},{8,10},{9,11},{10,... | collective-permute-start | bytes 589832 | tf_op jit(solution)/shard_map/ppermute | solution.py:260
  57.9 6.2 %collective-permute-start.12 = (bf16[256,512]{1,0:T(8,128)(2,1)S(1)}, bf16[256,512]{1,0:T(8,128)(2,1)S(1)}, u32[]{:S(2)}, u32[]{:S(2)}) collective-permute-start(bf16[256,512]{1,0:T(8,128)(2,1)S(1)} %get-tuple-element.52), channel_id=1, source_target_pairs={{0,1},{1,0},{2,3},{3,2},{4,5},{5,4},{6,7},{7,6},{8,9},{9,8},{10,11... | collective-permute-start | bytes 786440 | tf_op jit(solution)/shard_map/ppermute | solution.py:260
  59.4 8.3 %collective-permute-start.16 = (bf16[256,512]{1,0:T(8,128)(2,1)S(1)}, bf16[256,512]{1,0:T(8,128)(2,1)S(1)}, u32[]{:S(2)}, u32[]{:S(2)}) collective-permute-start(bf16[256,512]{1,0:T(8,128)(2,1)S(1)} %collective-permute-done.15.refs_2_), channel_id=1, source_target_pairs={{0,16},{16,0},{1,17},{17,1},{2,18},{18,2},{3,19},{19,3},{4,20},{20... | collective-permute-start | bytes 786440 | tf_op jit(solution)/shard_map/ppermute | solution.py:398
  60.2 3.9 %collective-permute-start.11 = (bf16[384,256]{1,0:T(8,128)(2,1)S(1)}, bf16[384,256]{1,0:T(8,128)(2,1)S(1)}, u32[]{:S(2)}, u32[]{:S(2)}) collective-permute-start(bf16[384,256]{1,0:T(8,128)(2,1)S(1)} %get-tuple-element.51.refs_0_), channel_id=1, source_target_pairs={{0,1},{1,0},{2,3},{3,2},{4,5},{5,4},{6,7},{7,6},{8,9},{9,8},{10,11... | collective-permute-start | bytes 589832 | tf_op jit(solution)/shard_map/ppermute | solution.py:260
  64.1 3.6 %collective-permute-start.14 = (bf16[384,256]{1,0:T(8,128)(2,1)S(1)}, bf16[384,256]{1,0:T(8,128)(2,1)S(1)}, u32[]{:S(2)}, u32[]{:S(2)}) collective-permute-start(bf16[384,256]{1,0:T(8,128)(2,1)S(1)} %collective-permute-done.13.refs_0_), channel_id=1, source_target_pairs={{0,1},{1,0},{2,3},{3,2},{4,5},{5,4},{6,7},{7,6},{8,9},{9,8},{10,11... | collective-permute-start | bytes 589832 | tf_op jit(solution)/shard_map/ppermute | solution.py:260

commit v6 on v5

--- a/solution.py
+++ b/solution.py
@@ -19,20 +19,25 @@
 
 
 VMEM = pl.BlockSpec(memory_space=pltpu.VMEM)
+HBM = pl.BlockSpec(memory_space=pltpu.HBM)
 
 
 def shape_of(shape, dtype):
     return jax.ShapeDtypeStruct(shape, dtype)
 
 
-def call(body, operands, outs, limit=24 << 20):
+def call(body, operands, outs, held=(), scratch=(), limit=24 << 20):
     return pl.pallas_call(
         body,
         out_shape=tuple(outs),
-        in_specs=[VMEM] * len(operands),
+        in_specs=[HBM if n in held else VMEM for n in range(len(operands))],
         out_specs=(VMEM,) * len(outs),
+        scratch_shapes=scratch,
         compiler_params=pltpu.CompilerParams(vmem_limit_bytes=limit),
-    )(*operands)
+    )(*[
+        pltpu.with_memory_space_constraint(x, pltpu.HBM) if n in held else x
+        for n, x in enumerate(operands)
+    ])
 
 
 def wide(column):
@@ -73,21 +78,50 @@
     return sums, squares
 
 
-def early_kernel(*refs, offsets, kinds, biases, copies):
+def first_kernel(*refs, count, kinds, pieces, columns):
+    own = refs[0]
+    others = refs[1:count]
+    gain = refs[count]
+    small = refs[count + 1 : count + 3]
+    weights = refs[count + 3 : count + 3 + kinds]
+    w_out = refs[count + 3 + kinds]
+    outs = refs[count + 4 + kinds : -2]
+    held, sems = refs[-2:]
+    sums_out, outs = outs[: kinds + 1], outs[kinds + 1 :]
+    small_out, outs = outs[:2], outs[2:]
+    weights_out, outs = outs[:kinds], outs[kinds:]
+    pieces_out, biases = outs[: len(pieces)], outs[len(pieces) :]
+    me = lax.axis_index("tp")
+    moves = [(own, held), *zip(weights, weights_out), *zip(small, small_out)]
+    for k, out in zip(pieces, pieces_out):
+        peer = me ^ (3 - lax.axis_index("grp") if k is None else k)
+        at = pl.ds(pl.multiple_of(peer * columns, columns), columns)
+        moves.append((w_out.at[:, at], out))
+    moves = [pltpu.make_async_copy(src, dst, sems.at[n]) for n, (src, dst) in enumerate(moves)]
+    for move in moves:
+        move.start()
+    for d, out in enumerate(biases):
+        out[...] = pair_bias(out.shape[0], d)
+    for move in moves[: kinds + 1]:
+        move.wait()
+    sums, squares = sums_of((held, *others), gain, weights_out, range(count))
+    for out, total in zip(sums_out, sums):
+        out[...] = total
+    sums_out[kinds][...] = wide(squares)
+    for move in moves[kinds + 1 :]:
+        move.wait()
+
+
+def early_kernel(*refs, offsets, kinds):
     count = len(offsets)
     hidden = refs[:count]
     gain = refs[count]
     weights = refs[count + 1 : count + 1 + kinds]
-    small = refs[count + 1 + kinds : count + 1 + kinds + copies]
-    outs = refs[count + 1 + kinds + copies :]
+    outs = refs[count + 1 + kinds :]
     sums, squares = sums_of(hidden, gain, weights, offsets)
     for out, total in zip(outs[:kinds], sums):
         out[...] = total
     outs[kinds][...] = wide(squares)
-    for ref, out in zip(small, outs[kinds + 1 :]):
-        out[...] = ref[...]
-    for d, out in zip(biases, outs[kinds + 1 + copies :]):
-        out[...] = pair_bias(out.shape[0], d)
 
 
 def head_turn(values, gains, cosine, sine):
@@ -96,7 +130,7 @@
     return values * cosine + pltpu.roll(values, values.shape[1] // 2, 1) * sine
 
 
-def late_kernel(*refs, offsets, kinds, width):
+def late_kernel(*refs, offsets, kinds, width, given):
     count = len(offsets)
     hidden = refs[:count]
     gain = refs[count]
@@ -107,7 +141,15 @@
     gains = rest[kinds + 1 : 2 * kinds]
     cosine, sine = rest[2 * kinds : 2 * kinds + 2]
     outs = rest[2 * kinds + 2 :]
-    outs = [*outs[:-1], outs[-1].at[0], outs[-1].at[1]]
+    computed = before[0].shape[0]
+    tail = None
+    if given:
+        received, pair = outs[-2:]
+        outs = [pair.at[0], pair.at[1]]
+        pair[:, computed:, :] = received[...]
+    else:
+        pair, tail = outs[-2:]
+        outs = [*outs[:-2], pair.at[0], pair.at[1]]
     sums, squares = sums_of(hidden, gain, weights, offsets)
     scale = lax.rsqrt((squares + squares_before[...]) / width + EPSILON)
     head_width = gains[0].shape[1]
@@ -120,7 +162,9 @@
             values = (sums[n][:, lanes] + before[n][:, lanes]) * scale
             if n < kinds - 1:
                 values = head_turn(values, gains[n][h : h + 1, :], turn_c, turn_s)
-            outs[n][:, lanes] = values.astype(jnp.bfloat16)
+            outs[n][:computed, lanes] = values.astype(jnp.bfloat16)
+    if tail is not None:
+        tail[...] = pair[:, computed - tail.shape[1] :, :]
 
 
 def softmax_part(q, blocks, lanes, factor):
@@ -292,7 +336,6 @@
     count = lax.axis_size("tp")
     shards = lax.axis_size("sp")
     half = count // 2
-    me = lax.axis_index("tp")
     shard = lax.axis_index("sp")
     factor = head_width ** (-0.5) * LOG2_E
     reach = -(-KEYS_BEHIND * DILATIONS[-1] // rows)
@@ -303,7 +346,7 @@
     first = shard * rows
     steps = jnp.arange(rows, dtype=jnp.int32)
     tables = turn_tables((steps + first).astype(jnp.float32), head_width)
-    tables_before = turn_tables((steps + first - rows).astype(jnp.float32), head_width)
+    tables_before = turn_tables((steps[: rows - rows // 3 // 16 * 16] + first - rows).astype(jnp.float32), head_width)
     gain = norm_gain.astype(jnp.float32).reshape(count, piece)
     gains = (query_gain, key_gain)
     weights = (w_query, w_key, w_value)
@@ -316,44 +359,49 @@
     late = tuple(range(half, count))
     columns = w_out.shape[1] // count
     copies = lax.axis_size("grp")
-    copy = lax.axis_index("grp")
     shared = copies == 2 and count == 4
 
-    def piece_for(k):
-        return lax.dynamic_slice_in_dim(w_out, (me ^ k) * columns, columns, axis=1)
-
-    own_slice, near_slice = piece_for(0), [piece_for(k) for k in range(1, half)]
-    far_slice = [piece_for(3 - copy)] if shared else [piece_for(k) for k in late]
-
-    def begin(blocks, kinds, biases, copied):
-        return call(
-            functools.partial(
-                early_kernel, offsets=early, kinds=kinds, biases=biases, copies=len(copied)
-            ),
-            [*blocks, gain, *weights[3 - kinds :], *copied],
-            [sums] * kinds
-            + [lane_wide]
-            + [shape_of(x.shape, x.dtype) for x in copied]
-            + [square] * len(biases),
-        )
-
-    def finish(blocks, kinds, begun, turn):
-        return call(
-            functools.partial(late_kernel, offsets=late, kinds=kinds, width=piece * count),
-            [*blocks, gain, *weights[3 - kinds :], *begun, *gains[3 - kinds :], *turn],
-            [half_sum] * (kinds - 2) + [pair],
-        )
+    piece_keys = (0, *range(1, half), *((None,) if shared else late))
+    piece_shape = shape_of((w_out.shape[0], columns), w_out.dtype)
+    direct = rows // 3 // 16 * 16
+    hidden_rows = rows - direct
+    sums_before = shape_of((hidden_rows, local_width), jnp.float32)
+    wide_before = shape_of((hidden_rows, LANES), jnp.float32)
+    direct_pair = shape_of((2, direct, local_width), jnp.bfloat16)
 
     across = swap(hidden, half)
+    rows_to_send = hidden[:hidden_rows]
+    before = behind(rows_to_send, 1)
     own_near = near_blocks(hidden)
-    before = behind(hidden, 1)
-
-    begun = begin(own_near, 3, tuple(distances), gains)
-    gains = begun[4:6]
-    biases = begun[6:]
+
+    operands = [*own_near, gain, *gains, *weights, w_out]
+    fixed = [0, *range(half + 1, len(operands))]
+    moves = len(weights) + 3 + len(piece_keys)
+    begun = call(
+        functools.partial(first_kernel, count=half, kinds=3, pieces=piece_keys, columns=columns),
+        operands,
+        [sums] * 3
+        + [lane_wide]
+        + [shape_of(x.shape, x.dtype) for x in (*gains, *weights)]
+        + [piece_shape] * len(piece_keys)
+        + [square] * len(distances),
+        held=fixed,
+        scratch=[pltpu.VMEM(hidden.shape, hidden.dtype), pltpu.SemaphoreType.DMA((moves,))],
+    )
+    begun, rest = begun[:4], begun[4:]
+    gains, weights, rest = rest[:2], rest[2:5], rest[5:]
+    slices, biases = rest[: len(piece_keys)], rest[len(piece_keys) :]
+    own_slice, near_slice, far_slice = slices[0], slices[1:half], slices[half:]
+
     own_far = near_blocks(across)
     before_across = swap(before, half)
-    q, kv = finish(own_far, 3, begun[:4], tables)
+    width = piece * count
+    q, kv, tail = call(
+        functools.partial(late_kernel, offsets=late, kinds=3, width=width, given=False),
+        [*own_far, gain, *weights, *begun, *gains, *tables],
+        [half_sum, pair, direct_pair],
+    )
+    received = behind(tail, 1)
 
     if helped is not None:
         visitor = send(q, [(helped, 1)])
@@ -361,18 +409,23 @@
     else:
         far_blocks = [(behind(kv, d), biases[d]) for d in far]
 
-    begun_before = begin(near_blocks(before), 2, (), ())
+    begun_before = call(
+        functools.partial(early_kernel, offsets=early, kinds=2),
+        [*near_blocks(before), gain, *weights[1:]],
+        [sums_before] * 2 + [wide_before],
+    )
     before_far = near_blocks(before_across)
+    operands = [*before_far, gain, *weights[1:], *begun_before, gains[1], *tables_before, received]
+    late_before = functools.partial(late_kernel, offsets=late, kinds=2, width=width, given=True)
     given = []
     if helped is None:
-        (kv_before,) = finish(before_far, 2, begun_before, tables_before)
+        (kv_before,) = call(late_before, operands, [pair])
     else:
-        operands = [*before_far, gain, *weights[1:], *begun_before, gains[1], *tables_before]
         kv_before, out, logs = call(
             functools.partial(
                 late_help_kernel,
                 late_count=len(operands),
-                late=functools.partial(late_kernel, offsets=late, kinds=2, width=piece * count),
+                late=late_before,
                 help_now=functools.partial(
                     help_kernel, blocks=2, head_width=head_width, factor=factor, helper=1
                 ),

time: 69.3 us -> 58.8 us (0.85)
  the two profiles are of different devices: /device:TPU:8 before, /device:TPU:30 now
where the time goes in v6:
time: 58.8 us; the launch traced here: 58.6 us
  waiting for transfers between devices  31.9 us (54%)
  starting transfers between devices  14.8 us (25%)
  Pallas kernels  8.77 us (15%)
  other arithmetic  1.31 us (2%)
  local copies, waits for them, and re-layouts  1.03 us (2%)
  between operations  0.84 us (1%)
    ppermute x6, waiting for transfers between devices, send(): return lax.ppermute(value, 'sp', pairs)  20.8 us
    pallas_call x8, Pallas kernels, call(): pl.pallas_call(body, out_shape=tuple(outs), in_specs=[HBM if n in held el...  8.77 us
    ppermute x10, waiting for transfers between devices, swap(): return lax.ppermute(value, 'tp', [(i, i ^ distance) for i in range(count)])  8.6 us
    ppermute x6, starting transfers between devices, send(): return lax.ppermute(value, 'sp', pairs)  8.1 us
    ppermute x10, starting transfers between devices, swap(): return lax.ppermute(value, 'tp', [(i, i ^ distance) for i in range(count)])  4.59 us
    ppermute x1, waiting for transfers between devices, layer(): other = lax.ppermute(fetched, 'grp', [(0, 1), (1, 0)])  2.52 us
    ppermute x1, starting transfers between devices, layer(): fetched = lax.ppermute(far_slice[0], ('grp', 'tp'), routes)  1.56 us
    sin x2, other arithmetic, turn_tables(): return (jnp.cos(angles), jnp.sin(angles))  1.28 us
  transfers between devices with their start and end apart: 18, of which 6 were waited for; matrix products, arithmetic and copies ran while one was open for 4% of the time, Pallas kernels for 13%

profile of v6, /device:TPU:30, one launch (start us, length us, event | category | flops | bytes accessed | tf_op | source)
XLA Modules:
  0.0 58.6 jit_solution(17496891240421618851)
XLA Ops:
  0.6 0.0 copy-start
  0.6 0.6 %collective-permute-start = (bf16[384,512]{1,0:T(8,128)(2,1)}, bf16[384,512]{1,0:T(8,128)(2,1)S(1)}, u32[]{:S(2)}, u32[]{:S(2)}) collective-permute-start(bf16[384,512]{1,0:T(8,128)(2,1)} %refs_0_.1), channel_id=1, source_target_pairs={{0,2},{1,3},{2,0},{3,1},{4,6},{5,7},{6,4},{7,5},{8,10},{9,11},{10,... | collective-permute-start | bytes 1179656 | tf_op jit(solution)/shard_map/ppermute | solution.py:304
  1.2 1.0 %slice.6 = bf16[256,512]{1,0:T(8,128)(2,1)S(1)} slice(bf16[384,512]{1,0:T(8,128)(2,1)} %refs_0_.1), slice={[0:256], [0:512]} | slice | bytes 524288 | tf_op jit(solution)/shard_map/slice | solution.py:373
  2.2 1.3 %collective-permute-start.3 = (bf16[256,512]{1,0:T(8,128)(2,1)S(1)}, bf16[256,512]{1,0:T(8,128)(2,1)S(1)}, u32[]{:S(2)}, u32[]{:S(2)}) collective-permute-start(bf16[256,512]{1,0:T(8,128)(2,1)S(1)} %slice.6), channel_id=1, source_target_pairs={{0,4},{4,8},{8,12},{1,5},{5,9},{9,13},{2,6},{6,10},{10,14},{3,7},{... | collective-permute-start | bytes 786440 | tf_op jit(solution)/shard_map/ppermute | solution.py:308
  3.6 0.1 collective-permute-start.2
  3.7 8.3 %collective-permute-done.3.refs_0_ = bf16[256,512]{1,0:T(8,128)(2,1)S(1)} collective-permute-done((bf16[256,512]{1,0:T(8,128)(2,1)S(1)}, bf16[256,512]{1,0:T(8,128)(2,1)S(1)}, u32[]{:S(2)}, u32[]{:S(2)}) %collective-permute-start.3) | collective-permute-done | bytes 262176 | tf_op jit(solution)/shard_map/ppermute | solution.py:308
  11.9 1.5 %collective-permute-start.4 = (bf16[256,512]{1,0:T(8,128)(2,1)S(1)}, bf16[256,512]{1,0:T(8,128)(2,1)S(1)}, u32[]{:S(2)}, u32[]{:S(2)}) collective-permute-start(bf16[256,512]{1,0:T(8,128)(2,1)S(1)} %collective-permute-done.3.refs_0_), channel_id=1, source_target_pairs={{0,2},{1,3},{2,0},{3,1},{4,6},{5,7},{6,4},{7,5},{8,10},{9,11},{10,... | collective-permute-start | bytes 786440 | tf_op jit(solution)/shard_map/ppermute | solution.py:304
  13.4 0.0 collective-permute-done.refs_0_
  13.4 0.1 collective-permute-start.1
  13.5 0.8 %multiply_sine_fusion = (f32[384,64]{1,0:T(8,128)S(1)}, f32[384,64]{1,0:T(8,128)S(1)}) fusion(f32[64]{0:T(128)S(1)} %multiply_power_fusion, f32[384]{0:T(512)S(1)} %add_convert_fusion), kind=kLoop, calls=%fused_computation | loop fusion | flops 24576 | bytes 198400 | tf_op jit(solution)/shard_map/sin | solution.py:329
  14.2 0.0 copy-start.1
  14.3 0.6 collective-permute-start.6
  14.8 4.0 %collective-permute-done.4.refs_0_ = bf16[256,512]{1,0:T(8,128)(2,1)S(1)} collective-permute-done((bf16[256,512]{1,0:T(8,128)(2,1)S(1)}, bf16[256,512]{1,0:T(8,128)(2,1)S(1)}, u32[]{:S(2)}, u32[]{:S(2)}) %collective-permute-start.4) | collective-permute-done | bytes 262176 | tf_op jit(solution)/shard_map/ppermute | solution.py:304
  18.8 0.0 collective-permute-start.5
  18.9 0.0 collective-permute-done.2.refs_1_
  18.9 2.9 %shard_map.95 = (f32[384,256]{1,0:T(8,128)S(1)}, f32[384,256]{1,0:T(8,128)S(1)}, f32[384,256]{1,0:T(8,128)S(1)}, f32[384,128]{1,0:T(8,128)S(1)}, f32[2,128]{1,0:...) custom-call(bf16[384,512]{1,0:T(8,128)(2,1)} %refs_0_.1, ...), custom_call_target="tpu_custom_call" | custom-call | tf_op jit(solution)/shard_map/pallas_call | solution.py:30
  21.7 0.0 collective-permute-done.1.refs_1_
  21.7 1.2 %shard_map.96 = (bf16[384,256]{1,0:T(8,128)(2,1)S(1)}, bf16[2,384,256]{2,1,0:T(8,128)(2,1)S(1)}, bf16[2,128,256]{2,1,0:T(8,128)(2,1)S(1)}) custom-call(bf16[384,512]{1,0:T(8,128)(2,1)S(1)} %collective-permute-done.refs_0_, bf16[384,512]{1,0:T(8,128)(2,1)S(1)} %collective-permute-done.1.refs_1_, f32[4,512]{1,0:T(4,128)S(1)} %reshape.25.refs_2_, ...), custom_call_target="tpu_custom_call" | custom-call | tf_op jit(solution)/shard_map/pallas_call | solution.py:30
  23.0 2.3 %collective-permute-start.8 = (bf16[384,256]{1,0:T(8,128)(2,1)S(1)}, bf16[384,256]{1,0:T(8,128)(2,1)S(1)}, u32[]{:S(2)}, u32[]{:S(2)}) collective-permute-start(bf16[384,256]{1,0:T(8,128)(2,1)S(1)} %get-tuple-element.45.q), channel_id=1, source_target_pairs={{12,4},{13,5},{14,6},{15,7},{28,20},{29,21},{30,22},{31,23}} | collective-permute-start | bytes 589832 | tf_op jit(solution)/shard_map/ppermute | solution.py:308
  25.3 1.3 %collective-permute-start.7 = (bf16[2,128,256]{2,1,0:T(8,128)(2,1)S(1)}, bf16[2,128,256]{2,1,0:T(8,128)(2,1)S(1)}, u32[]{:S(2)}, u32[]{:S(2)}) collective-permute-start(bf16[2,128,256]{2,1,0:T(8,128)(2,1)S(1)} %get-tuple-element.51), channel_id=1, source_target_pairs={{0,4},{4,8},{8,12},{1,5},{5,9},{9,13},{2,6},{6,10},{10,14},{3,7},{... | collective-permute-start | bytes 393224 | tf_op jit(solution)/shard_map/ppermute | solution.py:308
  26.6 0.7 %collective-permute-start.9 = (bf16[2,384,256]{2,1,0:T(8,128)(2,1)S(1)}, bf16[2,384,256]{2,1,0:T(8,128)(2,1)S(1)}, u32[]{:S(2)}, u32[]{:S(2)}) collective-permute-start(bf16[2,384,256]{2,1,0:T(8,128)(2,1)S(1)} %get-tuple-element.46.refs_13_.refs_0_), channel_id=1, source_target_pairs={{0,8},{1,9},{2,10},{3,11},{16,24},{17,25},{18,26},{19,27}} | collective-permute-start | bytes 1179656 | tf_op jit(solution)/shard_map/ppermute | solution.py:308
  27.2 0.5 multiply_sine_fusion.1
  27.8 0.0 collective-permute-done.6.refs_1_
  27.8 0.5 shard_map.97
  28.2 0.0 collective-permute-done.5.refs_1_
  28.3 4.5 %collective-permute-done.7.refs_11_ = bf16[2,128,256]{2,1,0:T(8,128)(2,1)S(1)} collective-permute-done((bf16[2,128,256]{2,1,0:T(8,128)(2,1)S(1)}, bf16[2,128,256]{2,1,0:T(8,128)(2,1)S(1)}, u32[]{:S(2)}, u32[]{:S(2)}) %collective-permute-start.7) | collective-permute-done | bytes 131104 | tf_op jit(solution)/shard_map/ppermute | solution.py:308
  32.8 0.0 collective-permute-done.8.refs_12_
  32.8 0.6 %shard_map.98 = (bf16[2,384,256]{2,1,0:T(8,128)(2,1)S(1)}, bf16[384,256]{1,0:T(8,128)(2,1)S(1)}, f32[8,384]{1,0:T(8,128)S(1)}) custom-call(bf16[256,512]{1,0:T(8,128)(2,1)S(1)} %collective-permute-done.4.refs_0_, bf16[256,512]{1,0:T(8,128)(2,1)S(1)} %collective-permute-done.5.refs_1_, f32[4,512]{1,0:T(4,128)S(1)} %reshape.25.refs_2_, ...), custom_call_target="tpu_custom_call" | custom-call | tf_op jit(solution)/shard_map/pallas_call | solution.py:30
  33.4 1.3 %collective-permute-start.10 = (bf16[384,256]{1,0:T(8,128)(2,1)S(1)}, bf16[384,256]{1,0:T(8,128)(2,1)S(1)}, u32[]{:S(2)}, u32[]{:S(2)}) collective-permute-start(bf16[384,256]{1,0:T(8,128)(2,1)S(1)} %get-tuple-element.59), channel_id=1, source_target_pairs={{4,12},{5,13},{6,14},{7,15},{20,28},{21,29},{22,30},{23,31}} | collective-permute-start | bytes 589832 | tf_op jit(solution)/shard_map/ppermute | solution.py:308
  34.7 1.6 %collective-permute-start.16 = (bf16[256,512]{1,0:T(8,128)(2,1)S(1)}, bf16[256,512]{1,0:T(8,128)(2,1)S(1)}, u32[]{:S(2)}, u32[]{:S(2)}) collective-permute-start(bf16[256,512]{1,0:T(8,128)(2,1)S(1)} %get-tuple-element.68), channel_id=1, source_target_pairs={{0,3},{1,2},{2,1},{3,0},{16,18},{17,19},{18,16},{19,17},{4,7},{5,6... | collective-permute-start | bytes 786440 | tf_op jit(solution)/shard_map/ppermute | solution.py:450
  36.3 1.3 %collective-permute-start.11 = (f32[8,384]{1,0:T(8,128)S(1)}, f32[8,384]{1,0:T(8,128)S(1)}, u32[]{:S(2)}, u32[]{:S(2)}) collective-permute-start(f32[8,384]{1,0:T(8,128)S(1)} %get-tuple-element.60), channel_id=1, source_target_pairs={{4,12},{5,13},{6,14},{7,15},{20,28},{21,29},{22,30},{23,31}} | collective-permute-start | bytes 36872 | tf_op jit(solution)/shard_map/ppermute | solution.py:308
  37.6 1.3 %shard_map.99 = (f32[384,256]{1,0:T(8,128)S(1)}, f32[384,256]{1,0:T(8,128)S(1)}, f32[384,256]{1,0:T(8,128)S(1)}) custom-call(bf16[384,256]{1,0:T(8,128)(2,1)S(1)} %get-tuple-element.45.q, bf16[2,384,256]{2,1,0:T(8,128)(2,1)S(1)} %get-tuple-element.46.refs_13_.refs_0_, f32[384,384]{1,0:T(8,128)S(1)} %get-tuple-element.47.refs_1_, ...), custom_call_target="tpu_custom_call" | custom-call | tf_op jit(solution)/shard_map/pallas_call | solution.py:30
  38.9 8.0 %collective-permute-done.11.refs_6_ = f32[8,384]{1,0:T(8,128)S(1)} collective-permute-done((f32[8,384]{1,0:T(8,128)S(1)}, f32[8,384]{1,0:T(8,128)S(1)}, u32[]{:S(2)}, u32[]{:S(2)}) %collective-permute-start.11) | collective-permute-done | bytes 12320 | tf_op jit(solution)/shard_map/ppermute | solution.py:308
  46.9 0.0 collective-permute-done.10.refs_5_
  46.9 0.0 collective-permute-done.9.refs_3_
  46.9 0.3 shard_map.100
  47.2 1.6 %collective-permute-start.14 = (bf16[384,256]{1,0:T(8,128)(2,1)S(1)}, bf16[384,256]{1,0:T(8,128)(2,1)S(1)}, u32[]{:S(2)}, u32[]{:S(2)}) collective-permute-start(bf16[384,256]{1,0:T(8,128)(2,1)S(1)} %get-tuple-element.62.refs_0_), channel_id=1, source_target_pairs={{0,2},{1,3},{2,0},{3,1},{4,6},{5,7},{6,4},{7,5},{8,10},{9,11},{10,... | collective-permute-start | bytes 589832 | tf_op jit(solution)/shard_map/ppermute | solution.py:304
  48.7 0.0 collective-permute-start.13
  48.7 0.0 collective-permute-done.16.refs_2_
  48.7 0.5 collective-permute-start.17
  49.2 0.2 collective-permute-start.12
  49.5 4.6 %collective-permute-done.14.refs_0_ = bf16[384,256]{1,0:T(8,128)(2,1)S(1)} collective-permute-done((bf16[384,256]{1,0:T(8,128)(2,1)S(1)}, bf16[384,256]{1,0:T(8,128)(2,1)S(1)}, u32[]{:S(2)}, u32[]{:S(2)}) %collective-permute-start.14) | collective-permute-done | bytes 196640 | tf_op jit(solution)/shard_map/ppermute | solution.py:304
  54.0 0.0 collective-permute-start.15
  54.1 0.0 collective-permute-done.13.refs_3_
  54.1 0.0 collective-permute-done.12.refs_1_
  54.1 0.9 %shard_map.101 = (f32[384,512]{1,0:T(8,128)S(1)}, f32[2,384]{1,0:T(2,128)}) custom-call(f32[384,256]{1,0:T(8,128)S(1)} %get-tuple-element.61.logs, bf16[384,256]{1,0:T(8,128)(2,1)S(1)} %get-tuple-element.62.refs_0_, bf16[384,256]{1,0:T(8,128)(2,1)S(1)} %collective-permute-done.12.refs_1_, bf16[256,512]{1,0:T(8,128)(2,1)S(1)} %get-tuple-element.63.refs_2_, ...), custom_call_target="tpu_custom_call" | custom-call | tf_op jit(solution)/shard_map/pallas_call | solution.py:30
  54.9 2.5 %collective-permute-done.17.refs_3_ = bf16[256,512]{1,0:T(8,128)(2,1)S(1)} collective-permute-done((bf16[256,512]{1,0:T(8,128)(2,1)S(1)}, bf16[256,512]{1,0:T(8,128)(2,1)S(1)}, u32[]{:S(2)}, u32[]{:S(2)}) %collective-permute-start.17) | collective-permute-done | bytes 262176 | tf_op jit(solution)/shard_map/ppermute | solution.py:451
  57.4 1.1 %shard_map.102 = bf16[384,512]{1,0:T(8,128)(2,1)} custom-call(f32[384,512]{1,0:T(8,128)S(1)} %get-tuple-element.66.before, bf16[384,256]{1,0:T(8,128)(2,1)S(1)} %collective-permute-done.14.refs_0_, bf16[384,256]{1,0:T(8,128)(2,1)S(1)} %collective-permute-done.15.refs_1_, bf16[256,512]{1,0:T(8,128)(2,1)S(1)} %collective-permute-done.16.refs_2_, ...), custom_call_target="tpu_custom_call" | custom-call | tf_op jit(solution)/shard_map/pallas_call | solution.py:30
  (8 shorter events, 0.0 us)
Async XLA Ops:
  0.6 2.9 %copy-start = (bf16[384,512]{1,0:T(8,128)(2,1)S(1)}, bf16[384,512]{1,0:T(8,128)(2,1)}, u32[]{:S(2)}) copy-start(bf16[384,512]{1,0:T(8,128)(2,1)} %refs_0_.1) | copy-start | bytes 1179652
  0.6 12.8 %collective-permute-start = (bf16[384,512]{1,0:T(8,128)(2,1)}, bf16[384,512]{1,0:T(8,128)(2,1)S(1)}, u32[]{:S(2)}, u32[]{:S(2)}) collective-permute-start(bf16[384,512]{1,0:T(8,128)(2,1)} %refs_0_.1), channel_id=1, source_target_pairs={{0,2},{1,3},{2,0},{3,1},{4,6},{5,7},{6,4},{7,5},{8,10},{9,11},{10,... | collective-permute-start | bytes 1179656 | tf_op jit(solution)/shard_map/ppermute | solution.py:304
  2.2 9.7 %collective-permute-start.3 = (bf16[256,512]{1,0:T(8,128)(2,1)S(1)}, bf16[256,512]{1,0:T(8,128)(2,1)S(1)}, u32[]{:S(2)}, u32[]{:S(2)}) collective-permute-start(bf16[256,512]{1,0:T(8,128)(2,1)S(1)} %slice.6), channel_id=1, source_target_pairs={{0,4},{4,8},{8,12},{1,5},{5,9},{9,13},{2,6},{6,10},{10,14},{3,7},{... | collective-permute-start | bytes 786440 | tf_op jit(solution)/shard_map/ppermute | solution.py:308
  3.6 15.3 %collective-permute-start.2 = (bf16[384,512]{1,0:T(8,128)(2,1)S(1)}, bf16[384,512]{1,0:T(8,128)(2,1)S(1)}, u32[]{:S(2)}, u32[]{:S(2)}) collective-permute-start(bf16[384,512]{1,0:T(8,128)(2,1)S(1)} %copy-done), channel_id=1, source_target_pairs={{0,1},{1,0},{2,3},{3,2},{4,5},{5,4},{6,7},{7,6},{8,9},{9,8},{10,11... | collective-permute-start | bytes 1179656 | tf_op jit(solution)/shard_map/ppermute | solution.py:304
  11.9 6.9 %collective-permute-start.4 = (bf16[256,512]{1,0:T(8,128)(2,1)S(1)}, bf16[256,512]{1,0:T(8,128)(2,1)S(1)}, u32[]{:S(2)}, u32[]{:S(2)}) collective-permute-start(bf16[256,512]{1,0:T(8,128)(2,1)S(1)} %collective-permute-done.3.refs_0_), channel_id=1, source_target_pairs={{0,2},{1,3},{2,0},{3,1},{4,6},{5,7},{6,4},{7,5},{8,10},{9,11},{10,... | collective-permute-start | bytes 786440 | tf_op jit(solution)/shard_map/ppermute | solution.py:304
  13.4 8.3 %collective-permute-start.1 = (bf16[384,512]{1,0:T(8,128)(2,1)S(1)}, bf16[384,512]{1,0:T(8,128)(2,1)S(1)}, u32[]{:S(2)}, u32[]{:S(2)}) collective-permute-start(bf16[384,512]{1,0:T(8,128)(2,1)S(1)} %collective-permute-done.refs_0_), channel_id=1, source_target_pairs={{0,1},{1,0},{2,3},{3,2},{4,5},{5,4},{6,7},{7,6},{8,9},{9,8},{10,11... | collective-permute-start | bytes 1179656 | tf_op jit(solution)/shard_map/ppermute | solution.py:304
  14.2 4.6 %copy-start.1 = (bf16[2048]{0:T(1024)(128)(2,1)S(1)}, bf16[2048]{0:T(1024)(128)(2,1)}, u32[]{:S(2)}) copy-start(bf16[2048]{0:T(1024)(128)(2,1)} %param.9) | copy-start | bytes 12292
  14.3 13.5 %collective-permute-start.6 = (bf16[256,512]{1,0:T(8,128)(2,1)S(1)}, bf16[256,512]{1,0:T(8,128)(2,1)S(1)}, u32[]{:S(2)}, u32[]{:S(2)}) collective-permute-start(bf16[256,512]{1,0:T(8,128)(2,1)S(1)} %collective-permute-done.3.refs_0_), channel_id=1, source_target_pairs={{0,1},{1,0},{2,3},{3,2},{4,5},{5,4},{6,7},{7,6},{8,9},{9,8},{10,11... | collective-permute-start | bytes 786440 | tf_op jit(solution)/shard_map/ppermute | solution.py:304
  18.8 9.4 %collective-permute-start.5 = (bf16[256,512]{1,0:T(8,128)(2,1)S(1)}, bf16[256,512]{1,0:T(8,128)(2,1)S(1)}, u32[]{:S(2)}, u32[]{:S(2)}) collective-permute-start(bf16[256,512]{1,0:T(8,128)(2,1)S(1)} %collective-permute-done.4.refs_0_), channel_id=1, source_target_pairs={{0,1},{1,0},{2,3},{3,2},{4,5},{5,4},{6,7},{7,6},{8,9},{9,8},{10,11... | collective-permute-start | bytes 786440 | tf_op jit(solution)/shard_map/ppermute | solution.py:304
  23.0 9.8 %collective-permute-start.8 = (bf16[384,256]{1,0:T(8,128)(2,1)S(1)}, bf16[384,256]{1,0:T(8,128)(2,1)S(1)}, u32[]{:S(2)}, u32[]{:S(2)}) collective-permute-start(bf16[384,256]{1,0:T(8,128)(2,1)S(1)} %get-tuple-element.45.q), channel_id=1, source_target_pairs={{12,4},{13,5},{14,6},{15,7},{28,20},{29,21},{30,22},{31,23}} | collective-permute-start | bytes 589832 | tf_op jit(solution)/shard_map/ppermute | solution.py:308
  25.3 7.5 %collective-permute-start.7 = (bf16[2,128,256]{2,1,0:T(8,128)(2,1)S(1)}, bf16[2,128,256]{2,1,0:T(8,128)(2,1)S(1)}, u32[]{:S(2)}, u32[]{:S(2)}) collective-permute-start(bf16[2,128,256]{2,1,0:T(8,128)(2,1)S(1)} %get-tuple-element.51), channel_id=1, source_target_pairs={{0,4},{4,8},{8,12},{1,5},{5,9},{9,13},{2,6},{6,10},{10,14},{3,7},{... | collective-permute-start | bytes 393224 | tf_op jit(solution)/shard_map/ppermute | solution.py:308
  26.6 20.3 %collective-permute-start.9 = (bf16[2,384,256]{2,1,0:T(8,128)(2,1)S(1)}, bf16[2,384,256]{2,1,0:T(8,128)(2,1)S(1)}, u32[]{:S(2)}, u32[]{:S(2)}) collective-permute-start(bf16[2,384,256]{2,1,0:T(8,128)(2,1)S(1)} %get-tuple-element.46.refs_13_.refs_0_), channel_id=1, source_target_pairs={{0,8},{1,9},{2,10},{3,11},{16,24},{17,25},{18,26},{19,27}} | collective-permute-start | bytes 1179656 | tf_op jit(solution)/shard_map/ppermute | solution.py:308
  33.4 13.5 %collective-permute-start.10 = (bf16[384,256]{1,0:T(8,128)(2,1)S(1)}, bf16[384,256]{1,0:T(8,128)(2,1)S(1)}, u32[]{:S(2)}, u32[]{:S(2)}) collective-permute-start(bf16[384,256]{1,0:T(8,128)(2,1)S(1)} %get-tuple-element.59), channel_id=1, source_target_pairs={{4,12},{5,13},{6,14},{7,15},{20,28},{21,29},{22,30},{23,31}} | collective-permute-start | bytes 589832 | tf_op jit(solution)/shard_map/ppermute | solution.py:308
  34.7 14.0 %collective-permute-start.16 = (bf16[256,512]{1,0:T(8,128)(2,1)S(1)}, bf16[256,512]{1,0:T(8,128)(2,1)S(1)}, u32[]{:S(2)}, u32[]{:S(2)}) collective-permute-start(bf16[256,512]{1,0:T(8,128)(2,1)S(1)} %get-tuple-element.68), channel_id=1, source_target_pairs={{0,3},{1,2},{2,1},{3,0},{16,18},{17,19},{18,16},{19,17},{4,7},{5,6... | collective-permute-start | bytes 786440 | tf_op jit(solution)/shard_map/ppermute | solution.py:450
  36.3 10.6 %collective-permute-start.11 = (f32[8,384]{1,0:T(8,128)S(1)}, f32[8,384]{1,0:T(8,128)S(1)}, u32[]{:S(2)}, u32[]{:S(2)}) collective-permute-start(f32[8,384]{1,0:T(8,128)S(1)} %get-tuple-element.60), channel_id=1, source_target_pairs={{4,12},{5,13},{6,14},{7,15},{20,28},{21,29},{22,30},{23,31}} | collective-permute-start | bytes 36872 | tf_op jit(solution)/shard_map/ppermute | solution.py:308
  47.2 6.9 %collective-permute-start.14 = (bf16[384,256]{1,0:T(8,128)(2,1)S(1)}, bf16[384,256]{1,0:T(8,128)(2,1)S(1)}, u32[]{:S(2)}, u32[]{:S(2)}) collective-permute-start(bf16[384,256]{1,0:T(8,128)(2,1)S(1)} %get-tuple-element.62.refs_0_), channel_id=1, source_target_pairs={{0,2},{1,3},{2,0},{3,1},{4,6},{5,7},{6,4},{7,5},{8,10},{9,11},{10,... | collective-permute-start | bytes 589832 | tf_op jit(solution)/shard_map/ppermute | solution.py:304
  48.7 5.3 %collective-permute-start.13 = (bf16[256,512]{1,0:T(8,128)(2,1)S(1)}, bf16[256,512]{1,0:T(8,128)(2,1)S(1)}, u32[]{:S(2)}, u32[]{:S(2)}) collective-permute-start(bf16[256,512]{1,0:T(8,128)(2,1)S(1)} %get-tuple-element.65), channel_id=1, source_target_pairs={{0,1},{1,0},{2,3},{3,2},{4,5},{5,4},{6,7},{7,6},{8,9},{9,8},{10,11... | collective-permute-start | bytes 786440 | tf_op jit(solution)/shard_map/ppermute | solution.py:304
  48.7 8.7 %collective-permute-start.17 = (bf16[256,512]{1,0:T(8,128)(2,1)S(1)}, bf16[256,512]{1,0:T(8,128)(2,1)S(1)}, u32[]{:S(2)}, u32[]{:S(2)}) collective-permute-start(bf16[256,512]{1,0:T(8,128)(2,1)S(1)} %collective-permute-done.16.refs_2_), channel_id=1, source_target_pairs={{0,16},{16,0},{1,17},{17,1},{2,18},{18,2},{3,19},{19,3},{4,20},{20... | collective-permute-start | bytes 786440 | tf_op jit(solution)/shard_map/ppermute | solution.py:451
  49.2 4.8 %collective-permute-start.12 = (bf16[384,256]{1,0:T(8,128)(2,1)S(1)}, bf16[384,256]{1,0:T(8,128)(2,1)S(1)}, u32[]{:S(2)}, u32[]{:S(2)}) collective-permute-start(bf16[384,256]{1,0:T(8,128)(2,1)S(1)} %get-tuple-element.62.refs_0_), channel_id=1, source_target_pairs={{0,1},{1,0},{2,3},{3,2},{4,5},{5,4},{6,7},{7,6},{8,9},{9,8},{10,11... | collective-permute-start | bytes 589832 | tf_op jit(solution)/shard_map/ppermute | solution.py:304
  54.0 3.4 %collective-permute-start.15 = (bf16[384,256]{1,0:T(8,128)(2,1)S(1)}, bf16[384,256]{1,0:T(8,128)(2,1)S(1)}, u32[]{:S(2)}, u32[]{:S(2)}) collective-permute-start(bf16[384,256]{1,0:T(8,128)(2,1)S(1)} %collective-permute-done.14.refs_0_), channel_id=1, source_target_pairs={{0,1},{1,0},{2,3},{3,2},{4,5},{5,4},{6,7},{7,6},{8,9},{9,8},{10,11... | collective-permute-start | bytes 589832 | tf_op jit(solution)/shard_map/ppermute | solution.py:304

commit v7 on v6

--- a/solution.py
+++ b/solution.py
@@ -130,7 +130,7 @@
     return values * cosine + pltpu.roll(values, values.shape[1] // 2, 1) * sine
 
 
-def late_kernel(*refs, offsets, kinds, width, given):
+def late_kernel(*refs, offsets, kinds, width):
     count = len(offsets)
     hidden = refs[:count]
     gain = refs[count]
@@ -141,15 +141,7 @@
     gains = rest[kinds + 1 : 2 * kinds]
     cosine, sine = rest[2 * kinds : 2 * kinds + 2]
     outs = rest[2 * kinds + 2 :]
-    computed = before[0].shape[0]
-    tail = None
-    if given:
-        received, pair = outs[-2:]
-        outs = [pair.at[0], pair.at[1]]
-        pair[:, computed:, :] = received[...]
-    else:
-        pair, tail = outs[-2:]
-        outs = [*outs[:-2], pair.at[0], pair.at[1]]
+    outs = [*outs[:-1], outs[-1].at[0], outs[-1].at[1]]
     sums, squares = sums_of(hidden, gain, weights, offsets)
     scale = lax.rsqrt((squares + squares_before[...]) / width + EPSILON)
     head_width = gains[0].shape[1]
@@ -162,9 +154,7 @@
             values = (sums[n][:, lanes] + before[n][:, lanes]) * scale
             if n < kinds - 1:
                 values = head_turn(values, gains[n][h : h + 1, :], turn_c, turn_s)
-            outs[n][:computed, lanes] = values.astype(jnp.bfloat16)
-    if tail is not None:
-        tail[...] = pair[:, computed - tail.shape[1] :, :]
+            outs[n][:, lanes] = values.astype(jnp.bfloat16)
 
 
 def softmax_part(q, blocks, lanes, factor):
@@ -346,7 +336,7 @@
     first = shard * rows
     steps = jnp.arange(rows, dtype=jnp.int32)
     tables = turn_tables((steps + first).astype(jnp.float32), head_width)
-    tables_before = turn_tables((steps[: rows - rows // 3 // 16 * 16] + first - rows).astype(jnp.float32), head_width)
+    tables_before = turn_tables((steps + first - rows).astype(jnp.float32), head_width)
     gain = norm_gain.astype(jnp.float32).reshape(count, piece)
     gains = (query_gain, key_gain)
     weights = (w_query, w_key, w_value)
@@ -363,15 +353,8 @@
 
     piece_keys = (0, *range(1, half), *((None,) if shared else late))
     piece_shape = shape_of((w_out.shape[0], columns), w_out.dtype)
-    direct = rows // 3 // 16 * 16
-    hidden_rows = rows - direct
-    sums_before = shape_of((hidden_rows, local_width), jnp.float32)
-    wide_before = shape_of((hidden_rows, LANES), jnp.float32)
-    direct_pair = shape_of((2, direct, local_width), jnp.bfloat16)
-
     across = swap(hidden, half)
-    rows_to_send = hidden[:hidden_rows]
-    before = behind(rows_to_send, 1)
+    before = behind(hidden, 1)
     own_near = near_blocks(hidden)
 
     operands = [*own_near, gain, *gains, *weights, w_out]
@@ -396,12 +379,11 @@
     own_far = near_blocks(across)
     before_across = swap(before, half)
     width = piece * count
-    q, kv, tail = call(
-        functools.partial(late_kernel, offsets=late, kinds=3, width=width, given=False),
+    q, kv = call(
+        functools.partial(late_kernel, offsets=late, kinds=3, width=width),
         [*own_far, gain, *weights, *begun, *gains, *tables],
-        [half_sum, pair, direct_pair],
-    )
-    received = behind(tail, 1)
+        [half_sum, pair],
+    )
 
     if helped is not None:
         visitor = send(q, [(helped, 1)])
@@ -412,11 +394,11 @@
     begun_before = call(
         functools.partial(early_kernel, offsets=early, kinds=2),
         [*near_blocks(before), gain, *weights[1:]],
-        [sums_before] * 2 + [wide_before],
+        [sums] * 2 + [lane_wide],
     )
     before_far = near_blocks(before_across)
-    operands = [*before_far, gain, *weights[1:], *begun_before, gains[1], *tables_before, received]
-    late_before = functools.partial(late_kernel, offsets=late, kinds=2, width=width, given=True)
+    operands = [*before_far, gain, *weights[1:], *begun_before, gains[1], *tables_before]
+    late_before = functools.partial(late_kernel, offsets=late, kinds=2, width=width)
     given = []
     if helped is None:
         (kv_before,) = call(late_before, operands, [pair])
@@ -442,7 +424,6 @@
         [sums] * 3,
     )
 
-    *far_slice, _ = lax.optimization_barrier((*far_slice, begun_before[2]))
     *near_slice, _ = lax.optimization_barrier((*near_slice, begun_before[2]))
     near_pieces = [own_slice] + [swap(x, k + 1) for k, x in enumerate(near_slice)]
     if shared:

time: 58.8 us -> 61 us (1.037)
  the two profiles are of different devices: /device:TPU:30 before, /device:TPU:8 now
where the time goes in v7:
time: 61 us; the launch traced here: 60.8 us
  waiting for transfers between devices  32.3 us (53%)
  starting transfers between devices  15.3 us (25%)
  Pallas kernels  10.3 us (17%)
  other arithmetic  1.45 us (2%)
  between operations  0.75 us (1%)
  local copies, waits for them, and re-layouts  0.7 us (1%)
    ppermute x5, waiting for transfers between devices, send(): return lax.ppermute(value, 'sp', pairs)  17 us
    pallas_call x8, Pallas kernels, call(): pl.pallas_call(body, out_shape=tuple(outs), in_specs=[HBM if n in held el...  10.3 us
    ppermute x10, waiting for transfers between devices, swap(): return lax.ppermute(value, 'tp', [(i, i ^ distance) for i in range(count)])  10.2 us
    ppermute x5, starting transfers between devices, send(): return lax.ppermute(value, 'sp', pairs)  8.04 us
    ppermute x10, starting transfers between devices, swap(): return lax.ppermute(value, 'tp', [(i, i ^ distance) for i in range(count)])  5.13 us
    ppermute x1, waiting for transfers between devices, layer(): other = lax.ppermute(fetched, 'grp', [(0, 1), (1, 0)])  3.19 us
    ppermute x1, waiting for transfers between devices, layer(): fetched = lax.ppermute(far_slice[0], ('grp', 'tp'), routes)  1.92 us
    sin x1, other arithmetic, turn_tables(): return (jnp.cos(angles), jnp.sin(angles))  1.43 us
  transfers between devices with their start and end apart: 17, of which 7 were waited for; matrix products, arithmetic and copies ran while one was open for 4% of the time, Pallas kernels for 15%

profile of v7, /device:TPU:8, one launch (start us, length us, event | category | flops | bytes accessed | tf_op | source)
XLA Modules:
  0.0 60.8 jit_solution(200949469487352764)
XLA Ops:
  0.6 3.5 %collective-permute-start.3 = (bf16[384,512]{1,0:T(8,128)(2,1)}, bf16[384,512]{1,0:T(8,128)(2,1)S(1)}, u32[]{:S(2)}, u32[]{:S(2)}) collective-permute-start(bf16[384,512]{1,0:T(8,128)(2,1)} %refs_0_.1), channel_id=1, source_target_pairs={{0,4},{4,8},{8,12},{1,5},{5,9},{9,13},{2,6},{6,10},{10,14},{3,7},{... | collective-permute-start | bytes 1179656 | tf_op jit(solution)/shard_map/ppermute | solution.py:298
  4.1 1.6 %collective-permute-start = (bf16[384,512]{1,0:T(8,128)(2,1)}, bf16[384,512]{1,0:T(8,128)(2,1)S(1)}, u32[]{:S(2)}, u32[]{:S(2)}) collective-permute-start(bf16[384,512]{1,0:T(8,128)(2,1)} %refs_0_.1), channel_id=1, source_target_pairs={{0,2},{1,3},{2,0},{3,1},{4,6},{5,7},{6,4},{7,5},{8,10},{9,11},{10,... | collective-permute-start | bytes 1179656 | tf_op jit(solution)/shard_map/ppermute | solution.py:294
  5.7 7.9 %collective-permute-done.3.refs_0_ = bf16[384,512]{1,0:T(8,128)(2,1)S(1)} collective-permute-done((bf16[384,512]{1,0:T(8,128)(2,1)}, bf16[384,512]{1,0:T(8,128)(2,1)S(1)}, u32[]{:S(2)}, u32[]{:S(2)}) %collective-permute-start.3) | collective-permute-done | bytes 393248 | tf_op jit(solution)/shard_map/ppermute | solution.py:298
  13.6 1.5 %collective-permute-start.4 = (bf16[384,512]{1,0:T(8,128)(2,1)S(1)}, bf16[384,512]{1,0:T(8,128)(2,1)S(1)}, u32[]{:S(2)}, u32[]{:S(2)}) collective-permute-start(bf16[384,512]{1,0:T(8,128)(2,1)S(1)} %collective-permute-done.3.refs_0_), channel_id=1, source_target_pairs={{0,2},{1,3},{2,0},{3,1},{4,6},{5,7},{6,4},{7,5},{8,10},{9,11},{10,... | collective-permute-start | bytes 1179656 | tf_op jit(solution)/shard_map/ppermute | solution.py:294
  15.1 0.0 collective-permute-start.2
  15.1 0.0 collective-permute-done.refs_0_
  15.1 0.5 collective-permute-start.1
  15.6 0.7 %reshape.28.refs_2_ = f32[4,512]{1,0:T(4,128)S(1)} reshape(bf16[2048]{0:T(1024)(128)(2,1)} %param.9) | data formatting | bytes 12288 | tf_op jit(solution)/shard_map/reshape | solution.py:340
  16.3 0.0 collective-permute-start.6
  16.3 7.3 %collective-permute-done.4.refs_0_ = bf16[384,512]{1,0:T(8,128)(2,1)S(1)} collective-permute-done((bf16[384,512]{1,0:T(8,128)(2,1)S(1)}, bf16[384,512]{1,0:T(8,128)(2,1)S(1)}, u32[]{:S(2)}, u32[]{:S(2)}) %collective-permute-start.4) | collective-permute-done | bytes 393248 | tf_op jit(solution)/shard_map/ppermute | solution.py:294
  23.6 0.0 collective-permute-start.5
  23.6 1.4 %multiply_sine_fusion = (f32[384,64]{1,0:T(8,128)S(1)}, f32[384,64]{1,0:T(8,128)S(1)}, f32[384,64]{1,0:T(8,128)S(1)}, f32[384,64]{1,0:T(8,128)S(1)}) fusion(f32[384]{0:T(512)S(1)} %get-tuple-element.72, f32[64]{0:T(128)S(1)} %multiply_power_fusion, f32[384]{0:T(512)S(1)} %get-tuple-element.73), kind=kLoop, calls=%fused_computation | loop fusion | flops 49152 | bytes 396544 | tf_op jit(solution)/shard_map/sin | solution.py:319
  25.0 0.0 collective-permute-done.2.refs_1_
  25.0 2.9 %shard_map.95 = (f32[384,256]{1,0:T(8,128)S(1)}, f32[384,256]{1,0:T(8,128)S(1)}, f32[384,256]{1,0:T(8,128)S(1)}, f32[384,128]{1,0:T(8,128)S(1)}, f32[2,128]{1,0:...) custom-call(bf16[384,512]{1,0:T(8,128)(2,1)} %refs_0_.1, ...), custom_call_target="tpu_custom_call" | custom-call | tf_op jit(solution)/shard_map/pallas_call | solution.py:30
  27.9 0.0 collective-permute-done.1.refs_1_
  27.9 1.2 %shard_map.96 = (bf16[384,256]{1,0:T(8,128)(2,1)S(1)}, bf16[2,384,256]{2,1,0:T(8,128)(2,1)S(1)}) custom-call(bf16[384,512]{1,0:T(8,128)(2,1)S(1)} %collective-permute-done.refs_0_, bf16[384,512]{1,0:T(8,128)(2,1)S(1)} %collective-permute-done.1.refs_1_, f32[4,512]{1,0:T(4,128)S(1)} %reshape.28.refs_2_, bf16[2048,256]{1,0:T(8,128)(2,1)S(1)} %get-tuple-element.34.refs_3_, ...), custom_call_target="tpu_custom_call" | custom-call | tf_op jit(solution)/shard_map/pallas_call | solution.py:30
  29.1 1.3 %collective-permute-start.7 = (bf16[384,256]{1,0:T(8,128)(2,1)S(1)}, bf16[384,256]{1,0:T(8,128)(2,1)S(1)}, u32[]{:S(2)}, u32[]{:S(2)}) collective-permute-start(bf16[384,256]{1,0:T(8,128)(2,1)S(1)} %get-tuple-element.43.q), channel_id=1, source_target_pairs={{12,4},{13,5},{14,6},{15,7},{28,20},{29,21},{30,22},{31,23}} | collective-permute-start | bytes 589832 | tf_op jit(solution)/shard_map/ppermute | solution.py:298
  30.4 0.7 %collective-permute-start.8 = (bf16[2,384,256]{2,1,0:T(8,128)(2,1)S(1)}, bf16[2,384,256]{2,1,0:T(8,128)(2,1)S(1)}, u32[]{:S(2)}, u32[]{:S(2)}) collective-permute-start(bf16[2,384,256]{2,1,0:T(8,128)(2,1)S(1)} %get-tuple-element.44.refs_12_.refs_0_), channel_id=1, source_target_pairs={{0,8},{1,9},{2,10},{3,11},{16,24},{17,25},{18,26},{19,27}} | collective-permute-start | bytes 1179656 | tf_op jit(solution)/shard_map/ppermute | solution.py:298
  31.1 0.0 collective-permute-done.6.refs_1_
  31.1 0.6 shard_map.97
  31.7 7.5 %collective-permute-done.7.refs_11_ = bf16[384,256]{1,0:T(8,128)(2,1)S(1)} collective-permute-done((bf16[384,256]{1,0:T(8,128)(2,1)S(1)}, bf16[384,256]{1,0:T(8,128)(2,1)S(1)}, u32[]{:S(2)}, u32[]{:S(2)}) %collective-permute-start.7) | collective-permute-done | bytes 196640 | tf_op jit(solution)/shard_map/ppermute | solution.py:298
  39.2 0.0 collective-permute-done.5.refs_1_
  39.2 2.2 %shard_map.98 = (bf16[2,384,256]{2,1,0:T(8,128)(2,1)S(1)}, bf16[384,256]{1,0:T(8,128)(2,1)S(1)}, f32[8,384]{1,0:T(8,128)S(1)}) custom-call(bf16[384,512]{1,0:T(8,128)(2,1)S(1)} %collective-permute-done.4.refs_0_, bf16[384,512]{1,0:T(8,128)(2,1)S(1)} %collective-permute-done.5.refs_1_, f32[4,512]{1,0:T(4,128)S(1)} %reshape.28.refs_2_, ...), custom_call_target="tpu_custom_call" | custom-call | tf_op jit(solution)/shard_map/pallas_call | solution.py:30
  41.4 1.3 %collective-permute-start.9 = (bf16[384,256]{1,0:T(8,128)(2,1)S(1)}, bf16[384,256]{1,0:T(8,128)(2,1)S(1)}, u32[]{:S(2)}, u32[]{:S(2)}) collective-permute-start(bf16[384,256]{1,0:T(8,128)(2,1)S(1)} %get-tuple-element.56), channel_id=1, source_target_pairs={{4,12},{5,13},{6,14},{7,15},{20,28},{21,29},{22,30},{23,31}} | collective-permute-start | bytes 589832 | tf_op jit(solution)/shard_map/ppermute | solution.py:298
  42.7 0.8 %collective-permute-start.15 = (bf16[256,512]{1,0:T(8,128)(2,1)S(1)}, bf16[256,512]{1,0:T(8,128)(2,1)S(1)}, u32[]{:S(2)}, u32[]{:S(2)}) collective-permute-start(bf16[256,512]{1,0:T(8,128)(2,1)S(1)} %get-tuple-element.64), channel_id=1, source_target_pairs={{0,3},{1,2},{2,1},{3,0},{16,18},{17,19},{18,16},{19,17},{4,7},{5,6... | collective-permute-start | bytes 786440 | tf_op jit(solution)/shard_map/ppermute | solution.py:431
  43.5 1.3 %collective-permute-start.10 = (f32[8,384]{1,0:T(8,128)S(1)}, f32[8,384]{1,0:T(8,128)S(1)}, u32[]{:S(2)}, u32[]{:S(2)}) collective-permute-start(f32[8,384]{1,0:T(8,128)S(1)} %get-tuple-element.57), channel_id=1, source_target_pairs={{4,12},{5,13},{6,14},{7,15},{20,28},{21,29},{22,30},{23,31}} | collective-permute-start | bytes 36872 | tf_op jit(solution)/shard_map/ppermute | solution.py:298
  44.8 1.3 %shard_map.99 = (f32[384,256]{1,0:T(8,128)S(1)}, f32[384,256]{1,0:T(8,128)S(1)}, f32[384,256]{1,0:T(8,128)S(1)}) custom-call(bf16[384,256]{1,0:T(8,128)(2,1)S(1)} %get-tuple-element.43.q, bf16[2,384,256]{2,1,0:T(8,128)(2,1)S(1)} %get-tuple-element.44.refs_12_.refs_0_, f32[384,384]{1,0:T(8,128)S(1)} %get-tuple-element.45.refs_1_, ...), custom_call_target="tpu_custom_call" | custom-call | tf_op jit(solution)/shard_map/pallas_call | solution.py:30
  46.1 0.0 collective-permute-done.8.refs_3_
  46.1 1.6 %collective-permute-done.10.refs_6_ = f32[8,384]{1,0:T(8,128)S(1)} collective-permute-done((f32[8,384]{1,0:T(8,128)S(1)}, f32[8,384]{1,0:T(8,128)S(1)}, u32[]{:S(2)}, u32[]{:S(2)}) %collective-permute-start.10) | collective-permute-done | bytes 12320 | tf_op jit(solution)/shard_map/ppermute | solution.py:298
  47.7 0.0 collective-permute-done.9.refs_5_
  47.7 0.2 shard_map.100
  47.9 1.6 %collective-permute-start.13 = (bf16[384,256]{1,0:T(8,128)(2,1)S(1)}, bf16[384,256]{1,0:T(8,128)(2,1)S(1)}, u32[]{:S(2)}, u32[]{:S(2)}) collective-permute-start(bf16[384,256]{1,0:T(8,128)(2,1)S(1)} %get-tuple-element.59.refs_0_), channel_id=1, source_target_pairs={{0,2},{1,3},{2,0},{3,1},{4,6},{5,7},{6,4},{7,5},{8,10},{9,11},{10,... | collective-permute-start | bytes 589832 | tf_op jit(solution)/shard_map/ppermute | solution.py:294
  49.4 0.0 collective-permute-start.12
  49.4 1.9 %collective-permute-done.15.refs_2_ = bf16[256,512]{1,0:T(8,128)(2,1)S(1)} collective-permute-done((bf16[256,512]{1,0:T(8,128)(2,1)S(1)}, bf16[256,512]{1,0:T(8,128)(2,1)S(1)}, u32[]{:S(2)}, u32[]{:S(2)}) %collective-permute-start.15) | collective-permute-done | bytes 262176 | tf_op jit(solution)/shard_map/ppermute | solution.py:431
  51.4 1.3 %collective-permute-start.16 = (bf16[256,512]{1,0:T(8,128)(2,1)S(1)}, bf16[256,512]{1,0:T(8,128)(2,1)S(1)}, u32[]{:S(2)}, u32[]{:S(2)}) collective-permute-start(bf16[256,512]{1,0:T(8,128)(2,1)S(1)} %collective-permute-done.15.refs_2_), channel_id=1, source_target_pairs={{0,16},{16,0},{1,17},{17,1},{2,18},{18,2},{3,19},{19,3},{4,20},{20... | collective-permute-start | bytes 786440 | tf_op jit(solution)/shard_map/ppermute | solution.py:432
  52.7 0.0 collective-permute-start.11
  52.7 2.9 %collective-permute-done.13.refs_0_ = bf16[384,256]{1,0:T(8,128)(2,1)S(1)} collective-permute-done((bf16[384,256]{1,0:T(8,128)(2,1)S(1)}, bf16[384,256]{1,0:T(8,128)(2,1)S(1)}, u32[]{:S(2)}, u32[]{:S(2)}) %collective-permute-start.13) | collective-permute-done | bytes 196640 | tf_op jit(solution)/shard_map/ppermute | solution.py:294
  55.6 0.0 collective-permute-start.14
  55.6 0.0 collective-permute-done.12.refs_3_
  55.6 0.0 collective-permute-done.11.refs_1_
  55.6 0.9 %shard_map.101 = (f32[384,512]{1,0:T(8,128)S(1)}, f32[2,384]{1,0:T(2,128)}) custom-call(f32[384,256]{1,0:T(8,128)S(1)} %get-tuple-element.58.logs, bf16[384,256]{1,0:T(8,128)(2,1)S(1)} %get-tuple-element.59.refs_0_, bf16[384,256]{1,0:T(8,128)(2,1)S(1)} %collective-permute-done.11.refs_1_, bf16[256,512]{1,0:T(8,128)(2,1)S(1)} %get-tuple-element.60.refs_2_, ...), custom_call_target="tpu_custom_call" | custom-call | tf_op jit(solution)/shard_map/pallas_call | solution.py:30
  56.5 3.2 %collective-permute-done.16.refs_3_ = bf16[256,512]{1,0:T(8,128)(2,1)S(1)} collective-permute-done((bf16[256,512]{1,0:T(8,128)(2,1)S(1)}, bf16[256,512]{1,0:T(8,128)(2,1)S(1)}, u32[]{:S(2)}, u32[]{:S(2)}) %collective-permute-start.16) | collective-permute-done | bytes 262176 | tf_op jit(solution)/shard_map/ppermute | solution.py:432
  59.7 0.0 collective-permute-done.14.refs_1_
  59.7 1.1 %shard_map.102 = bf16[384,512]{1,0:T(8,128)(2,1)} custom-call(f32[384,512]{1,0:T(8,128)S(1)} %get-tuple-element.63.before, bf16[384,256]{1,0:T(8,128)(2,1)S(1)} %collective-permute-done.13.refs_0_, bf16[384,256]{1,0:T(8,128)(2,1)S(1)} %collective-permute-done.14.refs_1_, bf16[256,512]{1,0:T(8,128)(2,1)S(1)} %collective-permute-done.15.refs_2_, ...), custom_call_target="tpu_custom_call" | custom-call | tf_op jit(solution)/shard_map/pallas_call | solution.py:30
  (2 shorter events, 0.0 us)
Async XLA Ops:
  0.6 13.0 %collective-permute-start.3 = (bf16[384,512]{1,0:T(8,128)(2,1)}, bf16[384,512]{1,0:T(8,128)(2,1)S(1)}, u32[]{:S(2)}, u32[]{:S(2)}) collective-permute-start(bf16[384,512]{1,0:T(8,128)(2,1)} %refs_0_.1), channel_id=1, source_target_pairs={{0,4},{4,8},{8,12},{1,5},{5,9},{9,13},{2,6},{6,10},{10,14},{3,7},{... | collective-permute-start | bytes 1179656 | tf_op jit(solution)/shard_map/ppermute | solution.py:298
  4.1 11.0 %collective-permute-start = (bf16[384,512]{1,0:T(8,128)(2,1)}, bf16[384,512]{1,0:T(8,128)(2,1)S(1)}, u32[]{:S(2)}, u32[]{:S(2)}) collective-permute-start(bf16[384,512]{1,0:T(8,128)(2,1)} %refs_0_.1), channel_id=1, source_target_pairs={{0,2},{1,3},{2,0},{3,1},{4,6},{5,7},{6,4},{7,5},{8,10},{9,11},{10,... | collective-permute-start | bytes 1179656 | tf_op jit(solution)/shard_map/ppermute | solution.py:294
  13.6 10.0 %collective-permute-start.4 = (bf16[384,512]{1,0:T(8,128)(2,1)S(1)}, bf16[384,512]{1,0:T(8,128)(2,1)S(1)}, u32[]{:S(2)}, u32[]{:S(2)}) collective-permute-start(bf16[384,512]{1,0:T(8,128)(2,1)S(1)} %collective-permute-done.3.refs_0_), channel_id=1, source_target_pairs={{0,2},{1,3},{2,0},{3,1},{4,6},{5,7},{6,4},{7,5},{8,10},{9,11},{10,... | collective-permute-start | bytes 1179656 | tf_op jit(solution)/shard_map/ppermute | solution.py:294
  15.1 10.0 %collective-permute-start.2 = (bf16[384,512]{1,0:T(8,128)(2,1)}, bf16[384,512]{1,0:T(8,128)(2,1)S(1)}, u32[]{:S(2)}, u32[]{:S(2)}) collective-permute-start(bf16[384,512]{1,0:T(8,128)(2,1)} %refs_0_.1), channel_id=1, source_target_pairs={{0,1},{1,0},{2,3},{3,2},{4,5},{5,4},{6,7},{7,6},{8,9},{9,8},{10,11... | collective-permute-start | bytes 1179656 | tf_op jit(solution)/shard_map/ppermute | solution.py:294
  15.1 12.8 %collective-permute-start.1 = (bf16[384,512]{1,0:T(8,128)(2,1)S(1)}, bf16[384,512]{1,0:T(8,128)(2,1)S(1)}, u32[]{:S(2)}, u32[]{:S(2)}) collective-permute-start(bf16[384,512]{1,0:T(8,128)(2,1)S(1)} %collective-permute-done.refs_0_), channel_id=1, source_target_pairs={{0,1},{1,0},{2,3},{3,2},{4,5},{5,4},{6,7},{7,6},{8,9},{9,8},{10,11... | collective-permute-start | bytes 1179656 | tf_op jit(solution)/shard_map/ppermute | solution.py:294
  16.3 14.8 %collective-permute-start.6 = (bf16[384,512]{1,0:T(8,128)(2,1)S(1)}, bf16[384,512]{1,0:T(8,128)(2,1)S(1)}, u32[]{:S(2)}, u32[]{:S(2)}) collective-permute-start(bf16[384,512]{1,0:T(8,128)(2,1)S(1)} %collective-permute-done.3.refs_0_), channel_id=1, source_target_pairs={{0,1},{1,0},{2,3},{3,2},{4,5},{5,4},{6,7},{7,6},{8,9},{9,8},{10,11... | collective-permute-start | bytes 1179656 | tf_op jit(solution)/shard_map/ppermute | solution.py:294
  23.6 15.7 %collective-permute-start.5 = (bf16[384,512]{1,0:T(8,128)(2,1)S(1)}, bf16[384,512]{1,0:T(8,128)(2,1)S(1)}, u32[]{:S(2)}, u32[]{:S(2)}) collective-permute-start(bf16[384,512]{1,0:T(8,128)(2,1)S(1)} %collective-permute-done.4.refs_0_), channel_id=1, source_target_pairs={{0,1},{1,0},{2,3},{3,2},{4,5},{5,4},{6,7},{7,6},{8,9},{9,8},{10,11... | collective-permute-start | bytes 1179656 | tf_op jit(solution)/shard_map/ppermute | solution.py:294
  29.1 10.1 %collective-permute-start.7 = (bf16[384,256]{1,0:T(8,128)(2,1)S(1)}, bf16[384,256]{1,0:T(8,128)(2,1)S(1)}, u32[]{:S(2)}, u32[]{:S(2)}) collective-permute-start(bf16[384,256]{1,0:T(8,128)(2,1)S(1)} %get-tuple-element.43.q), channel_id=1, source_target_pairs={{12,4},{13,5},{14,6},{15,7},{28,20},{29,21},{30,22},{31,23}} | collective-permute-start | bytes 589832 | tf_op jit(solution)/shard_map/ppermute | solution.py:298
  30.4 15.7 %collective-permute-start.8 = (bf16[2,384,256]{2,1,0:T(8,128)(2,1)S(1)}, bf16[2,384,256]{2,1,0:T(8,128)(2,1)S(1)}, u32[]{:S(2)}, u32[]{:S(2)}) collective-permute-start(bf16[2,384,256]{2,1,0:T(8,128)(2,1)S(1)} %get-tuple-element.44.refs_12_.refs_0_), channel_id=1, source_target_pairs={{0,8},{1,9},{2,10},{3,11},{16,24},{17,25},{18,26},{19,27}} | collective-permute-start | bytes 1179656 | tf_op jit(solution)/shard_map/ppermute | solution.py:298
  41.4 6.3 %collective-permute-start.9 = (bf16[384,256]{1,0:T(8,128)(2,1)S(1)}, bf16[384,256]{1,0:T(8,128)(2,1)S(1)}, u32[]{:S(2)}, u32[]{:S(2)}) collective-permute-start(bf16[384,256]{1,0:T(8,128)(2,1)S(1)} %get-tuple-element.56), channel_id=1, source_target_pairs={{4,12},{5,13},{6,14},{7,15},{20,28},{21,29},{22,30},{23,31}} | collective-permute-start | bytes 589832 | tf_op jit(solution)/shard_map/ppermute | solution.py:298
  42.7 8.6 %collective-permute-start.15 = (bf16[256,512]{1,0:T(8,128)(2,1)S(1)}, bf16[256,512]{1,0:T(8,128)(2,1)S(1)}, u32[]{:S(2)}, u32[]{:S(2)}) collective-permute-start(bf16[256,512]{1,0:T(8,128)(2,1)S(1)} %get-tuple-element.64), channel_id=1, source_target_pairs={{0,3},{1,2},{2,1},{3,0},{16,18},{17,19},{18,16},{19,17},{4,7},{5,6... | collective-permute-start | bytes 786440 | tf_op jit(solution)/shard_map/ppermute | solution.py:431
  43.5 4.2 %collective-permute-start.10 = (f32[8,384]{1,0:T(8,128)S(1)}, f32[8,384]{1,0:T(8,128)S(1)}, u32[]{:S(2)}, u32[]{:S(2)}) collective-permute-start(f32[8,384]{1,0:T(8,128)S(1)} %get-tuple-element.57), channel_id=1, source_target_pairs={{4,12},{5,13},{6,14},{7,15},{20,28},{21,29},{22,30},{23,31}} | collective-permute-start | bytes 36872 | tf_op jit(solution)/shard_map/ppermute | solution.py:298
  47.9 7.7 %collective-permute-start.13 = (bf16[384,256]{1,0:T(8,128)(2,1)S(1)}, bf16[384,256]{1,0:T(8,128)(2,1)S(1)}, u32[]{:S(2)}, u32[]{:S(2)}) collective-permute-start(bf16[384,256]{1,0:T(8,128)(2,1)S(1)} %get-tuple-element.59.refs_0_), channel_id=1, source_target_pairs={{0,2},{1,3},{2,0},{3,1},{4,6},{5,7},{6,4},{7,5},{8,10},{9,11},{10,... | collective-permute-start | bytes 589832 | tf_op jit(solution)/shard_map/ppermute | solution.py:294
  49.4 6.2 %collective-permute-start.12 = (bf16[256,512]{1,0:T(8,128)(2,1)S(1)}, bf16[256,512]{1,0:T(8,128)(2,1)S(1)}, u32[]{:S(2)}, u32[]{:S(2)}) collective-permute-start(bf16[256,512]{1,0:T(8,128)(2,1)S(1)} %get-tuple-element.62), channel_id=1, source_target_pairs={{0,1},{1,0},{2,3},{3,2},{4,5},{5,4},{6,7},{7,6},{8,9},{9,8},{10,11... | collective-permute-start | bytes 786440 | tf_op jit(solution)/shard_map/ppermute | solution.py:294
  51.4 8.3 %collective-permute-start.16 = (bf16[256,512]{1,0:T(8,128)(2,1)S(1)}, bf16[256,512]{1,0:T(8,128)(2,1)S(1)}, u32[]{:S(2)}, u32[]{:S(2)}) collective-permute-start(bf16[256,512]{1,0:T(8,128)(2,1)S(1)} %collective-permute-done.15.refs_2_), channel_id=1, source_target_pairs={{0,16},{16,0},{1,17},{17,1},{2,18},{18,2},{3,19},{19,3},{4,20},{20... | collective-permute-start | bytes 786440 | tf_op jit(solution)/shard_map/ppermute | solution.py:432
  52.7 2.9 %collective-permute-start.11 = (bf16[384,256]{1,0:T(8,128)(2,1)S(1)}, bf16[384,256]{1,0:T(8,128)(2,1)S(1)}, u32[]{:S(2)}, u32[]{:S(2)}) collective-permute-start(bf16[384,256]{1,0:T(8,128)(2,1)S(1)} %get-tuple-element.59.refs_0_), channel_id=1, source_target_pairs={{0,1},{1,0},{2,3},{3,2},{4,5},{5,4},{6,7},{7,6},{8,9},{9,8},{10,11... | collective-permute-start | bytes 589832 | tf_op jit(solution)/shard_map/ppermute | solution.py:294
  55.6 4.1 %collective-permute-start.14 = (bf16[384,256]{1,0:T(8,128)(2,1)S(1)}, bf16[384,256]{1,0:T(8,128)(2,1)S(1)}, u32[]{:S(2)}, u32[]{:S(2)}) collective-permute-start(bf16[384,256]{1,0:T(8,128)(2,1)S(1)} %collective-permute-done.13.refs_0_), channel_id=1, source_target_pairs={{0,1},{1,0},{2,3},{3,2},{4,5},{5,4},{6,7},{7,6},{8,9},{9,8},{10,11... | collective-permute-start | bytes 589832 | tf_op jit(solution)/shard_map/ppermute | solution.py:294

commit v8 on v7

--- a/solution.py
+++ b/solution.py
@@ -195,18 +195,24 @@
     return [slice(h * head_width, (h + 1) * head_width) for h in range(count)]
 
 
-def near_kernel(q, *refs, distances, head_width, factor):
-    count = len(distances)
-    tops, totals, accs = refs[2 * count :]
-    for lanes in head_lanes(q, head_width):
-        blocks = []
-        for n, d in enumerate(distances):
-            bias = refs[2 * n + 1][...]
-            blocks.append((refs[2 * n], jnp.where(lax.axis_index("sp") >= d, bias, MASKED) if d else bias))
-        top, total, acc = softmax_part(q, blocks, lanes, factor)
-        tops[:, lanes] = wide(top)
-        totals[:, lanes] = wide(total)
-        accs[:, lanes] = acc
+def near_kernel(q, kv, bias, kv_before, bias_before, *refs, last, head_width, factor):
+    shard = lax.axis_index("sp")
+    tops, totals, accs = refs[-3:]
+
+    def work(previous):
+        for lanes in head_lanes(q, head_width):
+            seen = jnp.where(shard >= 1, bias_before[...], MASKED)
+            blocks = [(kv, bias[...]), (previous, seen)]
+            top, total, acc = softmax_part(q, blocks, lanes, factor)
+            tops[:, lanes] = wide(top)
+            totals[:, lanes] = wide(total)
+            accs[:, lanes] = acc
+
+    if last is None:
+        work(kv_before)
+    else:
+        pl.when(shard == last)(lambda: work(refs[0]))
+        pl.when(shard != last)(lambda: work(kv_before))
 
 
 def help_kernel(q, *refs, blocks, head_width, factor, helper):
@@ -354,7 +360,10 @@
     piece_keys = (0, *range(1, half), *((None,) if shared else late))
     piece_shape = shape_of((w_out.shape[0], columns), w_out.dtype)
     across = swap(hidden, half)
-    before = behind(hidden, 1)
+    if helped is None:
+        before = behind(hidden, 1)
+    else:
+        before = send(hidden, [(n, n + 1) for n in range(shards - 2)])
     own_near = near_blocks(hidden)
 
     operands = [*own_near, gain, *gains, *weights, w_out]
@@ -377,7 +386,11 @@
     own_slice, near_slice, far_slice = slices[0], slices[1:half], slices[half:]
 
     own_far = near_blocks(across)
-    before_across = swap(before, half)
+    if helped is None:
+        before_across = swap(before, half)
+    else:
+        inner = [(n * count + t, n * count + (t ^ half)) for n in (1, 2) for t in range(count)]
+        before_across = lax.ppermute(before, ("sp", "tp"), inner)
     width = piece * count
     q, kv = call(
         functools.partial(late_kernel, offsets=late, kinds=3, width=width),
@@ -388,8 +401,10 @@
     if helped is not None:
         visitor = send(q, [(helped, 1)])
         far_blocks = [(send(kv, [(0, 2)]), biases[2])]
+        direct = [send(kv, [(shards - 2, shards - 1)])]
     else:
         far_blocks = [(behind(kv, d), biases[d]) for d in far]
+        direct = []
 
     begun_before = call(
         functools.partial(early_kernel, offsets=early, kinds=2),
@@ -418,9 +433,9 @@
         given = [send(out, [(1, helped)]), send(logs, [(1, helped)])]
     near = call(
         functools.partial(
-            near_kernel, distances=(0, 1), head_width=head_width, factor=factor
+            near_kernel, last=helped, head_width=head_width, factor=factor
         ),
-        [q, kv, biases[0], kv_before, biases[1]],
+        [q, kv, biases[0], kv_before, biases[1], *direct],
         [sums] * 3,
     )
 
@@ -429,6 +444,7 @@
     if shared:
         routes = [(g * 4 + t, g * 4 + (t ^ (3 - g))) for g in range(2) for t in range(4)]
         fetched = lax.ppermute(far_slice[0], ("grp", "tp"), routes)
+        fetched, _ = lax.optimization_barrier((fetched, near[0]))
         other = lax.ppermute(fetched, "grp", [(0, 1), (1, 0)])
         far_pieces = [fetched, other]
     else:

time: 61 us -> 66.9 us (1.097)
  the two profiles are of different devices: /device:TPU:8 before, /device:TPU:24 now
where the time goes in v8:
time: 66.9 us; the launch traced here: 66.6 us
  waiting for transfers between devices  28.3 us (42%)
  starting transfers between devices  26.2 us (39%)
  Pallas kernels  9.19 us (14%)
  other arithmetic  1.45 us (2%)
  between operations  0.79 us (1%)
  local copies, waits for them, and re-layouts  0.7 us (1%)
    ppermute x6, starting transfers between devices, send(): return lax.ppermute(value, 'sp', pairs)  19.2 us
    ppermute x6, waiting for transfers between devices, send(): return lax.ppermute(value, 'sp', pairs)  13.4 us
    ppermute x9, waiting for transfers between devices, swap(): return lax.ppermute(value, 'tp', [(i, i ^ distance) for i in range(count)])  12.4 us
    pallas_call x8, Pallas kernels, call(): pl.pallas_call(body, out_shape=tuple(outs), in_specs=[HBM if n in held el...  9.19 us
    ppermute x9, starting transfers between devices, swap(): return lax.ppermute(value, 'tp', [(i, i ^ distance) for i in range(count)])  4 us
    ppermute x1, waiting for transfers between devices, layer(): other = lax.ppermute(fetched, 'grp', [(0, 1), (1, 0)])  2.51 us
    ppermute x1, starting transfers between devices, layer(): other = lax.ppermute(fetched, 'grp', [(0, 1), (1, 0)])  1.52 us
    sin x1, other arithmetic, turn_tables(): return (jnp.cos(angles), jnp.sin(angles))  1.43 us
  transfers between devices with their start and end apart: 18, of which 6 were waited for; matrix products, arithmetic and copies ran while one was open for 3% of the time, Pallas kernels for 12%

profile of v8, /device:TPU:24, one launch (start us, length us, event | category | flops | bytes accessed | tf_op | source)
XLA Modules:
  0.0 66.6 jit_solution(15107618871378888048)
XLA Ops:
  0.6 0.7 %collective-permute-start.3 = (bf16[384,512]{1,0:T(8,128)(2,1)}, bf16[384,512]{1,0:T(8,128)(2,1)S(1)}, u32[]{:S(2)}, u32[]{:S(2)}) collective-permute-start(bf16[384,512]{1,0:T(8,128)(2,1)} %refs_0_.1), channel_id=1, source_target_pairs={{0,4},{4,8},{1,5},{5,9},{2,6},{6,10},{3,7},{7,11},{16,20},{20,24},... | collective-permute-start | bytes 1179656 | tf_op jit(solution)/shard_map/ppermute | solution.py:304
  1.3 1.6 %collective-permute-start = (bf16[384,512]{1,0:T(8,128)(2,1)}, bf16[384,512]{1,0:T(8,128)(2,1)S(1)}, u32[]{:S(2)}, u32[]{:S(2)}) collective-permute-start(bf16[384,512]{1,0:T(8,128)(2,1)} %refs_0_.1), channel_id=1, source_target_pairs={{0,2},{1,3},{2,0},{3,1},{4,6},{5,7},{6,4},{7,5},{8,10},{9,11},{10,... | collective-permute-start | bytes 1179656 | tf_op jit(solution)/shard_map/ppermute | solution.py:300
  2.9 0.0 collective-permute-done.3.refs_0_
  2.9 0.7 %collective-permute-start.4 = (bf16[384,512]{1,0:T(8,128)(2,1)S(1)}, bf16[384,512]{1,0:T(8,128)(2,1)S(1)}, u32[]{:S(2)}, u32[]{:S(2)}) collective-permute-start(bf16[384,512]{1,0:T(8,128)(2,1)S(1)} %collective-permute-done.3.refs_0_), channel_id=1, source_target_pairs={{4,6},{5,7},{6,4},{7,5},{8,10},{9,11},{10,8},{11,9},{20,22},{21,23... | collective-permute-start | bytes 1179656 | tf_op jit(solution)/shard_map/ppermute | solution.py:393
  3.6 0.1 collective-permute-start.2
  3.6 8.8 %collective-permute-done.refs_0_ = bf16[384,512]{1,0:T(8,128)(2,1)S(1)} collective-permute-done((bf16[384,512]{1,0:T(8,128)(2,1)}, bf16[384,512]{1,0:T(8,128)(2,1)S(1)}, u32[]{:S(2)}, u32[]{:S(2)}) %collective-permute-start) | collective-permute-done | bytes 393248 | tf_op jit(solution)/shard_map/ppermute | solution.py:300
  12.5 0.0 collective-permute-start.1
  12.5 0.7 %reshape.28.refs_2_ = f32[4,512]{1,0:T(4,128)S(1)} reshape(bf16[2048]{0:T(1024)(128)(2,1)} %param.9) | data formatting | bytes 12288 | tf_op jit(solution)/shard_map/reshape | solution.py:346
  13.2 0.5 collective-permute-start.6
  13.7 0.0 collective-permute-done.4.refs_0_
  13.7 0.1 collective-permute-start.5
  13.8 1.4 %multiply_sine_fusion = (f32[384,64]{1,0:T(8,128)S(1)}, f32[384,64]{1,0:T(8,128)S(1)}, f32[384,64]{1,0:T(8,128)S(1)}, f32[384,64]{1,0:T(8,128)S(1)}) fusion(f32[384]{0:T(512)S(1)} %get-tuple-element.74, f32[64]{0:T(128)S(1)} %multiply_power_fusion, f32[384]{0:T(512)S(1)} %get-tuple-element.75), kind=kLoop, calls=%fused_computation | loop fusion | flops 49152 | bytes 396544 | tf_op jit(solution)/shard_map/sin | solution.py:325
  15.2 0.0 collective-permute-done.2.refs_1_
  15.2 2.9 %shard_map.95 = (f32[384,256]{1,0:T(8,128)S(1)}, f32[384,256]{1,0:T(8,128)S(1)}, f32[384,256]{1,0:T(8,128)S(1)}, f32[384,128]{1,0:T(8,128)S(1)}, f32[2,128]{1,0:...) custom-call(bf16[384,512]{1,0:T(8,128)(2,1)} %refs_0_.1, ...), custom_call_target="tpu_custom_call" | custom-call | tf_op jit(solution)/shard_map/pallas_call | solution.py:30
  18.1 0.0 collective-permute-done.1.refs_1_
  18.1 1.2 %shard_map.96 = (bf16[384,256]{1,0:T(8,128)(2,1)S(1)}, bf16[2,384,256]{2,1,0:T(8,128)(2,1)S(1)}) custom-call(bf16[384,512]{1,0:T(8,128)(2,1)S(1)} %collective-permute-done.refs_0_, bf16[384,512]{1,0:T(8,128)(2,1)S(1)} %collective-permute-done.1.refs_1_, f32[4,512]{1,0:T(4,128)S(1)} %reshape.28.refs_2_, bf16[2048,256]{1,0:T(8,128)(2,1)S(1)} %get-tuple-element.35.refs_3_, ...), custom_call_target="tpu_custom_call" | custom-call | tf_op jit(solution)/shard_map/pallas_call | solution.py:30
  19.3 14.0 %collective-permute-start.7 = (bf16[384,256]{1,0:T(8,128)(2,1)S(1)}, bf16[384,256]{1,0:T(8,128)(2,1)S(1)}, u32[]{:S(2)}, u32[]{:S(2)}) collective-permute-start(bf16[384,256]{1,0:T(8,128)(2,1)S(1)} %get-tuple-element.44.q), channel_id=1, source_target_pairs={{12,4},{13,5},{14,6},{15,7},{28,20},{29,21},{30,22},{31,23}} | collective-permute-start | bytes 589832 | tf_op jit(solution)/shard_map/ppermute | solution.py:304
  33.3 1.3 %collective-permute-start.8 = (bf16[2,384,256]{2,1,0:T(8,128)(2,1)S(1)}, bf16[2,384,256]{2,1,0:T(8,128)(2,1)S(1)}, u32[]{:S(2)}, u32[]{:S(2)}) collective-permute-start(bf16[2,384,256]{2,1,0:T(8,128)(2,1)S(1)} %get-tuple-element.45.refs_12_.kv), channel_id=1, source_target_pairs={{8,12},{9,13},{10,14},{11,15},{24,28},{25,29},{26,30},{27,31}} | collective-permute-start | bytes 1179656 | tf_op jit(solution)/shard_map/ppermute | solution.py:304
  34.6 0.7 %collective-permute-start.9 = (bf16[2,384,256]{2,1,0:T(8,128)(2,1)S(1)}, bf16[2,384,256]{2,1,0:T(8,128)(2,1)S(1)}, u32[]{:S(2)}, u32[]{:S(2)}) collective-permute-start(bf16[2,384,256]{2,1,0:T(8,128)(2,1)S(1)} %get-tuple-element.45.refs_12_.kv), channel_id=1, source_target_pairs={{0,8},{1,9},{2,10},{3,11},{16,24},{17,25},{18,26},{19,27}} | collective-permute-start | bytes 1179656 | tf_op jit(solution)/shard_map/ppermute | solution.py:304
  35.3 0.0 collective-permute-done.6.refs_1_
  35.3 0.6 shard_map.97
  35.9 2.2 %collective-permute-done.7.refs_11_ = bf16[384,256]{1,0:T(8,128)(2,1)S(1)} collective-permute-done((bf16[384,256]{1,0:T(8,128)(2,1)S(1)}, bf16[384,256]{1,0:T(8,128)(2,1)S(1)}, u32[]{:S(2)}, u32[]{:S(2)}) %collective-permute-start.7) | collective-permute-done | bytes 196640 | tf_op jit(solution)/shard_map/ppermute | solution.py:304
  38.1 0.0 collective-permute-done.5.refs_1_
  38.1 0.9 %shard_map.98 = (bf16[2,384,256]{2,1,0:T(8,128)(2,1)S(1)}, bf16[384,256]{1,0:T(8,128)(2,1)S(1)}, f32[8,384]{1,0:T(8,128)S(1)}) custom-call(bf16[384,512]{1,0:T(8,128)(2,1)S(1)} %collective-permute-done.4.refs_0_, bf16[384,512]{1,0:T(8,128)(2,1)S(1)} %collective-permute-done.5.refs_1_, f32[4,512]{1,0:T(4,128)S(1)} %reshape.28.refs_2_, ...), custom_call_target="tpu_custom_call" | custom-call | tf_op jit(solution)/shard_map/pallas_call | solution.py:30
  39.0 1.3 %collective-permute-start.10 = (bf16[384,256]{1,0:T(8,128)(2,1)S(1)}, bf16[384,256]{1,0:T(8,128)(2,1)S(1)}, u32[]{:S(2)}, u32[]{:S(2)}) collective-permute-start(bf16[384,256]{1,0:T(8,128)(2,1)S(1)} %get-tuple-element.57), channel_id=1, source_target_pairs={{4,12},{5,13},{6,14},{7,15},{20,28},{21,29},{22,30},{23,31}} | collective-permute-start | bytes 589832 | tf_op jit(solution)/shard_map/ppermute | solution.py:304
  40.3 0.8 %collective-permute-start.16 = (bf16[256,512]{1,0:T(8,128)(2,1)S(1)}, bf16[256,512]{1,0:T(8,128)(2,1)S(1)}, u32[]{:S(2)}, u32[]{:S(2)}) collective-permute-start(bf16[256,512]{1,0:T(8,128)(2,1)S(1)} %get-tuple-element.65), channel_id=1, source_target_pairs={{0,3},{1,2},{2,1},{3,0},{16,18},{17,19},{18,16},{19,17},{4,7},{5,6... | collective-permute-start | bytes 786440 | tf_op jit(solution)/shard_map/ppermute | solution.py:446
  41.2 1.3 %collective-permute-start.11 = (f32[8,384]{1,0:T(8,128)S(1)}, f32[8,384]{1,0:T(8,128)S(1)}, u32[]{:S(2)}, u32[]{:S(2)}) collective-permute-start(f32[8,384]{1,0:T(8,128)S(1)} %get-tuple-element.58), channel_id=1, source_target_pairs={{4,12},{5,13},{6,14},{7,15},{20,28},{21,29},{22,30},{23,31}} | collective-permute-start | bytes 36872 | tf_op jit(solution)/shard_map/ppermute | solution.py:304
  42.4 4.1 %collective-permute-done.8.refs_0_ = bf16[2,384,256]{2,1,0:T(8,128)(2,1)S(1)} collective-permute-done((bf16[2,384,256]{2,1,0:T(8,128)(2,1)S(1)}, bf16[2,384,256]{2,1,0:T(8,128)(2,1)S(1)}, u32[]{:S(2)}, u32[]{:S(2)}) %collective-permute-start.8) | collective-permute-done | bytes 393248 | tf_op jit(solution)/shard_map/ppermute | solution.py:304
  46.5 1.3 %shard_map.99 = (f32[384,256]{1,0:T(8,128)S(1)}, f32[384,256]{1,0:T(8,128)S(1)}, f32[384,256]{1,0:T(8,128)S(1)}) custom-call(bf16[384,256]{1,0:T(8,128)(2,1)S(1)} %get-tuple-element.44.q, bf16[2,384,256]{2,1,0:T(8,128)(2,1)S(1)} %get-tuple-element.45.refs_12_.kv, f32[384,384]{1,0:T(8,128)S(1)} %get-tuple-element.46.bias, ...), custom_call_target="tpu_custom_call" | custom-call | tf_op jit(solution)/shard_map/pallas_call | solution.py:30
  47.8 0.0 collective-permute-done.9.refs_3_
  47.8 7.1 %collective-permute-done.11.refs_6_ = f32[8,384]{1,0:T(8,128)S(1)} collective-permute-done((f32[8,384]{1,0:T(8,128)S(1)}, f32[8,384]{1,0:T(8,128)S(1)}, u32[]{:S(2)}, u32[]{:S(2)}) %collective-permute-start.11) | collective-permute-done | bytes 12320 | tf_op jit(solution)/shard_map/ppermute | solution.py:304
  54.9 0.0 collective-permute-done.10.refs_5_
  54.9 0.3 shard_map.100
  55.2 1.6 %collective-permute-start.14 = (bf16[384,256]{1,0:T(8,128)(2,1)S(1)}, bf16[384,256]{1,0:T(8,128)(2,1)S(1)}, u32[]{:S(2)}, u32[]{:S(2)}) collective-permute-start(bf16[384,256]{1,0:T(8,128)(2,1)S(1)} %get-tuple-element.60.refs_0_), channel_id=1, source_target_pairs={{0,2},{1,3},{2,0},{3,1},{4,6},{5,7},{6,4},{7,5},{8,10},{9,11},{10,... | collective-permute-start | bytes 589832 | tf_op jit(solution)/shard_map/ppermute | solution.py:300
  56.8 0.0 collective-permute-start.13
  56.8 0.0 collective-permute-done.16.refs_2_
  56.8 1.5 %collective-permute-start.17 = (bf16[256,512]{1,0:T(8,128)(2,1)S(1)}, bf16[256,512]{1,0:T(8,128)(2,1)S(1)}, u32[]{:S(2)}, u32[]{:S(2)}) collective-permute-start(bf16[256,512]{1,0:T(8,128)(2,1)S(1)} %collective-permute-done.16.refs_2_), channel_id=1, source_target_pairs={{0,16},{16,0},{1,17},{17,1},{2,18},{18,2},{3,19},{19,3},{4,20},{20... | collective-permute-start | bytes 786440 | tf_op jit(solution)/shard_map/ppermute | solution.py:448
  58.3 0.2 collective-permute-start.12
  58.5 3.6 %collective-permute-done.14.refs_0_ = bf16[384,256]{1,0:T(8,128)(2,1)S(1)} collective-permute-done((bf16[384,256]{1,0:T(8,128)(2,1)S(1)}, bf16[384,256]{1,0:T(8,128)(2,1)S(1)}, u32[]{:S(2)}, u32[]{:S(2)}) %collective-permute-start.14) | collective-permute-done | bytes 196640 | tf_op jit(solution)/shard_map/ppermute | solution.py:300
  62.1 0.0 collective-permute-start.15
  62.1 0.0 collective-permute-done.13.refs_3_
  62.1 0.0 collective-permute-done.12.refs_1_
  62.1 0.9 %shard_map.101 = (f32[384,512]{1,0:T(8,128)S(1)}, f32[2,384]{1,0:T(2,128)}) custom-call(f32[384,256]{1,0:T(8,128)S(1)} %get-tuple-element.59.logs, bf16[384,256]{1,0:T(8,128)(2,1)S(1)} %get-tuple-element.60.refs_0_, bf16[384,256]{1,0:T(8,128)(2,1)S(1)} %collective-permute-done.12.refs_1_, bf16[256,512]{1,0:T(8,128)(2,1)S(1)} %get-tuple-element.61.refs_2_, ...), custom_call_target="tpu_custom_call" | custom-call | tf_op jit(solution)/shard_map/pallas_call | solution.py:30
  63.0 2.5 %collective-permute-done.17.refs_3_ = bf16[256,512]{1,0:T(8,128)(2,1)S(1)} collective-permute-done((bf16[256,512]{1,0:T(8,128)(2,1)S(1)}, bf16[256,512]{1,0:T(8,128)(2,1)S(1)}, u32[]{:S(2)}, u32[]{:S(2)}) %collective-permute-start.17) | collective-permute-done | bytes 262176 | tf_op jit(solution)/shard_map/ppermute | solution.py:448
  65.5 0.0 collective-permute-done.15.refs_1_
  65.5 1.1 %shard_map.102 = bf16[384,512]{1,0:T(8,128)(2,1)} custom-call(f32[384,512]{1,0:T(8,128)S(1)} %get-tuple-element.64.before, bf16[384,256]{1,0:T(8,128)(2,1)S(1)} %collective-permute-done.14.refs_0_, bf16[384,256]{1,0:T(8,128)(2,1)S(1)} %collective-permute-done.15.refs_1_, bf16[256,512]{1,0:T(8,128)(2,1)S(1)} %collective-permute-done.16.refs_2_, ...), custom_call_target="tpu_custom_call" | custom-call | tf_op jit(solution)/shard_map/pallas_call | solution.py:30
  (2 shorter events, 0.0 us)
Async XLA Ops:
  0.6 2.3 %collective-permute-start.3 = (bf16[384,512]{1,0:T(8,128)(2,1)}, bf16[384,512]{1,0:T(8,128)(2,1)S(1)}, u32[]{:S(2)}, u32[]{:S(2)}) collective-permute-start(bf16[384,512]{1,0:T(8,128)(2,1)} %refs_0_.1), channel_id=1, source_target_pairs={{0,4},{4,8},{1,5},{5,9},{2,6},{6,10},{3,7},{7,11},{16,20},{20,24},... | collective-permute-start | bytes 1179656 | tf_op jit(solution)/shard_map/ppermute | solution.py:304
  1.3 11.1 %collective-permute-start = (bf16[384,512]{1,0:T(8,128)(2,1)}, bf16[384,512]{1,0:T(8,128)(2,1)S(1)}, u32[]{:S(2)}, u32[]{:S(2)}) collective-permute-start(bf16[384,512]{1,0:T(8,128)(2,1)} %refs_0_.1), channel_id=1, source_target_pairs={{0,2},{1,3},{2,0},{3,1},{4,6},{5,7},{6,4},{7,5},{8,10},{9,11},{10,... | collective-permute-start | bytes 1179656 | tf_op jit(solution)/shard_map/ppermute | solution.py:300
  2.9 10.8 %collective-permute-start.4 = (bf16[384,512]{1,0:T(8,128)(2,1)S(1)}, bf16[384,512]{1,0:T(8,128)(2,1)S(1)}, u32[]{:S(2)}, u32[]{:S(2)}) collective-permute-start(bf16[384,512]{1,0:T(8,128)(2,1)S(1)} %collective-permute-done.3.refs_0_), channel_id=1, source_target_pairs={{4,6},{5,7},{6,4},{7,5},{8,10},{9,11},{10,8},{11,9},{20,22},{21,23... | collective-permute-start | bytes 1179656 | tf_op jit(solution)/shard_map/ppermute | solution.py:393
  3.6 11.6 %collective-permute-start.2 = (bf16[384,512]{1,0:T(8,128)(2,1)}, bf16[384,512]{1,0:T(8,128)(2,1)S(1)}, u32[]{:S(2)}, u32[]{:S(2)}) collective-permute-start(bf16[384,512]{1,0:T(8,128)(2,1)} %refs_0_.1), channel_id=1, source_target_pairs={{0,1},{1,0},{2,3},{3,2},{4,5},{5,4},{6,7},{7,6},{8,9},{9,8},{10,11... | collective-permute-start | bytes 1179656 | tf_op jit(solution)/shard_map/ppermute | solution.py:300
  12.5 5.6 %collective-permute-start.1 = (bf16[384,512]{1,0:T(8,128)(2,1)S(1)}, bf16[384,512]{1,0:T(8,128)(2,1)S(1)}, u32[]{:S(2)}, u32[]{:S(2)}) collective-permute-start(bf16[384,512]{1,0:T(8,128)(2,1)S(1)} %collective-permute-done.refs_0_), channel_id=1, source_target_pairs={{0,1},{1,0},{2,3},{3,2},{4,5},{5,4},{6,7},{7,6},{8,9},{9,8},{10,11... | collective-permute-start | bytes 1179656 | tf_op jit(solution)/shard_map/ppermute | solution.py:300
  13.2 22.1 %collective-permute-start.6 = (bf16[384,512]{1,0:T(8,128)(2,1)S(1)}, bf16[384,512]{1,0:T(8,128)(2,1)S(1)}, u32[]{:S(2)}, u32[]{:S(2)}) collective-permute-start(bf16[384,512]{1,0:T(8,128)(2,1)S(1)} %collective-permute-done.3.refs_0_), channel_id=1, source_target_pairs={{0,1},{1,0},{2,3},{3,2},{4,5},{5,4},{6,7},{7,6},{8,9},{9,8},{10,11... | collective-permute-start | bytes 1179656 | tf_op jit(solution)/shard_map/ppermute | solution.py:300
  13.7 24.4 %collective-permute-start.5 = (bf16[384,512]{1,0:T(8,128)(2,1)S(1)}, bf16[384,512]{1,0:T(8,128)(2,1)S(1)}, u32[]{:S(2)}, u32[]{:S(2)}) collective-permute-start(bf16[384,512]{1,0:T(8,128)(2,1)S(1)} %collective-permute-done.4.refs_0_), channel_id=1, source_target_pairs={{0,1},{1,0},{2,3},{3,2},{4,5},{5,4},{6,7},{7,6},{8,9},{9,8},{10,11... | collective-permute-start | bytes 1179656 | tf_op jit(solution)/shard_map/ppermute | solution.py:300
  19.3 18.8 %collective-permute-start.7 = (bf16[384,256]{1,0:T(8,128)(2,1)S(1)}, bf16[384,256]{1,0:T(8,128)(2,1)S(1)}, u32[]{:S(2)}, u32[]{:S(2)}) collective-permute-start(bf16[384,256]{1,0:T(8,128)(2,1)S(1)} %get-tuple-element.44.q), channel_id=1, source_target_pairs={{12,4},{13,5},{14,6},{15,7},{28,20},{29,21},{30,22},{31,23}} | collective-permute-start | bytes 589832 | tf_op jit(solution)/shard_map/ppermute | solution.py:304
  33.3 13.2 %collective-permute-start.8 = (bf16[2,384,256]{2,1,0:T(8,128)(2,1)S(1)}, bf16[2,384,256]{2,1,0:T(8,128)(2,1)S(1)}, u32[]{:S(2)}, u32[]{:S(2)}) collective-permute-start(bf16[2,384,256]{2,1,0:T(8,128)(2,1)S(1)} %get-tuple-element.45.refs_12_.kv), channel_id=1, source_target_pairs={{8,12},{9,13},{10,14},{11,15},{24,28},{25,29},{26,30},{27,31}} | collective-permute-start | bytes 1179656 | tf_op jit(solution)/shard_map/ppermute | solution.py:304
  34.6 13.2 %collective-permute-start.9 = (bf16[2,384,256]{2,1,0:T(8,128)(2,1)S(1)}, bf16[2,384,256]{2,1,0:T(8,128)(2,1)S(1)}, u32[]{:S(2)}, u32[]{:S(2)}) collective-permute-start(bf16[2,384,256]{2,1,0:T(8,128)(2,1)S(1)} %get-tuple-element.45.refs_12_.kv), channel_id=1, source_target_pairs={{0,8},{1,9},{2,10},{3,11},{16,24},{17,25},{18,26},{19,27}} | collective-permute-start | bytes 1179656 | tf_op jit(solution)/shard_map/ppermute | solution.py:304
  39.0 15.9 %collective-permute-start.10 = (bf16[384,256]{1,0:T(8,128)(2,1)S(1)}, bf16[384,256]{1,0:T(8,128)(2,1)S(1)}, u32[]{:S(2)}, u32[]{:S(2)}) collective-permute-start(bf16[384,256]{1,0:T(8,128)(2,1)S(1)} %get-tuple-element.57), channel_id=1, source_target_pairs={{4,12},{5,13},{6,14},{7,15},{20,28},{21,29},{22,30},{23,31}} | collective-permute-start | bytes 589832 | tf_op jit(solution)/shard_map/ppermute | solution.py:304
  40.3 16.4 %collective-permute-start.16 = (bf16[256,512]{1,0:T(8,128)(2,1)S(1)}, bf16[256,512]{1,0:T(8,128)(2,1)S(1)}, u32[]{:S(2)}, u32[]{:S(2)}) collective-permute-start(bf16[256,512]{1,0:T(8,128)(2,1)S(1)} %get-tuple-element.65), channel_id=1, source_target_pairs={{0,3},{1,2},{2,1},{3,0},{16,18},{17,19},{18,16},{19,17},{4,7},{5,6... | collective-permute-start | bytes 786440 | tf_op jit(solution)/shard_map/ppermute | solution.py:446
  41.2 13.8 %collective-permute-start.11 = (f32[8,384]{1,0:T(8,128)S(1)}, f32[8,384]{1,0:T(8,128)S(1)}, u32[]{:S(2)}, u32[]{:S(2)}) collective-permute-start(f32[8,384]{1,0:T(8,128)S(1)} %get-tuple-element.58), channel_id=1, source_target_pairs={{4,12},{5,13},{6,14},{7,15},{20,28},{21,29},{22,30},{23,31}} | collective-permute-start | bytes 36872 | tf_op jit(solution)/shard_map/ppermute | solution.py:304
  55.2 6.9 %collective-permute-start.14 = (bf16[384,256]{1,0:T(8,128)(2,1)S(1)}, bf16[384,256]{1,0:T(8,128)(2,1)S(1)}, u32[]{:S(2)}, u32[]{:S(2)}) collective-permute-start(bf16[384,256]{1,0:T(8,128)(2,1)S(1)} %get-tuple-element.60.refs_0_), channel_id=1, source_target_pairs={{0,2},{1,3},{2,0},{3,1},{4,6},{5,7},{6,4},{7,5},{8,10},{9,11},{10,... | collective-permute-start | bytes 589832 | tf_op jit(solution)/shard_map/ppermute | solution.py:300
  56.8 5.3 %collective-permute-start.13 = (bf16[256,512]{1,0:T(8,128)(2,1)S(1)}, bf16[256,512]{1,0:T(8,128)(2,1)S(1)}, u32[]{:S(2)}, u32[]{:S(2)}) collective-permute-start(bf16[256,512]{1,0:T(8,128)(2,1)S(1)} %get-tuple-element.63), channel_id=1, source_target_pairs={{0,1},{1,0},{2,3},{3,2},{4,5},{5,4},{6,7},{7,6},{8,9},{9,8},{10,11... | collective-permute-start | bytes 786440 | tf_op jit(solution)/shard_map/ppermute | solution.py:300
  56.8 8.7 %collective-permute-start.17 = (bf16[256,512]{1,0:T(8,128)(2,1)S(1)}, bf16[256,512]{1,0:T(8,128)(2,1)S(1)}, u32[]{:S(2)}, u32[]{:S(2)}) collective-permute-start(bf16[256,512]{1,0:T(8,128)(2,1)S(1)} %collective-permute-done.16.refs_2_), channel_id=1, source_target_pairs={{0,16},{16,0},{1,17},{17,1},{2,18},{18,2},{3,19},{19,3},{4,20},{20... | collective-permute-start | bytes 786440 | tf_op jit(solution)/shard_map/ppermute | solution.py:448
  58.3 3.8 %collective-permute-start.12 = (bf16[384,256]{1,0:T(8,128)(2,1)S(1)}, bf16[384,256]{1,0:T(8,128)(2,1)S(1)}, u32[]{:S(2)}, u32[]{:S(2)}) collective-permute-start(bf16[384,256]{1,0:T(8,128)(2,1)S(1)} %get-tuple-element.60.refs_0_), channel_id=1, source_target_pairs={{0,1},{1,0},{2,3},{3,2},{4,5},{5,4},{6,7},{7,6},{8,9},{9,8},{10,11... | collective-permute-start | bytes 589832 | tf_op jit(solution)/shard_map/ppermute | solution.py:300
  62.1 3.4 %collective-permute-start.15 = (bf16[384,256]{1,0:T(8,128)(2,1)S(1)}, bf16[384,256]{1,0:T(8,128)(2,1)S(1)}, u32[]{:S(2)}, u32[]{:S(2)}) collective-permute-start(bf16[384,256]{1,0:T(8,128)(2,1)S(1)} %collective-permute-done.14.refs_0_), channel_id=1, source_target_pairs={{0,1},{1,0},{2,3},{3,2},{4,5},{5,4},{6,7},{7,6},{8,9},{9,8},{10,11... | collective-permute-start | bytes 589832 | tf_op jit(solution)/shard_map/ppermute | solution.py:300

commit v9 on v7

--- a/solution.py
+++ b/solution.py
@@ -209,24 +209,39 @@
         accs[:, lanes] = acc
 
 
-def help_kernel(q, *refs, blocks, head_width, factor, helper):
+def help_kernel(q, *refs, blocks, head_width, factor):
     out, logs = refs[2 * blocks :]
 
-    @pl.when(lax.axis_index("sp") == helper)
-    def _():
-        for h, lanes in enumerate(head_lanes(q, head_width)):
-            ready = [(refs[2 * n], refs[2 * n + 1][...]) for n in range(blocks)]
-            top, total, acc = softmax_part(q, ready, lanes, factor)
-            out[:, lanes] = (acc / total).astype(jnp.bfloat16)
-            logs[h : h + 1, :] = wide(top + jnp.log2(total)).T[:1, :]
-
-
-def late_help_kernel(*refs, late_count, late, help_now):
+    for h, lanes in enumerate(head_lanes(q, head_width)):
+        ready = [(refs[2 * n], refs[2 * n + 1][...]) for n in range(blocks)]
+        top, total, acc = softmax_part(q, ready, lanes, factor)
+        out[:, lanes] = (acc / total).astype(jnp.bfloat16)
+        logs[h : h + 1, :] = wide(top + jnp.log2(total)).T[:1, :]
+
+
+def late_help_kernel(*refs, late_count, late, help_now, helper):
     late_in, rest = refs[:late_count], refs[late_count:]
     q, kv, bias, bias_before = rest[:4]
     kv_before, out, logs = rest[4:]
-    late(*late_in, kv_before)
-    help_now(q, kv, bias, kv_before, bias_before, out, logs)
+
+    @pl.when(lax.axis_index("sp") == helper)
+    def _():
+        late(*late_in, kv_before)
+        help_now(q, kv, bias, kv_before, bias_before, out, logs)
+
+
+def near_late_kernel(q, kv, bias, kv_helper, bias_before, *refs, late, near, helper):
+    late_in, outs, held = refs[:-4], refs[-4:-1], refs[-1]
+    ready = lax.axis_index("sp") == helper
+
+    @pl.when(ready)
+    def _():
+        near(q, kv, bias, kv_helper, bias_before, *outs)
+
+    @pl.when(jnp.logical_not(ready))
+    def _():
+        late(*late_in, held)
+        near(q, kv, bias, held, bias_before, *outs)
 
 
 def final_kernel(q, *refs, far, only, helped, head_width, factor):
@@ -407,29 +422,36 @@
             functools.partial(
                 late_help_kernel,
                 late_count=len(operands),
+                helper=1,
                 late=late_before,
                 help_now=functools.partial(
-                    help_kernel, blocks=2, head_width=head_width, factor=factor, helper=1
+                    help_kernel, blocks=2, head_width=head_width, factor=factor
                 ),
             ),
             [*operands, visitor, kv, biases[2], biases[3]],
             [pair, half_sum, shape_of((8, rows), jnp.float32)],
         )
         given = [send(out, [(1, helped)]), send(logs, [(1, helped)])]
-    near = call(
-        functools.partial(
-            near_kernel, distances=(0, 1), head_width=head_width, factor=factor
-        ),
-        [q, kv, biases[0], kv_before, biases[1]],
-        [sums] * 3,
-    )
-
-    *near_slice, _ = lax.optimization_barrier((*near_slice, begun_before[2]))
+    near_part = functools.partial(
+        near_kernel, distances=(0, 1), head_width=head_width, factor=factor
+    )
+    near_in = [q, kv, biases[0], kv_before, biases[1]]
+    if helped is None:
+        near = call(near_part, near_in, [sums] * 3)
+    else:
+        near = call(
+            functools.partial(near_late_kernel, late=late_before, near=near_part, helper=1),
+            [*near_in, *operands],
+            [sums] * 3,
+            scratch=[pltpu.VMEM(pair.shape, pair.dtype)],
+        )
+
     near_pieces = [own_slice] + [swap(x, k + 1) for k, x in enumerate(near_slice)]
     if shared:
         routes = [(g * 4 + t, g * 4 + (t ^ (3 - g))) for g in range(2) for t in range(4)]
         fetched = lax.ppermute(far_slice[0], ("grp", "tp"), routes)
-        other = lax.ppermute(fetched, "grp", [(0, 1), (1, 0)])
+        later, _ = lax.optimization_barrier((fetched, near[0]))
+        other = lax.ppermute(later, "grp", [(0, 1), (1, 0)])
         far_pieces = [fetched, other]
     else:
         far_pieces = [swap(x, k) for k, x in zip(late, far_slice)]

time: 61 us -> 61.2 us (level)
  no operation moved by 1% of the time
where the time goes in v9:
time: 61.2 us; the launch traced here: 61 us
  waiting for transfers between devices  31.9 us (52%)
  starting transfers between devices  15.7 us (26%)
  Pallas kernels  10.5 us (17%)
  other arithmetic  1.45 us (2%)
  between operations  0.75 us (1%)
  local copies, waits for them, and re-layouts  0.7 us (1%)
    ppermute x5, waiting for transfers between devices, send(): return lax.ppermute(value, 'sp', pairs)  16.8 us
    pallas_call x8, Pallas kernels, call(): pl.pallas_call(body, out_shape=tuple(outs), in_specs=[HBM if n in held el...  10.5 us
    ppermute x10, waiting for transfers between devices, swap(): return lax.ppermute(value, 'tp', [(i, i ^ distance) for i in range(count)])  9.85 us
    ppermute x5, starting transfers between devices, send(): return lax.ppermute(value, 'sp', pairs)  8.04 us
    ppermute x10, starting transfers between devices, swap(): return lax.ppermute(value, 'tp', [(i, i ^ distance) for i in range(count)])  5.19 us
    ppermute x1, waiting for transfers between devices, layer(): other = lax.ppermute(later, 'grp', [(0, 1), (1, 0)])  3.12 us
    ppermute x1, waiting for transfers between devices, layer(): fetched = lax.ppermute(far_slice[0], ('grp', 'tp'), routes)  2.08 us
    ppermute x1, starting transfers between devices, layer(): other = lax.ppermute(later, 'grp', [(0, 1), (1, 0)])  1.69 us
  transfers between devices with their start and end apart: 17, of which 7 were waited for; matrix products, arithmetic and copies ran while one was open for 4% of the time, Pallas kernels for 15%

profile of v9, /device:TPU:8, one launch (start us, length us, event | category | flops | bytes accessed | tf_op | source)
XLA Modules:
  0.0 61.0 jit_solution(16199946458014209117)
XLA Ops:
  0.6 3.5 %collective-permute-start.3 = (bf16[384,512]{1,0:T(8,128)(2,1)}, bf16[384,512]{1,0:T(8,128)(2,1)S(1)}, u32[]{:S(2)}, u32[]{:S(2)}) collective-permute-start(bf16[384,512]{1,0:T(8,128)(2,1)} %refs_0_.1), channel_id=1, source_target_pairs={{0,4},{4,8},{8,12},{1,5},{5,9},{9,13},{2,6},{6,10},{10,14},{3,7},{... | collective-permute-start | bytes 1179656 | tf_op jit(solution)/shard_map/ppermute | solution.py:313
  4.1 1.6 %collective-permute-start = (bf16[384,512]{1,0:T(8,128)(2,1)}, bf16[384,512]{1,0:T(8,128)(2,1)S(1)}, u32[]{:S(2)}, u32[]{:S(2)}) collective-permute-start(bf16[384,512]{1,0:T(8,128)(2,1)} %refs_0_.1), channel_id=1, source_target_pairs={{0,2},{1,3},{2,0},{3,1},{4,6},{5,7},{6,4},{7,5},{8,10},{9,11},{10,... | collective-permute-start | bytes 1179656 | tf_op jit(solution)/shard_map/ppermute | solution.py:309
  5.7 7.9 %collective-permute-done.3.refs_0_ = bf16[384,512]{1,0:T(8,128)(2,1)S(1)} collective-permute-done((bf16[384,512]{1,0:T(8,128)(2,1)}, bf16[384,512]{1,0:T(8,128)(2,1)S(1)}, u32[]{:S(2)}, u32[]{:S(2)}) %collective-permute-start.3) | collective-permute-done | bytes 393248 | tf_op jit(solution)/shard_map/ppermute | solution.py:313
  13.6 1.5 %collective-permute-start.4 = (bf16[384,512]{1,0:T(8,128)(2,1)S(1)}, bf16[384,512]{1,0:T(8,128)(2,1)S(1)}, u32[]{:S(2)}, u32[]{:S(2)}) collective-permute-start(bf16[384,512]{1,0:T(8,128)(2,1)S(1)} %collective-permute-done.3.refs_0_), channel_id=1, source_target_pairs={{0,2},{1,3},{2,0},{3,1},{4,6},{5,7},{6,4},{7,5},{8,10},{9,11},{10,... | collective-permute-start | bytes 1179656 | tf_op jit(solution)/shard_map/ppermute | solution.py:309
  15.1 0.0 collective-permute-start.2
  15.1 0.0 collective-permute-done.refs_0_
  15.1 0.5 collective-permute-start.1
  15.6 0.7 %reshape.28.refs_2_ = f32[4,512]{1,0:T(4,128)S(1)} reshape(bf16[2048]{0:T(1024)(128)(2,1)} %param.9) | data formatting | bytes 12288 | tf_op jit(solution)/shard_map/reshape | solution.py:355
  16.3 0.0 collective-permute-start.6
  16.3 7.3 %collective-permute-done.4.refs_0_ = bf16[384,512]{1,0:T(8,128)(2,1)S(1)} collective-permute-done((bf16[384,512]{1,0:T(8,128)(2,1)S(1)}, bf16[384,512]{1,0:T(8,128)(2,1)S(1)}, u32[]{:S(2)}, u32[]{:S(2)}) %collective-permute-start.4) | collective-permute-done | bytes 393248 | tf_op jit(solution)/shard_map/ppermute | solution.py:309
  23.6 0.0 collective-permute-start.5
  23.6 1.4 %multiply_sine_fusion = (f32[384,64]{1,0:T(8,128)S(1)}, f32[384,64]{1,0:T(8,128)S(1)}, f32[384,64]{1,0:T(8,128)S(1)}, f32[384,64]{1,0:T(8,128)S(1)}) fusion(f32[384]{0:T(512)S(1)} %get-tuple-element.72, f32[64]{0:T(128)S(1)} %multiply_power_fusion, f32[384]{0:T(512)S(1)} %get-tuple-element.73), kind=kLoop, calls=%fused_computation | loop fusion | flops 49152 | bytes 396544 | tf_op jit(solution)/shard_map/sin | solution.py:334
  25.0 0.0 collective-permute-done.2.refs_1_
  25.0 2.9 %shard_map.95 = (f32[384,256]{1,0:T(8,128)S(1)}, f32[384,256]{1,0:T(8,128)S(1)}, f32[384,256]{1,0:T(8,128)S(1)}, f32[384,128]{1,0:T(8,128)S(1)}, f32[2,128]{1,0:...) custom-call(bf16[384,512]{1,0:T(8,128)(2,1)} %refs_0_.1, ...), custom_call_target="tpu_custom_call" | custom-call | tf_op jit(solution)/shard_map/pallas_call | solution.py:30
  27.9 0.0 collective-permute-done.1.refs_1_
  27.9 1.2 %shard_map.96 = (bf16[384,256]{1,0:T(8,128)(2,1)S(1)}, bf16[2,384,256]{2,1,0:T(8,128)(2,1)S(1)}) custom-call(bf16[384,512]{1,0:T(8,128)(2,1)S(1)} %collective-permute-done.refs_0_, bf16[384,512]{1,0:T(8,128)(2,1)S(1)} %collective-permute-done.1.refs_1_, f32[4,512]{1,0:T(4,128)S(1)} %reshape.28.refs_2_, bf16[2048,256]{1,0:T(8,128)(2,1)S(1)} %get-tuple-element.34.refs_3_, ...), custom_call_target="tpu_custom_call" | custom-call | tf_op jit(solution)/shard_map/pallas_call | solution.py:30
  29.1 1.3 %collective-permute-start.7 = (bf16[384,256]{1,0:T(8,128)(2,1)S(1)}, bf16[384,256]{1,0:T(8,128)(2,1)S(1)}, u32[]{:S(2)}, u32[]{:S(2)}) collective-permute-start(bf16[384,256]{1,0:T(8,128)(2,1)S(1)} %get-tuple-element.43.q), channel_id=1, source_target_pairs={{12,4},{13,5},{14,6},{15,7},{28,20},{29,21},{30,22},{31,23}} | collective-permute-start | bytes 589832 | tf_op jit(solution)/shard_map/ppermute | solution.py:313
  30.4 0.7 %collective-permute-start.8 = (bf16[2,384,256]{2,1,0:T(8,128)(2,1)S(1)}, bf16[2,384,256]{2,1,0:T(8,128)(2,1)S(1)}, u32[]{:S(2)}, u32[]{:S(2)}) collective-permute-start(bf16[2,384,256]{2,1,0:T(8,128)(2,1)S(1)} %get-tuple-element.44.refs_12_.kv), channel_id=1, source_target_pairs={{0,8},{1,9},{2,10},{3,11},{16,24},{17,25},{18,26},{19,27}} | collective-permute-start | bytes 1179656 | tf_op jit(solution)/shard_map/ppermute | solution.py:313
  31.1 0.0 collective-permute-done.6.refs_1_
  31.1 0.6 shard_map.97
  31.7 7.5 %collective-permute-done.7.refs_11_ = bf16[384,256]{1,0:T(8,128)(2,1)S(1)} collective-permute-done((bf16[384,256]{1,0:T(8,128)(2,1)S(1)}, bf16[384,256]{1,0:T(8,128)(2,1)S(1)}, u32[]{:S(2)}, u32[]{:S(2)}) %collective-permute-start.7) | collective-permute-done | bytes 196640 | tf_op jit(solution)/shard_map/ppermute | solution.py:313
  39.2 0.0 collective-permute-done.5.refs_1_
  39.3 2.3 %shard_map.98 = (bf16[2,384,256]{2,1,0:T(8,128)(2,1)S(1)}, bf16[384,256]{1,0:T(8,128)(2,1)S(1)}, f32[8,384]{1,0:T(8,128)S(1)}) custom-call(bf16[384,512]{1,0:T(8,128)(2,1)S(1)} %collective-permute-done.4.refs_0_, bf16[384,512]{1,0:T(8,128)(2,1)S(1)} %collective-permute-done.5.refs_1_, f32[4,512]{1,0:T(4,128)S(1)} %reshape.28.refs_2_, ...), custom_call_target="tpu_custom_call" | custom-call | tf_op jit(solution)/shard_map/pallas_call | solution.py:30
  41.6 1.3 %collective-permute-start.9 = (bf16[384,256]{1,0:T(8,128)(2,1)S(1)}, bf16[384,256]{1,0:T(8,128)(2,1)S(1)}, u32[]{:S(2)}, u32[]{:S(2)}) collective-permute-start(bf16[384,256]{1,0:T(8,128)(2,1)S(1)} %get-tuple-element.56), channel_id=1, source_target_pairs={{4,12},{5,13},{6,14},{7,15},{20,28},{21,29},{22,30},{23,31}} | collective-permute-start | bytes 589832 | tf_op jit(solution)/shard_map/ppermute | solution.py:313
  42.9 0.8 %collective-permute-start.15 = (bf16[256,512]{1,0:T(8,128)(2,1)S(1)}, bf16[256,512]{1,0:T(8,128)(2,1)S(1)}, u32[]{:S(2)}, u32[]{:S(2)}) collective-permute-start(bf16[256,512]{1,0:T(8,128)(2,1)S(1)} %get-tuple-element.63), channel_id=1, source_target_pairs={{0,3},{1,2},{2,1},{3,0},{16,18},{17,19},{18,16},{19,17},{4,7},{5,6... | collective-permute-start | bytes 786440 | tf_op jit(solution)/shard_map/ppermute | solution.py:452
  43.7 1.3 %collective-permute-start.10 = (f32[8,384]{1,0:T(8,128)S(1)}, f32[8,384]{1,0:T(8,128)S(1)}, u32[]{:S(2)}, u32[]{:S(2)}) collective-permute-start(f32[8,384]{1,0:T(8,128)S(1)} %get-tuple-element.57), channel_id=1, source_target_pairs={{4,12},{5,13},{6,14},{7,15},{20,28},{21,29},{22,30},{23,31}} | collective-permute-start | bytes 36872 | tf_op jit(solution)/shard_map/ppermute | solution.py:313
  45.0 1.3 %shard_map.99 = (f32[384,256]{1,0:T(8,128)S(1)}, f32[384,256]{1,0:T(8,128)S(1)}, f32[384,256]{1,0:T(8,128)S(1)}) custom-call(bf16[384,256]{1,0:T(8,128)(2,1)S(1)} %get-tuple-element.43.q, bf16[2,384,256]{2,1,0:T(8,128)(2,1)S(1)} %get-tuple-element.44.refs_12_.kv, f32[384,384]{1,0:T(8,128)S(1)} %get-tuple-element.45.bias, ...), custom_call_target="tpu_custom_call" | custom-call | tf_op jit(solution)/shard_map/pallas_call | solution.py:30
  46.3 0.0 collective-permute-done.8.refs_3_
  46.3 1.4 %collective-permute-done.10.refs_6_ = f32[8,384]{1,0:T(8,128)S(1)} collective-permute-done((f32[8,384]{1,0:T(8,128)S(1)}, f32[8,384]{1,0:T(8,128)S(1)}, u32[]{:S(2)}, u32[]{:S(2)}) %collective-permute-start.10) | collective-permute-done | bytes 12320 | tf_op jit(solution)/shard_map/ppermute | solution.py:313
  47.7 0.0 collective-permute-done.9.refs_5_
  47.7 0.2 shard_map.100
  47.9 1.6 %collective-permute-start.13 = (bf16[384,256]{1,0:T(8,128)(2,1)S(1)}, bf16[384,256]{1,0:T(8,128)(2,1)S(1)}, u32[]{:S(2)}, u32[]{:S(2)}) collective-permute-start(bf16[384,256]{1,0:T(8,128)(2,1)S(1)} %get-tuple-element.59.refs_0_), channel_id=1, source_target_pairs={{0,2},{1,3},{2,0},{3,1},{4,6},{5,7},{6,4},{7,5},{8,10},{9,11},{10,... | collective-permute-start | bytes 589832 | tf_op jit(solution)/shard_map/ppermute | solution.py:309
  49.4 0.0 collective-permute-start.12
  49.4 2.1 %collective-permute-done.15.refs_2_ = bf16[256,512]{1,0:T(8,128)(2,1)S(1)} collective-permute-done((bf16[256,512]{1,0:T(8,128)(2,1)S(1)}, bf16[256,512]{1,0:T(8,128)(2,1)S(1)}, u32[]{:S(2)}, u32[]{:S(2)}) %collective-permute-start.15) | collective-permute-done | bytes 262176 | tf_op jit(solution)/shard_map/ppermute | solution.py:452
  51.5 1.7 %collective-permute-start.16 = (bf16[256,512]{1,0:T(8,128)(2,1)S(1)}, bf16[256,512]{1,0:T(8,128)(2,1)S(1)}, u32[]{:S(2)}, u32[]{:S(2)}) collective-permute-start(bf16[256,512]{1,0:T(8,128)(2,1)S(1)} %collective-permute-done.15.refs_2_), channel_id=1, source_target_pairs={{0,16},{16,0},{1,17},{17,1},{2,18},{18,2},{3,19},{19,3},{4,20},{20... | collective-permute-start | bytes 786440 | tf_op jit(solution)/shard_map/ppermute | solution.py:454
  53.2 0.0 collective-permute-start.11
  53.2 2.6 %collective-permute-done.13.refs_0_ = bf16[384,256]{1,0:T(8,128)(2,1)S(1)} collective-permute-done((bf16[384,256]{1,0:T(8,128)(2,1)S(1)}, bf16[384,256]{1,0:T(8,128)(2,1)S(1)}, u32[]{:S(2)}, u32[]{:S(2)}) %collective-permute-start.13) | collective-permute-done | bytes 196640 | tf_op jit(solution)/shard_map/ppermute | solution.py:309
  55.8 0.1 collective-permute-start.14
  55.9 0.0 collective-permute-done.12.refs_3_
  55.9 0.0 collective-permute-done.11.refs_1_
  55.9 0.9 %shard_map.101 = (f32[384,512]{1,0:T(8,128)S(1)}, f32[2,384]{1,0:T(2,128)}) custom-call(f32[384,256]{1,0:T(8,128)S(1)} %get-tuple-element.58.logs, bf16[384,256]{1,0:T(8,128)(2,1)S(1)} %get-tuple-element.59.refs_0_, bf16[384,256]{1,0:T(8,128)(2,1)S(1)} %collective-permute-done.11.refs_1_, bf16[256,512]{1,0:T(8,128)(2,1)S(1)} %get-tuple-element.60.refs_2_, ...), custom_call_target="tpu_custom_call" | custom-call | tf_op jit(solution)/shard_map/pallas_call | solution.py:30
  56.7 3.1 %collective-permute-done.16.refs_3_ = bf16[256,512]{1,0:T(8,128)(2,1)S(1)} collective-permute-done((bf16[256,512]{1,0:T(8,128)(2,1)S(1)}, bf16[256,512]{1,0:T(8,128)(2,1)S(1)}, u32[]{:S(2)}, u32[]{:S(2)}) %collective-permute-start.16) | collective-permute-done | bytes 262176 | tf_op jit(solution)/shard_map/ppermute | solution.py:454
  59.9 0.0 collective-permute-done.14.refs_1_
  59.9 1.1 %shard_map.102 = bf16[384,512]{1,0:T(8,128)(2,1)} custom-call(f32[384,512]{1,0:T(8,128)S(1)} %get-tuple-element.62.before, bf16[384,256]{1,0:T(8,128)(2,1)S(1)} %collective-permute-done.13.refs_0_, bf16[384,256]{1,0:T(8,128)(2,1)S(1)} %collective-permute-done.14.refs_1_, bf16[256,512]{1,0:T(8,128)(2,1)S(1)} %collective-permute-done.15.refs_2_, ...), custom_call_target="tpu_custom_call" | custom-call | tf_op jit(solution)/shard_map/pallas_call | solution.py:30
  (2 shorter events, 0.0 us)
Async XLA Ops:
  0.6 13.0 %collective-permute-start.3 = (bf16[384,512]{1,0:T(8,128)(2,1)}, bf16[384,512]{1,0:T(8,128)(2,1)S(1)}, u32[]{:S(2)}, u32[]{:S(2)}) collective-permute-start(bf16[384,512]{1,0:T(8,128)(2,1)} %refs_0_.1), channel_id=1, source_target_pairs={{0,4},{4,8},{8,12},{1,5},{5,9},{9,13},{2,6},{6,10},{10,14},{3,7},{... | collective-permute-start | bytes 1179656 | tf_op jit(solution)/shard_map/ppermute | solution.py:313
  4.1 11.0 %collective-permute-start = (bf16[384,512]{1,0:T(8,128)(2,1)}, bf16[384,512]{1,0:T(8,128)(2,1)S(1)}, u32[]{:S(2)}, u32[]{:S(2)}) collective-permute-start(bf16[384,512]{1,0:T(8,128)(2,1)} %refs_0_.1), channel_id=1, source_target_pairs={{0,2},{1,3},{2,0},{3,1},{4,6},{5,7},{6,4},{7,5},{8,10},{9,11},{10,... | collective-permute-start | bytes 1179656 | tf_op jit(solution)/shard_map/ppermute | solution.py:309
  13.6 10.0 %collective-permute-start.4 = (bf16[384,512]{1,0:T(8,128)(2,1)S(1)}, bf16[384,512]{1,0:T(8,128)(2,1)S(1)}, u32[]{:S(2)}, u32[]{:S(2)}) collective-permute-start(bf16[384,512]{1,0:T(8,128)(2,1)S(1)} %collective-permute-done.3.refs_0_), channel_id=1, source_target_pairs={{0,2},{1,3},{2,0},{3,1},{4,6},{5,7},{6,4},{7,5},{8,10},{9,11},{10,... | collective-permute-start | bytes 1179656 | tf_op jit(solution)/shard_map/ppermute | solution.py:309
  15.1 10.0 %collective-permute-start.2 = (bf16[384,512]{1,0:T(8,128)(2,1)}, bf16[384,512]{1,0:T(8,128)(2,1)S(1)}, u32[]{:S(2)}, u32[]{:S(2)}) collective-permute-start(bf16[384,512]{1,0:T(8,128)(2,1)} %refs_0_.1), channel_id=1, source_target_pairs={{0,1},{1,0},{2,3},{3,2},{4,5},{5,4},{6,7},{7,6},{8,9},{9,8},{10,11... | collective-permute-start | bytes 1179656 | tf_op jit(solution)/shard_map/ppermute | solution.py:309
  15.1 12.8 %collective-permute-start.1 = (bf16[384,512]{1,0:T(8,128)(2,1)S(1)}, bf16[384,512]{1,0:T(8,128)(2,1)S(1)}, u32[]{:S(2)}, u32[]{:S(2)}) collective-permute-start(bf16[384,512]{1,0:T(8,128)(2,1)S(1)} %collective-permute-done.refs_0_), channel_id=1, source_target_pairs={{0,1},{1,0},{2,3},{3,2},{4,5},{5,4},{6,7},{7,6},{8,9},{9,8},{10,11... | collective-permute-start | bytes 1179656 | tf_op jit(solution)/shard_map/ppermute | solution.py:309
  16.3 14.8 %collective-permute-start.6 = (bf16[384,512]{1,0:T(8,128)(2,1)S(1)}, bf16[384,512]{1,0:T(8,128)(2,1)S(1)}, u32[]{:S(2)}, u32[]{:S(2)}) collective-permute-start(bf16[384,512]{1,0:T(8,128)(2,1)S(1)} %collective-permute-done.3.refs_0_), channel_id=1, source_target_pairs={{0,1},{1,0},{2,3},{3,2},{4,5},{5,4},{6,7},{7,6},{8,9},{9,8},{10,11... | collective-permute-start | bytes 1179656 | tf_op jit(solution)/shard_map/ppermute | solution.py:309
  23.6 15.7 %collective-permute-start.5 = (bf16[384,512]{1,0:T(8,128)(2,1)S(1)}, bf16[384,512]{1,0:T(8,128)(2,1)S(1)}, u32[]{:S(2)}, u32[]{:S(2)}) collective-permute-start(bf16[384,512]{1,0:T(8,128)(2,1)S(1)} %collective-permute-done.4.refs_0_), channel_id=1, source_target_pairs={{0,1},{1,0},{2,3},{3,2},{4,5},{5,4},{6,7},{7,6},{8,9},{9,8},{10,11... | collective-permute-start | bytes 1179656 | tf_op jit(solution)/shard_map/ppermute | solution.py:309
  29.1 10.1 %collective-permute-start.7 = (bf16[384,256]{1,0:T(8,128)(2,1)S(1)}, bf16[384,256]{1,0:T(8,128)(2,1)S(1)}, u32[]{:S(2)}, u32[]{:S(2)}) collective-permute-start(bf16[384,256]{1,0:T(8,128)(2,1)S(1)} %get-tuple-element.43.q), channel_id=1, source_target_pairs={{12,4},{13,5},{14,6},{15,7},{28,20},{29,21},{30,22},{31,23}} | collective-permute-start | bytes 589832 | tf_op jit(solution)/shard_map/ppermute | solution.py:313
  30.4 15.9 %collective-permute-start.8 = (bf16[2,384,256]{2,1,0:T(8,128)(2,1)S(1)}, bf16[2,384,256]{2,1,0:T(8,128)(2,1)S(1)}, u32[]{:S(2)}, u32[]{:S(2)}) collective-permute-start(bf16[2,384,256]{2,1,0:T(8,128)(2,1)S(1)} %get-tuple-element.44.refs_12_.kv), channel_id=1, source_target_pairs={{0,8},{1,9},{2,10},{3,11},{16,24},{17,25},{18,26},{19,27}} | collective-permute-start | bytes 1179656 | tf_op jit(solution)/shard_map/ppermute | solution.py:313
  41.6 6.1 %collective-permute-start.9 = (bf16[384,256]{1,0:T(8,128)(2,1)S(1)}, bf16[384,256]{1,0:T(8,128)(2,1)S(1)}, u32[]{:S(2)}, u32[]{:S(2)}) collective-permute-start(bf16[384,256]{1,0:T(8,128)(2,1)S(1)} %get-tuple-element.56), channel_id=1, source_target_pairs={{4,12},{5,13},{6,14},{7,15},{20,28},{21,29},{22,30},{23,31}} | collective-permute-start | bytes 589832 | tf_op jit(solution)/shard_map/ppermute | solution.py:313
  42.9 8.6 %collective-permute-start.15 = (bf16[256,512]{1,0:T(8,128)(2,1)S(1)}, bf16[256,512]{1,0:T(8,128)(2,1)S(1)}, u32[]{:S(2)}, u32[]{:S(2)}) collective-permute-start(bf16[256,512]{1,0:T(8,128)(2,1)S(1)} %get-tuple-element.63), channel_id=1, source_target_pairs={{0,3},{1,2},{2,1},{3,0},{16,18},{17,19},{18,16},{19,17},{4,7},{5,6... | collective-permute-start | bytes 786440 | tf_op jit(solution)/shard_map/ppermute | solution.py:452
  43.7 4.0 %collective-permute-start.10 = (f32[8,384]{1,0:T(8,128)S(1)}, f32[8,384]{1,0:T(8,128)S(1)}, u32[]{:S(2)}, u32[]{:S(2)}) collective-permute-start(f32[8,384]{1,0:T(8,128)S(1)} %get-tuple-element.57), channel_id=1, source_target_pairs={{4,12},{5,13},{6,14},{7,15},{20,28},{21,29},{22,30},{23,31}} | collective-permute-start | bytes 36872 | tf_op jit(solution)/shard_map/ppermute | solution.py:313
  47.9 7.9 %collective-permute-start.13 = (bf16[384,256]{1,0:T(8,128)(2,1)S(1)}, bf16[384,256]{1,0:T(8,128)(2,1)S(1)}, u32[]{:S(2)}, u32[]{:S(2)}) collective-permute-start(bf16[384,256]{1,0:T(8,128)(2,1)S(1)} %get-tuple-element.59.refs_0_), channel_id=1, source_target_pairs={{0,2},{1,3},{2,0},{3,1},{4,6},{5,7},{6,4},{7,5},{8,10},{9,11},{10,... | collective-permute-start | bytes 589832 | tf_op jit(solution)/shard_map/ppermute | solution.py:309
  49.4 6.4 %collective-permute-start.12 = (bf16[256,512]{1,0:T(8,128)(2,1)S(1)}, bf16[256,512]{1,0:T(8,128)(2,1)S(1)}, u32[]{:S(2)}, u32[]{:S(2)}) collective-permute-start(bf16[256,512]{1,0:T(8,128)(2,1)S(1)} %get-tuple-element.61), channel_id=1, source_target_pairs={{0,1},{1,0},{2,3},{3,2},{4,5},{5,4},{6,7},{7,6},{8,9},{9,8},{10,11... | collective-permute-start | bytes 786440 | tf_op jit(solution)/shard_map/ppermute | solution.py:309
  51.5 8.3 %collective-permute-start.16 = (bf16[256,512]{1,0:T(8,128)(2,1)S(1)}, bf16[256,512]{1,0:T(8,128)(2,1)S(1)}, u32[]{:S(2)}, u32[]{:S(2)}) collective-permute-start(bf16[256,512]{1,0:T(8,128)(2,1)S(1)} %collective-permute-done.15.refs_2_), channel_id=1, source_target_pairs={{0,16},{16,0},{1,17},{17,1},{2,18},{18,2},{3,19},{19,3},{4,20},{20... | collective-permute-start | bytes 786440 | tf_op jit(solution)/shard_map/ppermute | solution.py:454
  53.2 2.6 %collective-permute-start.11 = (bf16[384,256]{1,0:T(8,128)(2,1)S(1)}, bf16[384,256]{1,0:T(8,128)(2,1)S(1)}, u32[]{:S(2)}, u32[]{:S(2)}) collective-permute-start(bf16[384,256]{1,0:T(8,128)(2,1)S(1)} %get-tuple-element.59.refs_0_), channel_id=1, source_target_pairs={{0,1},{1,0},{2,3},{3,2},{4,5},{5,4},{6,7},{7,6},{8,9},{9,8},{10,11... | collective-permute-start | bytes 589832 | tf_op jit(solution)/shard_map/ppermute | solution.py:309
  55.8 4.1 %collective-permute-start.14 = (bf16[384,256]{1,0:T(8,128)(2,1)S(1)}, bf16[384,256]{1,0:T(8,128)(2,1)S(1)}, u32[]{:S(2)}, u32[]{:S(2)}) collective-permute-start(bf16[384,256]{1,0:T(8,128)(2,1)S(1)} %collective-permute-done.13.refs_0_), channel_id=1, source_target_pairs={{0,1},{1,0},{2,3},{3,2},{4,5},{5,4},{6,7},{7,6},{8,9},{9,8},{10,11... | collective-permute-start | bytes 589832 | tf_op jit(solution)/shard_map/ppermute | solution.py:309

commit v10 on v9

--- a/solution.py
+++ b/solution.py
@@ -93,10 +93,10 @@
     pieces_out, biases = outs[: len(pieces)], outs[len(pieces) :]
     me = lax.axis_index("tp")
     moves = [(own, held), *zip(weights, weights_out), *zip(small, small_out)]
-    for k, out in zip(pieces, pieces_out):
+    for (k, start), out in zip(pieces, pieces_out):
         peer = me ^ (3 - lax.axis_index("grp") if k is None else k)
         at = pl.ds(pl.multiple_of(peer * columns, columns), columns)
-        moves.append((w_out.at[:, at], out))
+        moves.append((w_out.at[pl.ds(start, out.shape[0]), at], out))
     moves = [pltpu.make_async_copy(src, dst, sems.at[n]) for n, (src, dst) in enumerate(moves)]
     for move in moves:
         move.start()
@@ -300,7 +300,11 @@
         crossed = lax.axis_index("grp") == 0
         low, high = blocks
         blocks = [jnp.where(crossed, high, low), jnp.where(crossed, low, high)]
-    total = before[...] + products(blocks, refs[count : 2 * count])
+        halves = [ref[...] for ref in refs[count:-1]]
+        pieces = [jnp.concatenate(halves[:2], axis=0), jnp.concatenate(halves[2:], axis=0)]
+    else:
+        pieces = refs[count : 2 * count]
+    total = before[...] + products(blocks, pieces)
     refs[-1][...] = total.astype(jnp.bfloat16)
 
 
@@ -366,8 +370,11 @@
     copies = lax.axis_size("grp")
     shared = copies == 2 and count == 4
 
-    piece_keys = (0, *range(1, half), *((None,) if shared else late))
-    piece_shape = shape_of((w_out.shape[0], columns), w_out.dtype)
+    cut = w_out.shape[0] // 2 if shared else w_out.shape[0]
+    piece_keys = tuple((k, 0) for k in range(half))
+    piece_keys += ((None, 0), (None, cut)) if shared else tuple((k, 0) for k in late)
+    piece_shapes = [shape_of((w_out.shape[0], columns), w_out.dtype)] * half
+    piece_shapes += [shape_of((cut, columns), w_out.dtype)] * (len(piece_keys) - half)
     across = swap(hidden, half)
     before = behind(hidden, 1)
     own_near = near_blocks(hidden)
@@ -381,7 +388,7 @@
         [sums] * 3
         + [lane_wide]
         + [shape_of(x.shape, x.dtype) for x in (*gains, *weights)]
-        + [piece_shape] * len(piece_keys)
+        + piece_shapes
         + [square] * len(distances),
         held=fixed,
         scratch=[pltpu.VMEM(hidden.shape, hidden.dtype), pltpu.SemaphoreType.DMA((moves,))],
@@ -449,10 +456,9 @@
     near_pieces = [own_slice] + [swap(x, k + 1) for k, x in enumerate(near_slice)]
     if shared:
         routes = [(g * 4 + t, g * 4 + (t ^ (3 - g))) for g in range(2) for t in range(4)]
-        fetched = lax.ppermute(far_slice[0], ("grp", "tp"), routes)
-        later, _ = lax.optimization_barrier((fetched, near[0]))
-        other = lax.ppermute(later, "grp", [(0, 1), (1, 0)])
-        far_pieces = [fetched, other]
+        first_half = lax.ppermute(far_slice[0], ("grp", "tp"), routes)
+        first_other = lax.ppermute(first_half, "grp", [(0, 1), (1, 0)])
+        last_half = lax.ppermute(far_slice[1], ("grp", "tp"), routes)
     else:
         far_pieces = [swap(x, k) for k, x in zip(late, far_slice)]
 
@@ -469,6 +475,10 @@
         [half_sum, sums],
     )
     attended_across = swap(attended, half)
+    if shared:
+        later, _ = lax.optimization_barrier((last_half, logs))
+        last_other = lax.ppermute(later, "grp", [(0, 1), (1, 0)])
+        far_pieces = [first_half, last_half, first_other, last_other]
     mixed_shape = (rows, columns)
     partial_mix, log_rows = call(
         functools.partial(mix_early_kernel, count=half),

time: 61.2 us -> 70.1 us (1.15)
  the two profiles are of different devices: /device:TPU:8 before, /device:TPU:24 now
where the time goes in v10:
time: 70.1 us; the launch traced here: 69.9 us
  waiting for transfers between devices  40.8 us (58%)
  starting transfers between devices  16.7 us (24%)
  Pallas kernels  9.41 us (13%)
  other arithmetic  1.45 us (2%)
  between operations  0.75 us (1%)
    ppermute x5, waiting for transfers between devices, send(): return lax.ppermute(value, 'sp', pairs)  20.8 us
    ppermute x10, waiting for transfers between devices, swap(): return lax.ppermute(value, 'tp', [(i, i ^ distance) for i in range(count)])  11.3 us
    pallas_call x8, Pallas kernels, call(): pl.pallas_call(body, out_shape=tuple(outs), in_specs=[HBM if n in held el...  9.41 us
    ppermute x5, starting transfers between devices, send(): return lax.ppermute(value, 'sp', pairs)  6.81 us
    ppermute x10, starting transfers between devices, swap(): return lax.ppermute(value, 'tp', [(i, i ^ distance) for i in range(count)])  5.63 us
    ppermute x1, waiting for transfers between devices, layer(): first_other = lax.ppermute(first_half, 'grp', [(0, 1), (1, 0)])  3.45 us
    ppermute x1, waiting for transfers between devices, layer(): first_half = lax.ppermute(far_slice[0], ('grp', 'tp'), routes)  3.05 us
    ppermute x1, starting transfers between devices, layer(): first_other = lax.ppermute(first_half, 'grp', [(0, 1), (1, 0)])  2.51 us
  transfers between devices with their start and end apart: 19, of which 8 were waited for; matrix products, arithmetic and copies ran while one was open for 3% of the time, Pallas kernels for 11%

profile of v10, /device:TPU:24, one launch (start us, length us, event | category | flops | bytes accessed | tf_op | source)
XLA Modules:
  0.0 69.9 jit_solution(17853299145337261243)
XLA Ops:
  0.6 1.3 %collective-permute-start.3 = (bf16[384,512]{1,0:T(8,128)(2,1)}, bf16[384,512]{1,0:T(8,128)(2,1)S(1)}, u32[]{:S(2)}, u32[]{:S(2)}) collective-permute-start(bf16[384,512]{1,0:T(8,128)(2,1)} %refs_0_.1), channel_id=1, source_target_pairs={{0,4},{4,8},{8,12},{1,5},{5,9},{9,13},{2,6},{6,10},{10,14},{3,7},{... | collective-permute-start | bytes 1179656 | tf_op jit(solution)/shard_map/ppermute | solution.py:317
  1.9 1.6 %collective-permute-start = (bf16[384,512]{1,0:T(8,128)(2,1)}, bf16[384,512]{1,0:T(8,128)(2,1)S(1)}, u32[]{:S(2)}, u32[]{:S(2)}) collective-permute-start(bf16[384,512]{1,0:T(8,128)(2,1)} %refs_0_.1), channel_id=1, source_target_pairs={{0,2},{1,3},{2,0},{3,1},{4,6},{5,7},{6,4},{7,5},{8,10},{9,11},{10,... | collective-permute-start | bytes 1179656 | tf_op jit(solution)/shard_map/ppermute | solution.py:313
  3.5 10.1 %collective-permute-done.3.refs_0_ = bf16[384,512]{1,0:T(8,128)(2,1)S(1)} collective-permute-done((bf16[384,512]{1,0:T(8,128)(2,1)}, bf16[384,512]{1,0:T(8,128)(2,1)S(1)}, u32[]{:S(2)}, u32[]{:S(2)}) %collective-permute-start.3) | collective-permute-done | bytes 393248 | tf_op jit(solution)/shard_map/ppermute | solution.py:317
  13.6 1.5 %collective-permute-start.4 = (bf16[384,512]{1,0:T(8,128)(2,1)S(1)}, bf16[384,512]{1,0:T(8,128)(2,1)S(1)}, u32[]{:S(2)}, u32[]{:S(2)}) collective-permute-start(bf16[384,512]{1,0:T(8,128)(2,1)S(1)} %collective-permute-done.3.refs_0_), channel_id=1, source_target_pairs={{0,2},{1,3},{2,0},{3,1},{4,6},{5,7},{6,4},{7,5},{8,10},{9,11},{10,... | collective-permute-start | bytes 1179656 | tf_op jit(solution)/shard_map/ppermute | solution.py:313
  15.1 0.0 collective-permute-start.2
  15.1 0.0 collective-permute-done.refs_0_
  15.1 0.5 collective-permute-start.1
  15.6 0.7 %reshape.28.refs_2_ = f32[4,512]{1,0:T(4,128)S(1)} reshape(bf16[2048]{0:T(1024)(128)(2,1)} %param.9) | data formatting | bytes 12288 | tf_op jit(solution)/shard_map/reshape | solution.py:359
  16.3 0.0 collective-permute-start.6
  16.3 7.3 %collective-permute-done.4.refs_0_ = bf16[384,512]{1,0:T(8,128)(2,1)S(1)} collective-permute-done((bf16[384,512]{1,0:T(8,128)(2,1)S(1)}, bf16[384,512]{1,0:T(8,128)(2,1)S(1)}, u32[]{:S(2)}, u32[]{:S(2)}) %collective-permute-start.4) | collective-permute-done | bytes 393248 | tf_op jit(solution)/shard_map/ppermute | solution.py:313
  23.6 0.0 collective-permute-start.5
  23.6 1.4 %multiply_sine_fusion = (f32[384,64]{1,0:T(8,128)S(1)}, f32[384,64]{1,0:T(8,128)S(1)}, f32[384,64]{1,0:T(8,128)S(1)}, f32[384,64]{1,0:T(8,128)S(1)}) fusion(f32[384]{0:T(512)S(1)} %get-tuple-element.74, f32[64]{0:T(128)S(1)} %multiply_power_fusion, f32[384]{0:T(512)S(1)} %get-tuple-element.75), kind=kLoop, calls=%fused_computation | loop fusion | flops 49152 | bytes 396544 | tf_op jit(solution)/shard_map/sin | solution.py:338
  25.0 0.0 collective-permute-done.2.refs_1_
  25.0 2.9 %shard_map.95 = (f32[384,256]{1,0:T(8,128)S(1)}, f32[384,256]{1,0:T(8,128)S(1)}, f32[384,256]{1,0:T(8,128)S(1)}, f32[384,128]{1,0:T(8,128)S(1)}, f32[2,128]{1,0:...) custom-call(bf16[384,512]{1,0:T(8,128)(2,1)} %refs_0_.1, ...), custom_call_target="tpu_custom_call" | custom-call | tf_op jit(solution)/shard_map/pallas_call | solution.py:30
  27.9 0.0 collective-permute-done.1.refs_1_
  27.9 1.2 %shard_map.96 = (bf16[384,256]{1,0:T(8,128)(2,1)S(1)}, bf16[2,384,256]{2,1,0:T(8,128)(2,1)S(1)}) custom-call(bf16[384,512]{1,0:T(8,128)(2,1)S(1)} %collective-permute-done.refs_0_, bf16[384,512]{1,0:T(8,128)(2,1)S(1)} %collective-permute-done.1.refs_1_, f32[4,512]{1,0:T(4,128)S(1)} %reshape.28.refs_2_, bf16[2048,256]{1,0:T(8,128)(2,1)S(1)} %get-tuple-element.35.refs_3_, ...), custom_call_target="tpu_custom_call" | custom-call | tf_op jit(solution)/shard_map/pallas_call | solution.py:30
  29.2 2.3 %collective-permute-start.7 = (bf16[384,256]{1,0:T(8,128)(2,1)S(1)}, bf16[384,256]{1,0:T(8,128)(2,1)S(1)}, u32[]{:S(2)}, u32[]{:S(2)}) collective-permute-start(bf16[384,256]{1,0:T(8,128)(2,1)S(1)} %get-tuple-element.44.q), channel_id=1, source_target_pairs={{12,4},{13,5},{14,6},{15,7},{28,20},{29,21},{30,22},{31,23}} | collective-permute-start | bytes 589832 | tf_op jit(solution)/shard_map/ppermute | solution.py:317
  31.4 0.7 collective-permute-start.8
  32.1 0.0 collective-permute-done.6.refs_1_
  32.1 0.6 shard_map.97
  32.7 3.5 %collective-permute-done.7.refs_11_ = bf16[384,256]{1,0:T(8,128)(2,1)S(1)} collective-permute-done((bf16[384,256]{1,0:T(8,128)(2,1)S(1)}, bf16[384,256]{1,0:T(8,128)(2,1)S(1)}, u32[]{:S(2)}, u32[]{:S(2)}) %collective-permute-start.7) | collective-permute-done | bytes 196640 | tf_op jit(solution)/shard_map/ppermute | solution.py:317
  36.2 0.0 collective-permute-done.5.refs_1_
  36.2 1.3 %collective-permute-start.9 = (bf16[384,256]{1,0:T(8,128)(2,1)S(1)}, bf16[384,256]{1,0:T(8,128)(2,1)S(1)}, u32[]{:S(2)}, u32[]{:S(2)}) collective-permute-start(bf16[384,256]{1,0:T(8,128)(2,1)S(1)} %get-tuple-element.57), channel_id=1, source_target_pairs={{4,12},{5,13},{6,14},{7,15},{20,28},{21,29},{22,30},{23,31}} | collective-permute-start | bytes 589832 | tf_op jit(solution)/shard_map/ppermute | solution.py:317
  37.5 1.3 %collective-permute-start.10 = (f32[8,384]{1,0:T(8,128)S(1)}, f32[8,384]{1,0:T(8,128)S(1)}, u32[]{:S(2)}, u32[]{:S(2)}) collective-permute-start(f32[8,384]{1,0:T(8,128)S(1)} %get-tuple-element.58), channel_id=1, source_target_pairs={{4,12},{5,13},{6,14},{7,15},{20,28},{21,29},{22,30},{23,31}} | collective-permute-start | bytes 36872 | tf_op jit(solution)/shard_map/ppermute | solution.py:317
  38.8 2.5 %shard_map.99 = (f32[384,256]{1,0:T(8,128)S(1)}, f32[384,256]{1,0:T(8,128)S(1)}, f32[384,256]{1,0:T(8,128)S(1)}) custom-call(bf16[384,256]{1,0:T(8,128)(2,1)S(1)} %get-tuple-element.44.q, bf16[2,384,256]{2,1,0:T(8,128)(2,1)S(1)} %get-tuple-element.45.refs_12_.kv, f32[384,384]{1,0:T(8,128)S(1)} %get-tuple-element.46.bias, ...), custom_call_target="tpu_custom_call" | custom-call | tf_op jit(solution)/shard_map/pallas_call | solution.py:30
  41.3 0.0 collective-permute-done.8.refs_3_
  41.3 7.2 %collective-permute-done.10.refs_6_ = f32[8,384]{1,0:T(8,128)S(1)} collective-permute-done((f32[8,384]{1,0:T(8,128)S(1)}, f32[8,384]{1,0:T(8,128)S(1)}, u32[]{:S(2)}, u32[]{:S(2)}) %collective-permute-start.10) | collective-permute-done | bytes 12320 | tf_op jit(solution)/shard_map/ppermute | solution.py:317
  48.5 0.0 collective-permute-done.9.refs_5_
  48.5 0.3 shard_map.100
  48.8 1.6 %collective-permute-start.13 = (bf16[384,256]{1,0:T(8,128)(2,1)S(1)}, bf16[384,256]{1,0:T(8,128)(2,1)S(1)}, u32[]{:S(2)}, u32[]{:S(2)}) collective-permute-start(bf16[384,256]{1,0:T(8,128)(2,1)S(1)} %get-tuple-element.60.refs_0_), channel_id=1, source_target_pairs={{0,2},{1,3},{2,0},{3,1},{4,6},{5,7},{6,4},{7,5},{8,10},{9,11},{10,... | collective-permute-start | bytes 589832 | tf_op jit(solution)/shard_map/ppermute | solution.py:313
  50.4 0.0 collective-permute-start.16
  50.4 1.7 %collective-permute-start.15 = (bf16[128,512]{1,0:T(8,128)(2,1)S(1)}, bf16[128,512]{1,0:T(8,128)(2,1)S(1)}, u32[]{:S(2)}, u32[]{:S(2)}) collective-permute-start(bf16[128,512]{1,0:T(8,128)(2,1)S(1)} %get-tuple-element.64), channel_id=1, source_target_pairs={{0,3},{1,2},{2,1},{3,0},{16,18},{17,19},{18,16},{19,17},{4,7},{5,6... | collective-permute-start | bytes 393224 | tf_op jit(solution)/shard_map/ppermute | solution.py:459
  52.1 0.0 collective-permute-start.12
  52.1 0.5 collective-permute-start.11
  52.6 4.0 %collective-permute-done.13.refs_0_ = bf16[384,256]{1,0:T(8,128)(2,1)S(1)} collective-permute-done((bf16[384,256]{1,0:T(8,128)(2,1)S(1)}, bf16[384,256]{1,0:T(8,128)(2,1)S(1)}, u32[]{:S(2)}, u32[]{:S(2)}) %collective-permute-start.13) | collective-permute-done | bytes 196640 | tf_op jit(solution)/shard_map/ppermute | solution.py:313
  56.7 0.0 collective-permute-start.14
  56.7 3.1 %collective-permute-done.15.refs_2_ = bf16[128,512]{1,0:T(8,128)(2,1)S(1)} collective-permute-done((bf16[128,512]{1,0:T(8,128)(2,1)S(1)}, bf16[128,512]{1,0:T(8,128)(2,1)S(1)}, u32[]{:S(2)}, u32[]{:S(2)}) %collective-permute-start.15) | collective-permute-done | bytes 131104 | tf_op jit(solution)/shard_map/ppermute | solution.py:459
  59.7 2.5 %collective-permute-start.17 = (bf16[128,512]{1,0:T(8,128)(2,1)S(1)}, bf16[128,512]{1,0:T(8,128)(2,1)S(1)}, u32[]{:S(2)}, u32[]{:S(2)}) collective-permute-start(bf16[128,512]{1,0:T(8,128)(2,1)S(1)} %collective-permute-done.15.refs_2_), channel_id=1, source_target_pairs={{0,16},{16,0},{1,17},{17,1},{2,18},{18,2},{3,19},{19,3},{4,20},{20... | collective-permute-start | bytes 393224 | tf_op jit(solution)/shard_map/ppermute | solution.py:460
  62.2 0.0 collective-permute-done.16.refs_3_
  62.2 0.0 collective-permute-start.18
  62.2 0.0 collective-permute-done.12.refs_3_
  62.3 0.0 collective-permute-done.11.refs_1_
  62.3 0.9 %shard_map.101 = (f32[384,512]{1,0:T(8,128)S(1)}, f32[2,384]{1,0:T(2,128)}) custom-call(f32[384,256]{1,0:T(8,128)S(1)} %get-tuple-element.59.logs, bf16[384,256]{1,0:T(8,128)(2,1)S(1)} %get-tuple-element.60.refs_0_, bf16[384,256]{1,0:T(8,128)(2,1)S(1)} %collective-permute-done.11.refs_1_, bf16[256,512]{1,0:T(8,128)(2,1)S(1)} %get-tuple-element.61.refs_2_, ...), custom_call_target="tpu_custom_call" | custom-call | tf_op jit(solution)/shard_map/pallas_call | solution.py:30
  63.1 3.4 %collective-permute-done.17.refs_4_ = bf16[128,512]{1,0:T(8,128)(2,1)S(1)} collective-permute-done((bf16[128,512]{1,0:T(8,128)(2,1)S(1)}, bf16[128,512]{1,0:T(8,128)(2,1)S(1)}, u32[]{:S(2)}, u32[]{:S(2)}) %collective-permute-start.17) | collective-permute-done | bytes 131104 | tf_op jit(solution)/shard_map/ppermute | solution.py:460
  66.6 2.2 %collective-permute-done.18.refs_5_ = bf16[128,512]{1,0:T(8,128)(2,1)S(1)} collective-permute-done((bf16[128,512]{1,0:T(8,128)(2,1)S(1)}, bf16[128,512]{1,0:T(8,128)(2,1)S(1)}, u32[]{:S(2)}, u32[]{:S(2)}) %collective-permute-start.18) | collective-permute-done | bytes 131104 | tf_op jit(solution)/shard_map/ppermute | solution.py:480
  68.7 0.0 collective-permute-done.14.refs_1_
  68.7 1.1 %shard_map.102 = bf16[384,512]{1,0:T(8,128)(2,1)} custom-call(f32[384,512]{1,0:T(8,128)S(1)} %get-tuple-element.63.before, bf16[384,256]{1,0:T(8,128)(2,1)S(1)} %collective-permute-done.13.refs_0_, bf16[384,256]{1,0:T(8,128)(2,1)S(1)} %collective-permute-done.14.refs_1_, bf16[128,512]{1,0:T(8,128)(2,1)S(1)} %collective-permute-done.15.refs_2_, ...), custom_call_target="tpu_custom_call" | custom-call | tf_op jit(solution)/shard_map/pallas_call | solution.py:30
  (3 shorter events, 0.0 us)
Async XLA Ops:
  0.6 13.0 %collective-permute-start.3 = (bf16[384,512]{1,0:T(8,128)(2,1)}, bf16[384,512]{1,0:T(8,128)(2,1)S(1)}, u32[]{:S(2)}, u32[]{:S(2)}) collective-permute-start(bf16[384,512]{1,0:T(8,128)(2,1)} %refs_0_.1), channel_id=1, source_target_pairs={{0,4},{4,8},{8,12},{1,5},{5,9},{9,13},{2,6},{6,10},{10,14},{3,7},{... | collective-permute-start | bytes 1179656 | tf_op jit(solution)/shard_map/ppermute | solution.py:317
  1.9 13.2 %collective-permute-start = (bf16[384,512]{1,0:T(8,128)(2,1)}, bf16[384,512]{1,0:T(8,128)(2,1)S(1)}, u32[]{:S(2)}, u32[]{:S(2)}) collective-permute-start(bf16[384,512]{1,0:T(8,128)(2,1)} %refs_0_.1), channel_id=1, source_target_pairs={{0,2},{1,3},{2,0},{3,1},{4,6},{5,7},{6,4},{7,5},{8,10},{9,11},{10,... | collective-permute-start | bytes 1179656 | tf_op jit(solution)/shard_map/ppermute | solution.py:313
  13.6 10.0 %collective-permute-start.4 = (bf16[384,512]{1,0:T(8,128)(2,1)S(1)}, bf16[384,512]{1,0:T(8,128)(2,1)S(1)}, u32[]{:S(2)}, u32[]{:S(2)}) collective-permute-start(bf16[384,512]{1,0:T(8,128)(2,1)S(1)} %collective-permute-done.3.refs_0_), channel_id=1, source_target_pairs={{0,2},{1,3},{2,0},{3,1},{4,6},{5,7},{6,4},{7,5},{8,10},{9,11},{10,... | collective-permute-start | bytes 1179656 | tf_op jit(solution)/shard_map/ppermute | solution.py:313
  15.1 10.0 %collective-permute-start.2 = (bf16[384,512]{1,0:T(8,128)(2,1)}, bf16[384,512]{1,0:T(8,128)(2,1)S(1)}, u32[]{:S(2)}, u32[]{:S(2)}) collective-permute-start(bf16[384,512]{1,0:T(8,128)(2,1)} %refs_0_.1), channel_id=1, source_target_pairs={{0,1},{1,0},{2,3},{3,2},{4,5},{5,4},{6,7},{7,6},{8,9},{9,8},{10,11... | collective-permute-start | bytes 1179656 | tf_op jit(solution)/shard_map/ppermute | solution.py:313
  15.1 12.8 %collective-permute-start.1 = (bf16[384,512]{1,0:T(8,128)(2,1)S(1)}, bf16[384,512]{1,0:T(8,128)(2,1)S(1)}, u32[]{:S(2)}, u32[]{:S(2)}) collective-permute-start(bf16[384,512]{1,0:T(8,128)(2,1)S(1)} %collective-permute-done.refs_0_), channel_id=1, source_target_pairs={{0,1},{1,0},{2,3},{3,2},{4,5},{5,4},{6,7},{7,6},{8,9},{9,8},{10,11... | collective-permute-start | bytes 1179656 | tf_op jit(solution)/shard_map/ppermute | solution.py:313
  16.3 15.8 %collective-permute-start.6 = (bf16[384,512]{1,0:T(8,128)(2,1)S(1)}, bf16[384,512]{1,0:T(8,128)(2,1)S(1)}, u32[]{:S(2)}, u32[]{:S(2)}) collective-permute-start(bf16[384,512]{1,0:T(8,128)(2,1)S(1)} %collective-permute-done.3.refs_0_), channel_id=1, source_target_pairs={{0,1},{1,0},{2,3},{3,2},{4,5},{5,4},{6,7},{7,6},{8,9},{9,8},{10,11... | collective-permute-start | bytes 1179656 | tf_op jit(solution)/shard_map/ppermute | solution.py:313
  23.6 12.6 %collective-permute-start.5 = (bf16[384,512]{1,0:T(8,128)(2,1)S(1)}, bf16[384,512]{1,0:T(8,128)(2,1)S(1)}, u32[]{:S(2)}, u32[]{:S(2)}) collective-permute-start(bf16[384,512]{1,0:T(8,128)(2,1)S(1)} %collective-permute-done.4.refs_0_), channel_id=1, source_target_pairs={{0,1},{1,0},{2,3},{3,2},{4,5},{5,4},{6,7},{7,6},{8,9},{9,8},{10,11... | collective-permute-start | bytes 1179656 | tf_op jit(solution)/shard_map/ppermute | solution.py:313
  29.2 7.1 %collective-permute-start.7 = (bf16[384,256]{1,0:T(8,128)(2,1)S(1)}, bf16[384,256]{1,0:T(8,128)(2,1)S(1)}, u32[]{:S(2)}, u32[]{:S(2)}) collective-permute-start(bf16[384,256]{1,0:T(8,128)(2,1)S(1)} %get-tuple-element.44.q), channel_id=1, source_target_pairs={{12,4},{13,5},{14,6},{15,7},{28,20},{29,21},{30,22},{31,23}} | collective-permute-start | bytes 589832 | tf_op jit(solution)/shard_map/ppermute | solution.py:317
  31.4 9.9 %collective-permute-start.8 = (bf16[2,384,256]{2,1,0:T(8,128)(2,1)S(1)}, bf16[2,384,256]{2,1,0:T(8,128)(2,1)S(1)}, u32[]{:S(2)}, u32[]{:S(2)}) collective-permute-start(bf16[2,384,256]{2,1,0:T(8,128)(2,1)S(1)} %get-tuple-element.45.refs_12_.kv), channel_id=1, source_target_pairs={{0,8},{1,9},{2,10},{3,11},{16,24},{17,25},{18,26},{19,27}} | collective-permute-start | bytes 1179656 | tf_op jit(solution)/shard_map/ppermute | solution.py:317
  36.2 12.3 %collective-permute-start.9 = (bf16[384,256]{1,0:T(8,128)(2,1)S(1)}, bf16[384,256]{1,0:T(8,128)(2,1)S(1)}, u32[]{:S(2)}, u32[]{:S(2)}) collective-permute-start(bf16[384,256]{1,0:T(8,128)(2,1)S(1)} %get-tuple-element.57), channel_id=1, source_target_pairs={{4,12},{5,13},{6,14},{7,15},{20,28},{21,29},{22,30},{23,31}} | collective-permute-start | bytes 589832 | tf_op jit(solution)/shard_map/ppermute | solution.py:317
  37.5 11.0 %collective-permute-start.10 = (f32[8,384]{1,0:T(8,128)S(1)}, f32[8,384]{1,0:T(8,128)S(1)}, u32[]{:S(2)}, u32[]{:S(2)}) collective-permute-start(f32[8,384]{1,0:T(8,128)S(1)} %get-tuple-element.58), channel_id=1, source_target_pairs={{4,12},{5,13},{6,14},{7,15},{20,28},{21,29},{22,30},{23,31}} | collective-permute-start | bytes 36872 | tf_op jit(solution)/shard_map/ppermute | solution.py:317
  48.8 7.8 %collective-permute-start.13 = (bf16[384,256]{1,0:T(8,128)(2,1)S(1)}, bf16[384,256]{1,0:T(8,128)(2,1)S(1)}, u32[]{:S(2)}, u32[]{:S(2)}) collective-permute-start(bf16[384,256]{1,0:T(8,128)(2,1)S(1)} %get-tuple-element.60.refs_0_), channel_id=1, source_target_pairs={{0,2},{1,3},{2,0},{3,1},{4,6},{5,7},{6,4},{7,5},{8,10},{9,11},{10,... | collective-permute-start | bytes 589832 | tf_op jit(solution)/shard_map/ppermute | solution.py:313
  50.4 11.9 %collective-permute-start.16 = (bf16[128,512]{1,0:T(8,128)(2,1)S(1)}, bf16[128,512]{1,0:T(8,128)(2,1)S(1)}, u32[]{:S(2)}, u32[]{:S(2)}) collective-permute-start(bf16[128,512]{1,0:T(8,128)(2,1)S(1)} %get-tuple-element.65), channel_id=1, source_target_pairs={{0,3},{1,2},{2,1},{3,0},{16,18},{17,19},{18,16},{19,17},{4,7},{5,6... | collective-permute-start | bytes 393224 | tf_op jit(solution)/shard_map/ppermute | solution.py:461
  50.4 9.3 %collective-permute-start.15 = (bf16[128,512]{1,0:T(8,128)(2,1)S(1)}, bf16[128,512]{1,0:T(8,128)(2,1)S(1)}, u32[]{:S(2)}, u32[]{:S(2)}) collective-permute-start(bf16[128,512]{1,0:T(8,128)(2,1)S(1)} %get-tuple-element.64), channel_id=1, source_target_pairs={{0,3},{1,2},{2,1},{3,0},{16,18},{17,19},{18,16},{19,17},{4,7},{5,6... | collective-permute-start | bytes 393224 | tf_op jit(solution)/shard_map/ppermute | solution.py:459
  52.1 10.1 %collective-permute-start.12 = (bf16[256,512]{1,0:T(8,128)(2,1)S(1)}, bf16[256,512]{1,0:T(8,128)(2,1)S(1)}, u32[]{:S(2)}, u32[]{:S(2)}) collective-permute-start(bf16[256,512]{1,0:T(8,128)(2,1)S(1)} %get-tuple-element.62), channel_id=1, source_target_pairs={{0,1},{1,0},{2,3},{3,2},{4,5},{5,4},{6,7},{7,6},{8,9},{9,8},{10,11... | collective-permute-start | bytes 786440 | tf_op jit(solution)/shard_map/ppermute | solution.py:313
  52.1 10.1 %collective-permute-start.11 = (bf16[384,256]{1,0:T(8,128)(2,1)S(1)}, bf16[384,256]{1,0:T(8,128)(2,1)S(1)}, u32[]{:S(2)}, u32[]{:S(2)}) collective-permute-start(bf16[384,256]{1,0:T(8,128)(2,1)S(1)} %get-tuple-element.60.refs_0_), channel_id=1, source_target_pairs={{0,1},{1,0},{2,3},{3,2},{4,5},{5,4},{6,7},{7,6},{8,9},{9,8},{10,11... | collective-permute-start | bytes 589832 | tf_op jit(solution)/shard_map/ppermute | solution.py:313
  56.7 12.1 %collective-permute-start.14 = (bf16[384,256]{1,0:T(8,128)(2,1)S(1)}, bf16[384,256]{1,0:T(8,128)(2,1)S(1)}, u32[]{:S(2)}, u32[]{:S(2)}) collective-permute-start(bf16[384,256]{1,0:T(8,128)(2,1)S(1)} %collective-permute-done.13.refs_0_), channel_id=1, source_target_pairs={{0,1},{1,0},{2,3},{3,2},{4,5},{5,4},{6,7},{7,6},{8,9},{9,8},{10,11... | collective-permute-start | bytes 589832 | tf_op jit(solution)/shard_map/ppermute | solution.py:313
  59.7 6.9 %collective-permute-start.17 = (bf16[128,512]{1,0:T(8,128)(2,1)S(1)}, bf16[128,512]{1,0:T(8,128)(2,1)S(1)}, u32[]{:S(2)}, u32[]{:S(2)}) collective-permute-start(bf16[128,512]{1,0:T(8,128)(2,1)S(1)} %collective-permute-done.15.refs_2_), channel_id=1, source_target_pairs={{0,16},{16,0},{1,17},{17,1},{2,18},{18,2},{3,19},{19,3},{4,20},{20... | collective-permute-start | bytes 393224 | tf_op jit(solution)/shard_map/ppermute | solution.py:460
  62.2 6.5 %collective-permute-start.18 = (bf16[128,512]{1,0:T(8,128)(2,1)S(1)}, bf16[128,512]{1,0:T(8,128)(2,1)S(1)}, u32[]{:S(2)}, u32[]{:S(2)}) collective-permute-start(bf16[128,512]{1,0:T(8,128)(2,1)S(1)} %collective-permute-done.16.refs_3_), channel_id=1, source_target_pairs={{0,16},{16,0},{1,17},{17,1},{2,18},{18,2},{3,19},{19,3},{4,20},{20... | collective-permute-start | bytes 393224 | tf_op jit(solution)/shard_map/ppermute | solution.py:480

commit v11 on v10

--- a/solution.py
+++ b/solution.py
@@ -112,16 +112,15 @@
         move.wait()
 
 
-def early_kernel(*refs, offsets, kinds):
+def early_kernel(*refs, offsets, kinds, carried=False):
     count = len(offsets)
     hidden = refs[:count]
     gain = refs[count]
     weights = refs[count + 1 : count + 1 + kinds]
-    outs = refs[count + 1 + kinds :]
+    prior, outs = refs[count + 1 + kinds : -kinds - 1], refs[-kinds - 1 :]
     sums, squares = sums_of(hidden, gain, weights, offsets)
-    for out, total in zip(outs[:kinds], sums):
-        out[...] = total
-    outs[kinds][...] = wide(squares)
+    for n, total in enumerate((*sums, wide(squares))):
+        outs[n][...] = total + prior[n][...] if carried else total
 
 
 def head_turn(values, gains, cosine, sine):
@@ -419,8 +418,13 @@
         [sums] * 2 + [lane_wide],
     )
     before_far = near_blocks(before_across)
-    operands = [*before_far, gain, *weights[1:], *begun_before, gains[1], *tables_before]
-    late_before = functools.partial(late_kernel, offsets=late, kinds=2, width=width)
+    begun_before = call(
+        functools.partial(early_kernel, offsets=late[:1], kinds=2, carried=True),
+        [before_far[0], gain, *weights[1:], *begun_before],
+        [sums] * 2 + [lane_wide],
+    )
+    operands = [*before_far[1:], gain, *weights[1:], *begun_before, gains[1], *tables_before]
+    late_before = functools.partial(late_kernel, offsets=late[1:], kinds=2, width=width)
     given = []
     if helped is None:
         (kv_before,) = call(late_before, operands, [pair])

time: 70.1 us -> 69.2 us (0.987)
  waiting for transfers between devices: 40.8 us -> 38.3 us
  starting transfers between devices: 16.7 us -> 18.4 us
    ppermute x1, starting transfers between devices: 0.02 us -> 1.67 us  [layer(): last_other = lax.ppermute(later, 'grp', [(0, 1), (1, 0)])]
    ppermute x1, waiting for transfers between devices: 3.45 us -> 1.8 us  [layer(): first_other = lax.ppermute(first_half, 'grp', [(0, 1), (1, 0)])]
    ppermute x1, waiting for transfers between devices: 3.05 us -> 1.8 us  [layer(): first_half = lax.ppermute(far_slice[0], ('grp', 'tp'), routes)]
    ppermute x1, starting transfers between devices: 1.74 us -> 0.66 us  [layer(): first_half = lax.ppermute(far_slice[0], ('grp', 'tp'), routes)]
    ppermute x1, starting transfers between devices: 0.01 us -> 1.09 us  [layer(): last_half = lax.ppermute(far_slice[1], ('grp', 'tp'), routes)]
    pallas_call x8 -> x9, Pallas kernels: 9.41 us -> 9.32 us  [call(): pl.pallas_call(body, out_shape=tuple(outs), in_specs=[HBM if n in held el...]
where the time goes in v11:
time: 69.2 us; the launch traced here: 68.9 us
  waiting for transfers between devices  38.3 us (55%)
  starting transfers between devices  18.4 us (27%)
  Pallas kernels  9.32 us (13%)
  other arithmetic  1.45 us (2%)
  between operations  0.76 us (1%)
  local copies, waits for them, and re-layouts  0.7 us (1%)
    ppermute x5, waiting for transfers between devices, send(): return lax.ppermute(value, 'sp', pairs)  20.9 us
    ppermute x10, waiting for transfers between devices, swap(): return lax.ppermute(value, 'tp', [(i, i ^ distance) for i in range(count)])  11.3 us
    pallas_call x9, Pallas kernels, call(): pl.pallas_call(body, out_shape=tuple(outs), in_specs=[HBM if n in held el...  9.32 us
    ppermute x5, starting transfers between devices, send(): return lax.ppermute(value, 'sp', pairs)  6.8 us
    ppermute x10, starting transfers between devices, swap(): return lax.ppermute(value, 'tp', [(i, i ^ distance) for i in range(count)])  5.62 us
    ppermute x1, starting transfers between devices, layer(): first_other = lax.ppermute(first_half, 'grp', [(0, 1), (1, 0)])  2.51 us
    ppermute x1, waiting for transfers between devices, layer(): last_other = lax.ppermute(later, 'grp', [(0, 1), (1, 0)])  2.47 us
    ppermute x1, waiting for transfers between devices, layer(): first_half = lax.ppermute(far_slice[0], ('grp', 'tp'), routes)  1.8 us
  transfers between devices with their start and end apart: 19, of which 8 were waited for; matrix products, arithmetic and copies ran while one was open for 3% of the time, Pallas kernels for 11%

profile of v11, /device:TPU:24, one launch (start us, length us, event | category | flops | bytes accessed | tf_op | source)
XLA Modules:
  0.0 68.9 jit_solution(11006153667375681478)
XLA Ops:
  0.6 1.3 %collective-permute-start.3 = (bf16[384,512]{1,0:T(8,128)(2,1)}, bf16[384,512]{1,0:T(8,128)(2,1)S(1)}, u32[]{:S(2)}, u32[]{:S(2)}) collective-permute-start(bf16[384,512]{1,0:T(8,128)(2,1)} %refs_0_.1), channel_id=1, source_target_pairs={{0,4},{4,8},{8,12},{1,5},{5,9},{9,13},{2,6},{6,10},{10,14},{3,7},{... | collective-permute-start | bytes 1179656 | tf_op jit(solution)/shard_map/ppermute | solution.py:316
  1.9 1.6 %collective-permute-start = (bf16[384,512]{1,0:T(8,128)(2,1)}, bf16[384,512]{1,0:T(8,128)(2,1)S(1)}, u32[]{:S(2)}, u32[]{:S(2)}) collective-permute-start(bf16[384,512]{1,0:T(8,128)(2,1)} %refs_0_.1), channel_id=1, source_target_pairs={{0,2},{1,3},{2,0},{3,1},{4,6},{5,7},{6,4},{7,5},{8,10},{9,11},{10,... | collective-permute-start | bytes 1179656 | tf_op jit(solution)/shard_map/ppermute | solution.py:312
  3.5 10.1 %collective-permute-done.3.refs_0_ = bf16[384,512]{1,0:T(8,128)(2,1)S(1)} collective-permute-done((bf16[384,512]{1,0:T(8,128)(2,1)}, bf16[384,512]{1,0:T(8,128)(2,1)S(1)}, u32[]{:S(2)}, u32[]{:S(2)}) %collective-permute-start.3) | collective-permute-done | bytes 393248 | tf_op jit(solution)/shard_map/ppermute | solution.py:316
  13.6 1.5 %collective-permute-start.4 = (bf16[384,512]{1,0:T(8,128)(2,1)S(1)}, bf16[384,512]{1,0:T(8,128)(2,1)S(1)}, u32[]{:S(2)}, u32[]{:S(2)}) collective-permute-start(bf16[384,512]{1,0:T(8,128)(2,1)S(1)} %collective-permute-done.3.refs_0_), channel_id=1, source_target_pairs={{0,2},{1,3},{2,0},{3,1},{4,6},{5,7},{6,4},{7,5},{8,10},{9,11},{10,... | collective-permute-start | bytes 1179656 | tf_op jit(solution)/shard_map/ppermute | solution.py:312
  15.1 0.0 collective-permute-start.2
  15.1 0.0 collective-permute-done.refs_0_
  15.1 0.5 collective-permute-start.1
  15.6 0.7 %reshape.28.refs_2_.refs_1_ = f32[4,512]{1,0:T(4,128)S(1)} reshape(bf16[2048]{0:T(1024)(128)(2,1)} %param.9) | data formatting | bytes 12288 | tf_op jit(solution)/shard_map/reshape | solution.py:358
  16.3 0.0 collective-permute-start.6
  16.3 7.3 %collective-permute-done.4.refs_0_ = bf16[384,512]{1,0:T(8,128)(2,1)S(1)} collective-permute-done((bf16[384,512]{1,0:T(8,128)(2,1)S(1)}, bf16[384,512]{1,0:T(8,128)(2,1)S(1)}, u32[]{:S(2)}, u32[]{:S(2)}) %collective-permute-start.4) | collective-permute-done | bytes 393248 | tf_op jit(solution)/shard_map/ppermute | solution.py:312
  23.6 0.0 collective-permute-start.5
  23.6 1.4 %multiply_sine_fusion = (f32[384,64]{1,0:T(8,128)S(1)}, f32[384,64]{1,0:T(8,128)S(1)}, f32[384,64]{1,0:T(8,128)S(1)}, f32[384,64]{1,0:T(8,128)S(1)}) fusion(f32[384]{0:T(512)S(1)} %get-tuple-element.80, f32[64]{0:T(128)S(1)} %multiply_power_fusion, f32[384]{0:T(512)S(1)} %get-tuple-element.81), kind=kLoop, calls=%fused_computation | loop fusion | flops 49152 | bytes 396544 | tf_op jit(solution)/shard_map/sin | solution.py:337
  25.0 0.0 collective-permute-done.2.refs_1_
  25.0 2.9 %shard_map.95 = (f32[384,256]{1,0:T(8,128)S(1)}, f32[384,256]{1,0:T(8,128)S(1)}, f32[384,256]{1,0:T(8,128)S(1)}, f32[384,128]{1,0:T(8,128)S(1)}, f32[2,128]{1,0:...) custom-call(bf16[384,512]{1,0:T(8,128)(2,1)} %refs_0_.1, ...), custom_call_target="tpu_custom_call" | custom-call | tf_op jit(solution)/shard_map/pallas_call | solution.py:30
  27.9 0.0 collective-permute-done.1.refs_1_
  27.9 1.2 %shard_map.96 = (bf16[384,256]{1,0:T(8,128)(2,1)S(1)}, bf16[2,384,256]{2,1,0:T(8,128)(2,1)S(1)}) custom-call(bf16[384,512]{1,0:T(8,128)(2,1)S(1)} %collective-permute-done.refs_0_, bf16[384,512]{1,0:T(8,128)(2,1)S(1)} %collective-permute-done.1.refs_1_, f32[4,512]{1,0:T(4,128)S(1)} %reshape.28.refs_2_.refs_1_, ...), custom_call_target="tpu_custom_call" | custom-call | tf_op jit(solution)/shard_map/pallas_call | solution.py:30
  29.2 2.3 %collective-permute-start.7 = (bf16[384,256]{1,0:T(8,128)(2,1)S(1)}, bf16[384,256]{1,0:T(8,128)(2,1)S(1)}, u32[]{:S(2)}, u32[]{:S(2)}) collective-permute-start(bf16[384,256]{1,0:T(8,128)(2,1)S(1)} %get-tuple-element.47.q), channel_id=1, source_target_pairs={{12,4},{13,5},{14,6},{15,7},{28,20},{29,21},{30,22},{31,23}} | collective-permute-start | bytes 589832 | tf_op jit(solution)/shard_map/ppermute | solution.py:316
  31.4 0.7 collective-permute-start.8
  32.1 0.0 collective-permute-done.6.refs_1_
  32.1 0.6 shard_map.97
  32.7 0.4 shard_map.98
  33.1 3.1 %collective-permute-done.7.refs_10_ = bf16[384,256]{1,0:T(8,128)(2,1)S(1)} collective-permute-done((bf16[384,256]{1,0:T(8,128)(2,1)S(1)}, bf16[384,256]{1,0:T(8,128)(2,1)S(1)}, u32[]{:S(2)}, u32[]{:S(2)}) %collective-permute-start.7) | collective-permute-done | bytes 196640 | tf_op jit(solution)/shard_map/ppermute | solution.py:316
  36.2 0.0 collective-permute-done.5.refs_0_
  36.2 1.3 %collective-permute-start.9 = (bf16[384,256]{1,0:T(8,128)(2,1)S(1)}, bf16[384,256]{1,0:T(8,128)(2,1)S(1)}, u32[]{:S(2)}, u32[]{:S(2)}) collective-permute-start(bf16[384,256]{1,0:T(8,128)(2,1)S(1)} %get-tuple-element.63), channel_id=1, source_target_pairs={{4,12},{5,13},{6,14},{7,15},{20,28},{21,29},{22,30},{23,31}} | collective-permute-start | bytes 589832 | tf_op jit(solution)/shard_map/ppermute | solution.py:316
  37.5 1.3 %collective-permute-start.10 = (f32[8,384]{1,0:T(8,128)S(1)}, f32[8,384]{1,0:T(8,128)S(1)}, u32[]{:S(2)}, u32[]{:S(2)}) collective-permute-start(f32[8,384]{1,0:T(8,128)S(1)} %get-tuple-element.64), channel_id=1, source_target_pairs={{4,12},{5,13},{6,14},{7,15},{20,28},{21,29},{22,30},{23,31}} | collective-permute-start | bytes 36872 | tf_op jit(solution)/shard_map/ppermute | solution.py:316
  38.8 2.0 %shard_map.100 = (f32[384,256]{1,0:T(8,128)S(1)}, f32[384,256]{1,0:T(8,128)S(1)}, f32[384,256]{1,0:T(8,128)S(1)}) custom-call(bf16[384,256]{1,0:T(8,128)(2,1)S(1)} %get-tuple-element.47.q, bf16[2,384,256]{2,1,0:T(8,128)(2,1)S(1)} %get-tuple-element.48.refs_11_.kv, f32[384,384]{1,0:T(8,128)S(1)} %get-tuple-element.49.bias, ...), custom_call_target="tpu_custom_call" | custom-call | tf_op jit(solution)/shard_map/pallas_call | solution.py:30
  40.8 0.0 collective-permute-done.8.refs_3_
  40.8 7.7 %collective-permute-done.10.refs_6_ = f32[8,384]{1,0:T(8,128)S(1)} collective-permute-done((f32[8,384]{1,0:T(8,128)S(1)}, f32[8,384]{1,0:T(8,128)S(1)}, u32[]{:S(2)}, u32[]{:S(2)}) %collective-permute-start.10) | collective-permute-done | bytes 12320 | tf_op jit(solution)/shard_map/ppermute | solution.py:316
  48.5 0.0 collective-permute-done.9.refs_5_
  48.5 0.3 shard_map.101
  48.8 1.5 %collective-permute-start.13 = (bf16[384,256]{1,0:T(8,128)(2,1)S(1)}, bf16[384,256]{1,0:T(8,128)(2,1)S(1)}, u32[]{:S(2)}, u32[]{:S(2)}) collective-permute-start(bf16[384,256]{1,0:T(8,128)(2,1)S(1)} %get-tuple-element.66.refs_0_), channel_id=1, source_target_pairs={{0,2},{1,3},{2,0},{3,1},{4,6},{5,7},{6,4},{7,5},{8,10},{9,11},{10,... | collective-permute-start | bytes 589832 | tf_op jit(solution)/shard_map/ppermute | solution.py:312
  50.4 0.0 collective-permute-start.12
  50.4 0.7 collective-permute-start.15
  51.0 1.1 %collective-permute-start.16 = (bf16[128,512]{1,0:T(8,128)(2,1)S(1)}, bf16[128,512]{1,0:T(8,128)(2,1)S(1)}, u32[]{:S(2)}, u32[]{:S(2)}) collective-permute-start(bf16[128,512]{1,0:T(8,128)(2,1)S(1)} %get-tuple-element.71), channel_id=1, source_target_pairs={{0,3},{1,2},{2,1},{3,0},{16,18},{17,19},{18,16},{19,17},{4,7},{5,6... | collective-permute-start | bytes 393224 | tf_op jit(solution)/shard_map/ppermute | solution.py:465
  52.1 0.5 collective-permute-start.11
  52.6 4.0 %collective-permute-done.13.refs_0_ = bf16[384,256]{1,0:T(8,128)(2,1)S(1)} collective-permute-done((bf16[384,256]{1,0:T(8,128)(2,1)S(1)}, bf16[384,256]{1,0:T(8,128)(2,1)S(1)}, u32[]{:S(2)}, u32[]{:S(2)}) %collective-permute-start.13) | collective-permute-done | bytes 196640 | tf_op jit(solution)/shard_map/ppermute | solution.py:312
  56.7 0.0 collective-permute-start.14
  56.7 1.8 %collective-permute-done.15.refs_2_ = bf16[128,512]{1,0:T(8,128)(2,1)S(1)} collective-permute-done((bf16[128,512]{1,0:T(8,128)(2,1)S(1)}, bf16[128,512]{1,0:T(8,128)(2,1)S(1)}, u32[]{:S(2)}, u32[]{:S(2)}) %collective-permute-start.15) | collective-permute-done | bytes 131104 | tf_op jit(solution)/shard_map/ppermute | solution.py:463
  58.5 2.5 %collective-permute-start.17 = (bf16[128,512]{1,0:T(8,128)(2,1)S(1)}, bf16[128,512]{1,0:T(8,128)(2,1)S(1)}, u32[]{:S(2)}, u32[]{:S(2)}) collective-permute-start(bf16[128,512]{1,0:T(8,128)(2,1)S(1)} %collective-permute-done.15.refs_2_), channel_id=1, source_target_pairs={{0,16},{16,0},{1,17},{17,1},{2,18},{18,2},{3,19},{19,3},{4,20},{20... | collective-permute-start | bytes 393224 | tf_op jit(solution)/shard_map/ppermute | solution.py:464
  61.0 0.0 collective-permute-done.16.refs_3_
  61.0 1.7 %collective-permute-start.18 = (bf16[128,512]{1,0:T(8,128)(2,1)S(1)}, bf16[128,512]{1,0:T(8,128)(2,1)S(1)}, u32[]{:S(2)}, u32[]{:S(2)}) collective-permute-start(bf16[128,512]{1,0:T(8,128)(2,1)S(1)} %collective-permute-done.16.refs_3_), channel_id=1, source_target_pairs={{0,16},{16,0},{1,17},{17,1},{2,18},{18,2},{3,19},{19,3},{4,20},{20... | collective-permute-start | bytes 393224 | tf_op jit(solution)/shard_map/ppermute | solution.py:484
  62.7 0.0 collective-permute-done.12.refs_3_
  62.7 0.0 collective-permute-done.11.refs_1_
  62.7 0.9 %shard_map.102 = (f32[384,512]{1,0:T(8,128)S(1)}, f32[2,384]{1,0:T(2,128)}) custom-call(f32[384,256]{1,0:T(8,128)S(1)} %get-tuple-element.65.logs, bf16[384,256]{1,0:T(8,128)(2,1)S(1)} %get-tuple-element.66.refs_0_, bf16[384,256]{1,0:T(8,128)(2,1)S(1)} %collective-permute-done.11.refs_1_, bf16[256,512]{1,0:T(8,128)(2,1)S(1)} %get-tuple-element.67.refs_2_, ...), custom_call_target="tpu_custom_call" | custom-call | tf_op jit(solution)/shard_map/pallas_call | solution.py:30
  63.5 1.8 %collective-permute-done.17.refs_4_ = bf16[128,512]{1,0:T(8,128)(2,1)S(1)} collective-permute-done((bf16[128,512]{1,0:T(8,128)(2,1)S(1)}, bf16[128,512]{1,0:T(8,128)(2,1)S(1)}, u32[]{:S(2)}, u32[]{:S(2)}) %collective-permute-start.17) | collective-permute-done | bytes 131104 | tf_op jit(solution)/shard_map/ppermute | solution.py:464
  65.3 2.5 %collective-permute-done.18.refs_5_ = bf16[128,512]{1,0:T(8,128)(2,1)S(1)} collective-permute-done((bf16[128,512]{1,0:T(8,128)(2,1)S(1)}, bf16[128,512]{1,0:T(8,128)(2,1)S(1)}, u32[]{:S(2)}, u32[]{:S(2)}) %collective-permute-start.18) | collective-permute-done | bytes 131104 | tf_op jit(solution)/shard_map/ppermute | solution.py:484
  67.8 0.0 collective-permute-done.14.refs_1_
  67.8 1.1 %shard_map.103 = bf16[384,512]{1,0:T(8,128)(2,1)} custom-call(f32[384,512]{1,0:T(8,128)S(1)} %get-tuple-element.69.before, bf16[384,256]{1,0:T(8,128)(2,1)S(1)} %collective-permute-done.13.refs_0_, bf16[384,256]{1,0:T(8,128)(2,1)S(1)} %collective-permute-done.14.refs_1_, bf16[128,512]{1,0:T(8,128)(2,1)S(1)} %collective-permute-done.15.refs_2_, ...), custom_call_target="tpu_custom_call" | custom-call | tf_op jit(solution)/shard_map/pallas_call | solution.py:30
  (3 shorter events, 0.0 us)
Async XLA Ops:
  0.6 13.0 %collective-permute-start.3 = (bf16[384,512]{1,0:T(8,128)(2,1)}, bf16[384,512]{1,0:T(8,128)(2,1)S(1)}, u32[]{:S(2)}, u32[]{:S(2)}) collective-permute-start(bf16[384,512]{1,0:T(8,128)(2,1)} %refs_0_.1), channel_id=1, source_target_pairs={{0,4},{4,8},{8,12},{1,5},{5,9},{9,13},{2,6},{6,10},{10,14},{3,7},{... | collective-permute-start | bytes 1179656 | tf_op jit(solution)/shard_map/ppermute | solution.py:316
  1.9 13.2 %collective-permute-start = (bf16[384,512]{1,0:T(8,128)(2,1)}, bf16[384,512]{1,0:T(8,128)(2,1)S(1)}, u32[]{:S(2)}, u32[]{:S(2)}) collective-permute-start(bf16[384,512]{1,0:T(8,128)(2,1)} %refs_0_.1), channel_id=1, source_target_pairs={{0,2},{1,3},{2,0},{3,1},{4,6},{5,7},{6,4},{7,5},{8,10},{9,11},{10,... | collective-permute-start | bytes 1179656 | tf_op jit(solution)/shard_map/ppermute | solution.py:312
  13.6 10.0 %collective-permute-start.4 = (bf16[384,512]{1,0:T(8,128)(2,1)S(1)}, bf16[384,512]{1,0:T(8,128)(2,1)S(1)}, u32[]{:S(2)}, u32[]{:S(2)}) collective-permute-start(bf16[384,512]{1,0:T(8,128)(2,1)S(1)} %collective-permute-done.3.refs_0_), channel_id=1, source_target_pairs={{0,2},{1,3},{2,0},{3,1},{4,6},{5,7},{6,4},{7,5},{8,10},{9,11},{10,... | collective-permute-start | bytes 1179656 | tf_op jit(solution)/shard_map/ppermute | solution.py:312
  15.1 10.0 %collective-permute-start.2 = (bf16[384,512]{1,0:T(8,128)(2,1)}, bf16[384,512]{1,0:T(8,128)(2,1)S(1)}, u32[]{:S(2)}, u32[]{:S(2)}) collective-permute-start(bf16[384,512]{1,0:T(8,128)(2,1)} %refs_0_.1), channel_id=1, source_target_pairs={{0,1},{1,0},{2,3},{3,2},{4,5},{5,4},{6,7},{7,6},{8,9},{9,8},{10,11... | collective-permute-start | bytes 1179656 | tf_op jit(solution)/shard_map/ppermute | solution.py:312
  15.1 12.9 %collective-permute-start.1 = (bf16[384,512]{1,0:T(8,128)(2,1)S(1)}, bf16[384,512]{1,0:T(8,128)(2,1)S(1)}, u32[]{:S(2)}, u32[]{:S(2)}) collective-permute-start(bf16[384,512]{1,0:T(8,128)(2,1)S(1)} %collective-permute-done.refs_0_), channel_id=1, source_target_pairs={{0,1},{1,0},{2,3},{3,2},{4,5},{5,4},{6,7},{7,6},{8,9},{9,8},{10,11... | collective-permute-start | bytes 1179656 | tf_op jit(solution)/shard_map/ppermute | solution.py:312
  16.3 15.8 %collective-permute-start.6 = (bf16[384,512]{1,0:T(8,128)(2,1)S(1)}, bf16[384,512]{1,0:T(8,128)(2,1)S(1)}, u32[]{:S(2)}, u32[]{:S(2)}) collective-permute-start(bf16[384,512]{1,0:T(8,128)(2,1)S(1)} %collective-permute-done.3.refs_0_), channel_id=1, source_target_pairs={{0,1},{1,0},{2,3},{3,2},{4,5},{5,4},{6,7},{7,6},{8,9},{9,8},{10,11... | collective-permute-start | bytes 1179656 | tf_op jit(solution)/shard_map/ppermute | solution.py:312
  23.6 12.6 %collective-permute-start.5 = (bf16[384,512]{1,0:T(8,128)(2,1)S(1)}, bf16[384,512]{1,0:T(8,128)(2,1)S(1)}, u32[]{:S(2)}, u32[]{:S(2)}) collective-permute-start(bf16[384,512]{1,0:T(8,128)(2,1)S(1)} %collective-permute-done.4.refs_0_), channel_id=1, source_target_pairs={{0,1},{1,0},{2,3},{3,2},{4,5},{5,4},{6,7},{7,6},{8,9},{9,8},{10,11... | collective-permute-start | bytes 1179656 | tf_op jit(solution)/shard_map/ppermute | solution.py:312
  29.2 7.1 %collective-permute-start.7 = (bf16[384,256]{1,0:T(8,128)(2,1)S(1)}, bf16[384,256]{1,0:T(8,128)(2,1)S(1)}, u32[]{:S(2)}, u32[]{:S(2)}) collective-permute-start(bf16[384,256]{1,0:T(8,128)(2,1)S(1)} %get-tuple-element.47.q), channel_id=1, source_target_pairs={{12,4},{13,5},{14,6},{15,7},{28,20},{29,21},{30,22},{31,23}} | collective-permute-start | bytes 589832 | tf_op jit(solution)/shard_map/ppermute | solution.py:316
  31.4 9.4 %collective-permute-start.8 = (bf16[2,384,256]{2,1,0:T(8,128)(2,1)S(1)}, bf16[2,384,256]{2,1,0:T(8,128)(2,1)S(1)}, u32[]{:S(2)}, u32[]{:S(2)}) collective-permute-start(bf16[2,384,256]{2,1,0:T(8,128)(2,1)S(1)} %get-tuple-element.48.refs_11_.kv), channel_id=1, source_target_pairs={{0,8},{1,9},{2,10},{3,11},{16,24},{17,25},{18,26},{19,27}} | collective-permute-start | bytes 1179656 | tf_op jit(solution)/shard_map/ppermute | solution.py:316
  36.2 12.3 %collective-permute-start.9 = (bf16[384,256]{1,0:T(8,128)(2,1)S(1)}, bf16[384,256]{1,0:T(8,128)(2,1)S(1)}, u32[]{:S(2)}, u32[]{:S(2)}) collective-permute-start(bf16[384,256]{1,0:T(8,128)(2,1)S(1)} %get-tuple-element.63), channel_id=1, source_target_pairs={{4,12},{5,13},{6,14},{7,15},{20,28},{21,29},{22,30},{23,31}} | collective-permute-start | bytes 589832 | tf_op jit(solution)/shard_map/ppermute | solution.py:316
  37.5 11.0 %collective-permute-start.10 = (f32[8,384]{1,0:T(8,128)S(1)}, f32[8,384]{1,0:T(8,128)S(1)}, u32[]{:S(2)}, u32[]{:S(2)}) collective-permute-start(f32[8,384]{1,0:T(8,128)S(1)} %get-tuple-element.64), channel_id=1, source_target_pairs={{4,12},{5,13},{6,14},{7,15},{20,28},{21,29},{22,30},{23,31}} | collective-permute-start | bytes 36872 | tf_op jit(solution)/shard_map/ppermute | solution.py:316
  48.8 7.8 %collective-permute-start.13 = (bf16[384,256]{1,0:T(8,128)(2,1)S(1)}, bf16[384,256]{1,0:T(8,128)(2,1)S(1)}, u32[]{:S(2)}, u32[]{:S(2)}) collective-permute-start(bf16[384,256]{1,0:T(8,128)(2,1)S(1)} %get-tuple-element.66.refs_0_), channel_id=1, source_target_pairs={{0,2},{1,3},{2,0},{3,1},{4,6},{5,7},{6,4},{7,5},{8,10},{9,11},{10,... | collective-permute-start | bytes 589832 | tf_op jit(solution)/shard_map/ppermute | solution.py:312
  50.4 12.3 %collective-permute-start.12 = (bf16[256,512]{1,0:T(8,128)(2,1)S(1)}, bf16[256,512]{1,0:T(8,128)(2,1)S(1)}, u32[]{:S(2)}, u32[]{:S(2)}) collective-permute-start(bf16[256,512]{1,0:T(8,128)(2,1)S(1)} %get-tuple-element.68), channel_id=1, source_target_pairs={{0,1},{1,0},{2,3},{3,2},{4,5},{5,4},{6,7},{7,6},{8,9},{9,8},{10,11... | collective-permute-start | bytes 786440 | tf_op jit(solution)/shard_map/ppermute | solution.py:312
  50.4 8.1 %collective-permute-start.15 = (bf16[128,512]{1,0:T(8,128)(2,1)S(1)}, bf16[128,512]{1,0:T(8,128)(2,1)S(1)}, u32[]{:S(2)}, u32[]{:S(2)}) collective-permute-start(bf16[128,512]{1,0:T(8,128)(2,1)S(1)} %get-tuple-element.70), channel_id=1, source_target_pairs={{0,3},{1,2},{2,1},{3,0},{16,18},{17,19},{18,16},{19,17},{4,7},{5,6... | collective-permute-start | bytes 393224 | tf_op jit(solution)/shard_map/ppermute | solution.py:463
  51.0 10.0 %collective-permute-start.16 = (bf16[128,512]{1,0:T(8,128)(2,1)S(1)}, bf16[128,512]{1,0:T(8,128)(2,1)S(1)}, u32[]{:S(2)}, u32[]{:S(2)}) collective-permute-start(bf16[128,512]{1,0:T(8,128)(2,1)S(1)} %get-tuple-element.71), channel_id=1, source_target_pairs={{0,3},{1,2},{2,1},{3,0},{16,18},{17,19},{18,16},{19,17},{4,7},{5,6... | collective-permute-start | bytes 393224 | tf_op jit(solution)/shard_map/ppermute | solution.py:465
  52.1 10.5 %collective-permute-start.11 = (bf16[384,256]{1,0:T(8,128)(2,1)S(1)}, bf16[384,256]{1,0:T(8,128)(2,1)S(1)}, u32[]{:S(2)}, u32[]{:S(2)}) collective-permute-start(bf16[384,256]{1,0:T(8,128)(2,1)S(1)} %get-tuple-element.66.refs_0_), channel_id=1, source_target_pairs={{0,1},{1,0},{2,3},{3,2},{4,5},{5,4},{6,7},{7,6},{8,9},{9,8},{10,11... | collective-permute-start | bytes 589832 | tf_op jit(solution)/shard_map/ppermute | solution.py:312
  56.7 11.1 %collective-permute-start.14 = (bf16[384,256]{1,0:T(8,128)(2,1)S(1)}, bf16[384,256]{1,0:T(8,128)(2,1)S(1)}, u32[]{:S(2)}, u32[]{:S(2)}) collective-permute-start(bf16[384,256]{1,0:T(8,128)(2,1)S(1)} %collective-permute-done.13.refs_0_), channel_id=1, source_target_pairs={{0,1},{1,0},{2,3},{3,2},{4,5},{5,4},{6,7},{7,6},{8,9},{9,8},{10,11... | collective-permute-start | bytes 589832 | tf_op jit(solution)/shard_map/ppermute | solution.py:312
  58.5 6.9 %collective-permute-start.17 = (bf16[128,512]{1,0:T(8,128)(2,1)S(1)}, bf16[128,512]{1,0:T(8,128)(2,1)S(1)}, u32[]{:S(2)}, u32[]{:S(2)}) collective-permute-start(bf16[128,512]{1,0:T(8,128)(2,1)S(1)} %collective-permute-done.15.refs_2_), channel_id=1, source_target_pairs={{0,16},{16,0},{1,17},{17,1},{2,18},{18,2},{3,19},{19,3},{4,20},{20... | collective-permute-start | bytes 393224 | tf_op jit(solution)/shard_map/ppermute | solution.py:464
  61.0 6.8 %collective-permute-start.18 = (bf16[128,512]{1,0:T(8,128)(2,1)S(1)}, bf16[128,512]{1,0:T(8,128)(2,1)S(1)}, u32[]{:S(2)}, u32[]{:S(2)}) collective-permute-start(bf16[128,512]{1,0:T(8,128)(2,1)S(1)} %collective-permute-done.16.refs_3_), channel_id=1, source_target_pairs={{0,16},{16,0},{1,17},{17,1},{2,18},{18,2},{3,19},{19,3},{4,20},{20... | collective-permute-start | bytes 393224 | tf_op jit(solution)/shard_map/ppermute | solution.py:484

commit v12 on v10

--- a/solution.py
+++ b/solution.py
@@ -370,11 +370,12 @@
     copies = lax.axis_size("grp")
     shared = copies == 2 and count == 4
 
-    cut = w_out.shape[0] // 2 if shared else w_out.shape[0]
+    cut = w_out.shape[0] * 3 // 8 if shared else w_out.shape[0]
     piece_keys = tuple((k, 0) for k in range(half))
     piece_keys += ((None, 0), (None, cut)) if shared else tuple((k, 0) for k in late)
     piece_shapes = [shape_of((w_out.shape[0], columns), w_out.dtype)] * half
-    piece_shapes += [shape_of((cut, columns), w_out.dtype)] * (len(piece_keys) - half)
+    sizes = (cut, w_out.shape[0] - cut) if shared else (cut,) * len(late)
+    piece_shapes += [shape_of((size, columns), w_out.dtype) for size in sizes]
     across = swap(hidden, half)
     before = behind(hidden, 1)
     own_near = near_blocks(hidden)

time: 70.1 us -> 69 us (0.984)
  waiting for transfers between devices: 40.8 us -> 38.8 us
  starting transfers between devices: 16.7 us -> 17.7 us
    ppermute x1, waiting for transfers between devices: 3.05 us -> 0.01 us  [layer(): first_half = lax.ppermute(far_slice[0], ('grp', 'tp'), routes)]
    ppermute x1, starting transfers between devices: 0.02 us -> 2.51 us  [layer(): last_other = lax.ppermute(later, 'grp', [(0, 1), (1, 0)])]
    ppermute x1, waiting for transfers between devices: 2.17 us -> 0.01 us  [layer(): last_other = lax.ppermute(later, 'grp', [(0, 1), (1, 0)])]
    ppermute x1, waiting for transfers between devices: 0.01 us -> 2 us  [layer(): last_half = lax.ppermute(far_slice[1], ('grp', 'tp'), routes)]
    ppermute x1, starting transfers between devices: 2.51 us -> 1.05 us  [layer(): first_other = lax.ppermute(first_half, 'grp', [(0, 1), (1, 0)])]
    ppermute x1, waiting for transfers between devices: 3.45 us -> 4.58 us  [layer(): first_other = lax.ppermute(first_half, 'grp', [(0, 1), (1, 0)])]
  transfers between devices with their start and end apart: 19 -> 19, of which waited for: 8 -> 7; matrix products, arithmetic and copies ran while one was open for 3% -> 3% of each run, Pallas kernels for 11% -> 12%
where the time goes in v12:
time: 69 us; the launch traced here: 68.8 us
  waiting for transfers between devices  38.8 us (56%)
  starting transfers between devices  17.7 us (26%)
  Pallas kernels  9.42 us (14%)
  other arithmetic  1.45 us (2%)
  between operations  0.75 us (1%)
  local copies, waits for them, and re-layouts  0.7 us (1%)
    ppermute x5, waiting for transfers between devices, send(): return lax.ppermute(value, 'sp', pairs)  20.8 us
    ppermute x10, waiting for transfers between devices, swap(): return lax.ppermute(value, 'tp', [(i, i ^ distance) for i in range(count)])  11.3 us
    pallas_call x8, Pallas kernels, call(): pl.pallas_call(body, out_shape=tuple(outs), in_specs=[HBM if n in held el...  9.42 us
    ppermute x5, starting transfers between devices, send(): return lax.ppermute(value, 'sp', pairs)  6.81 us
    ppermute x10, starting transfers between devices, swap(): return lax.ppermute(value, 'tp', [(i, i ^ distance) for i in range(count)])  5.77 us
    ppermute x1, waiting for transfers between devices, layer(): first_other = lax.ppermute(first_half, 'grp', [(0, 1), (1, 0)])  4.58 us
    ppermute x1, starting transfers between devices, layer(): last_other = lax.ppermute(later, 'grp', [(0, 1), (1, 0)])  2.51 us
    ppermute x1, waiting for transfers between devices, layer(): last_half = lax.ppermute(far_slice[1], ('grp', 'tp'), routes)  2 us
  transfers between devices with their start and end apart: 19, of which 7 were waited for; matrix products, arithmetic and copies ran while one was open for 3% of the time, Pallas kernels for 12%

profile of v12, /device:TPU:24, one launch (start us, length us, event | category | flops | bytes accessed | tf_op | source)
XLA Modules:
  0.0 68.8 jit_solution(2937826336859656389)
XLA Ops:
  0.6 1.3 %collective-permute-start.3 = (bf16[384,512]{1,0:T(8,128)(2,1)}, bf16[384,512]{1,0:T(8,128)(2,1)S(1)}, u32[]{:S(2)}, u32[]{:S(2)}) collective-permute-start(bf16[384,512]{1,0:T(8,128)(2,1)} %refs_0_.1), channel_id=1, source_target_pairs={{0,4},{4,8},{8,12},{1,5},{5,9},{9,13},{2,6},{6,10},{10,14},{3,7},{... | collective-permute-start | bytes 1179656 | tf_op jit(solution)/shard_map/ppermute | solution.py:317
  1.9 1.6 %collective-permute-start = (bf16[384,512]{1,0:T(8,128)(2,1)}, bf16[384,512]{1,0:T(8,128)(2,1)S(1)}, u32[]{:S(2)}, u32[]{:S(2)}) collective-permute-start(bf16[384,512]{1,0:T(8,128)(2,1)} %refs_0_.1), channel_id=1, source_target_pairs={{0,2},{1,3},{2,0},{3,1},{4,6},{5,7},{6,4},{7,5},{8,10},{9,11},{10,... | collective-permute-start | bytes 1179656 | tf_op jit(solution)/shard_map/ppermute | solution.py:313
  3.5 10.1 %collective-permute-done.3.refs_0_ = bf16[384,512]{1,0:T(8,128)(2,1)S(1)} collective-permute-done((bf16[384,512]{1,0:T(8,128)(2,1)}, bf16[384,512]{1,0:T(8,128)(2,1)S(1)}, u32[]{:S(2)}, u32[]{:S(2)}) %collective-permute-start.3) | collective-permute-done | bytes 393248 | tf_op jit(solution)/shard_map/ppermute | solution.py:317
  13.6 1.5 %collective-permute-start.4 = (bf16[384,512]{1,0:T(8,128)(2,1)S(1)}, bf16[384,512]{1,0:T(8,128)(2,1)S(1)}, u32[]{:S(2)}, u32[]{:S(2)}) collective-permute-start(bf16[384,512]{1,0:T(8,128)(2,1)S(1)} %collective-permute-done.3.refs_0_), channel_id=1, source_target_pairs={{0,2},{1,3},{2,0},{3,1},{4,6},{5,7},{6,4},{7,5},{8,10},{9,11},{10,... | collective-permute-start | bytes 1179656 | tf_op jit(solution)/shard_map/ppermute | solution.py:313
  15.1 0.0 collective-permute-start.2
  15.1 0.0 collective-permute-done.refs_0_
  15.1 0.5 collective-permute-start.1
  15.6 0.7 %reshape.28.refs_2_ = f32[4,512]{1,0:T(4,128)S(1)} reshape(bf16[2048]{0:T(1024)(128)(2,1)} %param.9) | data formatting | bytes 12288 | tf_op jit(solution)/shard_map/reshape | solution.py:359
  16.3 0.0 collective-permute-start.6
  16.3 7.3 %collective-permute-done.4.refs_0_ = bf16[384,512]{1,0:T(8,128)(2,1)S(1)} collective-permute-done((bf16[384,512]{1,0:T(8,128)(2,1)S(1)}, bf16[384,512]{1,0:T(8,128)(2,1)S(1)}, u32[]{:S(2)}, u32[]{:S(2)}) %collective-permute-start.4) | collective-permute-done | bytes 393248 | tf_op jit(solution)/shard_map/ppermute | solution.py:313
  23.6 0.0 collective-permute-start.5
  23.6 1.4 %multiply_sine_fusion = (f32[384,64]{1,0:T(8,128)S(1)}, f32[384,64]{1,0:T(8,128)S(1)}, f32[384,64]{1,0:T(8,128)S(1)}, f32[384,64]{1,0:T(8,128)S(1)}) fusion(f32[384]{0:T(512)S(1)} %get-tuple-element.74, f32[64]{0:T(128)S(1)} %multiply_power_fusion, f32[384]{0:T(512)S(1)} %get-tuple-element.75), kind=kLoop, calls=%fused_computation | loop fusion | flops 49152 | bytes 396544 | tf_op jit(solution)/shard_map/sin | solution.py:338
  25.0 0.0 collective-permute-done.2.refs_1_
  25.0 2.9 %shard_map.95 = (f32[384,256]{1,0:T(8,128)S(1)}, f32[384,256]{1,0:T(8,128)S(1)}, f32[384,256]{1,0:T(8,128)S(1)}, f32[384,128]{1,0:T(8,128)S(1)}, f32[2,128]{1,0:...) custom-call(bf16[384,512]{1,0:T(8,128)(2,1)} %refs_0_.1, ...), custom_call_target="tpu_custom_call" | custom-call | tf_op jit(solution)/shard_map/pallas_call | solution.py:30
  27.9 0.0 collective-permute-done.1.refs_1_
  27.9 1.2 %shard_map.96 = (bf16[384,256]{1,0:T(8,128)(2,1)S(1)}, bf16[2,384,256]{2,1,0:T(8,128)(2,1)S(1)}) custom-call(bf16[384,512]{1,0:T(8,128)(2,1)S(1)} %collective-permute-done.refs_0_, bf16[384,512]{1,0:T(8,128)(2,1)S(1)} %collective-permute-done.1.refs_1_, f32[4,512]{1,0:T(4,128)S(1)} %reshape.28.refs_2_, bf16[2048,256]{1,0:T(8,128)(2,1)S(1)} %get-tuple-element.35.refs_3_, ...), custom_call_target="tpu_custom_call" | custom-call | tf_op jit(solution)/shard_map/pallas_call | solution.py:30
  29.2 2.3 %collective-permute-start.7 = (bf16[384,256]{1,0:T(8,128)(2,1)S(1)}, bf16[384,256]{1,0:T(8,128)(2,1)S(1)}, u32[]{:S(2)}, u32[]{:S(2)}) collective-permute-start(bf16[384,256]{1,0:T(8,128)(2,1)S(1)} %get-tuple-element.44.q), channel_id=1, source_target_pairs={{12,4},{13,5},{14,6},{15,7},{28,20},{29,21},{30,22},{31,23}} | collective-permute-start | bytes 589832 | tf_op jit(solution)/shard_map/ppermute | solution.py:317
  31.4 0.7 collective-permute-start.8
  32.1 0.0 collective-permute-done.6.refs_1_
  32.1 0.6 shard_map.97
  32.7 3.5 %collective-permute-done.7.refs_11_ = bf16[384,256]{1,0:T(8,128)(2,1)S(1)} collective-permute-done((bf16[384,256]{1,0:T(8,128)(2,1)S(1)}, bf16[384,256]{1,0:T(8,128)(2,1)S(1)}, u32[]{:S(2)}, u32[]{:S(2)}) %collective-permute-start.7) | collective-permute-done | bytes 196640 | tf_op jit(solution)/shard_map/ppermute | solution.py:317
  36.2 0.0 collective-permute-done.5.refs_1_
  36.2 1.3 %collective-permute-start.9 = (bf16[384,256]{1,0:T(8,128)(2,1)S(1)}, bf16[384,256]{1,0:T(8,128)(2,1)S(1)}, u32[]{:S(2)}, u32[]{:S(2)}) collective-permute-start(bf16[384,256]{1,0:T(8,128)(2,1)S(1)} %get-tuple-element.57), channel_id=1, source_target_pairs={{4,12},{5,13},{6,14},{7,15},{20,28},{21,29},{22,30},{23,31}} | collective-permute-start | bytes 589832 | tf_op jit(solution)/shard_map/ppermute | solution.py:317
  37.5 1.3 %collective-permute-start.10 = (f32[8,384]{1,0:T(8,128)S(1)}, f32[8,384]{1,0:T(8,128)S(1)}, u32[]{:S(2)}, u32[]{:S(2)}) collective-permute-start(f32[8,384]{1,0:T(8,128)S(1)} %get-tuple-element.58), channel_id=1, source_target_pairs={{4,12},{5,13},{6,14},{7,15},{20,28},{21,29},{22,30},{23,31}} | collective-permute-start | bytes 36872 | tf_op jit(solution)/shard_map/ppermute | solution.py:317
  38.8 2.5 %shard_map.99 = (f32[384,256]{1,0:T(8,128)S(1)}, f32[384,256]{1,0:T(8,128)S(1)}, f32[384,256]{1,0:T(8,128)S(1)}) custom-call(bf16[384,256]{1,0:T(8,128)(2,1)S(1)} %get-tuple-element.44.q, bf16[2,384,256]{2,1,0:T(8,128)(2,1)S(1)} %get-tuple-element.45.refs_12_.kv, f32[384,384]{1,0:T(8,128)S(1)} %get-tuple-element.46.bias, ...), custom_call_target="tpu_custom_call" | custom-call | tf_op jit(solution)/shard_map/pallas_call | solution.py:30
  41.3 0.0 collective-permute-done.8.refs_3_
  41.3 7.2 %collective-permute-done.10.refs_6_ = f32[8,384]{1,0:T(8,128)S(1)} collective-permute-done((f32[8,384]{1,0:T(8,128)S(1)}, f32[8,384]{1,0:T(8,128)S(1)}, u32[]{:S(2)}, u32[]{:S(2)}) %collective-permute-start.10) | collective-permute-done | bytes 12320 | tf_op jit(solution)/shard_map/ppermute | solution.py:317
  48.5 0.0 collective-permute-done.9.refs_5_
  48.5 0.3 shard_map.100
  48.8 1.6 %collective-permute-start.13 = (bf16[384,256]{1,0:T(8,128)(2,1)S(1)}, bf16[384,256]{1,0:T(8,128)(2,1)S(1)}, u32[]{:S(2)}, u32[]{:S(2)}) collective-permute-start(bf16[384,256]{1,0:T(8,128)(2,1)S(1)} %get-tuple-element.60.refs_0_), channel_id=1, source_target_pairs={{0,2},{1,3},{2,0},{3,1},{4,6},{5,7},{6,4},{7,5},{8,10},{9,11},{10,... | collective-permute-start | bytes 589832 | tf_op jit(solution)/shard_map/ppermute | solution.py:313
  50.4 0.0 collective-permute-start.16
  50.4 0.6 collective-permute-start.12
  51.0 0.0 collective-permute-start.11
  51.0 1.6 %collective-permute-start.15 = (bf16[96,512]{1,0:T(8,128)(2,1)S(1)}, bf16[96,512]{1,0:T(8,128)(2,1)S(1)}, u32[]{:S(2)}, u32[]{:S(2)}) collective-permute-start(bf16[96,512]{1,0:T(8,128)(2,1)S(1)} %get-tuple-element.64), channel_id=1, source_target_pairs={{0,3},{1,2},{2,1},{3,0},{16,18},{17,19},{18,16},{19,17},{4,7},{5,6... | collective-permute-start | bytes 294920 | tf_op jit(solution)/shard_map/ppermute | solution.py:460
  52.6 4.0 %collective-permute-done.13.refs_0_ = bf16[384,256]{1,0:T(8,128)(2,1)S(1)} collective-permute-done((bf16[384,256]{1,0:T(8,128)(2,1)S(1)}, bf16[384,256]{1,0:T(8,128)(2,1)S(1)}, u32[]{:S(2)}, u32[]{:S(2)}) %collective-permute-start.13) | collective-permute-done | bytes 196640 | tf_op jit(solution)/shard_map/ppermute | solution.py:313
  56.7 0.0 collective-permute-start.14
  56.7 2.0 %collective-permute-done.16.refs_3_ = bf16[160,512]{1,0:T(8,128)(2,1)S(1)} collective-permute-done((bf16[160,512]{1,0:T(8,128)(2,1)S(1)}, bf16[160,512]{1,0:T(8,128)(2,1)S(1)}, u32[]{:S(2)}, u32[]{:S(2)}) %collective-permute-start.16) | collective-permute-done | bytes 163872 | tf_op jit(solution)/shard_map/ppermute | solution.py:462
  58.7 2.5 %collective-permute-start.18 = (bf16[160,512]{1,0:T(8,128)(2,1)S(1)}, bf16[160,512]{1,0:T(8,128)(2,1)S(1)}, u32[]{:S(2)}, u32[]{:S(2)}) collective-permute-start(bf16[160,512]{1,0:T(8,128)(2,1)S(1)} %collective-permute-done.16.refs_3_), channel_id=1, source_target_pairs={{0,16},{16,0},{1,17},{17,1},{2,18},{18,2},{3,19},{19,3},{4,20},{20... | collective-permute-start | bytes 491528 | tf_op jit(solution)/shard_map/ppermute | solution.py:481
  61.2 0.0 collective-permute-done.15.refs_2_
  61.2 1.0 %collective-permute-start.17 = (bf16[96,512]{1,0:T(8,128)(2,1)S(1)}, bf16[96,512]{1,0:T(8,128)(2,1)S(1)}, u32[]{:S(2)}, u32[]{:S(2)}) collective-permute-start(bf16[96,512]{1,0:T(8,128)(2,1)S(1)} %collective-permute-done.15.refs_2_), channel_id=1, source_target_pairs={{0,16},{16,0},{1,17},{17,1},{2,18},{18,2},{3,19},{19,3},{4,20},{20... | collective-permute-start | bytes 294920 | tf_op jit(solution)/shard_map/ppermute | solution.py:461
  62.2 0.0 collective-permute-done.12.refs_3_
  62.2 0.0 collective-permute-done.11.refs_1_
  62.2 0.9 %shard_map.101 = (f32[384,512]{1,0:T(8,128)S(1)}, f32[2,384]{1,0:T(2,128)}) custom-call(f32[384,256]{1,0:T(8,128)S(1)} %get-tuple-element.59.logs, bf16[384,256]{1,0:T(8,128)(2,1)S(1)} %get-tuple-element.60.refs_0_, bf16[384,256]{1,0:T(8,128)(2,1)S(1)} %collective-permute-done.11.refs_1_, bf16[256,512]{1,0:T(8,128)(2,1)S(1)} %get-tuple-element.61.refs_2_, ...), custom_call_target="tpu_custom_call" | custom-call | tf_op jit(solution)/shard_map/pallas_call | solution.py:30
  63.1 4.6 %collective-permute-done.17.refs_4_ = bf16[96,512]{1,0:T(8,128)(2,1)S(1)} collective-permute-done((bf16[96,512]{1,0:T(8,128)(2,1)S(1)}, bf16[96,512]{1,0:T(8,128)(2,1)S(1)}, u32[]{:S(2)}, u32[]{:S(2)}) %collective-permute-start.17) | collective-permute-done | bytes 98336 | tf_op jit(solution)/shard_map/ppermute | solution.py:461
  67.7 0.0 collective-permute-done.18.refs_5_
  67.7 0.0 collective-permute-done.14.refs_1_
  67.7 1.1 %shard_map.102 = bf16[384,512]{1,0:T(8,128)(2,1)} custom-call(f32[384,512]{1,0:T(8,128)S(1)} %get-tuple-element.63.before, bf16[384,256]{1,0:T(8,128)(2,1)S(1)} %collective-permute-done.13.refs_0_, bf16[384,256]{1,0:T(8,128)(2,1)S(1)} %collective-permute-done.14.refs_1_, bf16[96,512]{1,0:T(8,128)(2,1)S(1)} %collective-permute-done.15.refs_2_, ...), custom_call_target="tpu_custom_call" | custom-call | tf_op jit(solution)/shard_map/pallas_call | solution.py:30
  (3 shorter events, 0.0 us)
Async XLA Ops:
  0.6 13.0 %collective-permute-start.3 = (bf16[384,512]{1,0:T(8,128)(2,1)}, bf16[384,512]{1,0:T(8,128)(2,1)S(1)}, u32[]{:S(2)}, u32[]{:S(2)}) collective-permute-start(bf16[384,512]{1,0:T(8,128)(2,1)} %refs_0_.1), channel_id=1, source_target_pairs={{0,4},{4,8},{8,12},{1,5},{5,9},{9,13},{2,6},{6,10},{10,14},{3,7},{... | collective-permute-start | bytes 1179656 | tf_op jit(solution)/shard_map/ppermute | solution.py:317
  1.9 13.2 %collective-permute-start = (bf16[384,512]{1,0:T(8,128)(2,1)}, bf16[384,512]{1,0:T(8,128)(2,1)S(1)}, u32[]{:S(2)}, u32[]{:S(2)}) collective-permute-start(bf16[384,512]{1,0:T(8,128)(2,1)} %refs_0_.1), channel_id=1, source_target_pairs={{0,2},{1,3},{2,0},{3,1},{4,6},{5,7},{6,4},{7,5},{8,10},{9,11},{10,... | collective-permute-start | bytes 1179656 | tf_op jit(solution)/shard_map/ppermute | solution.py:313
  13.6 10.0 %collective-permute-start.4 = (bf16[384,512]{1,0:T(8,128)(2,1)S(1)}, bf16[384,512]{1,0:T(8,128)(2,1)S(1)}, u32[]{:S(2)}, u32[]{:S(2)}) collective-permute-start(bf16[384,512]{1,0:T(8,128)(2,1)S(1)} %collective-permute-done.3.refs_0_), channel_id=1, source_target_pairs={{0,2},{1,3},{2,0},{3,1},{4,6},{5,7},{6,4},{7,5},{8,10},{9,11},{10,... | collective-permute-start | bytes 1179656 | tf_op jit(solution)/shard_map/ppermute | solution.py:313
  15.1 10.0 %collective-permute-start.2 = (bf16[384,512]{1,0:T(8,128)(2,1)}, bf16[384,512]{1,0:T(8,128)(2,1)S(1)}, u32[]{:S(2)}, u32[]{:S(2)}) collective-permute-start(bf16[384,512]{1,0:T(8,128)(2,1)} %refs_0_.1), channel_id=1, source_target_pairs={{0,1},{1,0},{2,3},{3,2},{4,5},{5,4},{6,7},{7,6},{8,9},{9,8},{10,11... | collective-permute-start | bytes 1179656 | tf_op jit(solution)/shard_map/ppermute | solution.py:313
  15.1 12.8 %collective-permute-start.1 = (bf16[384,512]{1,0:T(8,128)(2,1)S(1)}, bf16[384,512]{1,0:T(8,128)(2,1)S(1)}, u32[]{:S(2)}, u32[]{:S(2)}) collective-permute-start(bf16[384,512]{1,0:T(8,128)(2,1)S(1)} %collective-permute-done.refs_0_), channel_id=1, source_target_pairs={{0,1},{1,0},{2,3},{3,2},{4,5},{5,4},{6,7},{7,6},{8,9},{9,8},{10,11... | collective-permute-start | bytes 1179656 | tf_op jit(solution)/shard_map/ppermute | solution.py:313
  16.3 15.8 %collective-permute-start.6 = (bf16[384,512]{1,0:T(8,128)(2,1)S(1)}, bf16[384,512]{1,0:T(8,128)(2,1)S(1)}, u32[]{:S(2)}, u32[]{:S(2)}) collective-permute-start(bf16[384,512]{1,0:T(8,128)(2,1)S(1)} %collective-permute-done.3.refs_0_), channel_id=1, source_target_pairs={{0,1},{1,0},{2,3},{3,2},{4,5},{5,4},{6,7},{7,6},{8,9},{9,8},{10,11... | collective-permute-start | bytes 1179656 | tf_op jit(solution)/shard_map/ppermute | solution.py:313
  23.6 12.6 %collective-permute-start.5 = (bf16[384,512]{1,0:T(8,128)(2,1)S(1)}, bf16[384,512]{1,0:T(8,128)(2,1)S(1)}, u32[]{:S(2)}, u32[]{:S(2)}) collective-permute-start(bf16[384,512]{1,0:T(8,128)(2,1)S(1)} %collective-permute-done.4.refs_0_), channel_id=1, source_target_pairs={{0,1},{1,0},{2,3},{3,2},{4,5},{5,4},{6,7},{7,6},{8,9},{9,8},{10,11... | collective-permute-start | bytes 1179656 | tf_op jit(solution)/shard_map/ppermute | solution.py:313
  29.2 7.1 %collective-permute-start.7 = (bf16[384,256]{1,0:T(8,128)(2,1)S(1)}, bf16[384,256]{1,0:T(8,128)(2,1)S(1)}, u32[]{:S(2)}, u32[]{:S(2)}) collective-permute-start(bf16[384,256]{1,0:T(8,128)(2,1)S(1)} %get-tuple-element.44.q), channel_id=1, source_target_pairs={{12,4},{13,5},{14,6},{15,7},{28,20},{29,21},{30,22},{31,23}} | collective-permute-start | bytes 589832 | tf_op jit(solution)/shard_map/ppermute | solution.py:317
  31.4 9.9 %collective-permute-start.8 = (bf16[2,384,256]{2,1,0:T(8,128)(2,1)S(1)}, bf16[2,384,256]{2,1,0:T(8,128)(2,1)S(1)}, u32[]{:S(2)}, u32[]{:S(2)}) collective-permute-start(bf16[2,384,256]{2,1,0:T(8,128)(2,1)S(1)} %get-tuple-element.45.refs_12_.kv), channel_id=1, source_target_pairs={{0,8},{1,9},{2,10},{3,11},{16,24},{17,25},{18,26},{19,27}} | collective-permute-start | bytes 1179656 | tf_op jit(solution)/shard_map/ppermute | solution.py:317
  36.2 12.3 %collective-permute-start.9 = (bf16[384,256]{1,0:T(8,128)(2,1)S(1)}, bf16[384,256]{1,0:T(8,128)(2,1)S(1)}, u32[]{:S(2)}, u32[]{:S(2)}) collective-permute-start(bf16[384,256]{1,0:T(8,128)(2,1)S(1)} %get-tuple-element.57), channel_id=1, source_target_pairs={{4,12},{5,13},{6,14},{7,15},{20,28},{21,29},{22,30},{23,31}} | collective-permute-start | bytes 589832 | tf_op jit(solution)/shard_map/ppermute | solution.py:317
  37.5 11.0 %collective-permute-start.10 = (f32[8,384]{1,0:T(8,128)S(1)}, f32[8,384]{1,0:T(8,128)S(1)}, u32[]{:S(2)}, u32[]{:S(2)}) collective-permute-start(f32[8,384]{1,0:T(8,128)S(1)} %get-tuple-element.58), channel_id=1, source_target_pairs={{4,12},{5,13},{6,14},{7,15},{20,28},{21,29},{22,30},{23,31}} | collective-permute-start | bytes 36872 | tf_op jit(solution)/shard_map/ppermute | solution.py:317
  48.8 7.8 %collective-permute-start.13 = (bf16[384,256]{1,0:T(8,128)(2,1)S(1)}, bf16[384,256]{1,0:T(8,128)(2,1)S(1)}, u32[]{:S(2)}, u32[]{:S(2)}) collective-permute-start(bf16[384,256]{1,0:T(8,128)(2,1)S(1)} %get-tuple-element.60.refs_0_), channel_id=1, source_target_pairs={{0,2},{1,3},{2,0},{3,1},{4,6},{5,7},{6,4},{7,5},{8,10},{9,11},{10,... | collective-permute-start | bytes 589832 | tf_op jit(solution)/shard_map/ppermute | solution.py:313
  50.4 8.3 %collective-permute-start.16 = (bf16[160,512]{1,0:T(8,128)(2,1)S(1)}, bf16[160,512]{1,0:T(8,128)(2,1)S(1)}, u32[]{:S(2)}, u32[]{:S(2)}) collective-permute-start(bf16[160,512]{1,0:T(8,128)(2,1)S(1)} %get-tuple-element.65), channel_id=1, source_target_pairs={{0,3},{1,2},{2,1},{3,0},{16,18},{17,19},{18,16},{19,17},{4,7},{5,6... | collective-permute-start | bytes 491528 | tf_op jit(solution)/shard_map/ppermute | solution.py:462
  50.4 11.8 %collective-permute-start.12 = (bf16[256,512]{1,0:T(8,128)(2,1)S(1)}, bf16[256,512]{1,0:T(8,128)(2,1)S(1)}, u32[]{:S(2)}, u32[]{:S(2)}) collective-permute-start(bf16[256,512]{1,0:T(8,128)(2,1)S(1)} %get-tuple-element.62), channel_id=1, source_target_pairs={{0,1},{1,0},{2,3},{3,2},{4,5},{5,4},{6,7},{7,6},{8,9},{9,8},{10,11... | collective-permute-start | bytes 786440 | tf_op jit(solution)/shard_map/ppermute | solution.py:313
  51.0 11.2 %collective-permute-start.11 = (bf16[384,256]{1,0:T(8,128)(2,1)S(1)}, bf16[384,256]{1,0:T(8,128)(2,1)S(1)}, u32[]{:S(2)}, u32[]{:S(2)}) collective-permute-start(bf16[384,256]{1,0:T(8,128)(2,1)S(1)} %get-tuple-element.60.refs_0_), channel_id=1, source_target_pairs={{0,1},{1,0},{2,3},{3,2},{4,5},{5,4},{6,7},{7,6},{8,9},{9,8},{10,11... | collective-permute-start | bytes 589832 | tf_op jit(solution)/shard_map/ppermute | solution.py:313
  51.0 10.1 %collective-permute-start.15 = (bf16[96,512]{1,0:T(8,128)(2,1)S(1)}, bf16[96,512]{1,0:T(8,128)(2,1)S(1)}, u32[]{:S(2)}, u32[]{:S(2)}) collective-permute-start(bf16[96,512]{1,0:T(8,128)(2,1)S(1)} %get-tuple-element.64), channel_id=1, source_target_pairs={{0,3},{1,2},{2,1},{3,0},{16,18},{17,19},{18,16},{19,17},{4,7},{5,6... | collective-permute-start | bytes 294920 | tf_op jit(solution)/shard_map/ppermute | solution.py:460
  56.7 11.0 %collective-permute-start.14 = (bf16[384,256]{1,0:T(8,128)(2,1)S(1)}, bf16[384,256]{1,0:T(8,128)(2,1)S(1)}, u32[]{:S(2)}, u32[]{:S(2)}) collective-permute-start(bf16[384,256]{1,0:T(8,128)(2,1)S(1)} %collective-permute-done.13.refs_0_), channel_id=1, source_target_pairs={{0,1},{1,0},{2,3},{3,2},{4,5},{5,4},{6,7},{7,6},{8,9},{9,8},{10,11... | collective-permute-start | bytes 589832 | tf_op jit(solution)/shard_map/ppermute | solution.py:313
  58.7 9.0 %collective-permute-start.18 = (bf16[160,512]{1,0:T(8,128)(2,1)S(1)}, bf16[160,512]{1,0:T(8,128)(2,1)S(1)}, u32[]{:S(2)}, u32[]{:S(2)}) collective-permute-start(bf16[160,512]{1,0:T(8,128)(2,1)S(1)} %collective-permute-done.16.refs_3_), channel_id=1, source_target_pairs={{0,16},{16,0},{1,17},{17,1},{2,18},{18,2},{3,19},{19,3},{4,20},{20... | collective-permute-start | bytes 491528 | tf_op jit(solution)/shard_map/ppermute | solution.py:481
  61.2 6.5 %collective-permute-start.17 = (bf16[96,512]{1,0:T(8,128)(2,1)S(1)}, bf16[96,512]{1,0:T(8,128)(2,1)S(1)}, u32[]{:S(2)}, u32[]{:S(2)}) collective-permute-start(bf16[96,512]{1,0:T(8,128)(2,1)S(1)} %collective-permute-done.15.refs_2_), channel_id=1, source_target_pairs={{0,16},{16,0},{1,17},{17,1},{2,18},{18,2},{3,19},{19,3},{4,20},{20... | collective-permute-start | bytes 294920 | tf_op jit(solution)/shard_map/ppermute | solution.py:461
